TPU v7x, 128 devices: a whole 4x4x4 slice. The times are simulated.
128 devices in a mesh: sp: 16 (over z, y), tp: 8 (over x, core).
Axes of the slice: x: 4, y: 4, z: 4, core: 2. Of those that a mesh axis runs over, the one named last changes fastest.
Arguments:
- queries: bfloat16 [12288, 2048], P('sp', 'tp'), may hold values from -11 to 11
- key_rows: bfloat16 [12288, 2048], P('sp', 'tp'), may hold values from -4.5 to 4.5
- value_rows: bfloat16 [12288, 2048], P('sp', 'tp'), may hold values from -6 to 6
- log_forget: float32 [12288, 32], P('sp', 'tp'), may hold values from -1477.56 to 0, as said below
- stream_in: bfloat16 [12288, 2048], P('sp'), may hold values from -6 to 6
- out_weight: bfloat16 [2048, 2048], P('tp'), may hold values from -0.52734375 to 0.52734375
- mix_gain: float32 [2048], replicated, may hold values from 0.1 to 1.9
- mix_bias: float32 [2048], replicated, may hold values from -3 to 3
- gate_weight: bfloat16 [2048, 5632], P('sp', 'tp'), may hold values from -0.125 to 0.125
- up_weight: bfloat16 [2048, 5632], P('sp', 'tp'), may hold values from -0.125 to 0.125
- down_weight: bfloat16 [5632, 2048], P('tp', 'sp'), may hold values from -0.15917969 to 0.15917969
- ffn_gain: float32 [2048], replicated, may hold values from 0.1 to 1.9
- ffn_bias: float32 [2048], replicated, may hold values from -3 to 3
Outputs:
- layer_out: bfloat16 [12288, 2048], P(('sp', 'tp'))
Inputs may be any that keep to these rules, and one draw needn't show every extreme that they name: `log_forget`: each column never rises along the positions.
All inputs are finite; a program needn't handle non-finite values.
Results may differ from a plain program's by a relative error of at most 0.015.
Values may be sent and summed in bfloat16 or wider, within the bound.
No kernel may reach another device: no remote copies, remote signals or barrier semaphores. Data moves between devices by JAX's collectives and lax.ppermute only.
A program may use at most 128 MiB of HBM per device.

v0:
```python
import jax
import jax.numpy as jnp
from jax import lax
from jax.sharding import PartitionSpec as P

ALPHA = 8.0**0.25
EPSILON = 1e-05


def laid_out(pieces, dim):
    lengths = list(pieces.shape[1:])
    lengths[dim] *= pieces.shape[0]
    return jnp.moveaxis(pieces, 0, dim).reshape(lengths)


def from_everyone(value, axis):
    copies = jnp.broadcast_to(value, (lax.axis_size(axis), *value.shape))
    return lax.all_to_all(copies, axis, split_axis=0, concat_axis=0, tiled=True)


def gathered_copies(value, axis, dim):
    return laid_out(from_everyone(value, axis), dim)


def in_one_piece(arrays, axis, dim, along):
    ends, at = ([], 0)
    for a in arrays[:-1]:
        at += a.shape[along]
        ends.append(at)
    both = jnp.concatenate(arrays, axis=along)
    return tuple(jnp.split(lax.all_gather(both, axis, axis=dim, tiled=True), ends, axis=along))


def in_blocks(value, dim, count):
    before, after = (value.shape[:dim], value.shape[dim + 1 :])
    return jnp.moveaxis(value.reshape(*before, count, -1, *after), dim, 0)


def sum_at_owner(value, axis, dim):
    pieces = in_blocks(value, dim, lax.axis_size(axis))
    arrived = lax.all_to_all(pieces, axis, split_axis=0, concat_axis=0, tiled=True)
    return arrived.astype(jnp.float32).sum(axis=0)


def layer_norm(matrix, norm_gain, norm_shift):
    centred = matrix - jnp.mean(matrix, axis=-1, keepdims=True)
    spread = jnp.mean(centred * centred, axis=-1, keepdims=True)
    return centred * lax.rsqrt(spread + EPSILON) * norm_gain + norm_shift


def attend(queries, key_rows, value_rows, log_forget):
    length, row_width = queries.shape
    head_count = log_forget.shape[1]
    head_dim = row_width // head_count
    score_scale = head_dim ** (-0.5)
    first_pos = lax.axis_index("sp") * length
    last_pos = first_pos + length
    query_heads = queries.reshape(length, head_count, head_dim)
    query_gates = log_forget.T
    query_pos = first_pos + jnp.arange(length, dtype=jnp.int32)
    gates_all = gathered_copies(log_forget, "sp", 0)
    initial = (
        jnp.full((head_count, length), -1e30, jnp.float32),
        jnp.zeros((head_count, length), jnp.float32),
        jnp.zeros((length, head_count, head_dim), jnp.float32),
    )
    running = initial
    key_piece, value_piece = in_one_piece((key_rows, value_rows), "sp", 0, 1)
    piece_len = key_piece.shape[0]
    shards = piece_len // length
    group_size = max(
        [
            count_try
            for count_try in range(1, shards + 1)
            if shards % count_try == 0 and count_try * length <= max(length, 512)
        ]
    )
    block_len = group_size * length
    blocks = piece_len // block_len
    key_blocks = key_piece.reshape(blocks, block_len, head_count, head_dim)
    value_blocks = value_piece.reshape(blocks, block_len, head_count, head_dim)
    gate_blocks = gates_all.reshape(blocks, block_len, head_count)
    block_starts = block_len * jnp.arange(blocks, dtype=jnp.int32)

    def one_block(running_state, packed):
        key_block, value_block, gate_block, block_start = packed

        def compute(state_in):
            highest, totals, weighted = state_in
            scores = (
                jnp.einsum(
                    "qhd,khd->hqk", query_heads, key_block, preferred_element_type=jnp.float32
                )
                * score_scale
            )
            scores = scores + query_gates[:, :, None] - gate_block.T[:, None, :]
            key_pos = block_start + jnp.arange(block_len, dtype=jnp.int32)
            allowed = (key_pos[None, :] <= query_pos[:, None])[None]
            masked = jnp.where(allowed, scores, -1e30)
            new_high = jnp.maximum(highest, jnp.max(masked, axis=2))
            weights = jnp.where(allowed, jnp.exp(masked - new_high[:, :, None]), 0.0)
            factor = jnp.exp(highest - new_high)
            totals = totals * factor + jnp.sum(weights, axis=2)
            weighted = weighted * factor.T[:, :, None] + jnp.einsum(
                "hqk,khd->qhd",
                weights.astype(jnp.bfloat16),
                value_block,
                preferred_element_type=jnp.float32,
            )
            return (new_high, totals, weighted)

        def keep_state(state_in):
            return state_in

        return (lax.cond(block_start < last_pos, compute, keep_state, running_state), None)

    running, unused = lax.scan(
        one_block, running, (key_blocks, value_blocks, gate_blocks, block_starts)
    )
    highest, totals, weighted = running
    return (weighted / totals.T[:, :, None]).reshape(length, row_width).astype(jnp.bfloat16)


def body(
    queries,
    key_rows,
    value_rows,
    log_forget,
    stream_in,
    out_weight,
    mix_gain,
    mix_bias,
    gate_weight,
    up_weight,
    down_weight,
    ffn_gain,
    ffn_bias,
):
    attended = attend(queries, key_rows, value_rows, log_forget)
    length = attended.shape[0]
    own_rows = length // lax.axis_size("tp")
    offset = lax.axis_index("tp") * own_rows
    summed = sum_at_owner(
        jnp.dot(attended, out_weight, preferred_element_type=jnp.float32).astype(jnp.bfloat16),
        "tp",
        0,
    )
    mix_out = lax.optimization_barrier(summed.astype(jnp.bfloat16)).astype(jnp.float32)
    stream_own = lax.dynamic_slice_in_dim(stream_in, offset, own_rows, 0)
    normed = layer_norm(
        ALPHA * stream_own.astype(jnp.float32) + mix_out, mix_gain, mix_bias
    ).astype(jnp.bfloat16)
    gathered = lax.all_gather(normed, "tp", axis=0, tiled=True)
    pieces = in_one_piece((gate_weight, up_weight), "sp", 0, 1)
    gate_part = jnp.dot(gathered, pieces[0], preferred_element_type=jnp.float32)
    up_part = jnp.dot(gathered, pieces[1], preferred_element_type=jnp.float32)
    hidden = (jax.nn.silu(gate_part) * up_part).astype(jnp.bfloat16)
    partial_terms = jnp.dot(
        hidden,
        lax.all_gather(down_weight, "sp", axis=1, tiled=True),
        preferred_element_type=jnp.float32,
    )
    lowered = lax.psum_scatter(
        partial_terms.astype(jnp.bfloat16), "tp", scatter_dimension=0, tiled=True
    ).astype(jnp.float32)
    lowered = lax.optimization_barrier(lowered.astype(jnp.bfloat16)).astype(jnp.float32)
    result = layer_norm(ALPHA * normed.astype(jnp.float32) + lowered, ffn_gain, ffn_bias)
    return result.astype(jnp.bfloat16)


def solution(mesh):
    placed = (
        P("sp", "tp"),
        P("sp", "tp"),
        P("sp", "tp"),
        P("sp", "tp"),
        P("sp", None),
        P("tp", None),
        P(),
        P(),
        P("sp", "tp"),
        P("sp", "tp"),
        P("tp", "sp"),
        P(),
        P(),
    )
    return jax.shard_map(
        body, mesh=mesh, in_specs=placed, out_specs=P(("sp", "tp"), None), check_vma=False
    )
```

profile of v0, /device:TPU:0, one launch (start us, length us, event | category | flops | bytes accessed | tf_op | source)
XLA Modules:
  0.0 604.3 jit_solution(4880820120093457124)
XLA Ops:
  6.5 0.0 copy-start
  6.5 0.0 all-gather.5.cloned.1.call-start
  6.5 2.2 pad_maximum_fusion
  8.7 0.0 all-gather.5.cloned.1.call-update
  8.8 0.0 all-gather.9.cloned.1.call-start
  8.8 1.8 pad_maximum_fusion.1
  10.6 0.0 all-gather.9.cloned.1.call-update
  10.6 1.4 broadcast_in_dim.56
  12.0 8.2 %all-to-all-start = ((f32[16,768,4]{1,2,0:T(4,128)}), f32[16,768,4]{1,2,0:T(4,128)S(1)}, u32[]{:S(2)}, u32[]{:S(2)}) async-start(f32[16,768,4]{1,2,0:T(4,128)} %broadcast_in_dim.56), calls=%async_computation | async-start | bytes 393216 | tf_op jit(solution)/shard_map/all_to_all | solution.py:18
  20.2 1.2 copy.18
  21.4 80.5 %all-gather.5.cloned.1.call-done = bf16[12288,512]{1,0:T(8,128)(2,1)} async-done(((bf16[768,512]{1,0:T(8,128)(2,1)}), bf16[12288,512]{1,0:T(8,128)(2,1)}) %all-gather.5.cloned.1.call-update) | async-done | bytes 12582928 | tf_op jit(solution)/shard_map/all_gather | solution.py:31
  101.9 10.1 %fusion.36 = (bf16[12288,256]{1,0:T(8,128)(2,1)}, bf16[12288,256]{1,0:T(8,128)(2,1)}) fusion(bf16[12288,512]{1,0:T(8,128)(2,1)} %all-gather.5.cloned.1.call-done), kind=kLoop, calls=%fused_computation.51 | loop fusion | bytes 25165824 | tf_op jit(solution)/shard_map/split | solution.py:31
  112.0 18.8 %reshape.82 = bf16[16,768,4,64]{3,2,1,0:T(4,128)(2,1)} reshape(bf16[12288,256]{1,0:T(8,128)(2,1)} %get-tuple-element.249) | data formatting | bytes 12582912 | tf_op jit(solution)/shard_map/reshape | solution.py:80
  130.8 18.1 %copy.20 = bf16[16,768,4,64]{1,3,2,0:T(8,128)(2,1)} copy(bf16[16,768,4,64]{3,2,1,0:T(4,128)(2,1)} %reshape.82) | data formatting | bytes 12582912
  148.9 18.8 %reshape.83 = bf16[16,768,4,64]{3,2,1,0:T(4,128)(2,1)} reshape(bf16[12288,256]{1,0:T(8,128)(2,1)} %get-tuple-element.248) | data formatting | bytes 12582912 | tf_op jit(solution)/shard_map/reshape | solution.py:81
  167.6 18.1 %copy.21 = bf16[16,768,4,64]{1,3,2,0:T(8,128)(2,1)} copy(bf16[16,768,4,64]{3,2,1,0:T(4,128)(2,1)} %reshape.83) | data formatting | bytes 12582912
  185.7 0.0 all-to-all-done
  185.7 0.1 broadcast_in_dim.55
  185.8 33.5 %while.15 = (s32[]{:T(128)}, f32[4,768]{1,0:T(4,128)S(1)}, f32[4,768]{1,0:T(4,128)S(1)}, f32[768,4,64]{0,2,1:T(8,128)S(1)}, s32[16]{0:T(128)S(1)}, /*index=5*/s3...) while((s32[]{:T(128)}, f32[4,768]{1,0:T(4,128)S(1)}, ...), condition=%wide.region_5.6_spmd.clone, body=%wide.region_0.5_spmd.clone.sunk | while | flops 649800192 | bytes 33738040 | solution.py:117
  185.8 0.6 dynamic_slice.50
  187.1 13.1 %conditional.3 = ((f32[4,768]{1,0:T(4,128)S(1)}, f32[4,768]{1,0:T(4,128)S(1)}, f32[768,4,64]{0,2,1:T(8,128)S(1)})) conditional(s32[]{:T(128)} %convert_element_type.100, (f32[4,768]{1,0:T(4,128)S(1)}, f32[4,768]{1,0:T(4,128)S(1)}, f32[768,4,64]{0,2,1:T(8,128)S(1)}) %tuple.41, (s32[]{:T(128)}, s32[]{:T(128)}, bf16[16,768,4,64]{1,3,2,0:T(8,128)(2,1)}, ...), branch_computations={%region_1.1_spmd, %region_2.4_spmd} | conditional | flops 649800192 | bytes 33734700 | solution.py:115
  187.1 0.7 iota_add_fusion
  187.7 0.4 broadcast_compare_fusion
  188.2 3.9 fusion.4
  192.0 4.6 fusion.11
  196.6 3.5 fusion.3
  200.2 0.6 dynamic_slice.50
  201.4 0.6 dynamic_slice.50
  202.7 0.6 dynamic_slice.50
  204.0 0.6 dynamic_slice.50
  205.3 0.6 dynamic_slice.50
  206.5 0.6 dynamic_slice.50
  207.8 0.6 dynamic_slice.50
  209.1 0.6 dynamic_slice.50
  210.4 0.6 dynamic_slice.50
  211.7 0.6 dynamic_slice.50
  212.9 0.6 dynamic_slice.50
  214.2 0.6 dynamic_slice.50
  215.5 0.6 dynamic_slice.50
  216.8 0.6 dynamic_slice.50
  218.0 0.6 dynamic_slice.50
  219.3 0.1 divide_convert_fusion
  219.4 2.7 convolution_convert_fusion.1
  222.1 4.6 all-to-all-start.1
  226.7 0.2 all-gather.7.cloned.1.call-start
  226.9 38.2 %all-to-all-done.1 = bf16[8,96,2048]{2,1,0:T(8,128)(2,1)} async-done(((bf16[8,96,2048]{2,1,0:T(8,128)(2,1)}), bf16[8,96,2048]{2,1,0:T(8,128)(2,1)}, u32[]{:S(2)}, u32[]{:S(2)}) %all-to-all-start.1) | async-done | bytes 3145760 | tf_op jit(solution)/shard_map/all_to_all | solution.py:41
  265.1 2.5 reduce_sum.59
  267.6 1.2 fusion.33
  268.8 1.3 multiply_reduce_fusion.1
  270.2 2.0 add_convert_fusion.1
  272.2 0.0 all-gather.7.cloned.1.call-update
  272.2 0.0 all-gather.11.cloned.1.call-start
  272.2 0.5 all-gather.11.cloned.1.call-update
  272.8 0.0 reduce-scatter.2.cloned.1.call-start
  272.8 0.0 all-gather.9.cloned.1.call-done
  272.8 220.0 %all-gather.7.cloned.1.call-done = bf16[768,2048]{1,0:T(8,128)(2,1)} async-done(((bf16[96,2048]{1,0:T(8,128)(2,1)}), bf16[768,2048]{1,0:T(8,128)(2,1)}) %all-gather.7.cloned.1.call-update) | async-done | bytes 3145744 | tf_op jit(solution)/shard_map/all_gather | solution.py:153
  492.8 6.5 %fusion.27 = f32[768,704]{0,1:T(8,128)} fusion(bf16[768,2048]{1,0:T(8,128)(2,1)} %all-gather.7.cloned.1.call-done, bf16[2048,1408]{0,1:T(8,128)(2,1)} %all-gather.9.cloned.1.call-done), kind=kOutput, calls=%fused_computation.31 | convolution fusion | flops 2214592512 | bytes 8192000 | tf_op jit(solution)/shard_map/dot_general | solution.py:155
  499.3 46.2 %all-gather.11.cloned.1.call-done = bf16[704,2048]{1,0:T(8,128)(2,1)} async-done(((bf16[704,128]{1,0:T(8,128)(2,1)}), bf16[704,2048]{1,0:T(8,128)(2,1)}) %all-gather.11.cloned.1.call-update) | async-done | bytes 2883600 | tf_op jit(solution)/shard_map/all_gather | solution.py:160
  545.5 12.4 %convolution_convert_fusion = bf16[768,2048]{1,0:T(8,128)(2,1)} fusion(bf16[704,2048]{1,0:T(8,128)(2,1)} %all-gather.11.cloned.1.call-done, f32[768,704]{0,1:T(8,128)} %fusion.27, bf16[768,2048]{1,0:T(8,128)(2,1)} %all-gather.7.cloned.1.call-done, bf16[2048,1408]{0,1:T(8,128)(2,1)} %all-gather.9.cloned.1.call-done), kind=kOutput, calls=%fused_computation.27 | convolution fusion | flops 4434001920 | bytes 14221312 | tf_op jit(solution)/shard_map/dot_general | solution.py:158
  557.9 0.0 reduce-scatter.2.cloned.1.call-update
  557.9 35.3 %reduce-scatter.2.cloned.1.call-done = bf16[96,2048]{1,0:T(8,128)(2,1)} async-done(((bf16[768,2048]{1,0:T(8,128)(2,1)}), bf16[96,2048]{1,0:T(8,128)(2,1)}) %reduce-scatter.2.cloned.1.call-update) | async-done | bytes 393232 | tf_op jit(solution)/shard_map/reduce_scatter | solution.py:163
  593.2 1.2 fusion.34
  594.4 1.3 multiply_reduce_fusion
  595.7 2.0 add_convert_fusion
  (55 shorter events, 0.3 us)
Async XLA Ops:
  6.5 212.9 %copy-start = (bf16[256,2048]{1,0:T(8,128)(2,1)S(1)}, bf16[256,2048]{1,0:T(8,128)(2,1)}, u32[]{:S(2)}) copy-start(bf16[256,2048]{1,0:T(8,128)(2,1)} %param.22) | copy-start | bytes 3145732
  6.5 95.4 %all-gather.5.cloned.1.call-start = ((), (), s32[]{:S(2)}) async-start(), calls=%async_computation.3 | async-start | bytes 13369344 | tf_op jit(solution)/shard_map/all_gather | solution.py:31
  8.8 264.1 %all-gather.9.cloned.1.call-start = ((), (), s32[]{:S(2)}) async-start(), calls=%async_computation.5 | async-start | bytes 6127616 | tf_op jit(solution)/shard_map/all_gather | solution.py:31
  12.0 173.7 %all-to-all-start = ((f32[16,768,4]{1,2,0:T(4,128)}), f32[16,768,4]{1,2,0:T(4,128)S(1)}, u32[]{:S(2)}, u32[]{:S(2)}) async-start(f32[16,768,4]{1,2,0:T(4,128)} %broadcast_in_dim.56), calls=%async_computation | async-start | bytes 393216 | tf_op jit(solution)/shard_map/all_to_all | solution.py:18
  167.6 18.2 %copy-start.2 = (f32[768,4]{0,1:T(4,128)S(1)}, f32[768,4]{0,1:T(4,128)}, u32[]{:S(2)}) copy-start(f32[768,4]{0,1:T(4,128)} %param.20) | copy-start | bytes 36868
  222.1 48.0 %copy-start.3 = (f32[2048]{0:T(1024)S(1)}, f32[2048]{0:T(1024)}, u32[]{:S(2)}) copy-start(f32[2048]{0:T(1024)} %param.24) | copy-start | bytes 24580
  222.1 48.0 %copy-start.4 = (f32[2048]{0:T(1024)S(1)}, f32[2048]{0:T(1024)}, u32[]{:S(2)}) copy-start(f32[2048]{0:T(1024)} %param.23) | copy-start | bytes 24580
  222.1 43.0 %all-to-all-start.1 = ((bf16[8,96,2048]{2,1,0:T(8,128)(2,1)}), bf16[8,96,2048]{2,1,0:T(8,128)(2,1)}, u32[]{:S(2)}, u32[]{:S(2)}) async-start(bf16[8,96,2048]{2,1,0:T(8,128)(2,1)} %bitcast.45), calls=%async_computation.1 | async-start | bytes 6291456 | tf_op jit(solution)/shard_map/all_to_all | solution.py:41
  226.7 266.1 %all-gather.7.cloned.1.call-start = ((), (), s32[]{:S(2)}) async-start(), calls=%async_computation.4 | async-start | bytes 3538944 | tf_op jit(solution)/shard_map/all_gather | solution.py:153
  272.2 273.3 %all-gather.11.cloned.1.call-start = ((), (), s32[]{:S(2)}) async-start(), calls=%async_computation.6 | async-start | bytes 3063808 | tf_op jit(solution)/shard_map/all_gather | solution.py:160
  272.8 320.4 %reduce-scatter.2.cloned.1.call-start = ((), (), s32[]{:S(2)}) async-start(), calls=%async_computation.7 | async-start | bytes 3538944 | tf_op jit(solution)/shard_map/reduce_scatter | solution.py:163
  499.3 93.9 %copy-start.1 = (bf16[96,2048]{1,0:T(8,128)(2,1)S(1)}, bf16[96,2048]{1,0:T(8,128)(2,1)}, u32[]{:S(2)}) copy-start(bf16[96,2048]{1,0:T(8,128)(2,1)} %add_convert_fusion.1) | copy-start | bytes 1179652
  499.3 96.4 %copy-start.5 = (f32[2048]{0:T(1024)S(1)}, f32[2048]{0:T(1024)}, u32[]{:S(2)}) copy-start(f32[2048]{0:T(1024)} %param.29) | copy-start | bytes 24580
  499.3 96.4 %copy-start.6 = (f32[2048]{0:T(1024)S(1)}, f32[2048]{0:T(1024)}, u32[]{:S(2)}) copy-start(f32[2048]{0:T(1024)} %param.28) | copy-start | bytes 24580
Sparse Core Ops, SparseCore 0:
  9.5 92.3 all-gather.4
  104.0 64.0 all-gather.8
  272.3 220.4 all-gather.6
  494.8 50.6 all-gather.10
  558.0 35.0 reduce-scatter.1
where the time goes:
time: 608 us; the launch traced here: 604 us
  waiting for transfers between devices  421 us (69%)
  local copies, waits for them, and re-layouts  95.9 us (16%)
  matrix products  30.1 us (5%)
  other arithmetic  20.1 us (3%)
  between operations  13.3 us (2%)
  starting transfers between devices  13.1 us (2%)
  loops' own time  11.1 us (2%)
    all_gather x1, waiting for transfers between devices, body(): gathered = lax.all_gather(normed, 'tp', axis=0, tiled=True)  220 us
    all_gather x2, waiting for transfers between devices, in_one_piece(): lax.all_gather(both, axis, axis=dim, tiled=True)  80.5 us
    all_gather x1, waiting for transfers between devices, body(): lax.all_gather(down_weight, 'sp', axis=1, tiled=True)  46.2 us
    all_to_all x1, waiting for transfers between devices, sum_at_owner(): lax.all_to_all(pieces, axis, split_axis=0, concat_axis=0, tiled=True)  38.2 us
    unnamed x17, local copies, waits for them, and re-layouts  37.4 us
    reduce_scatter x1, waiting for transfers between devices, body(): lax.psum_scatter(partial_terms.astype(jnp.bfloat16), 'tp', scatter_dimens...  35.3 us
    reshape x1, local copies, waits for them, and re-layouts, attend(): key_blocks = key_piece.reshape(blocks, block_len, head_count, head_dim)  18.8 us
    reshape x1, local copies, waits for them, and re-layouts, attend(): value_blocks = value_piece.reshape(blocks, block_len, head_count, head_dim)  18.8 us
  transfers between devices with their start and end apart: 7, of which 5 were waited for; matrix products, arithmetic and copies ran while one was open for 21% of the time, Pallas kernels for 0%

commit v1 on v0

v1 whole, which is shorter than its diff:
```python
import functools
import jax
import jax.numpy as jnp
import numpy as np
from jax import lax
from jax.experimental import pallas as pl
from jax.experimental.pallas import tpu as pltpu
from jax.sharding import Mesh, PartitionSpec as P

ALPHA = 8.0**0.25
EPSILON = 1e-05
F32 = jnp.float32
BF16 = jnp.bfloat16

ROWS = 768
SUB = 192
HALF = 96
HD = 64
NSH = 16
PACK = 800
TILE = 256
TILES = SUB * NSH // TILE


def vmem():
    return pl.BlockSpec(memory_space=pltpu.VMEM)


def smem():
    return pl.BlockSpec(memory_space=pltpu.SMEM)


def params(mb=60):
    return pltpu.CompilerParams(vmem_limit_bytes=mb * 1024 * 1024)


def pack_kernel(q_ref, k_ref, v_ref, g_ref, qo_ref, kvo_ref):
    for h in range(4):
        cols = slice(h * HD, (h + 1) * HD)
        kvo_ref[h, 0:ROWS, 0:HD] = k_ref[:, cols]
        kvo_ref[h, 0:ROWS, HD : 2 * HD] = v_ref[:, cols]
        for z in range(4):
            at = z * SUB
            qo_ref[z * 4 + h, :, 0:HD] = q_ref[at : at + HALF, cols]
            qo_ref[z * 4 + h, :, HD : 2 * HD] = q_ref[at + HALF : at + SUB, cols]
        chunks = [-g_ref[h : h + 1, c * 128 : (c + 1) * 128] for c in range(6)]
        value = jnp.concatenate(chunks, axis=0)
        first = value.astype(BF16).astype(F32)
        second = (value - first).astype(BF16).astype(F32)
        third = value - first - second
        rest = jnp.zeros((PACK - ROWS - 18, 128), F32)
        kvo_ref[h, ROWS:PACK, :] = jnp.concatenate(
            [first, second, third, rest], axis=0
        ).astype(BF16)


def pack(q, k, v, g):
    return pl.pallas_call(
        pack_kernel,
        out_shape=(
            jax.ShapeDtypeStruct((NSH, HALF, 128), BF16),
            jax.ShapeDtypeStruct((4, PACK, 128), BF16),
        ),
        in_specs=[vmem()] * 4,
        out_specs=(vmem(), vmem()),
        compiler_params=params(),
        cost_estimate=pl.CostEstimate(flops=10**6, bytes_accessed=2500000, transcendentals=0),
    )(q, k, v, g)


def unit_table():
    units = []
    for t in range(TILES):
        low = (TILE * t) // SUB
        for j in range(low + 2):
            units.append((t, j, int(j >= low), int(j == low + 1)))
    assert len(units) % 2 == 0
    count = len(units)
    units = [(0, 0, 0, 0)] + units + [units[-1]]
    return count, np.array(units, np.int32).T.copy()


UNITS, TABLE = unit_table()


def attend_kernel(
    tab, z_ref, q_ref, kv_ref, o_ref,
    kaug, vt, qrow, qt, qpos, oscr, s_a, s_b, p_a, p_b, al_a, al_b, top, acc,
):
    lane = lax.broadcasted_iota(jnp.int32, (128, 128), 1)

    def per_shard(s, carry):
        gates = kv_ref[s, ROWS:PACK, :].astype(F32)
        square = jnp.concatenate(
            [jnp.zeros((HD, 128), F32), gates, jnp.zeros((32, 128), F32)], axis=0
        )
        turned = square.T
        for c in range(6):
            part = kv_ref[s, c * 128 : (c + 1) * 128, :].astype(F32)
            mine = (lane == HD + c) | (lane == HD + 6 + c) | (lane == HD + 12 + c)
            kaug[s, c * 128 : (c + 1) * 128, :] = jnp.where(
                lane < HD, part, jnp.where(mine, turned, 0.0)
            ).astype(BF16)
            vt[s, :, c * 128 : (c + 1) * 128] = part.T.astype(BF16)
        vt[s, 48:64, :] = jnp.ones((16, ROWS), BF16)
        return carry

    lax.fori_loop(0, NSH, per_shard, 0)

    lane_h = lax.broadcasted_iota(jnp.int32, (HALF, 128), 1)

    def per_query(s, carry):
        both = q_ref[s].astype(F32) * (HD**-0.5)
        ones = jnp.where(lane_h < HD + 18, 1.0, 0.0)
        qrow[s, 0:HALF, :] = jnp.where(lane_h < HD, both, ones)
        qrow[s, HALF:SUB, :] = jnp.where(lane_h < HD, pltpu.roll(both, HD, 1), ones)
        return carry

    lax.fori_loop(0, NSH, per_query, 0)
    z = z_ref[0]
    lane_t = lax.broadcasted_iota(jnp.int32, (8, TILE), 1)
    for t in range(TILES):
        low = (TILE * t) // SUB
        edge = (low + 1) * SUB - TILE * t
        rows = jnp.concatenate(
            [
                qrow[low, SUB - edge : SUB, :],
                qrow[low + 1, 0 : TILE - edge, :],
            ],
            axis=0,
        )
        qt[t] = rows.T.astype(BF16)
        qpos[t] = z * SUB + jnp.where(
            lane_t < edge,
            low * ROWS + (SUB - edge) + lane_t,
            (low + 1) * ROWS + lane_t - edge,
        )
    acc[...] = jnp.zeros(acc.shape, F32)
    top[...] = jnp.full(top.shape, -1e30, F32)
    al_a[...] = jnp.zeros(al_a.shape, F32)
    al_b[...] = jnp.zeros(al_b.shape, F32)
    p_b[...] = jnp.zeros(p_b.shape, BF16)

    def scores(at, out):
        out[...] = jnp.dot(kaug[tab[1, at]], qt[tab[0, at]], preferred_element_type=F32)

    scores(1, s_a)

    def unit(at, s_now, s_next, p_before, p_now, al_before, al_now):
        def work(masked):
            scores(at + 1, s_next)
            j = tab[1, at]
            pv = jnp.dot(vt[tab[1, at - 1], 48:128, :], p_before[...], preferred_element_type=F32)
            acc[...] = acc[...] * al_before[0:1, :] + pv
            before = jnp.where(j == 0, -1e30, top[0:1, :])
            s = s_now[...]
            if masked:
                pos = j * ROWS + lax.broadcasted_iota(jnp.int32, (ROWS, TILE), 0)
                s = jnp.where(pos <= qpos[tab[0, at], 0:1, :], s, -1e30)
            high = jnp.maximum(before, jnp.max(s, axis=0, keepdims=True))
            p_now[...] = jnp.exp(s - high).astype(BF16)
            top[0:1, :] = high
            al_now[0:1, :] = jnp.exp(before - high)

        lax.cond(tab[2, at] == 1, lambda: work(True), lambda: work(False))
        finish(at - 1)

    def finish(at):
        @pl.when(tab[3, at] == 1)
        def _():
            good = acc[16:80, :] / acc[0:1, :]
            row = pl.multiple_of(tab[0, at] * TILE, TILE)
            full = jnp.concatenate([good, jnp.zeros((HD, TILE), F32)], axis=0)
            oscr[pl.ds(row, TILE), :] = full.T

    def pair(i, carry):
        unit(2 * i + 1, s_a, s_b, p_b, p_a, al_b, al_a)
        unit(2 * i + 2, s_b, s_a, p_a, p_b, al_a, al_b)
        return carry

    lax.fori_loop(0, UNITS // 2, pair, 0)
    pv = jnp.dot(vt[tab[1, UNITS], 48:128, :], p_b[...], preferred_element_type=F32)
    acc[...] = acc[...] * al_b[0:1, :] + pv
    finish(UNITS)

    def out(s, carry):
        row = pl.multiple_of(s * SUB, SUB)
        one = oscr[pl.ds(row, HALF), :]
        two = oscr[pl.ds(row + HALF, HALF), :]
        o_ref[s] = jnp.where(lane_h < HD, one, pltpu.roll(two, HD, 1)).astype(BF16)
        return carry

    lax.fori_loop(0, NSH, out, 0)


def attend(q, kv, z):
    return pl.pallas_call(
        attend_kernel,
        out_shape=jax.ShapeDtypeStruct((NSH, HALF, 128), BF16),
        in_specs=[smem(), smem(), vmem(), vmem()],
        out_specs=vmem(),
        scratch_shapes=[
            pltpu.VMEM((NSH, ROWS, 128), BF16),
            pltpu.VMEM((NSH, 128, ROWS), BF16),
            pltpu.VMEM((NSH, SUB, 128), F32),
            pltpu.VMEM((TILES, 128, TILE), BF16),
            pltpu.VMEM((TILES, 8, TILE), jnp.int32),
            pltpu.VMEM((SUB * NSH, 128), F32),
            pltpu.VMEM((ROWS, TILE), F32),
            pltpu.VMEM((ROWS, TILE), F32),
            pltpu.VMEM((ROWS, TILE), BF16),
            pltpu.VMEM((ROWS, TILE), BF16),
            pltpu.VMEM((8, TILE), F32),
            pltpu.VMEM((8, TILE), F32),
            pltpu.VMEM((8, TILE), F32),
            pltpu.VMEM((80, TILE), F32),
        ],
        compiler_params=params(),
        cost_estimate=pl.CostEstimate(
            flops=35 * 10**9, bytes_accessed=4 * 10**6, transcendentals=2 * 10**7
        ),
    )(jnp.asarray(TABLE), z, q, kv)


def spread_kernel(o_ref, a_ref):
    for z in range(4):
        for y in range(4):
            for half in range(2):
                a_ref[2 * z + half, :, y * HD : (y + 1) * HD] = o_ref[
                    4 * z + y, :, half * HD : (half + 1) * HD
                ]


def spread(o):
    return pl.pallas_call(
        spread_kernel,
        out_shape=jax.ShapeDtypeStruct((8, HALF, 256), BF16),
        in_specs=[vmem()],
        out_specs=vmem(),
        compiler_params=params(),
        cost_estimate=pl.CostEstimate(flops=10**5, bytes_accessed=800000, transcendentals=0),
    )(o)


def norm_rows(matrix, gain, shift):
    centred = matrix - jnp.mean(matrix, axis=-1, keepdims=True)
    spread_ = jnp.mean(centred * centred, axis=-1, keepdims=True)
    return centred * lax.rsqrt(spread_ + EPSILON) * gain + shift


def mix_kernel(place, a_ref, stream_ref, gain_ref, bias_ref, *rest):
    w_refs, n_ref = rest[:8], rest[8]
    total = None
    for i in range(8):
        term = jnp.dot(a_ref[place[i]], w_refs[i][...], preferred_element_type=F32)
        total = term if total is None else total + term
    mixed = total.astype(BF16).astype(F32)
    matrix = ALPHA * stream_ref[...].astype(F32) + mixed
    n_ref[...] = norm_rows(matrix, gain_ref[...], bias_ref[...]).astype(BF16)


def mix(place, own, att, stream, gain, bias, weights):
    def whole(shape):
        return pl.BlockSpec(shape, lambda i, place: (0,) * len(shape))

    return pl.pallas_call(
        mix_kernel,
        out_shape=jax.ShapeDtypeStruct((HALF, 2048), BF16),
        grid_spec=pltpu.PrefetchScalarGridSpec(
            num_scalar_prefetch=1,
            grid=(1,),
            in_specs=[
                whole((8, HALF, 256)),
                pl.BlockSpec((HALF, 2048), lambda i, place: (place[8], 0)),
                whole((1, 2048)),
                whole((1, 2048)),
            ]
            + [whole((256, 2048))] * 8,
            out_specs=whole((HALF, 2048)),
        ),
        compiler_params=params(),
        cost_estimate=pl.CostEstimate(
            flops=2 * HALF * 2048 * 2048, bytes_accessed=9 * 10**6, transcendentals=0
        ),
    )(place, att, stream, gain, bias, *weights)


def ffn_kernel(x_ref, w_ref, out_ref, w_in, w_out, h_scr):
    @pl.when(pl.program_id(0) == 0)
    def _():
        for s in range(NSH):
            w_in[:, s * 128 : (s + 1) * 128] = w_ref[s, 0:1408, :]
            w_out[:, s * 128 : (s + 1) * 128] = w_ref[s, 1408:2112, :]

    both = lax.dot_general(
        x_ref[...], w_in[...], (((1,), (1,)), ((), ())), preferred_element_type=F32
    )
    gate, up = both[:, 0:704], both[:, 704:1408]
    h_scr[...] = (gate / (1.0 + jnp.exp(-gate)) * up).astype(BF16)
    out_ref[...] = jnp.dot(h_scr[...], w_out[...], preferred_element_type=F32).astype(BF16)


def ffn(x, w, tile=192):
    return pl.pallas_call(
        ffn_kernel,
        out_shape=jax.ShapeDtypeStruct((ROWS, 2048), BF16),
        grid=(ROWS // tile,),
        in_specs=[
            pl.BlockSpec((tile, 2048), lambda i: (i, 0)),
            pl.BlockSpec((NSH, 2112, 128), lambda i: (0, 0, 0)),
        ],
        out_specs=pl.BlockSpec((tile, 2048), lambda i: (i, 0)),
        scratch_shapes=[
            pltpu.VMEM((1408, 2048), BF16),
            pltpu.VMEM((704, 2048), BF16),
            pltpu.VMEM((tile, 704), BF16),
        ],
        compiler_params=params(),
        cost_estimate=pl.CostEstimate(
            flops=6 * ROWS * 2048 * 704, bytes_accessed=15 * 10**6, transcendentals=10**6
        ),
    )(x, w)


def last_kernel(p_ref, n_ref, gain_ref, bias_ref, o_ref):
    total = p_ref[0].astype(F32)
    for i in range(1, 8):
        total = total + p_ref[i].astype(F32)
    lowered = total.astype(BF16).astype(F32)
    matrix = ALPHA * n_ref[...].astype(F32) + lowered
    o_ref[...] = norm_rows(matrix, gain_ref[...], bias_ref[...]).astype(BF16)


def last(parts, normed, gain, bias):
    return pl.pallas_call(
        last_kernel,
        out_shape=jax.ShapeDtypeStruct((HALF, 2048), BF16),
        in_specs=[vmem()] * 4,
        out_specs=vmem(),
        compiler_params=params(),
        cost_estimate=pl.CostEstimate(
            flops=4 * 10**6, bytes_accessed=4 * 10**6, transcendentals=0
        ),
    )(parts, normed, gain, bias)


def body(
    queries, key_rows, value_rows, log_forget, stream_in, out_weight, mix_gain, mix_bias,
    gate_weight, up_weight, down_weight, ffn_gain, ffn_bias,
):
    zi = lax.axis_index("z")
    xi = lax.axis_index("x")
    ci = lax.axis_index("c")
    q_pack, kv_pack = pack(queries, key_rows, value_rows, log_forget.T)
    kv_mine = lax.all_to_all(kv_pack, "y", split_axis=0, concat_axis=0, tiled=True)
    q_mine = lax.all_to_all(q_pack, ("z", "y"), split_axis=0, concat_axis=0, tiled=True)
    kv_all = lax.all_gather(kv_mine, "z", axis=0, tiled=True)

    shards = jnp.concatenate([gate_weight.T, up_weight.T, down_weight], axis=0)
    ffn_all = lax.all_gather(shards, ("z", "y"), axis=0, tiled=False)

    weights, places = [out_weight], [2 * xi + ci]
    for d in (1, 3, 2):
        ring = [(i, (i + d) % 4) for i in range(4)]
        weights.append(lax.ppermute(out_weight, "x", ring))
        places.append(2 * ((xi + 4 - d) % 4) + ci)
    for i in range(4):
        weights.append(lax.ppermute(weights[i], "c", [(0, 1), (1, 0)]))
        places.append(places[i] + 1 - 2 * ci)
    own = 2 * xi + ci
    place = jnp.stack(places + [own]).astype(jnp.int32)

    attended = attend(q_mine, kv_all, zi.astype(jnp.int32)[None])
    by_shard = lax.all_to_all(attended, ("z", "y"), split_axis=0, concat_axis=0, tiled=True)
    by_rows = lax.all_to_all(
        spread(by_shard), ("x", "c"), split_axis=0, concat_axis=0, tiled=True
    )
    normed = mix(
        place, own, by_rows, stream_in, mix_gain[None], mix_bias[None], weights
    )
    gathered = lax.all_gather(normed, ("x", "c"), axis=0, tiled=True)
    partial = ffn(gathered, ffn_all)
    parts = lax.all_to_all(
        partial.reshape(8, HALF, 2048), ("x", "c"), split_axis=0, concat_axis=0, tiled=True
    )
    return last(parts, normed, ffn_gain[None], ffn_bias[None])


def solution(mesh):
    fine = Mesh(mesh.devices.reshape(4, 4, 4, 2), ("z", "y", "x", "c"))
    sp, tp = ("z", "y"), ("x", "c")
    placed = (
        P(sp, tp), P(sp, tp), P(sp, tp), P(sp, tp), P(sp, None), P(tp, None), P(), P(),
        P(sp, tp), P(sp, tp), P(tp, sp), P(), P(),
    )
    return jax.shard_map(
        body, mesh=fine, in_specs=placed, out_specs=P(("z", "y", "x", "c"), None), check_vma=False
    )
```

time: 608 us -> 337 us (0.55)
  waiting for transfers between devices: 421 us -> 142 us
  local copies, waits for them, and re-layouts: 95.9 us -> 2.17 us
  Pallas kernels: 0 us -> 86 us
  blocking collectives: 0 us -> 77.3 us
  matrix products: 30.1 us -> 0 us
  other arithmetic: 20.1 us -> 0.84 us
  loops' own time: 11.1 us -> 0 us
    all_gather x4 -> x3, waiting for transfers between devices: 347 us -> 96.8 us  [the longest x1 74.3 us: body(): ffn_all = lax.all_gather(shards, ('z', 'y'), axis=0, tiled=False)]
    pallas_call x0 -> x6, Pallas kernels: none -> 86 us  [the longest x1 52.3 us: attend(): pl.pallas_call(attend_kernel, out_shape=jax.ShapeDtypeStruct((NSH, HALF,...]
    all_to_all x0 -> x3, blocking collectives: none -> 77.3 us  [the longest x1 42.9 us: body(): lax.all_to_all(partial.reshape(8, HALF, 2048), ('x', 'c'), split_axis=0,...]
    reshape x2 -> x0, local copies, waits for them, and re-layouts: 37.6 us -> none  [the longest x1 18.8 us: attend(): key_blocks = key_piece.reshape(blocks, block_len, head_count, head_dim)]
    ppermute x0 -> x7, waiting for transfers between devices: none -> 37.1 us  [the longest x3 37.1 us: body(): weights.append(lax.ppermute(out_weight, 'x', ring))]
    unnamed x17 -> x16, local copies, waits for them, and re-layouts: 37.4 us -> 1.48 us
    reduce_scatter x1 -> x0, waiting for transfers between devices: 35.3 us -> none  [body(): lax.psum_scatter(partial_terms.astype(jnp.bfloat16), 'tp', scatter_dimens...]
    all_to_all x2, waiting for transfers between devices: 38.2 us -> 8.04 us  [the longest x1 8.04 us: body(): lax.all_to_all(spread(by_shard), ('x', 'c'), split_axis=0, concat_axis=0,...]
  transfers between devices with their start and end apart: 7 -> 12, of which waited for: 5 -> 6; matrix products, arithmetic and copies ran while one was open for 21% -> 0% of each run, Pallas kernels for 0% -> 16%
where the time goes in v1:
time: 337 us; the launch traced here: 336 us
  waiting for transfers between devices  142 us (42%)
  Pallas kernels  86 us (26%)
  blocking collectives  77.3 us (23%)
  starting transfers between devices  14.8 us (4%)
  between operations  13.2 us (4%)
    all_gather x1, waiting for transfers between devices, body(): ffn_all = lax.all_gather(shards, ('z', 'y'), axis=0, tiled=False)  74.3 us
    pallas_call x1, Pallas kernels, attend(): pl.pallas_call(attend_kernel, out_shape=jax.ShapeDtypeStruct((NSH, HALF,...  52.3 us
    all_to_all x1, blocking collectives, body(): lax.all_to_all(partial.reshape(8, HALF, 2048), ('x', 'c'), split_axis=0,...  42.9 us
    ppermute x3, waiting for transfers between devices, body(): weights.append(lax.ppermute(out_weight, 'x', ring))  37.1 us
    all_gather x1, waiting for transfers between devices, body(): gathered = lax.all_gather(normed, ('x', 'c'), axis=0, tiled=True)  22.4 us
    pallas_call x1, Pallas kernels, ffn(): pl.pallas_call(ffn_kernel, out_shape=jax.ShapeDtypeStruct((ROWS, 2048), B...  18.2 us
    all_to_all x1, blocking collectives, body(): lax.all_to_all(kv_pack, 'y', split_axis=0, concat_axis=0, tiled=True)  17.3 us
    all_to_all x1, blocking collectives, body(): lax.all_to_all(attended, ('z', 'y'), split_axis=0, concat_axis=0, tiled=T...  17.1 us
  transfers between devices with their start and end apart: 12, of which 6 were waited for; matrix products, arithmetic and copies ran while one was open for 0% of the time, Pallas kernels for 16%

profile of v1, /device:TPU:0, one launch (start us, length us, event | category | flops | bytes accessed | tf_op | source)
XLA Modules:
  0.0 336.3 jit_solution(6986358320536963733)
XLA Ops:
  6.5 0.0 copy-start.1
  6.5 0.0 all-gather.5.cloned.1.call-start
  6.5 3.0 shard_map.136
  9.5 17.3 %all_to_all.25 = bf16[4,800,128]{2,1,0:T(8,128)(2,1)} all-to-all(bf16[4,800,128]{2,1,0:T(8,128)(2,1)} %get-tuple-element.8), channel_id=1, replica_groups=mesh['z'=4,'y'=4,'x'=4,'c'=2] {'y'}, dimensions={0} | all-to-all | bytes 1638400 | tf_op jit(solution)/shard_map/all_to_all | solution.py:355
  26.8 0.0 all-gather.5.cloned.1.call-update
  26.8 0.0 copy-done.1
  26.9 1.6 collective-permute-start
  28.4 1.7 collective-permute-start.1
  30.2 1.8 collective-permute-start.2
  32.0 6.0 %all-to-all-start = ((bf16[16,96,128]{2,1,0:T(8,128)(2,1)}), bf16[16,96,128]{2,1,0:T(8,128)(2,1)S(1)}, u32[]{:S(2)}, u32[]{:S(2)}) async-start(bf16[16,96,128]{2,1,0:T(8,128)(2,1)} %get-tuple-element.7), calls=%async_computation | async-start | bytes 786432 | tf_op jit(solution)/shard_map/all_to_all | solution.py:356
  38.0 0.1 collective-permute-start.3
  38.1 15.1 %collective-permute-done.rest_1_ = bf16[256,2048]{1,0:T(8,128)(2,1)S(1)} collective-permute-done((bf16[256,2048]{1,0:T(8,128)(2,1)S(1)}, bf16[256,2048]{1,0:T(8,128)(2,1)S(1)}, u32[]{:S(2)}, u32[]{:S(2)}) %collective-permute-start) | collective-permute-done | bytes 1048608 | tf_op jit(solution)/shard_map/ppermute | solution.py:365
  53.2 0.0 copy-start.2
  53.2 0.0 collective-permute-start.4
  53.2 20.2 %collective-permute-done.1.rest_2_ = bf16[256,2048]{1,0:T(8,128)(2,1)S(1)} collective-permute-done((bf16[256,2048]{1,0:T(8,128)(2,1)S(1)}, bf16[256,2048]{1,0:T(8,128)(2,1)S(1)}, u32[]{:S(2)}, u32[]{:S(2)}) %collective-permute-start.1) | collective-permute-done | bytes 1048608 | tf_op jit(solution)/shard_map/ppermute | solution.py:365
  73.4 0.0 copy-start.3
  73.4 0.0 collective-permute-start.5
  73.4 1.8 collective-permute-done.2.rest_3_
  75.2 0.0 collective-permute-start.6
  75.2 0.0 all-to-all-done.q_ref
  75.2 0.0 copy-start.4
  75.2 0.0 all-gather.5.cloned.1.call-done.kv_ref
  75.2 0.7 copy-done.4
  75.9 52.3 %shard_map.137 = bf16[16,96,128]{2,1,0:T(8,128)(2,1)} custom-call(s32[4,110]{1,0:T(4,128)} %constant.46.clone.tab, s32[1]{0:T(128)} %bitcast.8.z_ref, bf16[16,96,128]{2,1,0:T(8,128)(2,1)} %copy-done.4, bf16[16,800,128]{2,1,0:T(8,128)(2,1)} %all-gather.5.cloned.1.call-done.kv_ref), custom_call_target="tpu_custom_call" | custom-call | flops 35000000512 | bytes 4000000 | tf_op jit(solution)/shard_map/pallas_call | solution.py:197
  128.2 0.0 copy-done.2
  128.2 0.0 copy-done.3
  128.2 17.1 %all_to_all.26.o_ref = bf16[16,96,128]{2,1,0:T(8,128)(2,1)} all-to-all(bf16[16,96,128]{2,1,0:T(8,128)(2,1)} %shard_map.137), channel_id=1, replica_groups=mesh['z'=4,'y'=4,'x'=4,'c'=2] {'z','y'}, dimensions={0} | all-to-all | bytes 786432 | tf_op jit(solution)/shard_map/all_to_all | solution.py:374
  145.3 2.0 shard_map.138
  147.3 3.5 %all-to-all-start.3 = ((bf16[8,96,256]{2,1,0:T(8,128)(2,1)}), bf16[8,96,256]{2,1,0:T(8,128)(2,1)S(1)}, u32[]{:S(2)}, u32[]{:S(2)}) async-start(bf16[8,96,256]{2,1,0:T(8,128)(2,1)} %shard_map.138), calls=%async_computation.3 | async-start | bytes 786432 | tf_op jit(solution)/shard_map/all_to_all | solution.py:375
  150.8 0.0 all-gather.7.cloned.1.call-start
  150.9 0.7 stack.36.place
  151.6 0.0 collective-permute-done.3.rest_4_
  151.6 0.0 collective-permute-done.4.rest_5_
  151.6 0.0 collective-permute-done.5.rest_6_
  151.6 0.0 collective-permute-done.6.rest_7_
  151.6 8.0 %all-to-all-done.3.a_ref = bf16[8,96,256]{2,1,0:T(8,128)(2,1)S(1)} async-done(((bf16[8,96,256]{2,1,0:T(8,128)(2,1)}), bf16[8,96,256]{2,1,0:T(8,128)(2,1)S(1)}, u32[]{:S(2)}, u32[]{:S(2)}) %all-to-all-start.3) | async-done | bytes 393248 | tf_op jit(solution)/shard_map/all_to_all | solution.py:375
  159.6 0.0 copy-start
  159.6 0.7 copy-done
  160.4 0.0 copy-start.5
  160.4 0.0 copy-start.6
  160.4 0.0 copy-start.7
  160.4 7.0 %shard_map.139.n_ref = bf16[96,2048]{1,0:T(8,128)(2,1)} custom-call(s32[9]{0:T(128)} %stack.36.place, bf16[8,96,256]{2,1,0:T(8,128)(2,1)} %copy-done, bf16[768,2048]{1,0:T(8,128)(2,1)} %stream_ref.1, f32[1,2048]{1,0:T(1,128)} %bitcast.22, f32[1,2048]{1,0:T(1,128)} %bitcast.23, bf16[256,2048]{1,0:T(8,128)(2,1)} %rest_0_.1, bf16[256,2048]{1,0:T(8,128)(2,1)} %copy-done.2, ...), custom_call_target="tpu_custom_call" | custom-call | flops 805306368 | bytes 9000000 | tf_op jit(solution)/shard_map/pallas_call | solution.py:266
  167.3 0.0 all-gather.7.cloned.1.call-update
  167.4 0.0 all-gather.9.cloned.1.call-start
  167.4 0.0 copy-done.5
  167.4 0.0 copy-done.6
  167.4 0.0 copy-done.7
  167.4 0.8 pad_maximum_fusion
  168.3 0.0 all-gather.9.cloned.1.call-update
  168.3 22.4 %all-gather.7.cloned.1.call-done.x_ref = bf16[768,2048]{1,0:T(8,128)(2,1)} async-done(((bf16[96,2048]{1,0:T(8,128)(2,1)}), bf16[768,2048]{1,0:T(8,128)(2,1)}) %all-gather.7.cloned.1.call-update) | async-done | bytes 3145744 | tf_op jit(solution)/shard_map/all_gather | solution.py:381
  190.7 74.3 %all-gather.9.cloned.1.call-done = bf16[33792,128]{1,0:T(8,128)(2,1)} async-done(((bf16[2112,128]{1,0:T(8,128)(2,1)}), bf16[33792,128]{1,0:T(8,128)(2,1)}) %all-gather.9.cloned.1.call-update) | async-done | bytes 8650768 | tf_op jit(solution)/shard_map/all_gather | solution.py:360
  265.1 18.2 %shard_map.140 = bf16[768,2048]{1,0:T(8,128)(2,1)} custom-call(bf16[768,2048]{1,0:T(8,128)(2,1)} %all-gather.7.cloned.1.call-done.x_ref, bf16[16,2112,128]{2,1,0:T(8,128)(2,1)} %bitcast.26), custom_call_target="tpu_custom_call" | custom-call | flops 6643777536 | bytes 15000000 | tf_op jit(solution)/shard_map/pallas_call | solution.py:304
  283.3 42.9 %all_to_all.27.p_ref = bf16[8,96,2048]{2,1,0:T(8,128)(2,1)} all-to-all(bf16[8,96,2048]{2,1,0:T(8,128)(2,1)} %bitcast.18), channel_id=1, replica_groups=mesh['z'=4,'y'=4,'x'=4,'c'=2] {'x','c'}, dimensions={0} | all-to-all | bytes 6291456 | tf_op jit(solution)/shard_map/all_to_all | solution.py:383
  326.1 3.6 %shard_map.141 = bf16[96,2048]{1,0:T(8,128)(2,1)} custom-call(bf16[8,96,2048]{2,1,0:T(8,128)(2,1)} %all_to_all.27.p_ref, bf16[96,2048]{1,0:T(8,128)(2,1)} %shard_map.139.n_ref, f32[1,2048]{1,0:T(1,128)} %bitcast.24, f32[1,2048]{1,0:T(1,128)} %bitcast.25), custom_call_target="tpu_custom_call" | custom-call | flops 4000000 | bytes 4000000 | tf_op jit(solution)/shard_map/pallas_call | solution.py:335
Async XLA Ops:
  6.5 20.3 %copy-start.1 = (bf16[256,2048]{1,0:T(8,128)(2,1)S(1)}, bf16[256,2048]{1,0:T(8,128)(2,1)}, u32[]{:S(2)}) copy-start(bf16[256,2048]{1,0:T(8,128)(2,1)} %rest_0_.1) | copy-start | bytes 3145732
  6.5 68.7 %all-gather.5.cloned.1.call-start = ((), (), s32[]{:S(2)}) async-start(), calls=%async_computation.5 | async-start | bytes 4096000 | tf_op jit(solution)/shard_map/all_gather | solution.py:357
  26.9 26.3 %collective-permute-start = (bf16[256,2048]{1,0:T(8,128)(2,1)S(1)}, bf16[256,2048]{1,0:T(8,128)(2,1)S(1)}, u32[]{:S(2)}, u32[]{:S(2)}) collective-permute-start(bf16[256,2048]{1,0:T(8,128)(2,1)S(1)} %copy-done.1), channel_id=1, source_target_pairs={{0,2},{2,4},{4,6},{6,0},{1,3},{3,5},{5,7},{7,1},{8,10},{10,12},{12... | collective-permute-start | bytes 3145736 | tf_op jit(solution)/shard_map/ppermute | solution.py:365
  28.4 45.0 %collective-permute-start.1 = (bf16[256,2048]{1,0:T(8,128)(2,1)S(1)}, bf16[256,2048]{1,0:T(8,128)(2,1)S(1)}, u32[]{:S(2)}, u32[]{:S(2)}) collective-permute-start(bf16[256,2048]{1,0:T(8,128)(2,1)S(1)} %copy-done.1), channel_id=1, source_target_pairs={{0,6},{2,0},{4,2},{6,4},{1,7},{3,1},{5,3},{7,5},{8,14},{10,8},{12,... | collective-permute-start | bytes 3145736 | tf_op jit(solution)/shard_map/ppermute | solution.py:365
  30.2 45.0 %collective-permute-start.2 = (bf16[256,2048]{1,0:T(8,128)(2,1)S(1)}, bf16[256,2048]{1,0:T(8,128)(2,1)}, u32[]{:S(2)}, u32[]{:S(2)}) collective-permute-start(bf16[256,2048]{1,0:T(8,128)(2,1)S(1)} %copy-done.1), channel_id=1, source_target_pairs={{0,4},{2,6},{4,0},{6,2},{1,5},{3,7},{5,1},{7,3},{8,12},{10,14},{12... | collective-permute-start | bytes 3145736 | tf_op jit(solution)/shard_map/ppermute | solution.py:365
  32.0 43.2 %all-to-all-start = ((bf16[16,96,128]{2,1,0:T(8,128)(2,1)}), bf16[16,96,128]{2,1,0:T(8,128)(2,1)S(1)}, u32[]{:S(2)}, u32[]{:S(2)}) async-start(bf16[16,96,128]{2,1,0:T(8,128)(2,1)} %get-tuple-element.7), calls=%async_computation | async-start | bytes 786432 | tf_op jit(solution)/shard_map/all_to_all | solution.py:356
  38.0 113.6 %collective-permute-start.3 = (bf16[256,2048]{1,0:T(8,128)(2,1)S(1)}, bf16[256,2048]{1,0:T(8,128)(2,1)}, u32[]{:S(2)}, u32[]{:S(2)}) collective-permute-start(bf16[256,2048]{1,0:T(8,128)(2,1)S(1)} %copy-done.1), channel_id=1, source_target_pairs={{0,1},{1,0},{2,3},{3,2},{4,5},{5,4},{6,7},{7,6},{8,9},{9,8},{10,11... | collective-permute-start | bytes 3145736 | tf_op jit(solution)/shard_map/ppermute | solution.py:368
  53.2 75.0 %copy-start.2 = (bf16[256,2048]{1,0:T(8,128)(2,1)}, bf16[256,2048]{1,0:T(8,128)(2,1)S(1)}, u32[]{:S(2)}) copy-start(bf16[256,2048]{1,0:T(8,128)(2,1)S(1)} %collective-permute-done.rest_1_) | copy-start | bytes 3145732
  53.2 98.4 %collective-permute-start.4 = (bf16[256,2048]{1,0:T(8,128)(2,1)S(1)}, bf16[256,2048]{1,0:T(8,128)(2,1)}, u32[]{:S(2)}, u32[]{:S(2)}) collective-permute-start(bf16[256,2048]{1,0:T(8,128)(2,1)S(1)} %collective-permute-done.rest_1_), channel_id=1, source_target_pairs={{0,1},{1,0},{2,3},{3,2},{4,5},{5,4},{6,7},{7,6},{8,9},{9,8},{10,11... | collective-permute-start | bytes 3145736 | tf_op jit(solution)/shard_map/ppermute | solution.py:368
  73.4 54.8 %copy-start.3 = (bf16[256,2048]{1,0:T(8,128)(2,1)}, bf16[256,2048]{1,0:T(8,128)(2,1)S(1)}, u32[]{:S(2)}) copy-start(bf16[256,2048]{1,0:T(8,128)(2,1)S(1)} %collective-permute-done.1.rest_2_) | copy-start | bytes 3145732
  73.4 78.2 %collective-permute-start.5 = (bf16[256,2048]{1,0:T(8,128)(2,1)S(1)}, bf16[256,2048]{1,0:T(8,128)(2,1)}, u32[]{:S(2)}, u32[]{:S(2)}) collective-permute-start(bf16[256,2048]{1,0:T(8,128)(2,1)S(1)} %collective-permute-done.1.rest_2_), channel_id=1, source_target_pairs={{0,1},{1,0},{2,3},{3,2},{4,5},{5,4},{6,7},{7,6},{8,9},{9,8},{10,11... | collective-permute-start | bytes 3145736 | tf_op jit(solution)/shard_map/ppermute | solution.py:368
  75.2 76.4 %collective-permute-start.6 = (bf16[256,2048]{1,0:T(8,128)(2,1)}, bf16[256,2048]{1,0:T(8,128)(2,1)}, u32[]{:S(2)}, u32[]{:S(2)}) collective-permute-start(bf16[256,2048]{1,0:T(8,128)(2,1)} %collective-permute-done.2.rest_3_), channel_id=1, source_target_pairs={{0,1},{1,0},{2,3},{3,2},{4,5},{5,4},{6,7},{7,6},{8,9},{9,8},{10,11... | collective-permute-start | bytes 3145736 | tf_op jit(solution)/shard_map/ppermute | solution.py:368
  75.2 0.7 copy-start.4
  147.3 12.3 %all-to-all-start.3 = ((bf16[8,96,256]{2,1,0:T(8,128)(2,1)}), bf16[8,96,256]{2,1,0:T(8,128)(2,1)S(1)}, u32[]{:S(2)}, u32[]{:S(2)}) async-start(bf16[8,96,256]{2,1,0:T(8,128)(2,1)} %shard_map.138), calls=%async_computation.3 | async-start | bytes 786432 | tf_op jit(solution)/shard_map/all_to_all | solution.py:375
  150.8 39.9 %all-gather.7.cloned.1.call-start = ((), (), s32[]{:S(2)}) async-start(), calls=%async_computation.6 | async-start | bytes 3538944 | tf_op jit(solution)/shard_map/all_gather | solution.py:381
  159.6 0.7 copy-start
  160.4 7.0 %copy-start.5 = (bf16[704,128]{1,0:T(8,128)(2,1)S(1)}, bf16[704,128]{1,0:T(8,128)(2,1)}, u32[]{:S(2)}) copy-start(bf16[704,128]{1,0:T(8,128)(2,1)} %param.24) | copy-start | bytes 540676
  160.4 7.1 %copy-start.6 = (bf16[128,704]{0,1:T(8,128)(2,1)S(1)}, bf16[128,704]{0,1:T(8,128)(2,1)}, u32[]{:S(2)}) copy-start(bf16[128,704]{0,1:T(8,128)(2,1)} %param.23) | copy-start | bytes 540676
  160.4 7.1 %copy-start.7 = (bf16[128,704]{0,1:T(8,128)(2,1)S(1)}, bf16[128,704]{0,1:T(8,128)(2,1)}, u32[]{:S(2)}) copy-start(bf16[128,704]{0,1:T(8,128)(2,1)} %param.22) | copy-start | bytes 540676
  167.4 97.7 %all-gather.9.cloned.1.call-start = ((), (), s32[]{:S(2)}) async-start(), calls=%async_computation.7 | async-start | bytes 9191424 | tf_op jit(solution)/shard_map/all_gather | solution.py:360
Sparse Core Ops, SparseCore 0:
  27.0 44.5 all-gather.4
  167.5 23.1 all-gather.6
  192.9 72.1 all-gather.8

commit v2 on v1

v2 whole, which is shorter than its diff:
```python
import functools
import jax
import jax.numpy as jnp
import numpy as np
from jax import lax
from jax.experimental import pallas as pl
from jax.experimental.pallas import tpu as pltpu
from jax.sharding import Mesh, PartitionSpec as P


ALPHA = 8.0**0.25
EPSILON = 1e-05
F32 = jnp.float32
BF16 = jnp.bfloat16

ROWS = 768
SUB = 192
HALF = 96
HD = 64
NSH = 16
PACK = 800
TILE = 256
TILES = SUB * NSH // TILE


def vmem():
    return pl.BlockSpec(memory_space=pltpu.VMEM)


def smem():
    return pl.BlockSpec(memory_space=pltpu.SMEM)


def params(mb=60):
    return pltpu.CompilerParams(vmem_limit_bytes=mb * 1024 * 1024)


def pack_kernel(q_ref, k_ref, v_ref, g_ref, qo_ref, kvo_ref):
    for h in range(4):
        cols = slice(h * HD, (h + 1) * HD)
        kvo_ref[h, 0:ROWS, 0:HD] = k_ref[:, cols]
        kvo_ref[h, 0:ROWS, HD : 2 * HD] = v_ref[:, cols]
        for y in range(4):
            at = y * SUB
            qo_ref[h * 4 + y, :, 0:HD] = q_ref[at : at + HALF, cols]
            qo_ref[h * 4 + y, :, HD : 2 * HD] = q_ref[at + HALF : at + SUB, cols]
        chunks = [-g_ref[h : h + 1, c * 128 : (c + 1) * 128] for c in range(6)]
        value = jnp.concatenate(chunks, axis=0)
        first = value.astype(BF16).astype(F32)
        second = (value - first).astype(BF16).astype(F32)
        third = value - first - second
        rest = jnp.zeros((PACK - ROWS - 18, 128), F32)
        kvo_ref[h, ROWS:PACK, :] = jnp.concatenate(
            [first, second, third, rest], axis=0
        ).astype(BF16)


def pack(q, k, v, g):
    return pl.pallas_call(
        pack_kernel,
        out_shape=(
            jax.ShapeDtypeStruct((NSH, HALF, 128), BF16),
            jax.ShapeDtypeStruct((4, PACK, 128), BF16),
        ),
        in_specs=[vmem()] * 4,
        out_specs=(vmem(), vmem()),
        compiler_params=params(),
        cost_estimate=pl.CostEstimate(flops=10**6, bytes_accessed=2500000, transcendentals=0),
    )(q, k, v, g)


def unit_table(steps):
    tables, counts = [], []
    for y in range(4):
        units = []
        for t in range(TILES):
            low = (TILE * t) // SUB
            for i, d in enumerate(steps):
                for z in range(4):
                    s = z * 4 + (y + d) % 4
                    if s <= low + 1:
                        units.append((t, i * 4 + z, s, int(s >= low)))
        if len(units) % 2:
            units.append((0, 0, NSH - 1, 1))
        counts.append(len(units))
        tables.append([(0, 0, 0, 0)] + units + [units[-1]])
    width = max(len(u) for u in tables) + 1
    out = np.zeros((4, 4, width), np.int32)
    for y in range(4):
        out[y, :, : len(tables[y])] = np.array(tables[y], np.int32).T
        out[y, :, -1] = counts[y]
    return out


def attend_kernel(chunks, first, final, *refs):
    refs = list(refs)
    tab, y_ref = refs[:2]
    kv_refs = refs[2 : 2 + chunks]
    at = 2 + chunks
    if first:
        q_ref, qt, top, acc = refs[at : at + 4]
        at += 4
    else:
        qt, top_in, acc_in = refs[at : at + 3]
        at += 3
        if final:
            o_ref = refs[at]
            at += 1
        else:
            top, acc = refs[at : at + 2]
            at += 2
    kaug, vt, qpos, s_a, s_b, p_a, p_b, al_a, al_b = refs[at : at + 9]
    at += 9
    if first:
        qrow = refs[at]
    if final:
        top, acc, oscr = refs[at : at + 3]
    y = y_ref[0]
    lane = lax.broadcasted_iota(jnp.int32, (128, 128), 1)
    for i in range(chunks):
        kv_ref = kv_refs[i]

        def per_shard(s, carry):
            gates = kv_ref[s, ROWS:PACK, :].astype(F32)
            square = jnp.concatenate(
                [jnp.zeros((HD, 128), F32), gates, jnp.zeros((32, 128), F32)], axis=0
            )
            turned = square.T
            to = i * 4 + s
            for c in range(6):
                part = kv_ref[s, c * 128 : (c + 1) * 128, :].astype(F32)
                mine = (lane == HD + c) | (lane == HD + 6 + c) | (lane == HD + 12 + c)
                kaug[to, c * 128 : (c + 1) * 128, :] = jnp.where(
                    lane < HD, part, jnp.where(mine, turned, 0.0)
                ).astype(BF16)
                vt[to, :, c * 128 : (c + 1) * 128] = part.T.astype(BF16)
            vt[to, 48:64, :] = jnp.ones((16, ROWS), BF16)
            return carry

        lax.fori_loop(0, 4, per_shard, 0)

    lane_h = lax.broadcasted_iota(jnp.int32, (HALF, 128), 1)
    lane_t = lax.broadcasted_iota(jnp.int32, (8, TILE), 1)
    if first:

        def per_query(s, carry):
            both = q_ref[s].astype(F32) * (HD**-0.5)
            ones = jnp.where(lane_h < HD + 18, 1.0, 0.0)
            qrow[s, 0:HALF, :] = jnp.where(lane_h < HD, both, ones)
            qrow[s, HALF:SUB, :] = jnp.where(lane_h < HD, pltpu.roll(both, HD, 1), ones)
            return carry

        lax.fori_loop(0, NSH, per_query, 0)
    for t in range(TILES):
        low = (TILE * t) // SUB
        edge = (low + 1) * SUB - TILE * t
        qpos[t] = y * SUB + jnp.where(
            lane_t < edge,
            low * ROWS + (SUB - edge) + lane_t,
            (low + 1) * ROWS + lane_t - edge,
        )
        if first:
            rows = jnp.concatenate(
                [qrow[low, SUB - edge : SUB, :], qrow[low + 1, 0 : TILE - edge, :]], axis=0
            )
            qt[t] = rows.T.astype(BF16)
    if first:
        acc[...] = jnp.zeros(acc.shape, F32)
        top[...] = jnp.full(top.shape, -1e30, F32)
    else:
        acc[...] = acc_in[...]
        top[...] = top_in[...]
    al_b[...] = jnp.ones(al_b.shape, F32)
    p_b[...] = jnp.zeros(p_b.shape, BF16)

    def scores(u, out):
        out[...] = jnp.dot(kaug[tab[y, 1, u]], qt[tab[y, 0, u]], preferred_element_type=F32)

    def gather(u, p_before, al_before):
        t = tab[y, 0, u]
        pv = jnp.dot(vt[tab[y, 1, u], 48:128, :], p_before[...], preferred_element_type=F32)
        acc[t] = acc[t] * al_before[0:1, :] + pv

    scores(1, s_a)

    def unit(u, s_now, s_next, p_before, p_now, al_before, al_now):
        def work(masked):
            scores(u + 1, s_next)
            gather(u - 1, p_before, al_before)
            t = tab[y, 0, u]
            before = top[t, 0:1, :]
            s = s_now[...]
            if masked:
                pos = tab[y, 2, u] * ROWS + lax.broadcasted_iota(jnp.int32, (ROWS, TILE), 0)
                s = jnp.where(pos <= qpos[t, 0:1, :], s, -1e30)
            high = jnp.maximum(before, jnp.max(s, axis=0, keepdims=True))
            p_now[...] = jnp.exp(s - high).astype(BF16)
            top[t, 0:1, :] = high
            al_now[0:1, :] = jnp.exp(before - high)

        lax.cond(tab[y, 3, u] == 1, lambda: work(True), lambda: work(False))

    def pair(i, carry):
        unit(2 * i + 1, s_a, s_b, p_b, p_a, al_b, al_a)
        unit(2 * i + 2, s_b, s_a, p_a, p_b, al_a, al_b)
        return carry

    count = tab[y, 0, tab.shape[2] - 1]
    lax.fori_loop(0, count // 2, pair, 0)
    gather(count, p_b, al_b)

    if final:

        def finish(t, carry):
            good = acc[t, 16:80, :] / acc[t, 0:1, :]
            full = jnp.concatenate([good, jnp.zeros((HD, TILE), F32)], axis=0)
            oscr[pl.ds(pl.multiple_of(t * TILE, TILE), TILE), :] = full.T
            return carry

        lax.fori_loop(0, TILES, finish, 0)

        def out(s, carry):
            row = pl.multiple_of(s * SUB, SUB)
            one = oscr[pl.ds(row, HALF), :]
            two = oscr[pl.ds(row + HALF, HALF), :]
            o_ref[s] = jnp.where(lane_h < HD, one, pltpu.roll(two, HD, 1)).astype(BF16)
            return carry

        lax.fori_loop(0, NSH, out, 0)


def attend(y, steps, kvs, q=None, state=None, final=False):
    chunks, first = len(kvs), q is not None
    state_shapes = (
        jax.ShapeDtypeStruct((TILES, 8, TILE), F32),
        jax.ShapeDtypeStruct((TILES, 80, TILE), F32),
    )
    scratch = [
        pltpu.VMEM((4 * chunks, ROWS, 128), BF16),
        pltpu.VMEM((4 * chunks, 128, ROWS), BF16),
        pltpu.VMEM((TILES, 8, TILE), jnp.int32),
        pltpu.VMEM((ROWS, TILE), F32),
        pltpu.VMEM((ROWS, TILE), F32),
        pltpu.VMEM((ROWS, TILE), BF16),
        pltpu.VMEM((ROWS, TILE), BF16),
        pltpu.VMEM((8, TILE), F32),
        pltpu.VMEM((8, TILE), F32),
    ]
    if first:
        outs = (jax.ShapeDtypeStruct((TILES, 128, TILE), BF16),) + state_shapes
        scratch += [pltpu.VMEM((NSH, SUB, 128), F32)]
        rest = [q]
    elif final:
        outs = jax.ShapeDtypeStruct((NSH, HALF, 128), BF16)
        scratch += [pltpu.VMEM(s.shape, F32) for s in state_shapes]
        scratch += [pltpu.VMEM((SUB * NSH, 128), F32)]
        rest = list(state)
    else:
        outs = state_shapes
        rest = list(state)
    table = unit_table(steps)
    share = int(table[:, 0, -1].mean())
    return pl.pallas_call(
        functools.partial(attend_kernel, chunks, first, final),
        out_shape=outs,
        in_specs=[smem(), smem()] + [vmem()] * (chunks + len(rest)),
        out_specs=jax.tree.map(lambda _: vmem(), outs),
        scratch_shapes=scratch,
        compiler_params=params(),
        cost_estimate=pl.CostEstimate(
            flops=share * 4 * 10**8, bytes_accessed=3 * 10**6, transcendentals=share * 200000
        ),
    )(jnp.asarray(table), y, *kvs, *rest)


def spread_kernel(o_ref, a_ref):
    for z in range(4):
        for y in range(4):
            for half in range(2):
                a_ref[2 * y + half, :, z * HD : (z + 1) * HD] = o_ref[
                    4 * z + y, :, half * HD : (half + 1) * HD
                ]


def spread(o):
    return pl.pallas_call(
        spread_kernel,
        out_shape=jax.ShapeDtypeStruct((8, HALF, 256), BF16),
        in_specs=[vmem()],
        out_specs=vmem(),
        compiler_params=params(),
        cost_estimate=pl.CostEstimate(flops=10**5, bytes_accessed=800000, transcendentals=0),
    )(o)


def norm_rows(matrix, gain, shift):
    centred = matrix - jnp.mean(matrix, axis=-1, keepdims=True)
    spread_ = jnp.mean(centred * centred, axis=-1, keepdims=True)
    return centred * lax.rsqrt(spread_ + EPSILON) * gain + shift


def mix_kernel(place, a_ref, stream_ref, gain_ref, bias_ref, *rest):
    w_refs, n_ref = rest[:8], rest[8]
    total = None
    for i in range(8):
        term = jnp.dot(a_ref[place[i]], w_refs[i][...], preferred_element_type=F32)
        total = term if total is None else total + term
    mixed = total.astype(BF16).astype(F32)
    matrix = ALPHA * stream_ref[...].astype(F32) + mixed
    n_ref[...] = norm_rows(matrix, gain_ref[...], bias_ref[...]).astype(BF16)


def mix(place, att, stream, gain, bias, weights):
    def whole(shape):
        return pl.BlockSpec(shape, lambda i, place: (0,) * len(shape))

    return pl.pallas_call(
        mix_kernel,
        out_shape=jax.ShapeDtypeStruct((HALF, 2048), BF16),
        grid_spec=pltpu.PrefetchScalarGridSpec(
            num_scalar_prefetch=1,
            grid=(1,),
            in_specs=[
                whole((8, HALF, 256)),
                pl.BlockSpec((HALF, 2048), lambda i, place: (place[8], 0)),
                whole((1, 2048)),
                whole((1, 2048)),
            ]
            + [whole((256, 2048))] * 8,
            out_specs=whole((HALF, 2048)),
        ),
        compiler_params=params(),
        cost_estimate=pl.CostEstimate(
            flops=2 * HALF * 2048 * 2048, bytes_accessed=9 * 10**6, transcendentals=0
        ),
    )(place, att, stream, gain, bias, *weights)


def ffn_kernel(x_ref, w_ref, out_ref, w_in, w_out, h_scr):
    @pl.when(pl.program_id(0) == 0)
    def _():
        for s in range(NSH):
            w_in[:, s * 128 : (s + 1) * 128] = w_ref[s, 0:1408, :]
            w_out[:, s * 128 : (s + 1) * 128] = w_ref[s, 1408:2112, :]

    both = lax.dot_general(
        x_ref[...], w_in[...], (((1,), (1,)), ((), ())), preferred_element_type=F32
    )
    gate, up = both[:, 0:704], both[:, 704:1408]
    h_scr[...] = (gate / (1.0 + jnp.exp(-gate)) * up).astype(BF16)
    out_ref[...] = jnp.dot(h_scr[...], w_out[...], preferred_element_type=F32).astype(BF16)


def ffn(x, w, tile=192):
    return pl.pallas_call(
        ffn_kernel,
        out_shape=jax.ShapeDtypeStruct((ROWS, 2048), BF16),
        grid=(ROWS // tile,),
        in_specs=[
            pl.BlockSpec((tile, 2048), lambda i: (i, 0)),
            pl.BlockSpec((NSH, 2112, 128), lambda i: (0, 0, 0)),
        ],
        out_specs=pl.BlockSpec((tile, 2048), lambda i: (i, 0)),
        scratch_shapes=[
            pltpu.VMEM((1408, 2048), BF16),
            pltpu.VMEM((704, 2048), BF16),
            pltpu.VMEM((tile, 704), BF16),
        ],
        compiler_params=params(),
        cost_estimate=pl.CostEstimate(
            flops=6 * ROWS * 2048 * 704, bytes_accessed=15 * 10**6, transcendentals=10**6
        ),
    )(x, w)


def last_kernel(p_ref, n_ref, gain_ref, bias_ref, o_ref):
    total = p_ref[0].astype(F32)
    for i in range(1, 8):
        total = total + p_ref[i].astype(F32)
    lowered = total.astype(BF16).astype(F32)
    matrix = ALPHA * n_ref[...].astype(F32) + lowered
    o_ref[...] = norm_rows(matrix, gain_ref[...], bias_ref[...]).astype(BF16)


def last(parts, normed, gain, bias):
    return pl.pallas_call(
        last_kernel,
        out_shape=jax.ShapeDtypeStruct((HALF, 2048), BF16),
        in_specs=[vmem()] * 4,
        out_specs=vmem(),
        compiler_params=params(),
        cost_estimate=pl.CostEstimate(
            flops=4 * 10**6, bytes_accessed=4 * 10**6, transcendentals=0
        ),
    )(parts, normed, gain, bias)


def body(
    queries, key_rows, value_rows, log_forget, stream_in, out_weight, mix_gain, mix_bias,
    gate_weight, up_weight, down_weight, ffn_gain, ffn_bias,
):
    yi = lax.axis_index("y").astype(jnp.int32)[None]
    xi = lax.axis_index("x")
    ci = lax.axis_index("c")

    def turn(value, axis, d):
        return lax.ppermute(value, axis, [(i, (i + d) % 4) for i in range(4)])

    q_pack, kv_pack = pack(queries, key_rows, value_rows, log_forget.T)
    kv_own = lax.all_to_all(kv_pack, "z", split_axis=0, concat_axis=0, tiled=True)
    q_mine = lax.all_to_all(q_pack, ("z", "y"), split_axis=0, concat_axis=0, tiled=True)
    kv_back, kv_ahead = turn(kv_own, "y", 1), turn(kv_own, "y", 3)
    kv_far = turn(kv_own, "y", 2)

    shards = jnp.concatenate([gate_weight.T, up_weight.T, down_weight], axis=0)
    ffn_all = lax.all_gather(shards, ("z", "y"), axis=0, tiled=False)

    weights, places = [out_weight], [2 * xi + ci]
    for d in (1, 3, 2):
        weights.append(turn(out_weight, "x", d))
        places.append(2 * ((xi + 4 - d) % 4) + ci)
    for i in range(4):
        weights.append(lax.ppermute(weights[i], "c", [(0, 1), (1, 0)]))
        places.append(places[i] + 1 - 2 * ci)
    own = 2 * xi + ci
    place = jnp.stack(places + [own]).astype(jnp.int32)

    qt, *state = attend(yi, (0,), [kv_own], q=q_mine)
    state = attend(yi, (3, 1), [kv_back, kv_ahead], state=(qt, *state))
    attended = attend(yi, (2,), [kv_far], state=(qt, *state), final=True)
    by_shard = lax.all_to_all(attended, ("z", "y"), split_axis=0, concat_axis=0, tiled=True)
    by_rows = lax.all_to_all(
        spread(by_shard), ("x", "c"), split_axis=0, concat_axis=0, tiled=True
    )
    normed = mix(place, by_rows, stream_in, mix_gain[None], mix_bias[None], weights)
    gathered = lax.all_gather(normed, ("x", "c"), axis=0, tiled=True)
    partial = ffn(gathered, ffn_all)
    parts = lax.all_to_all(
        partial.reshape(8, HALF, 2048), ("x", "c"), split_axis=0, concat_axis=0, tiled=True
    )
    return last(parts, normed, ffn_gain[None], ffn_bias[None])


def solution(mesh):
    fine = Mesh(mesh.devices.reshape(4, 4, 4, 2), ("z", "y", "x", "c"))
    sp, tp = ("z", "y"), ("x", "c")
    placed = (
        P(sp, tp), P(sp, tp), P(sp, tp), P(sp, tp), P(sp, None), P(tp, None), P(), P(),
        P(sp, tp), P(sp, tp), P(tp, sp), P(), P(),
    )

    return jax.shard_map(
        body, mesh=fine, in_specs=placed, out_specs=P(("z", "y", "x", "c"), None), check_vma=False
    )
```

time: 337 us -> 337 us (level)
  waiting for transfers between devices: 142 us -> 126 us
  starting transfers between devices: 14.8 us -> 22.3 us
  Pallas kernels: 86 us -> 91.4 us
    ppermute x3 -> x6, waiting for transfers between devices: 37.1 us -> 19.8 us  [turn(): return lax.ppermute(value, axis, [(i, (i + d) % 4) for i in range(4)])]
    ppermute x3 -> x6, starting transfers between devices: 5.12 us -> 11.5 us  [turn(): return lax.ppermute(value, axis, [(i, (i + d) % 4) for i in range(4)])]
    pallas_call x1 -> x3, Pallas kernels: 52.3 us -> 57.6 us  [attend(): pl.pallas_call(functools.partial(attend_kernel, chunks, first, final), ou...]
  transfers between devices with their start and end apart: 12 -> 14, of which waited for: 6 -> 5; matrix products, arithmetic and copies ran while one was open for 0% -> 0% of each run, Pallas kernels for 16% -> 18%
where the time goes in v2:
time: 337 us; the launch traced here: 336 us
  waiting for transfers between devices  126 us (37%)
  Pallas kernels  91.4 us (27%)
  blocking collectives  80.2 us (24%)
  starting transfers between devices  22.3 us (7%)
  between operations  13.5 us (4%)
    all_gather x1, waiting for transfers between devices, body(): ffn_all = lax.all_gather(shards, ('z', 'y'), axis=0, tiled=False)  74.3 us
    pallas_call x3, Pallas kernels, attend(): pl.pallas_call(functools.partial(attend_kernel, chunks, first, final), ou...  57.6 us
    all_to_all x1, blocking collectives, body(): lax.all_to_all(partial.reshape(8, HALF, 2048), ('x', 'c'), split_axis=0,...  42.9 us
    all_gather x1, waiting for transfers between devices, body(): gathered = lax.all_gather(normed, ('x', 'c'), axis=0, tiled=True)  22.4 us
    ppermute x6, waiting for transfers between devices, turn(): return lax.ppermute(value, axis, [(i, (i + d) % 4) for i in range(4)])  19.8 us
    all_to_all x1, blocking collectives, body(): lax.all_to_all(attended, ('z', 'y'), split_axis=0, concat_axis=0, tiled=T...  19.2 us
    pallas_call x1, Pallas kernels, ffn(): pl.pallas_call(ffn_kernel, out_shape=jax.ShapeDtypeStruct((ROWS, 2048), B...  18.2 us
    all_to_all x1, blocking collectives, body(): lax.all_to_all(kv_pack, 'z', split_axis=0, concat_axis=0, tiled=True)  18.2 us
  transfers between devices with their start and end apart: 14, of which 5 were waited for; matrix products, arithmetic and copies ran while one was open for 0% of the time, Pallas kernels for 18%

profile of v2, /device:TPU:0, one launch (start us, length us, event | category | flops | bytes accessed | tf_op | source)
XLA Modules:
  0.0 336.0 jit_solution(5605876672077124893)
XLA Ops:
  6.5 0.0 copy-start.1
  6.5 3.0 shard_map.154
  9.5 18.2 %all_to_all.25.refs_2_ = bf16[4,800,128]{2,1,0:T(8,128)(2,1)} all-to-all(bf16[4,800,128]{2,1,0:T(8,128)(2,1)} %get-tuple-element.12), channel_id=1, replica_groups=mesh['z'=4,'y'=4,'x'=4,'c'=2] {'z'}, dimensions={0} | all-to-all | bytes 1638400 | tf_op jit(solution)/shard_map/all_to_all | solution.py:410
  27.7 5.3 %all-to-all-start.1 = ((bf16[16,96,128]{2,1,0:T(8,128)(2,1)}), bf16[16,96,128]{2,1,0:T(8,128)(2,1)S(1)}, u32[]{:S(2)}, u32[]{:S(2)}) async-start(bf16[16,96,128]{2,1,0:T(8,128)(2,1)} %get-tuple-element.13), calls=%async_computation.1 | async-start | bytes 786432 | tf_op jit(solution)/shard_map/all_to_all | solution.py:411
  33.0 0.0 copy-done.1
  33.0 1.6 collective-permute-start.3
  34.6 1.7 collective-permute-start.4
  36.3 1.8 collective-permute-start.5
  38.1 1.9 collective-permute-start.1
  40.0 1.3 collective-permute-start.2
  41.4 1.0 all-to-all-done.1.refs_3_
  42.4 0.0 copy-start.5
  42.4 0.7 copy-done.5
  43.1 0.0 copy-start.4
  43.1 16.7 %shard_map.155 = (bf16[12,128,256]{2,1,0:T(8,128)(2,1)}, f32[12,8,256]{2,1,0:T(8,128)}, f32[12,80,256]{2,1,0:T(8,128)}) custom-call(s32[4,4,33]{2,1,0:T(4,128)} %constant.49.clone.refs_0_, s32[1]{0:T(128)} %bitcast.8.refs_1_, bf16[4,800,128]{2,1,0:T(8,128)(2,1)} %all_to_all.25.refs_2_, bf16[16,96,128]{2,1,0:T(8,128)(2,1)} %copy-done.5), custom_call_target="tpu_custom_call" | custom-call | flops 10800000000 | bytes 3000000 | tf_op jit(solution)/shard_map/pallas_call | solution.py:263
  59.9 0.0 collective-permute-done.3.rest_1_
  59.9 0.0 copy-start.2
  59.9 0.0 collective-permute-start.6
  59.9 19.8 %collective-permute-done.4.rest_2_ = bf16[256,2048]{1,0:T(8,128)(2,1)S(1)} collective-permute-done((bf16[256,2048]{1,0:T(8,128)(2,1)S(1)}, bf16[256,2048]{1,0:T(8,128)(2,1)S(1)}, u32[]{:S(2)}, u32[]{:S(2)}) %collective-permute-start.4) | collective-permute-done | bytes 1048608 | tf_op jit(solution)/shard_map/ppermute | solution.py:407
  79.7 0.0 copy-done.4
  79.7 0.0 copy-start.3
  79.7 3.1 collective-permute-start
  82.8 0.0 collective-permute-done.5.rest_3_
  82.8 0.0 collective-permute-start.7
  82.8 0.0 collective-permute-done.1.refs_2_
  82.8 0.5 collective-permute-start.8
  83.3 0.0 collective-permute-done.2.refs_3_
  83.3 0.1 collective-permute-start.9
  83.4 24.8 %shard_map.156 = (f32[12,8,256]{2,1,0:T(8,128)}, f32[12,80,256]{2,1,0:T(8,128)}) custom-call(s32[4,4,59]{2,1,0:T(4,128)} %constant.50.clone.refs_0_, s32[1]{0:T(128)} %bitcast.8.refs_1_, bf16[4,800,128]{2,1,0:T(8,128)(2,1)} %collective-permute-done.1.refs_2_, bf16[4,800,128]{2,1,0:T(8,128)(2,1)} %collective-permute-done.2.refs_3_, ...), custom_call_target="tpu_custom_call" | custom-call | flops 21600000000 | bytes 3000000 | tf_op jit(solution)/shard_map/pallas_call | solution.py:263
  108.2 0.0 copy-done.2
  108.2 0.0 copy-done.3
  108.2 0.0 collective-permute-done.refs_2_
  108.2 16.2 %shard_map.157 = bf16[16,96,128]{2,1,0:T(8,128)(2,1)} custom-call(s32[4,4,33]{2,1,0:T(4,128)} %constant.51.clone.refs_0_, s32[1]{0:T(128)} %bitcast.8.refs_1_, bf16[4,800,128]{2,1,0:T(8,128)(2,1)} %collective-permute-done.refs_2_, bf16[12,128,256]{2,1,0:T(8,128)(2,1)} %get-tuple-element.14.refs_4_.refs_3_, f32[12,8,256]{2,1,0:T(8,128)} %get-tuple-element.17.refs_4_, ...), custom_call_target="tpu_custom_call" | custom-call | flops 10800000000 | bytes 3000000 | tf_op jit(solution)/shard_map/pallas_call | solution.py:263
  124.4 19.2 %all_to_all.26.o_ref = bf16[16,96,128]{2,1,0:T(8,128)(2,1)} all-to-all(bf16[16,96,128]{2,1,0:T(8,128)(2,1)} %shard_map.157), channel_id=1, replica_groups=mesh['z'=4,'y'=4,'x'=4,'c'=2] {'z','y'}, dimensions={0} | all-to-all | bytes 786432 | tf_op jit(solution)/shard_map/all_to_all | solution.py:431
  143.5 2.0 shard_map.158
  145.5 4.6 %all-to-all-start.3 = ((bf16[8,96,256]{2,1,0:T(8,128)(2,1)}), bf16[8,96,256]{2,1,0:T(8,128)(2,1)S(1)}, u32[]{:S(2)}, u32[]{:S(2)}) async-start(bf16[8,96,256]{2,1,0:T(8,128)(2,1)} %shard_map.158), calls=%async_computation.3 | async-start | bytes 786432 | tf_op jit(solution)/shard_map/all_to_all | solution.py:432
  150.1 0.2 all-gather.4.cloned.1.call-start
  150.4 0.7 stack.36.place
  151.1 0.0 collective-permute-done.6.rest_4_
  151.1 0.0 collective-permute-done.7.rest_5_
  151.1 0.0 collective-permute-done.8.rest_6_
  151.1 0.0 collective-permute-done.9.rest_7_
  151.1 8.0 %all-to-all-done.3.a_ref = bf16[8,96,256]{2,1,0:T(8,128)(2,1)S(1)} async-done(((bf16[8,96,256]{2,1,0:T(8,128)(2,1)}), bf16[8,96,256]{2,1,0:T(8,128)(2,1)S(1)}, u32[]{:S(2)}, u32[]{:S(2)}) %all-to-all-start.3) | async-done | bytes 393248 | tf_op jit(solution)/shard_map/all_to_all | solution.py:432
  159.1 0.0 copy-start
  159.1 0.7 copy-done
  159.8 0.0 copy-start.6
  159.8 0.0 copy-start.7
  159.8 0.0 copy-start.8
  159.8 7.0 %shard_map.159.n_ref = bf16[96,2048]{1,0:T(8,128)(2,1)} custom-call(s32[9]{0:T(128)} %stack.36.place, bf16[8,96,256]{2,1,0:T(8,128)(2,1)} %copy-done, bf16[768,2048]{1,0:T(8,128)(2,1)} %stream_ref.1, f32[1,2048]{1,0:T(1,128)} %bitcast.22, f32[1,2048]{1,0:T(1,128)} %bitcast.23, bf16[256,2048]{1,0:T(8,128)(2,1)} %rest_0_.1, bf16[256,2048]{1,0:T(8,128)(2,1)} %copy-done.2, ...), custom_call_target="tpu_custom_call" | custom-call | flops 805306368 | bytes 9000000 | tf_op jit(solution)/shard_map/pallas_call | solution.py:317
  166.8 0.0 all-gather.4.cloned.1.call-update
  166.8 0.0 all-gather.6.cloned.1.call-start
  166.8 0.0 copy-done.6
  166.9 0.0 copy-done.7
  166.9 0.0 copy-done.8
  166.9 0.8 pad_maximum_fusion
  167.7 0.0 all-gather.6.cloned.1.call-update
  167.7 22.4 %all-gather.4.cloned.1.call-done.x_ref = bf16[768,2048]{1,0:T(8,128)(2,1)} async-done(((bf16[96,2048]{1,0:T(8,128)(2,1)}), bf16[768,2048]{1,0:T(8,128)(2,1)}) %all-gather.4.cloned.1.call-update) | async-done | bytes 3145744 | tf_op jit(solution)/shard_map/all_gather | solution.py:436
  190.2 74.3 %all-gather.6.cloned.1.call-done = bf16[33792,128]{1,0:T(8,128)(2,1)} async-done(((bf16[2112,128]{1,0:T(8,128)(2,1)}), bf16[33792,128]{1,0:T(8,128)(2,1)}) %all-gather.6.cloned.1.call-update) | async-done | bytes 8650768 | tf_op jit(solution)/shard_map/all_gather | solution.py:416
  264.5 18.2 %shard_map.160 = bf16[768,2048]{1,0:T(8,128)(2,1)} custom-call(bf16[768,2048]{1,0:T(8,128)(2,1)} %all-gather.4.cloned.1.call-done.x_ref, bf16[16,2112,128]{2,1,0:T(8,128)(2,1)} %bitcast.26), custom_call_target="tpu_custom_call" | custom-call | flops 6643777536 | bytes 15000000 | tf_op jit(solution)/shard_map/pallas_call | solution.py:355
  282.7 42.9 %all_to_all.27.p_ref = bf16[8,96,2048]{2,1,0:T(8,128)(2,1)} all-to-all(bf16[8,96,2048]{2,1,0:T(8,128)(2,1)} %bitcast.18), channel_id=1, replica_groups=mesh['z'=4,'y'=4,'x'=4,'c'=2] {'x','c'}, dimensions={0} | all-to-all | bytes 6291456 | tf_op jit(solution)/shard_map/all_to_all | solution.py:438
  325.6 3.6 %shard_map.161 = bf16[96,2048]{1,0:T(8,128)(2,1)} custom-call(bf16[8,96,2048]{2,1,0:T(8,128)(2,1)} %all_to_all.27.p_ref, bf16[96,2048]{1,0:T(8,128)(2,1)} %shard_map.159.n_ref, f32[1,2048]{1,0:T(1,128)} %bitcast.24, f32[1,2048]{1,0:T(1,128)} %bitcast.25), custom_call_target="tpu_custom_call" | custom-call | flops 4000000 | bytes 4000000 | tf_op jit(solution)/shard_map/pallas_call | solution.py:386
Async XLA Ops:
  6.5 26.5 %copy-start.1 = (bf16[256,2048]{1,0:T(8,128)(2,1)S(1)}, bf16[256,2048]{1,0:T(8,128)(2,1)}, u32[]{:S(2)}) copy-start(bf16[256,2048]{1,0:T(8,128)(2,1)} %rest_0_.1) | copy-start | bytes 3145732
  27.7 14.7 %all-to-all-start.1 = ((bf16[16,96,128]{2,1,0:T(8,128)(2,1)}), bf16[16,96,128]{2,1,0:T(8,128)(2,1)S(1)}, u32[]{:S(2)}, u32[]{:S(2)}) async-start(bf16[16,96,128]{2,1,0:T(8,128)(2,1)} %get-tuple-element.13), calls=%async_computation.1 | async-start | bytes 786432 | tf_op jit(solution)/shard_map/all_to_all | solution.py:411
  33.0 26.9 %collective-permute-start.3 = (bf16[256,2048]{1,0:T(8,128)(2,1)S(1)}, bf16[256,2048]{1,0:T(8,128)(2,1)S(1)}, u32[]{:S(2)}, u32[]{:S(2)}) collective-permute-start(bf16[256,2048]{1,0:T(8,128)(2,1)S(1)} %copy-done.1), channel_id=1, source_target_pairs={{0,2},{2,4},{4,6},{6,0},{1,3},{3,5},{5,7},{7,1},{8,10},{10,12},{12... | collective-permute-start | bytes 3145736 | tf_op jit(solution)/shard_map/ppermute | solution.py:407
  34.6 45.1 %collective-permute-start.4 = (bf16[256,2048]{1,0:T(8,128)(2,1)S(1)}, bf16[256,2048]{1,0:T(8,128)(2,1)S(1)}, u32[]{:S(2)}, u32[]{:S(2)}) collective-permute-start(bf16[256,2048]{1,0:T(8,128)(2,1)S(1)} %copy-done.1), channel_id=1, source_target_pairs={{0,6},{2,0},{4,2},{6,4},{1,7},{3,1},{5,3},{7,5},{8,14},{10,8},{12,... | collective-permute-start | bytes 3145736 | tf_op jit(solution)/shard_map/ppermute | solution.py:407
  36.3 46.5 %collective-permute-start.5 = (bf16[256,2048]{1,0:T(8,128)(2,1)S(1)}, bf16[256,2048]{1,0:T(8,128)(2,1)}, u32[]{:S(2)}, u32[]{:S(2)}) collective-permute-start(bf16[256,2048]{1,0:T(8,128)(2,1)S(1)} %copy-done.1), channel_id=1, source_target_pairs={{0,4},{2,6},{4,0},{6,2},{1,5},{3,7},{5,1},{7,3},{8,12},{10,14},{12... | collective-permute-start | bytes 3145736 | tf_op jit(solution)/shard_map/ppermute | solution.py:407
  38.1 44.7 %collective-permute-start.1 = (bf16[4,800,128]{2,1,0:T(8,128)(2,1)}, bf16[4,800,128]{2,1,0:T(8,128)(2,1)}, u32[]{:S(2)}, u32[]{:S(2)}) collective-permute-start(bf16[4,800,128]{2,1,0:T(8,128)(2,1)} %all_to_all.25.refs_2_), channel_id=1, source_target_pairs={{0,8},{8,16},{16,24},{24,0},{1,9},{9,17},{17,25},{25,1},{2,10},{10... | collective-permute-start | bytes 2457608 | tf_op jit(solution)/shard_map/ppermute | solution.py:407
  40.0 43.3 %collective-permute-start.2 = (bf16[4,800,128]{2,1,0:T(8,128)(2,1)}, bf16[4,800,128]{2,1,0:T(8,128)(2,1)}, u32[]{:S(2)}, u32[]{:S(2)}) collective-permute-start(bf16[4,800,128]{2,1,0:T(8,128)(2,1)} %all_to_all.25.refs_2_), channel_id=1, source_target_pairs={{0,24},{8,0},{16,8},{24,16},{1,25},{9,1},{17,9},{25,17},{2,26},{10... | collective-permute-start | bytes 2457608 | tf_op jit(solution)/shard_map/ppermute | solution.py:407
  42.4 0.7 copy-start.5
  43.1 36.5 %copy-start.4 = (bf16[4,800,128]{2,1,0:T(8,128)(2,1)S(1)}, bf16[4,800,128]{2,1,0:T(8,128)(2,1)}, u32[]{:S(2)}) copy-start(bf16[4,800,128]{2,1,0:T(8,128)(2,1)} %all_to_all.25.refs_2_) | copy-start | bytes 2457604
  59.9 48.3 %copy-start.2 = (bf16[256,2048]{1,0:T(8,128)(2,1)}, bf16[256,2048]{1,0:T(8,128)(2,1)S(1)}, u32[]{:S(2)}) copy-start(bf16[256,2048]{1,0:T(8,128)(2,1)S(1)} %collective-permute-done.3.rest_1_) | copy-start | bytes 3145732
  59.9 91.2 %collective-permute-start.6 = (bf16[256,2048]{1,0:T(8,128)(2,1)S(1)}, bf16[256,2048]{1,0:T(8,128)(2,1)}, u32[]{:S(2)}, u32[]{:S(2)}) collective-permute-start(bf16[256,2048]{1,0:T(8,128)(2,1)S(1)} %copy-done.1), channel_id=1, source_target_pairs={{0,1},{1,0},{2,3},{3,2},{4,5},{5,4},{6,7},{7,6},{8,9},{9,8},{10,11... | collective-permute-start | bytes 3145736 | tf_op jit(solution)/shard_map/ppermute | solution.py:423
  79.7 28.5 %copy-start.3 = (bf16[256,2048]{1,0:T(8,128)(2,1)}, bf16[256,2048]{1,0:T(8,128)(2,1)S(1)}, u32[]{:S(2)}) copy-start(bf16[256,2048]{1,0:T(8,128)(2,1)S(1)} %collective-permute-done.4.rest_2_) | copy-start | bytes 3145732
  79.7 28.5 %collective-permute-start = (bf16[4,800,128]{2,1,0:T(8,128)(2,1)S(1)}, bf16[4,800,128]{2,1,0:T(8,128)(2,1)}, u32[]{:S(2)}, u32[]{:S(2)}) collective-permute-start(bf16[4,800,128]{2,1,0:T(8,128)(2,1)S(1)} %copy-done.4), channel_id=1, source_target_pairs={{0,16},{8,24},{16,0},{24,8},{1,17},{9,25},{17,1},{25,9},{2,18},{10... | collective-permute-start | bytes 2457608 | tf_op jit(solution)/shard_map/ppermute | solution.py:407
  82.8 68.3 %collective-permute-start.7 = (bf16[256,2048]{1,0:T(8,128)(2,1)S(1)}, bf16[256,2048]{1,0:T(8,128)(2,1)}, u32[]{:S(2)}, u32[]{:S(2)}) collective-permute-start(bf16[256,2048]{1,0:T(8,128)(2,1)S(1)} %collective-permute-done.3.rest_1_), channel_id=1, source_target_pairs={{0,1},{1,0},{2,3},{3,2},{4,5},{5,4},{6,7},{7,6},{8,9},{9,8},{10,11... | collective-permute-start | bytes 3145736 | tf_op jit(solution)/shard_map/ppermute | solution.py:423
  82.8 68.3 %collective-permute-start.8 = (bf16[256,2048]{1,0:T(8,128)(2,1)S(1)}, bf16[256,2048]{1,0:T(8,128)(2,1)}, u32[]{:S(2)}, u32[]{:S(2)}) collective-permute-start(bf16[256,2048]{1,0:T(8,128)(2,1)S(1)} %collective-permute-done.4.rest_2_), channel_id=1, source_target_pairs={{0,1},{1,0},{2,3},{3,2},{4,5},{5,4},{6,7},{7,6},{8,9},{9,8},{10,11... | collective-permute-start | bytes 3145736 | tf_op jit(solution)/shard_map/ppermute | solution.py:423
  83.3 67.8 %collective-permute-start.9 = (bf16[256,2048]{1,0:T(8,128)(2,1)}, bf16[256,2048]{1,0:T(8,128)(2,1)}, u32[]{:S(2)}, u32[]{:S(2)}) collective-permute-start(bf16[256,2048]{1,0:T(8,128)(2,1)} %collective-permute-done.5.rest_3_), channel_id=1, source_target_pairs={{0,1},{1,0},{2,3},{3,2},{4,5},{5,4},{6,7},{7,6},{8,9},{9,8},{10,11... | collective-permute-start | bytes 3145736 | tf_op jit(solution)/shard_map/ppermute | solution.py:423
  145.5 13.5 %all-to-all-start.3 = ((bf16[8,96,256]{2,1,0:T(8,128)(2,1)}), bf16[8,96,256]{2,1,0:T(8,128)(2,1)S(1)}, u32[]{:S(2)}, u32[]{:S(2)}) async-start(bf16[8,96,256]{2,1,0:T(8,128)(2,1)} %shard_map.158), calls=%async_computation.3 | async-start | bytes 786432 | tf_op jit(solution)/shard_map/all_to_all | solution.py:432
  150.1 40.0 %all-gather.4.cloned.1.call-start = ((), (), s32[]{:S(2)}) async-start(), calls=%async_computation.5 | async-start | bytes 3538944 | tf_op jit(solution)/shard_map/all_gather | solution.py:436
  159.1 0.7 copy-start
  159.8 7.0 %copy-start.6 = (bf16[704,128]{1,0:T(8,128)(2,1)S(1)}, bf16[704,128]{1,0:T(8,128)(2,1)}, u32[]{:S(2)}) copy-start(bf16[704,128]{1,0:T(8,128)(2,1)} %param.26) | copy-start | bytes 540676
  159.8 7.1 %copy-start.7 = (bf16[128,704]{0,1:T(8,128)(2,1)S(1)}, bf16[128,704]{0,1:T(8,128)(2,1)}, u32[]{:S(2)}) copy-start(bf16[128,704]{0,1:T(8,128)(2,1)} %param.25) | copy-start | bytes 540676
  159.8 7.1 %copy-start.8 = (bf16[128,704]{0,1:T(8,128)(2,1)S(1)}, bf16[128,704]{0,1:T(8,128)(2,1)}, u32[]{:S(2)}) copy-start(bf16[128,704]{0,1:T(8,128)(2,1)} %param.24) | copy-start | bytes 540676
  166.8 97.7 %all-gather.6.cloned.1.call-start = ((), (), s32[]{:S(2)}) async-start(), calls=%async_computation.6 | async-start | bytes 9191424 | tf_op jit(solution)/shard_map/all_gather | solution.py:416
Sparse Core Ops, SparseCore 0:
  166.9 23.2 all-gather.3
  192.3 72.1 all-gather.5

commit v3 on v2

--- a/solution.py
+++ b/solution.py
@@ -299,84 +299,153 @@
     return centred * lax.rsqrt(spread_ + EPSILON) * gain + shift
 
 
-def mix_kernel(place, a_ref, stream_ref, gain_ref, bias_ref, *rest):
-    w_refs, n_ref = rest[:8], rest[8]
-    total = None
-    for i in range(8):
-        term = jnp.dot(a_ref[place[i]], w_refs[i][...], preferred_element_type=F32)
-        total = term if total is None else total + term
-    mixed = total.astype(BF16).astype(F32)
-    matrix = ALPHA * stream_ref[...].astype(F32) + mixed
-    n_ref[...] = norm_rows(matrix, gain_ref[...], bias_ref[...]).astype(BF16)
-
-
-def mix(place, att, stream, gain, bias, weights):
-    def whole(shape):
-        return pl.BlockSpec(shape, lambda i, place: (0,) * len(shape))
-
+def mix_kernel(place, a_ref, stream_ref, gain_ref, bias_ref, same_ref, other_ref, n_ref, total):
+    c, x = place[0], pl.program_id(0)
+    term = jnp.dot(a_ref[2 * x + c], same_ref[0], preferred_element_type=F32)
+    term = term + jnp.dot(a_ref[2 * x + 1 - c], other_ref[0], preferred_element_type=F32)
+
+    @pl.when(x == 0)
+    def _():
+        total[...] = term
+
+    @pl.when(x > 0)
+    def _():
+        total[...] += term
+
+    @pl.when(x == 3)
+    def _():
+        mixed = total[...].astype(BF16).astype(F32)
+        matrix = ALPHA * stream_ref[...].astype(F32) + mixed
+        n_ref[...] = norm_rows(matrix, gain_ref[...], bias_ref[...]).astype(BF16)
+
+
+def whole(shape):
+    return pl.BlockSpec(shape, lambda i, place: (0,) * len(shape))
+
+
+def along(shape):
+    return pl.BlockSpec((1, *shape), lambda i, place: (i,) + (0,) * len(shape))
+
+
+def mix(place, att, stream, gain, bias, same, other):
     return pl.pallas_call(
         mix_kernel,
         out_shape=jax.ShapeDtypeStruct((HALF, 2048), BF16),
         grid_spec=pltpu.PrefetchScalarGridSpec(
             num_scalar_prefetch=1,
-            grid=(1,),
+            grid=(4,),
             in_specs=[
                 whole((8, HALF, 256)),
-                pl.BlockSpec((HALF, 2048), lambda i, place: (place[8], 0)),
+                pl.BlockSpec((HALF, 2048), lambda i, place: (place[1], 0)),
                 whole((1, 2048)),
                 whole((1, 2048)),
-            ]
-            + [whole((256, 2048))] * 8,
+                along((256, 2048)),
+                along((256, 2048)),
+            ],
             out_specs=whole((HALF, 2048)),
+            scratch_shapes=[pltpu.VMEM((HALF, 2048), F32)],
         ),
         compiler_params=params(),
         cost_estimate=pl.CostEstimate(
             flops=2 * HALF * 2048 * 2048, bytes_accessed=9 * 10**6, transcendentals=0
         ),
-    )(place, att, stream, gain, bias, *weights)
-
-
-def ffn_kernel(x_ref, w_ref, out_ref, w_in, w_out, h_scr):
-    @pl.when(pl.program_id(0) == 0)
+    )(place, att, stream, gain, bias, same, other)
+
+
+BLOCKS = 3
+
+
+def prepare_kernel(w_ref, in_ref, out_ref):
+    for j in range(BLOCKS):
+        live = min(256, 704 - 256 * j)
+        for part in range(2):
+            at = 704 * part + 256 * j
+            in_ref[j, :, 256 * part : 256 * part + live] = w_ref[0, at : at + live, :].T
+            if live < 256:
+                in_ref[j, :, 256 * part + live : 256 * part + 256] = jnp.zeros(
+                    (128, 256 - live), BF16
+                )
+        at = 1408 + 256 * j
+        out_ref[j, 0:live, :] = w_ref[0, at : at + live, :]
+        if live < 256:
+            out_ref[j, live:256, :] = jnp.zeros((256 - live, 128), BF16)
+
+
+def prepare(w):
+    return pl.pallas_call(
+        prepare_kernel,
+        out_shape=(
+            jax.ShapeDtypeStruct((BLOCKS, 2048, 512), BF16),
+            jax.ShapeDtypeStruct((BLOCKS, 256, 2048), BF16),
+        ),
+        grid=(NSH,),
+        in_specs=[pl.BlockSpec((1, 2112, 128), lambda s: (s, 0, 0))],
+        out_specs=(
+            pl.BlockSpec((BLOCKS, 128, 512), lambda s: (0, s, 0)),
+            pl.BlockSpec((BLOCKS, 256, 128), lambda s: (0, 0, s)),
+        ),
+        compiler_params=params(),
+        cost_estimate=pl.CostEstimate(
+            flops=10**9, bytes_accessed=17 * 10**6, transcendentals=0
+        ),
+    )(w)
+
+
+def ffn_kernel(count, place, *refs):
+    x_refs = refs[: 2 * count]
+    in_ref, out_ref, same_ref, other_ref, total = refs[2 * count :]
+    j = pl.program_id(0)
+    x = jnp.concatenate([r[0] for r in x_refs], axis=0)
+    both = jnp.dot(x, in_ref[0], preferred_element_type=F32)
+    gate, up = both[:, 0:256], both[:, 256:512]
+    hidden = (gate / (1.0 + jnp.exp(-gate)) * up).astype(BF16)
+    term = jnp.dot(hidden, out_ref[0], preferred_element_type=F32)
+
+    @pl.when(j == 0)
     def _():
-        for s in range(NSH):
-            w_in[:, s * 128 : (s + 1) * 128] = w_ref[s, 0:1408, :]
-            w_out[:, s * 128 : (s + 1) * 128] = w_ref[s, 1408:2112, :]
-
-    both = lax.dot_general(
-        x_ref[...], w_in[...], (((1,), (1,)), ((), ())), preferred_element_type=F32
-    )
-    gate, up = both[:, 0:704], both[:, 704:1408]
-    h_scr[...] = (gate / (1.0 + jnp.exp(-gate)) * up).astype(BF16)
-    out_ref[...] = jnp.dot(h_scr[...], w_out[...], preferred_element_type=F32).astype(BF16)
-
-
-def ffn(x, w, tile=192):
-    return pl.pallas_call(
-        ffn_kernel,
-        out_shape=jax.ShapeDtypeStruct((ROWS, 2048), BF16),
-        grid=(ROWS // tile,),
-        in_specs=[
-            pl.BlockSpec((tile, 2048), lambda i: (i, 0)),
-            pl.BlockSpec((NSH, 2112, 128), lambda i: (0, 0, 0)),
-        ],
-        out_specs=pl.BlockSpec((tile, 2048), lambda i: (i, 0)),
-        scratch_shapes=[
-            pltpu.VMEM((1408, 2048), BF16),
-            pltpu.VMEM((704, 2048), BF16),
-            pltpu.VMEM((tile, 704), BF16),
-        ],
+        total[...] = term
+
+    @pl.when(j == 1)
+    def _():
+        total[...] += term
+
+    @pl.when(j == BLOCKS - 1)
+    def _():
+        out = (total[...] + term).astype(BF16)
+        for i in range(count):
+            same_ref[i] = out[i * HALF : (i + 1) * HALF]
+            other_ref[i] = out[(count + i) * HALF : (count + i + 1) * HALF]
+
+
+def ffn(count, place, gathered, w_in, w_out):
+    def block(i):
+        return pl.BlockSpec((1, HALF, 2048), lambda g, place: (place[i], 0, 0))
+
+    shape = jax.ShapeDtypeStruct((count, HALF, 2048), BF16)
+    rows = 2 * count * HALF
+    return pl.pallas_call(
+        functools.partial(ffn_kernel, count),
+        out_shape=(shape, shape),
+        grid_spec=pltpu.PrefetchScalarGridSpec(
+            num_scalar_prefetch=1,
+            grid=(BLOCKS,),
+            in_specs=[block(i) for i in range(2 * count)]
+            + [along((2048, 512)), along((256, 2048))],
+            out_specs=(whole((count, HALF, 2048)),) * 2,
+            scratch_shapes=[pltpu.VMEM((rows, 2048), F32)],
+        ),
         compiler_params=params(),
         cost_estimate=pl.CostEstimate(
-            flops=6 * ROWS * 2048 * 704, bytes_accessed=15 * 10**6, transcendentals=10**6
-        ),
-    )(x, w)
-
-
-def last_kernel(p_ref, n_ref, gain_ref, bias_ref, o_ref):
-    total = p_ref[0].astype(F32)
-    for i in range(1, 8):
-        total = total + p_ref[i].astype(F32)
+            flops=6 * rows * 2048 * 704, bytes_accessed=10**7, transcendentals=rows * 704
+        ),
+    )(place, *([gathered] * (2 * count)), w_in, w_out)
+
+
+def last_kernel(n_ref, gain_ref, bias_ref, *refs):
+    o_ref = refs[-1]
+    total = refs[0][...].astype(F32)
+    for r in refs[1:-1]:
+        total = total + r[...].astype(F32)
     lowered = total.astype(BF16).astype(F32)
     matrix = ALPHA * n_ref[...].astype(F32) + lowered
     o_ref[...] = norm_rows(matrix, gain_ref[...], bias_ref[...]).astype(BF16)
@@ -386,13 +455,13 @@
     return pl.pallas_call(
         last_kernel,
         out_shape=jax.ShapeDtypeStruct((HALF, 2048), BF16),
-        in_specs=[vmem()] * 4,
+        in_specs=[vmem()] * (3 + len(parts)),
         out_specs=vmem(),
         compiler_params=params(),
         cost_estimate=pl.CostEstimate(
             flops=4 * 10**6, bytes_accessed=4 * 10**6, transcendentals=0
         ),
-    )(parts, normed, gain, bias)
+    )(normed, gain, bias, *parts)
 
 
 def body(
@@ -406,24 +475,18 @@
     def turn(value, axis, d):
         return lax.ppermute(value, axis, [(i, (i + d) % 4) for i in range(4)])
 
+    def swap(value):
+        return lax.ppermute(value, "c", [(0, 1), (1, 0)])
+
     q_pack, kv_pack = pack(queries, key_rows, value_rows, log_forget.T)
     kv_own = lax.all_to_all(kv_pack, "z", split_axis=0, concat_axis=0, tiled=True)
     q_mine = lax.all_to_all(q_pack, ("z", "y"), split_axis=0, concat_axis=0, tiled=True)
     kv_back, kv_ahead = turn(kv_own, "y", 1), turn(kv_own, "y", 3)
     kv_far = turn(kv_own, "y", 2)
-
+    w_same = lax.all_gather(out_weight, "x", axis=0, tiled=False)
+    w_other = swap(w_same)
     shards = jnp.concatenate([gate_weight.T, up_weight.T, down_weight], axis=0)
     ffn_all = lax.all_gather(shards, ("z", "y"), axis=0, tiled=False)
-
-    weights, places = [out_weight], [2 * xi + ci]
-    for d in (1, 3, 2):
-        weights.append(turn(out_weight, "x", d))
-        places.append(2 * ((xi + 4 - d) % 4) + ci)
-    for i in range(4):
-        weights.append(lax.ppermute(weights[i], "c", [(0, 1), (1, 0)]))
-        places.append(places[i] + 1 - 2 * ci)
-    own = 2 * xi + ci
-    place = jnp.stack(places + [own]).astype(jnp.int32)
 
     qt, *state = attend(yi, (0,), [kv_own], q=q_mine)
     state = attend(yi, (3, 1), [kv_back, kv_ahead], state=(qt, *state))
@@ -432,12 +495,29 @@
     by_rows = lax.all_to_all(
         spread(by_shard), ("x", "c"), split_axis=0, concat_axis=0, tiled=True
     )
-    normed = mix(place, by_rows, stream_in, mix_gain[None], mix_bias[None], weights)
-    gathered = lax.all_gather(normed, ("x", "c"), axis=0, tiled=True)
-    partial = ffn(gathered, ffn_all)
-    parts = lax.all_to_all(
-        partial.reshape(8, HALF, 2048), ("x", "c"), split_axis=0, concat_axis=0, tiled=True
-    )
+    place = jnp.stack([ci, 2 * xi + ci]).astype(jnp.int32)
+    normed = mix(place, by_rows, stream_in, mix_gain[None], mix_bias[None], w_same, w_other)
+    gathered = lax.all_gather(normed, ("x", "c"), axis=0, tiled=False)
+    w_in, w_out = prepare(ffn_all)
+
+    def chips(steps):
+        at = [2 * ((xi + d) % 4) for d in steps]
+        both = [i + ci for i in at] + [i + 1 - ci for i in at]
+        return jnp.stack(both).astype(jnp.int32)
+
+    def joined(one, two):
+        return (one.astype(F32) + two.astype(F32)).astype(BF16)
+
+    far_same, far_other = ffn(1, chips((2,)), gathered, w_in, w_out)
+    far_swapped = swap(far_other)
+    near_same, near_other = ffn(2, chips((1, 3)), gathered, w_in, w_out)
+    near_swapped = swap(near_other)
+    own_same, own_other = ffn(1, chips((0,)), gathered, w_in, w_out)
+    own_swapped = swap(own_other)
+    from_far = turn(joined(far_same[0], far_swapped[0]), "x", 2)
+    from_back = turn(joined(near_same[0], near_swapped[0]), "x", 1)
+    from_ahead = turn(joined(near_same[1], near_swapped[1]), "x", 3)
+    parts = [own_same[0], own_swapped[0], from_back, from_ahead, from_far]
     return last(parts, normed, ffn_gain[None], ffn_bias[None])
 
 

time: 337 us -> 247 us (0.73)
  waiting for transfers between devices: 126 us -> 52.4 us
  blocking collectives: 80.2 us -> 39.2 us
  Pallas kernels: 91.4 us -> 110 us
  other arithmetic: 0.84 us -> 4.74 us
    all_gather x1, waiting for transfers between devices: 74.3 us -> 0.01 us  [body(): ffn_all = lax.all_gather(shards, ('z', 'y'), axis=0, tiled=False)]
    all_to_all x1 -> x0, blocking collectives: 42.9 us -> none  [body(): lax.all_to_all(partial.reshape(8, HALF, 2048), ('x', 'c'), split_axis=0,...]
    pallas_call x1 -> x4, Pallas kernels: 18.2 us -> 37.9 us  [the longest x3 24.6 us: ffn(): pl.pallas_call(functools.partial(ffn_kernel, count), out_shape=(shape, sh...]
    all_gather x1 -> x2, waiting for transfers between devices: 22.4 us -> 27.4 us  [the longest x1 18.8 us: body(): w_same = lax.all_gather(out_weight, 'x', axis=0, tiled=False)]
    ppermute x6, waiting for transfers between devices: 19.8 us -> 16.1 us  [turn(): return lax.ppermute(value, axis, [(i, (i + d) % 4) for i in range(4)])]
  transfers between devices with their start and end apart: 14 -> 15, of which waited for: 5 -> 5; matrix products, arithmetic and copies ran while one was open for 0% -> 2% of each run, Pallas kernels for 18% -> 41%
where the time goes in v3:
time: 247 us; the launch traced here: 245 us
  Pallas kernels  110 us (45%)
  waiting for transfers between devices  52.4 us (21%)
  blocking collectives  39.2 us (16%)
  starting transfers between devices  20.7 us (8%)
  between operations  13.2 us (5%)
  other arithmetic  4.74 us (2%)
  local copies, waits for them, and re-layouts  4.17 us (2%)
    pallas_call x3, Pallas kernels, attend(): pl.pallas_call(functools.partial(attend_kernel, chunks, first, final), ou...  57.6 us
    pallas_call x3, Pallas kernels, ffn(): pl.pallas_call(functools.partial(ffn_kernel, count), out_shape=(shape, sh...  24.6 us
    all_to_all x1, blocking collectives, body(): lax.all_to_all(attended, ('z', 'y'), split_axis=0, concat_axis=0, tiled=T...  21.1 us
    all_gather x1, waiting for transfers between devices, body(): w_same = lax.all_gather(out_weight, 'x', axis=0, tiled=False)  18.8 us
    all_to_all x1, blocking collectives, body(): lax.all_to_all(kv_pack, 'z', split_axis=0, concat_axis=0, tiled=True)  18.1 us
    ppermute x6, waiting for transfers between devices, turn(): return lax.ppermute(value, axis, [(i, (i + d) % 4) for i in range(4)])  16.1 us
    pallas_call x1, Pallas kernels, prepare(): pl.pallas_call(prepare_kernel, out_shape=(jax.ShapeDtypeStruct((BLOCKS, 2...  13.2 us
    ppermute x6, starting transfers between devices, turn(): return lax.ppermute(value, axis, [(i, (i + d) % 4) for i in range(4)])  10.4 us
  transfers between devices with their start and end apart: 15, of which 5 were waited for; matrix products, arithmetic and copies ran while one was open for 2% of the time, Pallas kernels for 41%

profile of v3, /device:TPU:0, one launch (start us, length us, event | category | flops | bytes accessed | tf_op | source)
XLA Modules:
  0.0 244.9 jit_solution(10207837054022085907)
XLA Ops:
  6.5 0.0 all-gather.7.cloned.1.call-start
  6.5 0.7 all-gather.7.cloned.1.call-update
  7.3 0.0 all-gather.11.cloned.1.call-start
  7.3 1.9 pad_maximum_fusion
  9.2 0.0 all-gather.11.cloned.1.call-update
  9.3 2.9 %shard_map.154 = (bf16[16,96,128]{2,1,0:T(8,128)(2,1)}, bf16[4,800,128]{2,1,0:T(8,128)(2,1)}) custom-call(bf16[768,256]{1,0:T(8,128)(2,1)} %q_ref.1, bf16[768,256]{1,0:T(8,128)(2,1)} %k_ref.1, bf16[768,256]{1,0:T(8,128)(2,1)} %v_ref.1, f32[4,768]{1,0:T(4,128)} %bitcast.44), custom_call_target="tpu_custom_call" | custom-call | flops 1000000 | bytes 2500000 | tf_op jit(solution)/shard_map/pallas_call | solution.py:59
  12.1 18.1 %all_to_all.20.refs_2_ = bf16[4,800,128]{2,1,0:T(8,128)(2,1)S(1)} all-to-all(bf16[4,800,128]{2,1,0:T(8,128)(2,1)} %get-tuple-element.20), channel_id=1, replica_groups=mesh['z'=4,'y'=4,'x'=4,'c'=2] {'z'}, dimensions={0} | all-to-all | bytes 1638400 | tf_op jit(solution)/shard_map/all_to_all | solution.py:482
  30.2 0.0 copy-start.1
  30.2 5.2 %all-to-all-start.1 = ((bf16[16,96,128]{2,1,0:T(8,128)(2,1)}), bf16[16,96,128]{2,1,0:T(8,128)(2,1)S(1)}, u32[]{:S(2)}, u32[]{:S(2)}) async-start(bf16[16,96,128]{2,1,0:T(8,128)(2,1)} %get-tuple-element.21), calls=%async_computation.1 | async-start | bytes 786432 | tf_op jit(solution)/shard_map/all_to_all | solution.py:483
  35.4 1.9 collective-permute-start.1
  37.3 1.4 collective-permute-start.2
  38.7 2.1 collective-permute-start
  40.8 18.8 %all-gather.7.cloned.1.call-done = bf16[1024,2048]{1,0:T(8,128)(2,1)} async-done(((bf16[256,2048]{1,0:T(8,128)(2,1)}), bf16[1024,2048]{1,0:T(8,128)(2,1)}) %all-gather.7.cloned.1.call-update) | async-done | bytes 4194320 | tf_op jit(solution)/shard_map/all_gather | solution.py:486
  59.7 0.0 collective-permute-start.3
  59.7 0.0 all-to-all-done.1.refs_3_
  59.7 0.0 copy-done.1
  59.7 0.7 copy-done.3
  60.4 16.6 %shard_map.155 = (bf16[12,128,256]{2,1,0:T(8,128)(2,1)}, f32[12,8,256]{2,1,0:T(8,128)}, f32[12,80,256]{2,1,0:T(8,128)}) custom-call(s32[4,4,33]{2,1,0:T(4,128)} %constant.47.clone.refs_0_, s32[1]{0:T(128)} %bitcast.2.refs_1_, bf16[4,800,128]{2,1,0:T(8,128)(2,1)} %copy-done.1, bf16[16,96,128]{2,1,0:T(8,128)(2,1)} %copy-done.3), custom_call_target="tpu_custom_call" | custom-call | flops 10800000000 | bytes 3000000 | tf_op jit(solution)/shard_map/pallas_call | solution.py:263
  77.0 0.0 collective-permute-done.1.refs_2_
  77.0 0.0 collective-permute-done.2.refs_3_
  77.0 0.9 copy-done.10
  77.9 24.8 %shard_map.156 = (f32[12,8,256]{2,1,0:T(8,128)}, f32[12,80,256]{2,1,0:T(8,128)}) custom-call(s32[4,4,59]{2,1,0:T(4,128)} %constant.48.clone.refs_0_, s32[1]{0:T(128)} %bitcast.2.refs_1_, bf16[4,800,128]{2,1,0:T(8,128)(2,1)} %copy-done.10, bf16[4,800,128]{2,1,0:T(8,128)(2,1)} %collective-permute-done.2.refs_3_, ...), custom_call_target="tpu_custom_call" | custom-call | flops 21600000000 | bytes 3000000 | tf_op jit(solution)/shard_map/pallas_call | solution.py:263
  102.7 0.0 collective-permute-done.refs_2_
  102.7 0.9 copy-done.9
  103.6 16.3 %shard_map.157 = bf16[16,96,128]{2,1,0:T(8,128)(2,1)} custom-call(s32[4,4,33]{2,1,0:T(4,128)} %constant.49.clone.refs_0_, s32[1]{0:T(128)} %bitcast.2.refs_1_, bf16[4,800,128]{2,1,0:T(8,128)(2,1)} %copy-done.9, bf16[12,128,256]{2,1,0:T(8,128)(2,1)} %get-tuple-element.22.refs_4_.refs_3_, f32[12,8,256]{2,1,0:T(8,128)} %get-tuple-element.25.refs_4_, ...), custom_call_target="tpu_custom_call" | custom-call | flops 10800000000 | bytes 3000000 | tf_op jit(solution)/shard_map/pallas_call | solution.py:263
  119.8 21.1 %all_to_all.21.o_ref = bf16[16,96,128]{2,1,0:T(8,128)(2,1)} all-to-all(bf16[16,96,128]{2,1,0:T(8,128)(2,1)} %shard_map.157), channel_id=1, replica_groups=mesh['z'=4,'y'=4,'x'=4,'c'=2] {'z','y'}, dimensions={0} | all-to-all | bytes 786432 | tf_op jit(solution)/shard_map/all_to_all | solution.py:494
  141.0 2.0 shard_map.158
  143.0 4.2 %all-to-all-start.3 = ((bf16[8,96,256]{2,1,0:T(8,128)(2,1)}), bf16[8,96,256]{2,1,0:T(8,128)(2,1)S(1)}, u32[]{:S(2)}, u32[]{:S(2)}) async-start(bf16[8,96,256]{2,1,0:T(8,128)(2,1)} %shard_map.158), calls=%async_computation.3 | async-start | bytes 786432 | tf_op jit(solution)/shard_map/all_to_all | solution.py:495
  147.2 0.0 all-gather.9.cloned.1.call-start
  147.3 0.6 pad_add_fusion.place
  147.9 8.2 %all-to-all-done.3.a_ref = bf16[8,96,256]{2,1,0:T(8,128)(2,1)S(1)} async-done(((bf16[8,96,256]{2,1,0:T(8,128)(2,1)}), bf16[8,96,256]{2,1,0:T(8,128)(2,1)S(1)}, u32[]{:S(2)}, u32[]{:S(2)}) %all-to-all-start.3) | async-done | bytes 393248 | tf_op jit(solution)/shard_map/all_to_all | solution.py:495
  156.1 0.0 collective-permute-done.3.other_ref
  156.1 0.7 copy-done
  156.9 7.0 %shard_map.159.n_ref = bf16[96,2048]{1,0:T(8,128)(2,1)} custom-call(s32[2]{0:T(128)} %pad_add_fusion.place, bf16[8,96,256]{2,1,0:T(8,128)(2,1)} %copy-done, bf16[768,2048]{1,0:T(8,128)(2,1)} %stream_ref.1, f32[1,2048]{1,0:T(1,128)} %bitcast.45, f32[1,2048]{1,0:T(1,128)} %bitcast.46, bf16[4,256,2048]{2,1,0:T(8,128)(2,1)} %bitcast.39, ...), custom_call_target="tpu_custom_call" | custom-call | flops 805306368 | bytes 9000000 | tf_op jit(solution)/shard_map/pallas_call | solution.py:331
  163.9 0.0 all-gather.9.cloned.1.call-update
  164.0 0.6 pad_add_fusion.3.place
  164.6 0.6 pad_add_fusion.2.place
  165.2 13.2 %shard_map.160 = (bf16[3,2048,512]{2,1,0:T(8,128)(2,1)}, bf16[3,256,2048]{2,1,0:T(8,128)(2,1)}) custom-call(bf16[16,2112,128]{2,1,0:T(8,128)(2,1)} %bitcast.37), custom_call_target="tpu_custom_call" | custom-call | flops 1000000000 | bytes 17000000 | tf_op jit(solution)/shard_map/pallas_call | solution.py:375
  178.5 8.5 %all-gather.9.cloned.1.call-done = bf16[768,2048]{1,0:T(8,128)(2,1)} async-done(((bf16[96,2048]{1,0:T(8,128)(2,1)}), bf16[768,2048]{1,0:T(8,128)(2,1)}) %all-gather.9.cloned.1.call-update) | async-done | bytes 3145744 | tf_op jit(solution)/shard_map/all_gather | solution.py:500
  187.0 7.6 %shard_map.163 = (bf16[1,96,2048]{2,1,0:T(8,128)(2,1)}, bf16[1,96,2048]{2,1,0:T(8,128)(2,1)}) custom-call(s32[2]{0:T(128)} %pad_add_fusion.3.place, bf16[8,96,2048]{2,1,0:T(8,128)(2,1)} %bitcast.29, bf16[8,96,2048]{2,1,0:T(8,128)(2,1)} %bitcast.30, bf16[3,2048,512]{2,1,0:T(8,128)(2,1)} %get-tuple-element.27.refs_2_.refs_4_, ...), custom_call_target="tpu_custom_call" | custom-call | flops 1660944384 | bytes 10000000 | tf_op jit(solution)/shard_map/pallas_call | solution.py:426
  194.6 0.2 collective-permute-start.8
  194.8 9.4 %shard_map.162 = (bf16[2,96,2048]{2,1,0:T(8,128)(2,1)}, bf16[2,96,2048]{2,1,0:T(8,128)(2,1)}) custom-call(s32[4]{0:T(128)} %pad_add_fusion.2.place, bf16[8,96,2048]{2,1,0:T(8,128)(2,1)} %bitcast.31, bf16[8,96,2048]{2,1,0:T(8,128)(2,1)} %bitcast.32, bf16[8,96,2048]{2,1,0:T(8,128)(2,1)} %bitcast.33, bf16[8,96,2048]{2,1,0:T(8,128)(2,1)} %bitcast.34, ...), custom_call_target="tpu_custom_call" | custom-call | flops 3321888768 | bytes 10000000 | tf_op jit(solution)/shard_map/pallas_call | solution.py:426
  204.2 0.3 collective-permute-start.5
  204.5 0.6 pad_add_fusion.1.place
  205.1 7.7 %shard_map.161 = (bf16[1,96,2048]{2,1,0:T(8,128)(2,1)}, bf16[1,96,2048]{2,1,0:T(8,128)(2,1)}) custom-call(s32[2]{0:T(128)} %pad_add_fusion.1.place, bf16[8,96,2048]{2,1,0:T(8,128)(2,1)} %bitcast.35, bf16[8,96,2048]{2,1,0:T(8,128)(2,1)} %bitcast.36, bf16[3,2048,512]{2,1,0:T(8,128)(2,1)} %get-tuple-element.27.refs_2_.refs_4_, ...), custom_call_target="tpu_custom_call" | custom-call | flops 1660944384 | bytes 10000000 | tf_op jit(solution)/shard_map/pallas_call | solution.py:426
  212.8 0.2 collective-permute-start.4
  213.0 0.0 collective-permute-done.8
  213.0 0.0 copy-done.4
  213.0 0.1 fusion.2
  213.1 1.7 collective-permute-start.9
  214.8 0.0 collective-permute-done.5
  214.8 0.0 copy-done.2
  214.8 0.3 fusion.1
  215.0 1.0 collective-permute-start.6
  216.0 2.3 collective-permute-start.7
  218.3 0.0 collective-permute-done.4
  218.4 8.4 %collective-permute-done.9.refs_4_ = bf16[96,2048]{1,0:T(8,128)(2,1)S(1)} collective-permute-done((bf16[96,2048]{1,0:T(8,128)(2,1)S(1)}, bf16[96,2048]{1,0:T(8,128)(2,1)S(1)}, u32[]{:S(2)}, u32[]{:S(2)}) %collective-permute-start.9) | collective-permute-done | bytes 393248 | tf_op jit(solution)/shard_map/ppermute | solution.py:476
  226.7 7.7 %collective-permute-done.6.refs_2_ = bf16[96,2048]{1,0:T(8,128)(2,1)S(1)} collective-permute-done((bf16[96,2048]{1,0:T(8,128)(2,1)S(1)}, bf16[96,2048]{1,0:T(8,128)(2,1)S(1)}, u32[]{:S(2)}, u32[]{:S(2)}) %collective-permute-start.6) | collective-permute-done | bytes 393248 | tf_op jit(solution)/shard_map/ppermute | solution.py:476
  234.4 0.0 collective-permute-done.7.refs_3_
  234.4 0.0 copy-done.5
  234.4 0.0 copy-done.6
  234.4 0.7 copy-done.7
  235.2 0.2 copy-done.8
  235.3 3.0 %shard_map.164 = bf16[96,2048]{1,0:T(8,128)(2,1)} custom-call(bf16[96,2048]{1,0:T(8,128)(2,1)} %shard_map.159.n_ref, f32[1,2048]{1,0:T(1,128)} %bitcast.47, f32[1,2048]{1,0:T(1,128)} %bitcast.48, bf16[96,2048]{1,0:T(8,128)(2,1)} %bitcast.40, bf16[96,2048]{1,0:T(8,128)(2,1)} %bitcast.41, bf16[96,2048]{1,0:T(8,128)(2,1)} %copy-done.7, ...), custom_call_target="tpu_custom_call" | custom-call | flops 4000000 | bytes 4000000 | tf_op jit(solution)/shard_map/pallas_call | solution.py:455
  (11 shorter events, 0.0 us)
Async XLA Ops:
  6.5 53.1 %all-gather.7.cloned.1.call-start = ((), (), s32[]{:S(2)}) async-start(), calls=%async_computation.4 | async-start | bytes 5242880 | tf_op jit(solution)/shard_map/all_gather | solution.py:486
  7.3 158.0 %all-gather.11.cloned.1.call-start = ((), (), s32[]{:S(2)}) async-start(), calls=%async_computation.6 | async-start | bytes 9191424 | tf_op jit(solution)/shard_map/all_gather | solution.py:489
  30.2 29.5 %copy-start.1 = (bf16[4,800,128]{2,1,0:T(8,128)(2,1)}, bf16[4,800,128]{2,1,0:T(8,128)(2,1)S(1)}, u32[]{:S(2)}) copy-start(bf16[4,800,128]{2,1,0:T(8,128)(2,1)S(1)} %all_to_all.20.refs_2_) | copy-start | bytes 2457604
  30.2 29.5 %all-to-all-start.1 = ((bf16[16,96,128]{2,1,0:T(8,128)(2,1)}), bf16[16,96,128]{2,1,0:T(8,128)(2,1)S(1)}, u32[]{:S(2)}, u32[]{:S(2)}) async-start(bf16[16,96,128]{2,1,0:T(8,128)(2,1)} %get-tuple-element.21), calls=%async_computation.1 | async-start | bytes 786432 | tf_op jit(solution)/shard_map/all_to_all | solution.py:483
  35.4 41.6 %collective-permute-start.1 = (bf16[4,800,128]{2,1,0:T(8,128)(2,1)S(1)}, bf16[4,800,128]{2,1,0:T(8,128)(2,1)S(1)}, u32[]{:S(2)}, u32[]{:S(2)}) collective-permute-start(bf16[4,800,128]{2,1,0:T(8,128)(2,1)S(1)} %all_to_all.20.refs_2_), channel_id=1, source_target_pairs={{0,8},{8,16},{16,24},{24,0},{1,9},{9,17},{17,25},{25,1},{2,10},{10... | collective-permute-start | bytes 2457608 | tf_op jit(solution)/shard_map/ppermute | solution.py:476
  37.3 39.7 %collective-permute-start.2 = (bf16[4,800,128]{2,1,0:T(8,128)(2,1)S(1)}, bf16[4,800,128]{2,1,0:T(8,128)(2,1)}, u32[]{:S(2)}, u32[]{:S(2)}) collective-permute-start(bf16[4,800,128]{2,1,0:T(8,128)(2,1)S(1)} %all_to_all.20.refs_2_), channel_id=1, source_target_pairs={{0,24},{8,0},{16,8},{24,16},{1,25},{9,1},{17,9},{25,17},{2,26},{10... | collective-permute-start | bytes 2457608 | tf_op jit(solution)/shard_map/ppermute | solution.py:476
  38.7 64.0 %collective-permute-start = (bf16[4,800,128]{2,1,0:T(8,128)(2,1)S(1)}, bf16[4,800,128]{2,1,0:T(8,128)(2,1)S(1)}, u32[]{:S(2)}, u32[]{:S(2)}) collective-permute-start(bf16[4,800,128]{2,1,0:T(8,128)(2,1)S(1)} %all_to_all.20.refs_2_), channel_id=1, source_target_pairs={{0,16},{8,24},{16,0},{24,8},{1,17},{9,25},{17,1},{25,9},{2,18},{10... | collective-permute-start | bytes 2457608 | tf_op jit(solution)/shard_map/ppermute | solution.py:476
  59.7 96.5 %collective-permute-start.3 = (bf16[4,256,2048]{2,1,0:T(8,128)(2,1)}, bf16[4,256,2048]{2,1,0:T(8,128)(2,1)}, u32[]{:S(2)}, u32[]{:S(2)}) collective-permute-start(bf16[4,256,2048]{2,1,0:T(8,128)(2,1)} %bitcast.38), channel_id=1, source_target_pairs={{0,1},{1,0},{2,3},{3,2},{4,5},{5,4},{6,7},{7,6},{8,9},{9,8},{10,11... | collective-permute-start | bytes 12582920 | tf_op jit(solution)/shard_map/ppermute | solution.py:479
  59.7 0.7 copy-start.3
  77.0 0.9 copy-start.10
  102.7 0.9 copy-start.9
  143.0 13.2 %all-to-all-start.3 = ((bf16[8,96,256]{2,1,0:T(8,128)(2,1)}), bf16[8,96,256]{2,1,0:T(8,128)(2,1)S(1)}, u32[]{:S(2)}, u32[]{:S(2)}) async-start(bf16[8,96,256]{2,1,0:T(8,128)(2,1)} %shard_map.158), calls=%async_computation.3 | async-start | bytes 786432 | tf_op jit(solution)/shard_map/all_to_all | solution.py:495
  147.2 39.8 %all-gather.9.cloned.1.call-start = ((), (), s32[]{:S(2)}) async-start(), calls=%async_computation.5 | async-start | bytes 3538944 | tf_op jit(solution)/shard_map/all_gather | solution.py:500
  156.1 0.7 copy-start
  194.6 18.4 %collective-permute-start.8 = (bf16[1,96,2048]{2,1,0:T(8,128)(2,1)}, bf16[1,96,2048]{2,1,0:T(8,128)(2,1)S(1)}, u32[]{:S(2)}, u32[]{:S(2)}) collective-permute-start(bf16[1,96,2048]{2,1,0:T(8,128)(2,1)} %get-tuple-element.34), channel_id=1, source_target_pairs={{0,1},{1,0},{2,3},{3,2},{4,5},{5,4},{6,7},{7,6},{8,9},{9,8},{10,11... | collective-permute-start | bytes 1179656 | tf_op jit(solution)/shard_map/ppermute | solution.py:479
  204.2 10.6 %collective-permute-start.5 = (bf16[2,96,2048]{2,1,0:T(8,128)(2,1)}, bf16[2,96,2048]{2,1,0:T(8,128)(2,1)S(1)}, u32[]{:S(2)}, u32[]{:S(2)}) collective-permute-start(bf16[2,96,2048]{2,1,0:T(8,128)(2,1)} %get-tuple-element.32), channel_id=1, source_target_pairs={{0,1},{1,0},{2,3},{3,2},{4,5},{5,4},{6,7},{7,6},{8,9},{9,8},{10,11... | collective-permute-start | bytes 2359304 | tf_op jit(solution)/shard_map/ppermute | solution.py:479
  205.1 7.9 %copy-start.4 = (bf16[1,96,2048]{2,1,0:T(8,128)(2,1)S(1)}, bf16[1,96,2048]{2,1,0:T(8,128)(2,1)}, u32[]{:S(2)}) copy-start(bf16[1,96,2048]{2,1,0:T(8,128)(2,1)} %get-tuple-element.33) | copy-start | bytes 1179652
  205.1 9.7 %copy-start.2 = (bf16[2,96,2048]{2,1,0:T(8,128)(2,1)S(1)}, bf16[2,96,2048]{2,1,0:T(8,128)(2,1)}, u32[]{:S(2)}) copy-start(bf16[2,96,2048]{2,1,0:T(8,128)(2,1)} %get-tuple-element.31) | copy-start | bytes 2359300
  212.8 5.6 %collective-permute-start.4 = (bf16[1,96,2048]{2,1,0:T(8,128)(2,1)}, bf16[1,96,2048]{2,1,0:T(8,128)(2,1)S(1)}, u32[]{:S(2)}, u32[]{:S(2)}) collective-permute-start(bf16[1,96,2048]{2,1,0:T(8,128)(2,1)} %get-tuple-element.30), channel_id=1, source_target_pairs={{0,1},{1,0},{2,3},{3,2},{4,5},{5,4},{6,7},{7,6},{8,9},{9,8},{10,11... | collective-permute-start | bytes 1179656 | tf_op jit(solution)/shard_map/ppermute | solution.py:479
  213.1 13.6 %collective-permute-start.9 = (bf16[96,2048]{1,0:T(8,128)(2,1)S(1)}, bf16[96,2048]{1,0:T(8,128)(2,1)S(1)}, u32[]{:S(2)}, u32[]{:S(2)}) collective-permute-start(bf16[96,2048]{1,0:T(8,128)(2,1)S(1)} %fusion.2), channel_id=1, source_target_pairs={{0,4},{2,6},{4,0},{6,2},{1,5},{3,7},{5,1},{7,3},{8,12},{10,14},{12... | collective-permute-start | bytes 1179656 | tf_op jit(solution)/shard_map/ppermute | solution.py:476
  215.0 19.4 %collective-permute-start.6 = (bf16[96,2048]{1,0:T(8,128)(2,1)S(1)}, bf16[96,2048]{1,0:T(8,128)(2,1)S(1)}, u32[]{:S(2)}, u32[]{:S(2)}) collective-permute-start(bf16[96,2048]{1,0:T(8,128)(2,1)S(1)} %get-tuple-element.36), channel_id=1, source_target_pairs={{0,2},{2,4},{4,6},{6,0},{1,3},{3,5},{5,7},{7,1},{8,10},{10,12},{12... | collective-permute-start | bytes 1179656 | tf_op jit(solution)/shard_map/ppermute | solution.py:476
  216.0 18.4 %collective-permute-start.7 = (bf16[96,2048]{1,0:T(8,128)(2,1)S(1)}, bf16[96,2048]{1,0:T(8,128)(2,1)S(1)}, u32[]{:S(2)}, u32[]{:S(2)}) collective-permute-start(bf16[96,2048]{1,0:T(8,128)(2,1)S(1)} %get-tuple-element.35), channel_id=1, source_target_pairs={{0,6},{2,0},{4,2},{6,4},{1,7},{3,1},{5,3},{7,5},{8,14},{10,8},{12,... | collective-permute-start | bytes 1179656 | tf_op jit(solution)/shard_map/ppermute | solution.py:476
  218.4 16.1 %copy-start.5 = (bf16[1,96,2048]{2,1,0:T(8,128)(2,1)}, bf16[1,96,2048]{2,1,0:T(8,128)(2,1)S(1)}, u32[]{:S(2)}) copy-start(bf16[1,96,2048]{2,1,0:T(8,128)(2,1)S(1)} %collective-permute-done.4) | copy-start | bytes 1179652
  226.7 7.7 %copy-start.6 = (bf16[96,2048]{1,0:T(8,128)(2,1)}, bf16[96,2048]{1,0:T(8,128)(2,1)S(1)}, u32[]{:S(2)}) copy-start(bf16[96,2048]{1,0:T(8,128)(2,1)S(1)} %collective-permute-done.9.refs_4_) | copy-start | bytes 1179652
  234.4 0.8 copy-start.7
  234.4 0.9 copy-start.8
Sparse Core Ops, SparseCore 0:
  9.0 50.6 all-gather.6
  61.8 76.4 all-gather.10
  164.1 22.8 all-gather.8

commit v4 on v3

--- a/solution.py
+++ b/solution.py
@@ -31,7 +31,7 @@
     return pl.BlockSpec(memory_space=pltpu.SMEM)
 
 
-def params(mb=60):
+def params(mb):
     return pltpu.CompilerParams(vmem_limit_bytes=mb * 1024 * 1024)
 
 
@@ -64,7 +64,7 @@
         ),
         in_specs=[vmem()] * 4,
         out_specs=(vmem(), vmem()),
-        compiler_params=params(),
+        compiler_params=params(60),
         cost_estimate=pl.CostEstimate(flops=10**6, bytes_accessed=2500000, transcendentals=0),
     )(q, k, v, g)
 
@@ -266,7 +266,7 @@
         in_specs=[smem(), smem()] + [vmem()] * (chunks + len(rest)),
         out_specs=jax.tree.map(lambda _: vmem(), outs),
         scratch_shapes=scratch,
-        compiler_params=params(),
+        compiler_params=params(60),
         cost_estimate=pl.CostEstimate(
             flops=share * 4 * 10**8, bytes_accessed=3 * 10**6, transcendentals=share * 200000
         ),
@@ -288,7 +288,7 @@
         out_shape=jax.ShapeDtypeStruct((8, HALF, 256), BF16),
         in_specs=[vmem()],
         out_specs=vmem(),
-        compiler_params=params(),
+        compiler_params=params(60),
         cost_estimate=pl.CostEstimate(flops=10**5, bytes_accessed=800000, transcendentals=0),
     )(o)
 
@@ -345,7 +345,7 @@
             out_specs=whole((HALF, 2048)),
             scratch_shapes=[pltpu.VMEM((HALF, 2048), F32)],
         ),
-        compiler_params=params(),
+        compiler_params=params(60),
         cost_estimate=pl.CostEstimate(
             flops=2 * HALF * 2048 * 2048, bytes_accessed=9 * 10**6, transcendentals=0
         ),
@@ -355,7 +355,7 @@
 BLOCKS = 3
 
 
-def prepare_kernel(w_ref, in_ref, out_ref):
+def prepare_kernel(w_ref, in_ref):
     for j in range(BLOCKS):
         live = min(256, 704 - 256 * j)
         for part in range(2):
@@ -365,41 +365,33 @@
                 in_ref[j, :, 256 * part + live : 256 * part + 256] = jnp.zeros(
                     (128, 256 - live), BF16
                 )
-        at = 1408 + 256 * j
-        out_ref[j, 0:live, :] = w_ref[0, at : at + live, :]
-        if live < 256:
-            out_ref[j, live:256, :] = jnp.zeros((256 - live, 128), BF16)
 
 
 def prepare(w):
     return pl.pallas_call(
         prepare_kernel,
-        out_shape=(
-            jax.ShapeDtypeStruct((BLOCKS, 2048, 512), BF16),
-            jax.ShapeDtypeStruct((BLOCKS, 256, 2048), BF16),
-        ),
+        out_shape=jax.ShapeDtypeStruct((BLOCKS, 2048, 512), BF16),
         grid=(NSH,),
-        in_specs=[pl.BlockSpec((1, 2112, 128), lambda s: (s, 0, 0))],
-        out_specs=(
-            pl.BlockSpec((BLOCKS, 128, 512), lambda s: (0, s, 0)),
-            pl.BlockSpec((BLOCKS, 256, 128), lambda s: (0, 0, s)),
-        ),
-        compiler_params=params(),
+        in_specs=[pl.BlockSpec((1, 1408, 128), lambda s: (s, 0, 0))],
+        out_specs=pl.BlockSpec((BLOCKS, 128, 512), lambda s: (0, s, 0)),
+        compiler_params=params(60),
         cost_estimate=pl.CostEstimate(
-            flops=10**9, bytes_accessed=17 * 10**6, transcendentals=0
+            flops=10**9, bytes_accessed=11 * 10**6, transcendentals=0
         ),
     )(w)
 
 
 def ffn_kernel(count, place, *refs):
     x_refs = refs[: 2 * count]
-    in_ref, out_ref, same_ref, other_ref, total = refs[2 * count :]
+    in_ref, out_refs = refs[2 * count], refs[2 * count + 1 : 2 * count + 5]
+    same_ref, other_ref, total = refs[2 * count + 5 :]
     j = pl.program_id(0)
     x = jnp.concatenate([r[0] for r in x_refs], axis=0)
     both = jnp.dot(x, in_ref[0], preferred_element_type=F32)
     gate, up = both[:, 0:256], both[:, 256:512]
     hidden = (gate / (1.0 + jnp.exp(-gate)) * up).astype(BF16)
-    term = jnp.dot(hidden, out_ref[0], preferred_element_type=F32)
+    rows = [jnp.concatenate([r[s] for s in range(NSH)], axis=1) for r in out_refs]
+    term = jnp.dot(hidden, jnp.concatenate(rows, axis=0), preferred_element_type=F32)
 
     @pl.when(j == 0)
     def _():
@@ -417,9 +409,18 @@
             other_ref[i] = out[(count + i) * HALF : (count + i + 1) * HALF]
 
 
-def ffn(count, place, gathered, w_in, w_out):
-    def block(i):
-        return pl.BlockSpec((1, HALF, 2048), lambda g, place: (place[i], 0, 0))
+def ffn(steps, place, gathered, w_in, w_down):
+    count = len(steps)
+
+    def block(d, swapped):
+        def at(g, place):
+            x, c = place[2], place[0]
+            return (2 * lax.rem(x + d, 4) + (1 - c if swapped else c), 0, 0)
+
+        return pl.BlockSpec((1, HALF, 2048), at)
+
+    def down(i):
+        return pl.BlockSpec((NSH, 64, 128), lambda g, place: (0, jnp.minimum(4 * g + i, 10), 0))
 
     shape = jax.ShapeDtypeStruct((count, HALF, 2048), BF16)
     rows = 2 * count * HALF
@@ -429,16 +430,36 @@
         grid_spec=pltpu.PrefetchScalarGridSpec(
             num_scalar_prefetch=1,
             grid=(BLOCKS,),
-            in_specs=[block(i) for i in range(2 * count)]
-            + [along((2048, 512)), along((256, 2048))],
+            in_specs=[block(d, swapped) for swapped in (False, True) for d in steps]
+            + [along((2048, 512))]
+            + [down(i) for i in range(4)],
             out_specs=(whole((count, HALF, 2048)),) * 2,
             scratch_shapes=[pltpu.VMEM((rows, 2048), F32)],
         ),
-        compiler_params=params(),
+        compiler_params=params(60),
         cost_estimate=pl.CostEstimate(
             flops=6 * rows * 2048 * 704, bytes_accessed=10**7, transcendentals=rows * 704
         ),
-    )(place, *([gathered] * (2 * count)), w_in, w_out)
+    )(place, *([gathered] * (2 * count)), w_in, *([w_down] * 4))
+
+
+def join_kernel(count, *refs):
+    same_ref, other_ref = refs[:2]
+    for i in range(count):
+        refs[2 + i][...] = (same_ref[i].astype(F32) + other_ref[i].astype(F32)).astype(BF16)
+
+
+def join(same, other):
+    count = same.shape[0]
+    shape = jax.ShapeDtypeStruct((HALF, 2048), BF16)
+    return pl.pallas_call(
+        functools.partial(join_kernel, count),
+        out_shape=(shape,) * count,
+        in_specs=[vmem()] * 2,
+        out_specs=(vmem(),) * count,
+        compiler_params=params(60),
+        cost_estimate=pl.CostEstimate(flops=10**6, bytes_accessed=10**6, transcendentals=0),
+    )(same, other)
 
 
 def last_kernel(n_ref, gain_ref, bias_ref, *refs):
@@ -457,7 +478,7 @@
         out_shape=jax.ShapeDtypeStruct((HALF, 2048), BF16),
         in_specs=[vmem()] * (3 + len(parts)),
         out_specs=vmem(),
-        compiler_params=params(),
+        compiler_params=params(60),
         cost_estimate=pl.CostEstimate(
             flops=4 * 10**6, bytes_accessed=4 * 10**6, transcendentals=0
         ),
@@ -478,15 +499,17 @@
     def swap(value):
         return lax.ppermute(value, "c", [(0, 1), (1, 0)])
 
+    place = jnp.stack([ci, 2 * xi + ci, xi]).astype(jnp.int32)
+    w_same = lax.all_gather(out_weight, "x", axis=0, tiled=False)
     q_pack, kv_pack = pack(queries, key_rows, value_rows, log_forget.T)
+    q_mine = lax.all_to_all(q_pack, ("z", "y"), split_axis=0, concat_axis=0, tiled=True)
     kv_own = lax.all_to_all(kv_pack, "z", split_axis=0, concat_axis=0, tiled=True)
-    q_mine = lax.all_to_all(q_pack, ("z", "y"), split_axis=0, concat_axis=0, tiled=True)
     kv_back, kv_ahead = turn(kv_own, "y", 1), turn(kv_own, "y", 3)
     kv_far = turn(kv_own, "y", 2)
-    w_same = lax.all_gather(out_weight, "x", axis=0, tiled=False)
     w_other = swap(w_same)
-    shards = jnp.concatenate([gate_weight.T, up_weight.T, down_weight], axis=0)
-    ffn_all = lax.all_gather(shards, ("z", "y"), axis=0, tiled=False)
+    shards = jnp.concatenate([gate_weight.T, up_weight.T], axis=0)
+    gu_all = lax.all_gather(shards, ("z", "y"), axis=0, tiled=False)
+    w_down = lax.all_gather(down_weight, ("z", "y"), axis=0, tiled=False)
 
     qt, *state = attend(yi, (0,), [kv_own], q=q_mine)
     state = attend(yi, (3, 1), [kv_back, kv_ahead], state=(qt, *state))
@@ -495,28 +518,19 @@
     by_rows = lax.all_to_all(
         spread(by_shard), ("x", "c"), split_axis=0, concat_axis=0, tiled=True
     )
-    place = jnp.stack([ci, 2 * xi + ci]).astype(jnp.int32)
     normed = mix(place, by_rows, stream_in, mix_gain[None], mix_bias[None], w_same, w_other)
     gathered = lax.all_gather(normed, ("x", "c"), axis=0, tiled=False)
-    w_in, w_out = prepare(ffn_all)
-
-    def chips(steps):
-        at = [2 * ((xi + d) % 4) for d in steps]
-        both = [i + ci for i in at] + [i + 1 - ci for i in at]
-        return jnp.stack(both).astype(jnp.int32)
-
-    def joined(one, two):
-        return (one.astype(F32) + two.astype(F32)).astype(BF16)
-
-    far_same, far_other = ffn(1, chips((2,)), gathered, w_in, w_out)
+    w_in = prepare(gu_all)
+
+    far_same, far_other = ffn((2,), place, gathered, w_in, w_down)
     far_swapped = swap(far_other)
-    near_same, near_other = ffn(2, chips((1, 3)), gathered, w_in, w_out)
+    near_same, near_other = ffn((1, 3), place, gathered, w_in, w_down)
     near_swapped = swap(near_other)
-    own_same, own_other = ffn(1, chips((0,)), gathered, w_in, w_out)
+    own_same, own_other = ffn((0,), place, gathered, w_in, w_down)
     own_swapped = swap(own_other)
-    from_far = turn(joined(far_same[0], far_swapped[0]), "x", 2)
-    from_back = turn(joined(near_same[0], near_swapped[0]), "x", 1)
-    from_ahead = turn(joined(near_same[1], near_swapped[1]), "x", 3)
+    from_far = turn(join(far_same, far_swapped)[0], "x", 2)
+    near_back, near_ahead = join(near_same, near_swapped)
+    from_back, from_ahead = turn(near_back, "x", 1), turn(near_ahead, "x", 3)
     parts = [own_same[0], own_swapped[0], from_back, from_ahead, from_far]
     return last(parts, normed, ffn_gain[None], ffn_bias[None])
 

time: 247 us -> 261 us (1.057)
  waiting for transfers between devices: 52.4 us -> 80.7 us
  blocking collectives: 39.2 us -> 17.9 us
  starting transfers between devices: 20.7 us -> 25.4 us
  Pallas kernels: 110 us -> 113 us
    all_gather x1, waiting for transfers between devices: 8.53 us -> 27 us  [body(): gathered = lax.all_gather(normed, ('x', 'c'), axis=0, tiled=False)]
    all_to_all x1 -> x0, blocking collectives: 18.1 us -> none  [body(): lax.all_to_all(kv_pack, 'z', split_axis=0, concat_axis=0, tiled=True)]
    all_to_all x0 -> x1, waiting for transfers between devices: none -> 11.9 us  [body(): lax.all_to_all(kv_pack, 'z', split_axis=0, concat_axis=0, tiled=True)]
    all_to_all x0 -> x1, starting transfers between devices: none -> 5.42 us  [body(): lax.all_to_all(kv_pack, 'z', split_axis=0, concat_axis=0, tiled=True)]
    all_to_all x1, blocking collectives: 21.1 us -> 17.9 us  [body(): lax.all_to_all(attended, ('z', 'y'), split_axis=0, concat_axis=0, tiled=T...]
    pallas_call x1 -> x3, Pallas kernels: 13.2 us -> 16.2 us  [the longest x1 11.9 us: prepare(): pl.pallas_call(prepare_kernel, out_shape=jax.ShapeDtypeStruct((BLOCKS, 20...]
    ppermute x6, waiting for transfers between devices: 16.1 us -> 13.4 us  [turn(): return lax.ppermute(value, axis, [(i, (i + d) % 4) for i in range(4)])]
  transfers between devices with their start and end apart: 15 -> 17, of which waited for: 5 -> 6; matrix products, arithmetic and copies ran while one was open for 2% -> 1% of each run, Pallas kernels for 41% -> 39%
where the time goes in v4:
time: 261 us; the launch traced here: 259 us
  Pallas kernels  113 us (43%)
  waiting for transfers between devices  80.7 us (31%)
  starting transfers between devices  25.4 us (10%)
  blocking collectives  17.9 us (7%)
  between operations  13.2 us (5%)
  local copies, waits for them, and re-layouts  5.79 us (2%)
    pallas_call x3, Pallas kernels, attend(): pl.pallas_call(functools.partial(attend_kernel, chunks, first, final), ou...  57.5 us
    all_gather x1, waiting for transfers between devices, body(): gathered = lax.all_gather(normed, ('x', 'c'), axis=0, tiled=False)  27 us
    pallas_call x3, Pallas kernels, ffn(): pl.pallas_call(functools.partial(ffn_kernel, count), out_shape=(shape, sh...  24.7 us
    all_gather x1, waiting for transfers between devices, body(): w_same = lax.all_gather(out_weight, 'x', axis=0, tiled=False)  19 us
    all_to_all x1, blocking collectives, body(): lax.all_to_all(attended, ('z', 'y'), split_axis=0, concat_axis=0, tiled=T...  17.9 us
    ppermute x6, waiting for transfers between devices, turn(): return lax.ppermute(value, axis, [(i, (i + d) % 4) for i in range(4)])  13.4 us
    all_to_all x1, waiting for transfers between devices, body(): lax.all_to_all(kv_pack, 'z', split_axis=0, concat_axis=0, tiled=True)  11.9 us
    pallas_call x1, Pallas kernels, prepare(): pl.pallas_call(prepare_kernel, out_shape=jax.ShapeDtypeStruct((BLOCKS, 20...  11.9 us
  transfers between devices with their start and end apart: 17, of which 6 were waited for; matrix products, arithmetic and copies ran while one was open for 1% of the time, Pallas kernels for 39%

profile of v4, /device:TPU:0, one launch (start us, length us, event | category | flops | bytes accessed | tf_op | source)
XLA Modules:
  0.0 258.7 jit_solution(11788346208271743411)
XLA Ops:
  6.5 0.0 all-gather.9.cloned.1.call-start
  6.5 0.7 all-gather.9.cloned.1.call-update
  7.3 0.0 all-gather.13.cloned.1.call-start
  7.3 1.8 pad_maximum_fusion
  9.1 0.0 all-gather.13.cloned.1.call-update
  9.1 2.9 %shard_map.154 = (bf16[16,96,128]{2,1,0:T(8,128)(2,1)}, bf16[4,800,128]{2,1,0:T(8,128)(2,1)}) custom-call(bf16[768,256]{1,0:T(8,128)(2,1)} %q_ref.1, bf16[768,256]{1,0:T(8,128)(2,1)} %k_ref.1, bf16[768,256]{1,0:T(8,128)(2,1)} %v_ref.1, f32[4,768]{1,0:T(4,128)} %bitcast.44), custom_call_target="tpu_custom_call" | custom-call | flops 1000000 | bytes 2500000 | tf_op jit(solution)/shard_map/pallas_call | solution.py:59
  12.0 5.4 %all-to-all-start = ((bf16[4,800,128]{2,1,0:T(8,128)(2,1)}), bf16[4,800,128]{2,1,0:T(8,128)(2,1)S(1)}, u32[]{:S(2)}, u32[]{:S(2)}) async-start(bf16[4,800,128]{2,1,0:T(8,128)(2,1)} %get-tuple-element.20), calls=%async_computation | async-start | bytes 1638400 | tf_op jit(solution)/shard_map/all_to_all | solution.py:506
  17.4 0.0 all-gather.15.cloned.1.call-start
  17.4 0.7 all-gather.15.cloned.1.call-update
  18.1 11.9 %all-to-all-done.refs_2_ = bf16[4,800,128]{2,1,0:T(8,128)(2,1)S(1)} async-done(((bf16[4,800,128]{2,1,0:T(8,128)(2,1)}), bf16[4,800,128]{2,1,0:T(8,128)(2,1)S(1)}, u32[]{:S(2)}, u32[]{:S(2)}) %all-to-all-start) | async-done | bytes 819232 | tf_op jit(solution)/shard_map/all_to_all | solution.py:506
  30.1 5.2 %all-to-all-start.1 = ((bf16[16,96,128]{2,1,0:T(8,128)(2,1)}), bf16[16,96,128]{2,1,0:T(8,128)(2,1)S(1)}, u32[]{:S(2)}, u32[]{:S(2)}) async-start(bf16[16,96,128]{2,1,0:T(8,128)(2,1)} %get-tuple-element.21), calls=%async_computation.1 | async-start | bytes 786432 | tf_op jit(solution)/shard_map/all_to_all | solution.py:505
  35.3 1.9 collective-permute-start.1
  37.2 1.4 collective-permute-start.2
  38.6 2.1 collective-permute-start
  40.7 19.0 %all-gather.9.cloned.1.call-done = bf16[1024,2048]{1,0:T(8,128)(2,1)} async-done(((bf16[256,2048]{1,0:T(8,128)(2,1)}), bf16[1024,2048]{1,0:T(8,128)(2,1)}) %all-gather.9.cloned.1.call-update) | async-done | bytes 4194320 | tf_op jit(solution)/shard_map/all_gather | solution.py:503
  59.7 0.0 collective-permute-start.3
  59.7 0.0 all-to-all-done.1.refs_3_
  59.7 0.0 copy-done.1
  59.7 0.7 copy-done.3
  60.4 16.6 %shard_map.155 = (bf16[12,128,256]{2,1,0:T(8,128)(2,1)}, f32[12,8,256]{2,1,0:T(8,128)}, f32[12,80,256]{2,1,0:T(8,128)}) custom-call(s32[4,4,33]{2,1,0:T(4,128)} %constant.19.clone.refs_0_, s32[1]{0:T(128)} %bitcast.3.refs_1_, bf16[4,800,128]{2,1,0:T(8,128)(2,1)} %copy-done.1, bf16[16,96,128]{2,1,0:T(8,128)(2,1)} %copy-done.3), custom_call_target="tpu_custom_call" | custom-call | flops 10800000000 | bytes 3000000 | tf_op jit(solution)/shard_map/pallas_call | solution.py:263
  77.0 0.0 collective-permute-done.1.refs_2_
  77.0 0.0 collective-permute-done.2.refs_3_
  77.0 0.9 copy-done.10
  77.9 24.8 %shard_map.156 = (f32[12,8,256]{2,1,0:T(8,128)}, f32[12,80,256]{2,1,0:T(8,128)}) custom-call(s32[4,4,59]{2,1,0:T(4,128)} %constant.20.clone.refs_0_, s32[1]{0:T(128)} %bitcast.3.refs_1_, bf16[4,800,128]{2,1,0:T(8,128)(2,1)} %copy-done.10, bf16[4,800,128]{2,1,0:T(8,128)(2,1)} %collective-permute-done.2.refs_3_, ...), custom_call_target="tpu_custom_call" | custom-call | flops 21600000000 | bytes 3000000 | tf_op jit(solution)/shard_map/pallas_call | solution.py:263
  102.7 0.0 collective-permute-done.refs_2_
  102.7 0.9 copy-done.9
  103.6 16.2 %shard_map.157 = bf16[16,96,128]{2,1,0:T(8,128)(2,1)} custom-call(s32[4,4,33]{2,1,0:T(4,128)} %constant.21.clone.refs_0_, s32[1]{0:T(128)} %bitcast.3.refs_1_, bf16[4,800,128]{2,1,0:T(8,128)(2,1)} %copy-done.9, bf16[12,128,256]{2,1,0:T(8,128)(2,1)} %get-tuple-element.22.refs_4_.refs_3_, f32[12,8,256]{2,1,0:T(8,128)} %get-tuple-element.25.refs_4_, ...), custom_call_target="tpu_custom_call" | custom-call | flops 10800000000 | bytes 3000000 | tf_op jit(solution)/shard_map/pallas_call | solution.py:263
  119.8 17.9 %all_to_all.20.o_ref = bf16[16,96,128]{2,1,0:T(8,128)(2,1)} all-to-all(bf16[16,96,128]{2,1,0:T(8,128)(2,1)} %shard_map.157), channel_id=1, replica_groups=mesh['z'=4,'y'=4,'x'=4,'c'=2] {'z','y'}, dimensions={0} | all-to-all | bytes 786432 | tf_op jit(solution)/shard_map/all_to_all | solution.py:517
  137.7 2.0 shard_map.158
  139.7 3.5 %all-to-all-start.3 = ((bf16[8,96,256]{2,1,0:T(8,128)(2,1)}), bf16[8,96,256]{2,1,0:T(8,128)(2,1)S(1)}, u32[]{:S(2)}, u32[]{:S(2)}) async-start(bf16[8,96,256]{2,1,0:T(8,128)(2,1)} %shard_map.158), calls=%async_computation.3 | async-start | bytes 786432 | tf_op jit(solution)/shard_map/all_to_all | solution.py:518
  143.1 0.2 all-gather.11.cloned.1.call-start
  143.4 0.6 pad_add_fusion.place
  144.0 8.0 %all-to-all-done.3.a_ref = bf16[8,96,256]{2,1,0:T(8,128)(2,1)S(1)} async-done(((bf16[8,96,256]{2,1,0:T(8,128)(2,1)}), bf16[8,96,256]{2,1,0:T(8,128)(2,1)S(1)}, u32[]{:S(2)}, u32[]{:S(2)}) %all-to-all-start.3) | async-done | bytes 393248 | tf_op jit(solution)/shard_map/all_to_all | solution.py:518
  152.0 0.0 collective-permute-done.3.other_ref
  152.0 0.7 copy-done
  152.7 7.0 %shard_map.159.n_ref = bf16[96,2048]{1,0:T(8,128)(2,1)} custom-call(s32[3]{0:T(128)} %pad_add_fusion.place, bf16[8,96,256]{2,1,0:T(8,128)(2,1)} %copy-done, bf16[768,2048]{1,0:T(8,128)(2,1)} %stream_ref.1, f32[1,2048]{1,0:T(1,128)} %bitcast.45, f32[1,2048]{1,0:T(1,128)} %bitcast.46, bf16[4,256,2048]{2,1,0:T(8,128)(2,1)} %bitcast.39, ...), custom_call_target="tpu_custom_call" | custom-call | flops 805306368 | bytes 9000000 | tf_op jit(solution)/shard_map/pallas_call | solution.py:331
  159.8 0.0 all-gather.11.cloned.1.call-update
  159.8 0.0 all-gather.13.cloned.1.call-done
  159.8 11.9 %shard_map.160.refs_2_.refs_4_ = bf16[3,2048,512]{2,1,0:T(8,128)(2,1)} custom-call(bf16[16,1408,128]{2,1,0:T(8,128)(2,1)} %bitcast.37), custom_call_target="tpu_custom_call" | custom-call | flops 1000000000 | bytes 11000000 | tf_op jit(solution)/shard_map/pallas_call | solution.py:371
  171.7 27.0 %all-gather.11.cloned.1.call-done = bf16[768,2048]{1,0:T(8,128)(2,1)} async-done(((bf16[96,2048]{1,0:T(8,128)(2,1)}), bf16[768,2048]{1,0:T(8,128)(2,1)}) %all-gather.11.cloned.1.call-update) | async-done | bytes 3145744 | tf_op jit(solution)/shard_map/all_gather | solution.py:522
  198.7 9.5 %shard_map.162 = (bf16[2,96,2048]{2,1,0:T(8,128)(2,1)}, bf16[2,96,2048]{2,1,0:T(8,128)(2,1)}) custom-call(s32[3]{0:T(128)} %pad_add_fusion.place, bf16[8,96,2048]{2,1,0:T(8,128)(2,1)} %bitcast.29, bf16[8,96,2048]{2,1,0:T(8,128)(2,1)} %bitcast.30, bf16[8,96,2048]{2,1,0:T(8,128)(2,1)} %bitcast.31, bf16[8,96,2048]{2,1,0:T(8,128)(2,1)} %bitcast.32, ...), custom_call_target="tpu_custom_call" | custom-call | flops 3321888768 | bytes 10000000 | tf_op jit(solution)/shard_map/pallas_call | solution.py:427
  208.2 0.2 collective-permute-start.5
  208.5 7.6 %shard_map.164 = (bf16[1,96,2048]{2,1,0:T(8,128)(2,1)}, bf16[1,96,2048]{2,1,0:T(8,128)(2,1)}) custom-call(s32[3]{0:T(128)} %pad_add_fusion.place, bf16[8,96,2048]{2,1,0:T(8,128)(2,1)} %bitcast.33, bf16[8,96,2048]{2,1,0:T(8,128)(2,1)} %bitcast.34, bf16[3,2048,512]{2,1,0:T(8,128)(2,1)} %shard_map.160.refs_2_.refs_4_, bf16[16,704,128]{2,1,0:T(8,128)(2,1)} %bitcast.21, ...), custom_call_target="tpu_custom_call" | custom-call | flops 1660944384 | bytes 10000000 | tf_op jit(solution)/shard_map/pallas_call | solution.py:427
  216.1 0.3 collective-permute-start.8
  216.4 7.6 %shard_map.161 = (bf16[1,96,2048]{2,1,0:T(8,128)(2,1)}, bf16[1,96,2048]{2,1,0:T(8,128)(2,1)}) custom-call(s32[3]{0:T(128)} %pad_add_fusion.place, bf16[8,96,2048]{2,1,0:T(8,128)(2,1)} %bitcast.35, bf16[8,96,2048]{2,1,0:T(8,128)(2,1)} %bitcast.36, bf16[3,2048,512]{2,1,0:T(8,128)(2,1)} %shard_map.160.refs_2_.refs_4_, bf16[16,704,128]{2,1,0:T(8,128)(2,1)} %bitcast.25, ...), custom_call_target="tpu_custom_call" | custom-call | flops 1660944384 | bytes 10000000 | tf_op jit(solution)/shard_map/pallas_call | solution.py:427
  223.9 0.2 collective-permute-start.4
  224.2 0.0 collective-permute-done.8.refs_1_
  224.2 0.8 copy-done.4
  224.9 1.9 shard_map.165
  226.9 1.6 collective-permute-start.9
  228.5 0.0 collective-permute-done.5.refs_1_
  228.5 0.9 copy-done.2
  229.4 2.3 shard_map.163
  231.7 0.9 collective-permute-start.6
  232.6 2.3 collective-permute-start.7
  235.0 0.0 collective-permute-done.4
  235.0 5.7 %collective-permute-done.9.refs_4_ = bf16[96,2048]{1,0:T(8,128)(2,1)S(1)} collective-permute-done((bf16[96,2048]{1,0:T(8,128)(2,1)}, bf16[96,2048]{1,0:T(8,128)(2,1)S(1)}, u32[]{:S(2)}, u32[]{:S(2)}) %collective-permute-start.9) | collective-permute-done | bytes 393248 | tf_op jit(solution)/shard_map/ppermute | solution.py:497
  240.6 7.7 %collective-permute-done.6.refs_2_ = bf16[96,2048]{1,0:T(8,128)(2,1)S(1)} collective-permute-done((bf16[96,2048]{1,0:T(8,128)(2,1)}, bf16[96,2048]{1,0:T(8,128)(2,1)S(1)}, u32[]{:S(2)}, u32[]{:S(2)}) %collective-permute-start.6) | collective-permute-done | bytes 393248 | tf_op jit(solution)/shard_map/ppermute | solution.py:497
  248.3 0.0 collective-permute-done.7.refs_3_
  248.3 0.0 copy-done.5
  248.3 0.0 copy-done.6
  248.3 0.7 copy-done.7
  249.0 0.1 copy-done.8
  249.2 3.0 %shard_map.166 = bf16[96,2048]{1,0:T(8,128)(2,1)} custom-call(bf16[96,2048]{1,0:T(8,128)(2,1)} %shard_map.159.n_ref, f32[1,2048]{1,0:T(1,128)} %bitcast.47, f32[1,2048]{1,0:T(1,128)} %bitcast.48, bf16[96,2048]{1,0:T(8,128)(2,1)} %bitcast.40, bf16[96,2048]{1,0:T(8,128)(2,1)} %bitcast.41, bf16[96,2048]{1,0:T(8,128)(2,1)} %copy-done.7, ...), custom_call_target="tpu_custom_call" | custom-call | flops 4000000 | bytes 4000000 | tf_op jit(solution)/shard_map/pallas_call | solution.py:476
  (12 shorter events, 0.0 us)
Async XLA Ops:
  6.5 53.1 %all-gather.9.cloned.1.call-start = ((), (), s32[]{:S(2)}) async-start(), calls=%async_computation.4 | async-start | bytes 5242880 | tf_op jit(solution)/shard_map/all_gather | solution.py:503
  7.3 152.6 %all-gather.13.cloned.1.call-start = ((), (), s32[]{:S(2)}) async-start(), calls=%async_computation.6 | async-start | bytes 6127616 | tf_op jit(solution)/shard_map/all_gather | solution.py:511
  12.0 18.1 %all-to-all-start = ((bf16[4,800,128]{2,1,0:T(8,128)(2,1)}), bf16[4,800,128]{2,1,0:T(8,128)(2,1)S(1)}, u32[]{:S(2)}, u32[]{:S(2)}) async-start(bf16[4,800,128]{2,1,0:T(8,128)(2,1)} %get-tuple-element.20), calls=%async_computation | async-start | bytes 1638400 | tf_op jit(solution)/shard_map/all_to_all | solution.py:506
  17.4 154.3 %all-gather.15.cloned.1.call-start = ((), (), s32[]{:S(2)}) async-start(), calls=%async_computation.7 | async-start | bytes 3063808 | tf_op jit(solution)/shard_map/all_gather | solution.py:512
  30.1 29.6 %copy-start.1 = (bf16[4,800,128]{2,1,0:T(8,128)(2,1)}, bf16[4,800,128]{2,1,0:T(8,128)(2,1)S(1)}, u32[]{:S(2)}) copy-start(bf16[4,800,128]{2,1,0:T(8,128)(2,1)S(1)} %all-to-all-done.refs_2_) | copy-start | bytes 2457604
  30.1 29.6 %all-to-all-start.1 = ((bf16[16,96,128]{2,1,0:T(8,128)(2,1)}), bf16[16,96,128]{2,1,0:T(8,128)(2,1)S(1)}, u32[]{:S(2)}, u32[]{:S(2)}) async-start(bf16[16,96,128]{2,1,0:T(8,128)(2,1)} %get-tuple-element.21), calls=%async_computation.1 | async-start | bytes 786432 | tf_op jit(solution)/shard_map/all_to_all | solution.py:505
  35.3 41.8 %collective-permute-start.1 = (bf16[4,800,128]{2,1,0:T(8,128)(2,1)S(1)}, bf16[4,800,128]{2,1,0:T(8,128)(2,1)S(1)}, u32[]{:S(2)}, u32[]{:S(2)}) collective-permute-start(bf16[4,800,128]{2,1,0:T(8,128)(2,1)S(1)} %all-to-all-done.refs_2_), channel_id=1, source_target_pairs={{0,8},{8,16},{16,24},{24,0},{1,9},{9,17},{17,25},{25,1},{2,10},{10... | collective-permute-start | bytes 2457608 | tf_op jit(solution)/shard_map/ppermute | solution.py:497
  37.2 39.9 %collective-permute-start.2 = (bf16[4,800,128]{2,1,0:T(8,128)(2,1)S(1)}, bf16[4,800,128]{2,1,0:T(8,128)(2,1)}, u32[]{:S(2)}, u32[]{:S(2)}) collective-permute-start(bf16[4,800,128]{2,1,0:T(8,128)(2,1)S(1)} %all-to-all-done.refs_2_), channel_id=1, source_target_pairs={{0,24},{8,0},{16,8},{24,16},{1,25},{9,1},{17,9},{25,17},{2,26},{10... | collective-permute-start | bytes 2457608 | tf_op jit(solution)/shard_map/ppermute | solution.py:497
  38.6 64.1 %collective-permute-start = (bf16[4,800,128]{2,1,0:T(8,128)(2,1)S(1)}, bf16[4,800,128]{2,1,0:T(8,128)(2,1)S(1)}, u32[]{:S(2)}, u32[]{:S(2)}) collective-permute-start(bf16[4,800,128]{2,1,0:T(8,128)(2,1)S(1)} %all-to-all-done.refs_2_), channel_id=1, source_target_pairs={{0,16},{8,24},{16,0},{24,8},{1,17},{9,25},{17,1},{25,9},{2,18},{10... | collective-permute-start | bytes 2457608 | tf_op jit(solution)/shard_map/ppermute | solution.py:497
  59.7 92.3 %collective-permute-start.3 = (bf16[4,256,2048]{2,1,0:T(8,128)(2,1)}, bf16[4,256,2048]{2,1,0:T(8,128)(2,1)}, u32[]{:S(2)}, u32[]{:S(2)}) collective-permute-start(bf16[4,256,2048]{2,1,0:T(8,128)(2,1)} %bitcast.38), channel_id=1, source_target_pairs={{0,1},{1,0},{2,3},{3,2},{4,5},{5,4},{6,7},{7,6},{8,9},{9,8},{10,11... | collective-permute-start | bytes 12582920 | tf_op jit(solution)/shard_map/ppermute | solution.py:500
  59.7 0.7 copy-start.3
  77.0 0.9 copy-start.10
  102.7 0.9 copy-start.9
  139.7 12.3 %all-to-all-start.3 = ((bf16[8,96,256]{2,1,0:T(8,128)(2,1)}), bf16[8,96,256]{2,1,0:T(8,128)(2,1)S(1)}, u32[]{:S(2)}, u32[]{:S(2)}) async-start(bf16[8,96,256]{2,1,0:T(8,128)(2,1)} %shard_map.158), calls=%async_computation.3 | async-start | bytes 786432 | tf_op jit(solution)/shard_map/all_to_all | solution.py:518
  143.1 55.6 %all-gather.11.cloned.1.call-start = ((), (), s32[]{:S(2)}) async-start(), calls=%async_computation.5 | async-start | bytes 3538944 | tf_op jit(solution)/shard_map/all_gather | solution.py:522
  152.0 0.7 copy-start
  208.2 20.3 %collective-permute-start.5 = (bf16[2,96,2048]{2,1,0:T(8,128)(2,1)}, bf16[2,96,2048]{2,1,0:T(8,128)(2,1)S(1)}, u32[]{:S(2)}, u32[]{:S(2)}) collective-permute-start(bf16[2,96,2048]{2,1,0:T(8,128)(2,1)} %get-tuple-element.30), channel_id=1, source_target_pairs={{0,1},{1,0},{2,3},{3,2},{4,5},{5,4},{6,7},{7,6},{8,9},{9,8},{10,11... | collective-permute-start | bytes 2359304 | tf_op jit(solution)/shard_map/ppermute | solution.py:500
  216.1 8.1 %collective-permute-start.8 = (bf16[1,96,2048]{2,1,0:T(8,128)(2,1)}, bf16[1,96,2048]{2,1,0:T(8,128)(2,1)S(1)}, u32[]{:S(2)}, u32[]{:S(2)}) collective-permute-start(bf16[1,96,2048]{2,1,0:T(8,128)(2,1)} %get-tuple-element.34), channel_id=1, source_target_pairs={{0,1},{1,0},{2,3},{3,2},{4,5},{5,4},{6,7},{7,6},{8,9},{9,8},{10,11... | collective-permute-start | bytes 1179656 | tf_op jit(solution)/shard_map/ppermute | solution.py:500
  223.9 11.0 %collective-permute-start.4 = (bf16[1,96,2048]{2,1,0:T(8,128)(2,1)}, bf16[1,96,2048]{2,1,0:T(8,128)(2,1)S(1)}, u32[]{:S(2)}, u32[]{:S(2)}) collective-permute-start(bf16[1,96,2048]{2,1,0:T(8,128)(2,1)} %get-tuple-element.28), channel_id=1, source_target_pairs={{0,1},{1,0},{2,3},{3,2},{4,5},{5,4},{6,7},{7,6},{8,9},{9,8},{10,11... | collective-permute-start | bytes 1179656 | tf_op jit(solution)/shard_map/ppermute | solution.py:500
  224.2 0.8 copy-start.4
  226.9 13.7 %collective-permute-start.9 = (bf16[96,2048]{1,0:T(8,128)(2,1)}, bf16[96,2048]{1,0:T(8,128)(2,1)S(1)}, u32[]{:S(2)}, u32[]{:S(2)}) collective-permute-start(bf16[96,2048]{1,0:T(8,128)(2,1)} %shard_map.165), channel_id=1, source_target_pairs={{0,4},{2,6},{4,0},{6,2},{1,5},{3,7},{5,1},{7,3},{8,12},{10,14},{12... | collective-permute-start | bytes 1179656 | tf_op jit(solution)/shard_map/ppermute | solution.py:497
  228.5 0.9 copy-start.2
  231.7 16.6 %collective-permute-start.6 = (bf16[96,2048]{1,0:T(8,128)(2,1)}, bf16[96,2048]{1,0:T(8,128)(2,1)S(1)}, u32[]{:S(2)}, u32[]{:S(2)}) collective-permute-start(bf16[96,2048]{1,0:T(8,128)(2,1)} %get-tuple-element.31), channel_id=1, source_target_pairs={{0,2},{2,4},{4,6},{6,0},{1,3},{3,5},{5,7},{7,1},{8,10},{10,12},{12... | collective-permute-start | bytes 1179656 | tf_op jit(solution)/shard_map/ppermute | solution.py:497
  232.6 15.7 %collective-permute-start.7 = (bf16[96,2048]{1,0:T(8,128)(2,1)}, bf16[96,2048]{1,0:T(8,128)(2,1)S(1)}, u32[]{:S(2)}, u32[]{:S(2)}) collective-permute-start(bf16[96,2048]{1,0:T(8,128)(2,1)} %get-tuple-element.32), channel_id=1, source_target_pairs={{0,6},{2,0},{4,2},{6,4},{1,7},{3,1},{5,3},{7,5},{8,14},{10,8},{12,... | collective-permute-start | bytes 1179656 | tf_op jit(solution)/shard_map/ppermute | solution.py:497
  235.0 13.4 %copy-start.5 = (bf16[1,96,2048]{2,1,0:T(8,128)(2,1)}, bf16[1,96,2048]{2,1,0:T(8,128)(2,1)S(1)}, u32[]{:S(2)}) copy-start(bf16[1,96,2048]{2,1,0:T(8,128)(2,1)S(1)} %collective-permute-done.4) | copy-start | bytes 1179652
  240.6 7.7 %copy-start.6 = (bf16[96,2048]{1,0:T(8,128)(2,1)}, bf16[96,2048]{1,0:T(8,128)(2,1)S(1)}, u32[]{:S(2)}) copy-start(bf16[96,2048]{1,0:T(8,128)(2,1)S(1)} %collective-permute-done.9.refs_4_) | copy-start | bytes 1179652
  248.3 0.7 copy-start.7
  248.3 0.9 copy-start.8
Sparse Core Ops, SparseCore 0:
  9.0 50.6 all-gather.8
  61.8 59.7 all-gather.12
  123.8 46.6 all-gather.14
  172.0 26.6 all-gather.10

commit v5 on v4

--- a/solution.py
+++ b/solution.py
@@ -355,7 +355,8 @@
 BLOCKS = 3
 
 
-def prepare_kernel(w_ref, in_ref):
+def prepare_kernel(w_ref, in_ref, down_ref):
+    down_ref[...] = w_ref[:, 1408:2112, :]
     for j in range(BLOCKS):
         live = min(256, 704 - 256 * j)
         for part in range(2):
@@ -370,10 +371,16 @@
 def prepare(w):
     return pl.pallas_call(
         prepare_kernel,
-        out_shape=jax.ShapeDtypeStruct((BLOCKS, 2048, 512), BF16),
+        out_shape=(
+            jax.ShapeDtypeStruct((BLOCKS, 2048, 512), BF16),
+            jax.ShapeDtypeStruct((NSH, 704, 128), BF16),
+        ),
         grid=(NSH,),
-        in_specs=[pl.BlockSpec((1, 1408, 128), lambda s: (s, 0, 0))],
-        out_specs=pl.BlockSpec((BLOCKS, 128, 512), lambda s: (0, s, 0)),
+        in_specs=[pl.BlockSpec((1, 2112, 128), lambda s: (s, 0, 0))],
+        out_specs=(
+            pl.BlockSpec((BLOCKS, 128, 512), lambda s: (0, s, 0)),
+            pl.BlockSpec((1, 704, 128), lambda s: (s, 0, 0)),
+        ),
         compiler_params=params(60),
         cost_estimate=pl.CostEstimate(
             flops=10**9, bytes_accessed=11 * 10**6, transcendentals=0
@@ -443,23 +450,8 @@
     )(place, *([gathered] * (2 * count)), w_in, *([w_down] * 4))
 
 
-def join_kernel(count, *refs):
-    same_ref, other_ref = refs[:2]
-    for i in range(count):
-        refs[2 + i][...] = (same_ref[i].astype(F32) + other_ref[i].astype(F32)).astype(BF16)
-
-
-def join(same, other):
-    count = same.shape[0]
-    shape = jax.ShapeDtypeStruct((HALF, 2048), BF16)
-    return pl.pallas_call(
-        functools.partial(join_kernel, count),
-        out_shape=(shape,) * count,
-        in_specs=[vmem()] * 2,
-        out_specs=(vmem(),) * count,
-        compiler_params=params(60),
-        cost_estimate=pl.CostEstimate(flops=10**6, bytes_accessed=10**6, transcendentals=0),
-    )(same, other)
+def join(one, two):
+    return (one.astype(F32) + two.astype(F32)).astype(BF16)
 
 
 def last_kernel(n_ref, gain_ref, bias_ref, *refs):
@@ -507,9 +499,8 @@
     kv_back, kv_ahead = turn(kv_own, "y", 1), turn(kv_own, "y", 3)
     kv_far = turn(kv_own, "y", 2)
     w_other = swap(w_same)
-    shards = jnp.concatenate([gate_weight.T, up_weight.T], axis=0)
-    gu_all = lax.all_gather(shards, ("z", "y"), axis=0, tiled=False)
-    w_down = lax.all_gather(down_weight, ("z", "y"), axis=0, tiled=False)
+    shards = jnp.concatenate([gate_weight.T, up_weight.T, down_weight], axis=0)
+    ffn_all = lax.all_gather(shards, ("z", "y"), axis=0, tiled=False)
 
     qt, *state = attend(yi, (0,), [kv_own], q=q_mine)
     state = attend(yi, (3, 1), [kv_back, kv_ahead], state=(qt, *state))
@@ -520,7 +511,7 @@
     )
     normed = mix(place, by_rows, stream_in, mix_gain[None], mix_bias[None], w_same, w_other)
     gathered = lax.all_gather(normed, ("x", "c"), axis=0, tiled=False)
-    w_in = prepare(gu_all)
+    w_in, w_down = prepare(ffn_all)
 
     far_same, far_other = ffn((2,), place, gathered, w_in, w_down)
     far_swapped = swap(far_other)
@@ -528,9 +519,9 @@
     near_swapped = swap(near_other)
     own_same, own_other = ffn((0,), place, gathered, w_in, w_down)
     own_swapped = swap(own_other)
-    from_far = turn(join(far_same, far_swapped)[0], "x", 2)
-    near_back, near_ahead = join(near_same, near_swapped)
-    from_back, from_ahead = turn(near_back, "x", 1), turn(near_ahead, "x", 3)
+    from_far = turn(join(far_same[0], far_swapped[0]), "x", 2)
+    near = [join(near_same[i], near_swapped[i]) for i in range(2)]
+    from_back, from_ahead = turn(near[0], "x", 1), turn(near[1], "x", 3)
     parts = [own_same[0], own_swapped[0], from_back, from_ahead, from_far]
     return last(parts, normed, ffn_gain[None], ffn_bias[None])
 

time: 261 us -> 246 us (0.943)
  waiting for transfers between devices: 80.7 us -> 53.5 us
  blocking collectives: 17.9 us -> 39.2 us
  starting transfers between devices: 25.4 us -> 20.9 us
    all_to_all x0 -> x1, blocking collectives: none -> 18.1 us  [body(): lax.all_to_all(kv_pack, 'z', split_axis=0, concat_axis=0, tiled=True)]
    all_gather x1, waiting for transfers between devices: 27 us -> 9.68 us  [body(): gathered = lax.all_gather(normed, ('x', 'c'), axis=0, tiled=False)]
    all_to_all x1 -> x0, waiting for transfers between devices: 11.9 us -> none  [body(): lax.all_to_all(kv_pack, 'z', split_axis=0, concat_axis=0, tiled=True)]
    all_to_all x1 -> x0, starting transfers between devices: 5.42 us -> none  [body(): lax.all_to_all(kv_pack, 'z', split_axis=0, concat_axis=0, tiled=True)]
    all_to_all x1, blocking collectives: 17.9 us -> 21.1 us  [body(): lax.all_to_all(attended, ('z', 'y'), split_axis=0, concat_axis=0, tiled=T...]
    pallas_call x3 -> x1, Pallas kernels: 16.2 us -> 13.3 us  [prepare(): pl.pallas_call(prepare_kernel, out_shape=(jax.ShapeDtypeStruct((BLOCKS, 2...]
  transfers between devices with their start and end apart: 17 -> 15, of which waited for: 6 -> 5; matrix products, arithmetic and copies ran while one was open for 1% -> 1% of each run, Pallas kernels for 39% -> 41%
where the time goes in v5:
time: 246 us; the launch traced here: 244 us
  Pallas kernels  111 us (45%)
  waiting for transfers between devices  53.5 us (22%)
  blocking collectives  39.2 us (16%)
  starting transfers between devices  20.9 us (8%)
  between operations  13.2 us (5%)
  local copies, waits for them, and re-layouts  4.17 us (2%)
  other arithmetic  2.88 us (1%)
    pallas_call x3, Pallas kernels, attend(): pl.pallas_call(functools.partial(attend_kernel, chunks, first, final), ou...  57.6 us
    pallas_call x3, Pallas kernels, ffn(): pl.pallas_call(functools.partial(ffn_kernel, count), out_shape=(shape, sh...  24.7 us
    all_to_all x1, blocking collectives, body(): lax.all_to_all(attended, ('z', 'y'), split_axis=0, concat_axis=0, tiled=T...  21.1 us
    all_gather x1, waiting for transfers between devices, body(): w_same = lax.all_gather(out_weight, 'x', axis=0, tiled=False)  18.8 us
    all_to_all x1, blocking collectives, body(): lax.all_to_all(kv_pack, 'z', split_axis=0, concat_axis=0, tiled=True)  18.1 us
    ppermute x6, waiting for transfers between devices, turn(): return lax.ppermute(value, axis, [(i, (i + d) % 4) for i in range(4)])  15.9 us
    pallas_call x1, Pallas kernels, prepare(): pl.pallas_call(prepare_kernel, out_shape=(jax.ShapeDtypeStruct((BLOCKS, 2...  13.3 us
    ppermute x6, starting transfers between devices, turn(): return lax.ppermute(value, axis, [(i, (i + d) % 4) for i in range(4)])  10.4 us
  transfers between devices with their start and end apart: 15, of which 5 were waited for; matrix products, arithmetic and copies ran while one was open for 1% of the time, Pallas kernels for 41%

profile of v5, /device:TPU:0, one launch (start us, length us, event | category | flops | bytes accessed | tf_op | source)
XLA Modules:
  0.0 244.4 jit_solution(15380191572617304474)
XLA Ops:
  6.5 0.0 all-gather.7.cloned.1.call-start
  6.5 0.7 all-gather.7.cloned.1.call-update
  7.3 0.0 all-gather.11.cloned.1.call-start
  7.3 1.9 pad_maximum_fusion
  9.2 0.0 all-gather.11.cloned.1.call-update
  9.3 2.9 %shard_map.154 = (bf16[16,96,128]{2,1,0:T(8,128)(2,1)}, bf16[4,800,128]{2,1,0:T(8,128)(2,1)}) custom-call(bf16[768,256]{1,0:T(8,128)(2,1)} %q_ref.1, bf16[768,256]{1,0:T(8,128)(2,1)} %k_ref.1, bf16[768,256]{1,0:T(8,128)(2,1)} %v_ref.1, f32[4,768]{1,0:T(4,128)} %bitcast.37), custom_call_target="tpu_custom_call" | custom-call | flops 1000000 | bytes 2500000 | tf_op jit(solution)/shard_map/pallas_call | solution.py:59
  12.1 18.1 %all_to_all.20.refs_2_ = bf16[4,800,128]{2,1,0:T(8,128)(2,1)S(1)} all-to-all(bf16[4,800,128]{2,1,0:T(8,128)(2,1)} %get-tuple-element.20), channel_id=1, replica_groups=mesh['z'=4,'y'=4,'x'=4,'c'=2] {'z'}, dimensions={0} | all-to-all | bytes 1638400 | tf_op jit(solution)/shard_map/all_to_all | solution.py:498
  30.2 0.0 copy-start.1
  30.2 5.2 %all-to-all-start.1 = ((bf16[16,96,128]{2,1,0:T(8,128)(2,1)}), bf16[16,96,128]{2,1,0:T(8,128)(2,1)S(1)}, u32[]{:S(2)}, u32[]{:S(2)}) async-start(bf16[16,96,128]{2,1,0:T(8,128)(2,1)} %get-tuple-element.21), calls=%async_computation.1 | async-start | bytes 786432 | tf_op jit(solution)/shard_map/all_to_all | solution.py:497
  35.4 1.9 collective-permute-start.1
  37.3 1.4 collective-permute-start.2
  38.7 2.1 collective-permute-start
  40.8 18.8 %all-gather.7.cloned.1.call-done = bf16[1024,2048]{1,0:T(8,128)(2,1)} async-done(((bf16[256,2048]{1,0:T(8,128)(2,1)}), bf16[1024,2048]{1,0:T(8,128)(2,1)}) %all-gather.7.cloned.1.call-update) | async-done | bytes 4194320 | tf_op jit(solution)/shard_map/all_gather | solution.py:495
  59.7 0.0 collective-permute-start.3
  59.7 0.0 all-to-all-done.1.refs_3_
  59.7 0.0 copy-start.3
  59.7 0.0 copy-done.1
  59.7 0.7 copy-done.3
  60.4 16.6 %shard_map.155 = (bf16[12,128,256]{2,1,0:T(8,128)(2,1)}, f32[12,8,256]{2,1,0:T(8,128)}, f32[12,80,256]{2,1,0:T(8,128)}) custom-call(s32[4,4,33]{2,1,0:T(4,128)} %constant.19.clone.refs_0_, s32[1]{0:T(128)} %bitcast.3.refs_1_, bf16[4,800,128]{2,1,0:T(8,128)(2,1)} %copy-done.1, bf16[16,96,128]{2,1,0:T(8,128)(2,1)} %copy-done.3), custom_call_target="tpu_custom_call" | custom-call | flops 10800000000 | bytes 3000000 | tf_op jit(solution)/shard_map/pallas_call | solution.py:263
  77.0 0.0 collective-permute-done.1.refs_2_
  77.0 0.0 copy-start.10
  77.0 0.0 collective-permute-done.2.refs_3_
  77.0 0.9 copy-done.10
  77.9 24.8 %shard_map.156 = (f32[12,8,256]{2,1,0:T(8,128)}, f32[12,80,256]{2,1,0:T(8,128)}) custom-call(s32[4,4,59]{2,1,0:T(4,128)} %constant.20.clone.refs_0_, s32[1]{0:T(128)} %bitcast.3.refs_1_, bf16[4,800,128]{2,1,0:T(8,128)(2,1)} %copy-done.10, bf16[4,800,128]{2,1,0:T(8,128)(2,1)} %collective-permute-done.2.refs_3_, ...), custom_call_target="tpu_custom_call" | custom-call | flops 21600000000 | bytes 3000000 | tf_op jit(solution)/shard_map/pallas_call | solution.py:263
  102.7 0.0 collective-permute-done.refs_2_
  102.7 0.9 copy-done.9
  103.6 16.3 %shard_map.157 = bf16[16,96,128]{2,1,0:T(8,128)(2,1)} custom-call(s32[4,4,33]{2,1,0:T(4,128)} %constant.21.clone.refs_0_, s32[1]{0:T(128)} %bitcast.3.refs_1_, bf16[4,800,128]{2,1,0:T(8,128)(2,1)} %copy-done.9, bf16[12,128,256]{2,1,0:T(8,128)(2,1)} %get-tuple-element.22.refs_4_.refs_3_, f32[12,8,256]{2,1,0:T(8,128)} %get-tuple-element.25.refs_4_, ...), custom_call_target="tpu_custom_call" | custom-call | flops 10800000000 | bytes 3000000 | tf_op jit(solution)/shard_map/pallas_call | solution.py:263
  119.8 21.1 %all_to_all.21.o_ref = bf16[16,96,128]{2,1,0:T(8,128)(2,1)} all-to-all(bf16[16,96,128]{2,1,0:T(8,128)(2,1)} %shard_map.157), channel_id=1, replica_groups=mesh['z'=4,'y'=4,'x'=4,'c'=2] {'z','y'}, dimensions={0} | all-to-all | bytes 786432 | tf_op jit(solution)/shard_map/all_to_all | solution.py:508
  141.0 2.0 shard_map.158
  143.0 4.2 %all-to-all-start.3 = ((bf16[8,96,256]{2,1,0:T(8,128)(2,1)}), bf16[8,96,256]{2,1,0:T(8,128)(2,1)S(1)}, u32[]{:S(2)}, u32[]{:S(2)}) async-start(bf16[8,96,256]{2,1,0:T(8,128)(2,1)} %shard_map.158), calls=%async_computation.3 | async-start | bytes 786432 | tf_op jit(solution)/shard_map/all_to_all | solution.py:509
  147.2 0.0 all-gather.9.cloned.1.call-start
  147.3 0.6 pad_add_fusion.place
  147.9 8.3 %all-to-all-done.3.a_ref = bf16[8,96,256]{2,1,0:T(8,128)(2,1)S(1)} async-done(((bf16[8,96,256]{2,1,0:T(8,128)(2,1)}), bf16[8,96,256]{2,1,0:T(8,128)(2,1)S(1)}, u32[]{:S(2)}, u32[]{:S(2)}) %all-to-all-start.3) | async-done | bytes 393248 | tf_op jit(solution)/shard_map/all_to_all | solution.py:509
  156.1 0.0 collective-permute-done.3.other_ref
  156.1 0.7 copy-done
  156.9 7.1 %shard_map.159.n_ref = bf16[96,2048]{1,0:T(8,128)(2,1)} custom-call(s32[3]{0:T(128)} %pad_add_fusion.place, bf16[8,96,256]{2,1,0:T(8,128)(2,1)} %copy-done, bf16[768,2048]{1,0:T(8,128)(2,1)} %stream_ref.1, f32[1,2048]{1,0:T(1,128)} %bitcast.38, f32[1,2048]{1,0:T(1,128)} %bitcast.39, bf16[4,256,2048]{2,1,0:T(8,128)(2,1)} %bitcast.32, ...), custom_call_target="tpu_custom_call" | custom-call | flops 805306368 | bytes 9000000 | tf_op jit(solution)/shard_map/pallas_call | solution.py:331
  163.9 0.0 all-gather.9.cloned.1.call-update
  164.0 0.0 all-gather.11.cloned.1.call-done
  164.0 13.3 %shard_map.160 = (bf16[3,2048,512]{2,1,0:T(8,128)(2,1)}, bf16[16,704,128]{2,1,0:T(8,128)(2,1)}) custom-call(bf16[16,2112,128]{2,1,0:T(8,128)(2,1)} %bitcast.30), custom_call_target="tpu_custom_call" | custom-call | flops 1000000000 | bytes 11000000 | tf_op jit(solution)/shard_map/pallas_call | solution.py:372
  177.3 9.7 %all-gather.9.cloned.1.call-done = bf16[768,2048]{1,0:T(8,128)(2,1)} async-done(((bf16[96,2048]{1,0:T(8,128)(2,1)}), bf16[768,2048]{1,0:T(8,128)(2,1)}) %all-gather.9.cloned.1.call-update) | async-done | bytes 3145744 | tf_op jit(solution)/shard_map/all_gather | solution.py:513
  187.0 7.6 %shard_map.163 = (bf16[1,96,2048]{2,1,0:T(8,128)(2,1)}, bf16[1,96,2048]{2,1,0:T(8,128)(2,1)}) custom-call(s32[3]{0:T(128)} %pad_add_fusion.place, bf16[8,96,2048]{2,1,0:T(8,128)(2,1)} %bitcast.22, bf16[8,96,2048]{2,1,0:T(8,128)(2,1)} %bitcast.23, bf16[3,2048,512]{2,1,0:T(8,128)(2,1)} %get-tuple-element.27.refs_2_.refs_4_, ...), custom_call_target="tpu_custom_call" | custom-call | flops 1660944384 | bytes 10000000 | tf_op jit(solution)/shard_map/pallas_call | solution.py:434
  194.6 0.2 collective-permute-start.8
  194.8 9.6 %shard_map.162 = (bf16[2,96,2048]{2,1,0:T(8,128)(2,1)}, bf16[2,96,2048]{2,1,0:T(8,128)(2,1)}) custom-call(s32[3]{0:T(128)} %pad_add_fusion.place, bf16[8,96,2048]{2,1,0:T(8,128)(2,1)} %bitcast.24, bf16[8,96,2048]{2,1,0:T(8,128)(2,1)} %bitcast.25, bf16[8,96,2048]{2,1,0:T(8,128)(2,1)} %bitcast.26, bf16[8,96,2048]{2,1,0:T(8,128)(2,1)} %bitcast.27, ...), custom_call_target="tpu_custom_call" | custom-call | flops 3321888768 | bytes 10000000 | tf_op jit(solution)/shard_map/pallas_call | solution.py:434
  204.4 0.4 collective-permute-start.5
  204.7 7.6 %shard_map.161 = (bf16[1,96,2048]{2,1,0:T(8,128)(2,1)}, bf16[1,96,2048]{2,1,0:T(8,128)(2,1)}) custom-call(s32[3]{0:T(128)} %pad_add_fusion.place, bf16[8,96,2048]{2,1,0:T(8,128)(2,1)} %bitcast.28, bf16[8,96,2048]{2,1,0:T(8,128)(2,1)} %bitcast.29, bf16[3,2048,512]{2,1,0:T(8,128)(2,1)} %get-tuple-element.27.refs_2_.refs_4_, ...), custom_call_target="tpu_custom_call" | custom-call | flops 1660944384 | bytes 10000000 | tf_op jit(solution)/shard_map/pallas_call | solution.py:434
  212.3 0.4 collective-permute-start.4
  212.6 0.0 collective-permute-done.8
  212.6 0.0 copy-done.4
  212.6 0.1 fusion.2
  212.8 1.7 collective-permute-start.9
  214.4 0.0 collective-permute-done.5
  214.4 0.0 copy-done.2
  214.4 0.3 fusion.1
  214.7 1.0 collective-permute-start.6
  215.7 2.3 collective-permute-start.7
  218.0 0.0 collective-permute-done.4
  218.0 8.3 %collective-permute-done.9.refs_4_ = bf16[96,2048]{1,0:T(8,128)(2,1)S(1)} collective-permute-done((bf16[96,2048]{1,0:T(8,128)(2,1)S(1)}, bf16[96,2048]{1,0:T(8,128)(2,1)S(1)}, u32[]{:S(2)}, u32[]{:S(2)}) %collective-permute-start.9) | collective-permute-done | bytes 393248 | tf_op jit(solution)/shard_map/ppermute | solution.py:489
  226.4 7.6 %collective-permute-done.6.refs_2_ = bf16[96,2048]{1,0:T(8,128)(2,1)S(1)} collective-permute-done((bf16[96,2048]{1,0:T(8,128)(2,1)S(1)}, bf16[96,2048]{1,0:T(8,128)(2,1)S(1)}, u32[]{:S(2)}, u32[]{:S(2)}) %collective-permute-start.6) | collective-permute-done | bytes 393248 | tf_op jit(solution)/shard_map/ppermute | solution.py:489
  233.9 0.0 collective-permute-done.7.refs_3_
  233.9 0.0 copy-done.5
  233.9 0.0 copy-done.6
  234.0 0.7 copy-done.7
  234.7 0.2 copy-done.8
  234.9 3.0 %shard_map.164 = bf16[96,2048]{1,0:T(8,128)(2,1)} custom-call(bf16[96,2048]{1,0:T(8,128)(2,1)} %shard_map.159.n_ref, f32[1,2048]{1,0:T(1,128)} %bitcast.40, f32[1,2048]{1,0:T(1,128)} %bitcast.41, bf16[96,2048]{1,0:T(8,128)(2,1)} %bitcast.33, bf16[96,2048]{1,0:T(8,128)(2,1)} %bitcast.34, bf16[96,2048]{1,0:T(8,128)(2,1)} %copy-done.7, ...), custom_call_target="tpu_custom_call" | custom-call | flops 4000000 | bytes 4000000 | tf_op jit(solution)/shard_map/pallas_call | solution.py:468
  (8 shorter events, 0.0 us)
Async XLA Ops:
  6.5 53.1 %all-gather.7.cloned.1.call-start = ((), (), s32[]{:S(2)}) async-start(), calls=%async_computation.4 | async-start | bytes 5242880 | tf_op jit(solution)/shard_map/all_gather | solution.py:495
  7.3 156.7 %all-gather.11.cloned.1.call-start = ((), (), s32[]{:S(2)}) async-start(), calls=%async_computation.6 | async-start | bytes 9191424 | tf_op jit(solution)/shard_map/all_gather | solution.py:503
  30.2 29.5 %copy-start.1 = (bf16[4,800,128]{2,1,0:T(8,128)(2,1)}, bf16[4,800,128]{2,1,0:T(8,128)(2,1)S(1)}, u32[]{:S(2)}) copy-start(bf16[4,800,128]{2,1,0:T(8,128)(2,1)S(1)} %all_to_all.20.refs_2_) | copy-start | bytes 2457604
  30.2 29.5 %all-to-all-start.1 = ((bf16[16,96,128]{2,1,0:T(8,128)(2,1)}), bf16[16,96,128]{2,1,0:T(8,128)(2,1)S(1)}, u32[]{:S(2)}, u32[]{:S(2)}) async-start(bf16[16,96,128]{2,1,0:T(8,128)(2,1)} %get-tuple-element.21), calls=%async_computation.1 | async-start | bytes 786432 | tf_op jit(solution)/shard_map/all_to_all | solution.py:497
  35.4 41.6 %collective-permute-start.1 = (bf16[4,800,128]{2,1,0:T(8,128)(2,1)S(1)}, bf16[4,800,128]{2,1,0:T(8,128)(2,1)S(1)}, u32[]{:S(2)}, u32[]{:S(2)}) collective-permute-start(bf16[4,800,128]{2,1,0:T(8,128)(2,1)S(1)} %all_to_all.20.refs_2_), channel_id=1, source_target_pairs={{0,8},{8,16},{16,24},{24,0},{1,9},{9,17},{17,25},{25,1},{2,10},{10... | collective-permute-start | bytes 2457608 | tf_op jit(solution)/shard_map/ppermute | solution.py:489
  37.3 39.7 %collective-permute-start.2 = (bf16[4,800,128]{2,1,0:T(8,128)(2,1)S(1)}, bf16[4,800,128]{2,1,0:T(8,128)(2,1)}, u32[]{:S(2)}, u32[]{:S(2)}) collective-permute-start(bf16[4,800,128]{2,1,0:T(8,128)(2,1)S(1)} %all_to_all.20.refs_2_), channel_id=1, source_target_pairs={{0,24},{8,0},{16,8},{24,16},{1,25},{9,1},{17,9},{25,17},{2,26},{10... | collective-permute-start | bytes 2457608 | tf_op jit(solution)/shard_map/ppermute | solution.py:489
  38.7 64.0 %collective-permute-start = (bf16[4,800,128]{2,1,0:T(8,128)(2,1)S(1)}, bf16[4,800,128]{2,1,0:T(8,128)(2,1)S(1)}, u32[]{:S(2)}, u32[]{:S(2)}) collective-permute-start(bf16[4,800,128]{2,1,0:T(8,128)(2,1)S(1)} %all_to_all.20.refs_2_), channel_id=1, source_target_pairs={{0,16},{8,24},{16,0},{24,8},{1,17},{9,25},{17,1},{25,9},{2,18},{10... | collective-permute-start | bytes 2457608 | tf_op jit(solution)/shard_map/ppermute | solution.py:489
  59.7 96.5 %collective-permute-start.3 = (bf16[4,256,2048]{2,1,0:T(8,128)(2,1)}, bf16[4,256,2048]{2,1,0:T(8,128)(2,1)}, u32[]{:S(2)}, u32[]{:S(2)}) collective-permute-start(bf16[4,256,2048]{2,1,0:T(8,128)(2,1)} %bitcast.31), channel_id=1, source_target_pairs={{0,1},{1,0},{2,3},{3,2},{4,5},{5,4},{6,7},{7,6},{8,9},{9,8},{10,11... | collective-permute-start | bytes 12582920 | tf_op jit(solution)/shard_map/ppermute | solution.py:492
  59.7 0.7 copy-start.3
  77.0 0.9 copy-start.10
  102.7 0.9 copy-start.9
  143.0 13.2 %all-to-all-start.3 = ((bf16[8,96,256]{2,1,0:T(8,128)(2,1)}), bf16[8,96,256]{2,1,0:T(8,128)(2,1)S(1)}, u32[]{:S(2)}, u32[]{:S(2)}) async-start(bf16[8,96,256]{2,1,0:T(8,128)(2,1)} %shard_map.158), calls=%async_computation.3 | async-start | bytes 786432 | tf_op jit(solution)/shard_map/all_to_all | solution.py:509
  147.2 39.8 %all-gather.9.cloned.1.call-start = ((), (), s32[]{:S(2)}) async-start(), calls=%async_computation.5 | async-start | bytes 3538944 | tf_op jit(solution)/shard_map/all_gather | solution.py:513
  156.1 0.7 copy-start
  194.6 18.1 %collective-permute-start.8 = (bf16[1,96,2048]{2,1,0:T(8,128)(2,1)}, bf16[1,96,2048]{2,1,0:T(8,128)(2,1)S(1)}, u32[]{:S(2)}, u32[]{:S(2)}) collective-permute-start(bf16[1,96,2048]{2,1,0:T(8,128)(2,1)} %get-tuple-element.34), channel_id=1, source_target_pairs={{0,1},{1,0},{2,3},{3,2},{4,5},{5,4},{6,7},{7,6},{8,9},{9,8},{10,11... | collective-permute-start | bytes 1179656 | tf_op jit(solution)/shard_map/ppermute | solution.py:492
  204.4 8.3 %copy-start.4 = (bf16[1,96,2048]{2,1,0:T(8,128)(2,1)S(1)}, bf16[1,96,2048]{2,1,0:T(8,128)(2,1)}, u32[]{:S(2)}) copy-start(bf16[1,96,2048]{2,1,0:T(8,128)(2,1)} %get-tuple-element.33) | copy-start | bytes 1179652
  204.4 10.1 %copy-start.2 = (bf16[2,96,2048]{2,1,0:T(8,128)(2,1)S(1)}, bf16[2,96,2048]{2,1,0:T(8,128)(2,1)}, u32[]{:S(2)}) copy-start(bf16[2,96,2048]{2,1,0:T(8,128)(2,1)} %get-tuple-element.31) | copy-start | bytes 2359300
  204.4 10.1 %collective-permute-start.5 = (bf16[2,96,2048]{2,1,0:T(8,128)(2,1)}, bf16[2,96,2048]{2,1,0:T(8,128)(2,1)S(1)}, u32[]{:S(2)}, u32[]{:S(2)}) collective-permute-start(bf16[2,96,2048]{2,1,0:T(8,128)(2,1)} %get-tuple-element.32), channel_id=1, source_target_pairs={{0,1},{1,0},{2,3},{3,2},{4,5},{5,4},{6,7},{7,6},{8,9},{9,8},{10,11... | collective-permute-start | bytes 2359304 | tf_op jit(solution)/shard_map/ppermute | solution.py:492
  212.3 5.7 %collective-permute-start.4 = (bf16[1,96,2048]{2,1,0:T(8,128)(2,1)}, bf16[1,96,2048]{2,1,0:T(8,128)(2,1)S(1)}, u32[]{:S(2)}, u32[]{:S(2)}) collective-permute-start(bf16[1,96,2048]{2,1,0:T(8,128)(2,1)} %get-tuple-element.30), channel_id=1, source_target_pairs={{0,1},{1,0},{2,3},{3,2},{4,5},{5,4},{6,7},{7,6},{8,9},{9,8},{10,11... | collective-permute-start | bytes 1179656 | tf_op jit(solution)/shard_map/ppermute | solution.py:492
  212.8 13.6 %collective-permute-start.9 = (bf16[96,2048]{1,0:T(8,128)(2,1)S(1)}, bf16[96,2048]{1,0:T(8,128)(2,1)S(1)}, u32[]{:S(2)}, u32[]{:S(2)}) collective-permute-start(bf16[96,2048]{1,0:T(8,128)(2,1)S(1)} %fusion.2), channel_id=1, source_target_pairs={{0,4},{2,6},{4,0},{6,2},{1,5},{3,7},{5,1},{7,3},{8,12},{10,14},{12... | collective-permute-start | bytes 1179656 | tf_op jit(solution)/shard_map/ppermute | solution.py:489
  214.7 19.2 %collective-permute-start.6 = (bf16[96,2048]{1,0:T(8,128)(2,1)S(1)}, bf16[96,2048]{1,0:T(8,128)(2,1)S(1)}, u32[]{:S(2)}, u32[]{:S(2)}) collective-permute-start(bf16[96,2048]{1,0:T(8,128)(2,1)S(1)} %get-tuple-element.36), channel_id=1, source_target_pairs={{0,2},{2,4},{4,6},{6,0},{1,3},{3,5},{5,7},{7,1},{8,10},{10,12},{12... | collective-permute-start | bytes 1179656 | tf_op jit(solution)/shard_map/ppermute | solution.py:489
  215.7 18.2 %collective-permute-start.7 = (bf16[96,2048]{1,0:T(8,128)(2,1)S(1)}, bf16[96,2048]{1,0:T(8,128)(2,1)S(1)}, u32[]{:S(2)}, u32[]{:S(2)}) collective-permute-start(bf16[96,2048]{1,0:T(8,128)(2,1)S(1)} %get-tuple-element.35), channel_id=1, source_target_pairs={{0,6},{2,0},{4,2},{6,4},{1,7},{3,1},{5,3},{7,5},{8,14},{10,8},{12,... | collective-permute-start | bytes 1179656 | tf_op jit(solution)/shard_map/ppermute | solution.py:489
  218.0 15.9 %copy-start.5 = (bf16[1,96,2048]{2,1,0:T(8,128)(2,1)}, bf16[1,96,2048]{2,1,0:T(8,128)(2,1)S(1)}, u32[]{:S(2)}) copy-start(bf16[1,96,2048]{2,1,0:T(8,128)(2,1)S(1)} %collective-permute-done.4) | copy-start | bytes 1179652
  226.4 7.6 %copy-start.6 = (bf16[96,2048]{1,0:T(8,128)(2,1)}, bf16[96,2048]{1,0:T(8,128)(2,1)S(1)}, u32[]{:S(2)}) copy-start(bf16[96,2048]{1,0:T(8,128)(2,1)S(1)} %collective-permute-done.9.refs_4_) | copy-start | bytes 1179652
  233.9 0.8 copy-start.7
  233.9 0.9 copy-start.8
Sparse Core Ops, SparseCore 0:
  9.0 50.6 all-gather.6
  61.8 76.4 all-gather.10
  164.1 22.8 all-gather.8

commit v6 on v5

--- a/solution.py
+++ b/solution.py
@@ -20,6 +20,7 @@
 NSH = 16
 PACK = 800
 TILE = 256
+SPLIT = 1
 TILES = SUB * NSH // TILE
 
 
@@ -80,15 +81,20 @@
                     s = z * 4 + (y + d) % 4
                     if s <= low + 1:
                         units.append((t, i * 4 + z, s, int(s >= low)))
-        if len(units) % 2:
-            units.append((0, 0, NSH - 1, 1))
-        counts.append(len(units))
+        plain = [u for u in units if not u[3]]
+        held = [u for u in units if u[3]]
+        if len(plain) % 2:
+            held.insert(0, plain.pop())
+        if len(held) % 2:
+            held.append((0, 0, NSH - 1, 1))
+        units = plain + held
+        counts.append((len(plain) // 2, len(units) // 2))
         tables.append([(0, 0, 0, 0)] + units + [units[-1]])
     width = max(len(u) for u in tables) + 1
     out = np.zeros((4, 4, width), np.int32)
     for y in range(4):
         out[y, :, : len(tables[y])] = np.array(tables[y], np.int32).T
-        out[y, :, -1] = counts[y]
+        out[y, 0:2, -1] = counts[y]
     return out
 
 
@@ -109,8 +115,8 @@
         else:
             top, acc = refs[at : at + 2]
             at += 2
-    kaug, vt, qpos, s_a, s_b, p_a, p_b, al_a, al_b = refs[at : at + 9]
-    at += 9
+    kaug, vt, qpos, s_a, s_b, p_a, p_b, al_a, al_b, mx_a, mx_b = refs[at : at + 11]
+    at += 11
     if first:
         qrow = refs[at]
     if final:
@@ -173,41 +179,54 @@
     al_b[...] = jnp.ones(al_b.shape, F32)
     p_b[...] = jnp.zeros(p_b.shape, BF16)
 
-    def scores(u, out):
-        out[...] = jnp.dot(kaug[tab[y, 1, u]], qt[tab[y, 0, u]], preferred_element_type=F32)
+    def scores(u, out, most, masked):
+        rows = ROWS // SPLIT
+        high = None
+        for i in range(SPLIT):
+            part = slice(i * rows, (i + 1) * rows)
+            s = jnp.dot(
+                kaug[tab[y, 1, u], part, :], qt[tab[y, 0, u]], preferred_element_type=F32
+            )
+            if masked:
+                pos = tab[y, 2, u] * ROWS + i * rows
+                pos = pos + lax.broadcasted_iota(jnp.int32, (rows, TILE), 0)
+                s = jnp.where(pos <= qpos[tab[y, 0, u], 0:1, :], s, -1e30)
+            out[part, :] = s
+            here = jnp.max(s.reshape(rows // 8, 8, TILE), axis=0)
+            high = here if high is None else jnp.maximum(high, here)
+        most[...] = high
 
     def gather(u, p_before, al_before):
         t = tab[y, 0, u]
         pv = jnp.dot(vt[tab[y, 1, u], 48:128, :], p_before[...], preferred_element_type=F32)
         acc[t] = acc[t] * al_before[0:1, :] + pv
 
-    scores(1, s_a)
-
-    def unit(u, s_now, s_next, p_before, p_now, al_before, al_now):
-        def work(masked):
-            scores(u + 1, s_next)
-            gather(u - 1, p_before, al_before)
-            t = tab[y, 0, u]
-            before = top[t, 0:1, :]
-            s = s_now[...]
-            if masked:
-                pos = tab[y, 2, u] * ROWS + lax.broadcasted_iota(jnp.int32, (ROWS, TILE), 0)
-                s = jnp.where(pos <= qpos[t, 0:1, :], s, -1e30)
-            high = jnp.maximum(before, jnp.max(s, axis=0, keepdims=True))
-            p_now[...] = jnp.exp(s - high).astype(BF16)
-            top[t, 0:1, :] = high
-            al_now[0:1, :] = jnp.exp(before - high)
-
-        lax.cond(tab[y, 3, u] == 1, lambda: work(True), lambda: work(False))
-
-    def pair(i, carry):
-        unit(2 * i + 1, s_a, s_b, p_b, p_a, al_b, al_a)
-        unit(2 * i + 2, s_b, s_a, p_a, p_b, al_a, al_b)
-        return carry
-
-    count = tab[y, 0, tab.shape[2] - 1]
-    lax.fori_loop(0, count // 2, pair, 0)
-    gather(count, p_b, al_b)
+    def unit(u, now, later, before, masked):
+        s_now, p_now, al_now, mx_now = now
+        s_next, _, _, mx_next = later
+        _, p_before, al_before, _ = before
+        t = tab[y, 0, u]
+        old = top[t, 0:1, :]
+        high = jnp.maximum(old, jnp.max(mx_now[...], axis=0, keepdims=True))
+        top[t, 0:1, :] = high
+        al_now[0:1, :] = jnp.exp(old - high)
+        scores(u + 1, s_next, mx_next, masked)
+        p_now[...] = jnp.exp(s_now[...] - high).astype(BF16)
+        gather(u - 1, p_before, al_before)
+
+    one, two = (s_a, p_a, al_a, mx_a), (s_b, p_b, al_b, mx_b)
+    last_at = tab.shape[2] - 1
+    plain, pairs = tab[y, 0, last_at], tab[y, 1, last_at]
+    for masked, low, high in ((False, 0, plain), (True, plain, pairs)):
+
+        def pair(i, carry):
+            unit(2 * i + 1, one, two, two, masked)
+            unit(2 * i + 2, two, one, one, masked)
+            return carry
+
+        scores(2 * low + 1, s_a, mx_a, masked)
+        lax.fori_loop(low, high, pair, 0)
+    gather(2 * pairs, p_b, al_b)
 
     if final:
 
@@ -243,9 +262,7 @@
         pltpu.VMEM((ROWS, TILE), F32),
         pltpu.VMEM((ROWS, TILE), BF16),
         pltpu.VMEM((ROWS, TILE), BF16),
-        pltpu.VMEM((8, TILE), F32),
-        pltpu.VMEM((8, TILE), F32),
-    ]
+    ] + [pltpu.VMEM((8, TILE), F32)] * 4
     if first:
         outs = (jax.ShapeDtypeStruct((TILES, 128, TILE), BF16),) + state_shapes
         scratch += [pltpu.VMEM((NSH, SUB, 128), F32)]
@@ -259,7 +276,7 @@
         outs = state_shapes
         rest = list(state)
     table = unit_table(steps)
-    share = int(table[:, 0, -1].mean())
+    share = 2 * int(table[:, 1, -1].mean())
     return pl.pallas_call(
         functools.partial(attend_kernel, chunks, first, final),
         out_shape=outs,

time: 246 us -> 236 us (0.959)
  Pallas kernels: 111 us -> 99.6 us
    pallas_call x3, Pallas kernels: 57.6 us -> 46.7 us  [attend(): pl.pallas_call(functools.partial(attend_kernel, chunks, first, final), ou...]
  transfers between devices with their start and end apart: 15 -> 15, of which waited for: 5 -> 5; matrix products, arithmetic and copies ran while one was open for 1% -> 1% of each run, Pallas kernels for 41% -> 38%
where the time goes in v6:
time: 236 us; the launch traced here: 234 us
  Pallas kernels  99.6 us (42%)
  waiting for transfers between devices  53.7 us (23%)
  blocking collectives  40.4 us (17%)
  starting transfers between devices  20.1 us (9%)
  between operations  13.2 us (6%)
  local copies, waits for them, and re-layouts  4.17 us (2%)
  other arithmetic  2.88 us (1%)
    pallas_call x3, Pallas kernels, attend(): pl.pallas_call(functools.partial(attend_kernel, chunks, first, final), ou...  46.7 us
    pallas_call x3, Pallas kernels, ffn(): pl.pallas_call(functools.partial(ffn_kernel, count), out_shape=(shape, sh...  24.7 us
    all_to_all x1, blocking collectives, body(): lax.all_to_all(attended, ('z', 'y'), split_axis=0, concat_axis=0, tiled=T...  22.3 us
    all_gather x1, waiting for transfers between devices, body(): w_same = lax.all_gather(out_weight, 'x', axis=0, tiled=False)  18.8 us
    all_to_all x1, blocking collectives, body(): lax.all_to_all(kv_pack, 'z', split_axis=0, concat_axis=0, tiled=True)  18.1 us
    ppermute x6, waiting for transfers between devices, turn(): return lax.ppermute(value, axis, [(i, (i + d) % 4) for i in range(4)])  15.9 us
    pallas_call x1, Pallas kernels, prepare(): pl.pallas_call(prepare_kernel, out_shape=(jax.ShapeDtypeStruct((BLOCKS, 2...  13.2 us
    ppermute x6, starting transfers between devices, turn(): return lax.ppermute(value, axis, [(i, (i + d) % 4) for i in range(4)])  10.4 us
  transfers between devices with their start and end apart: 15, of which 5 were waited for; matrix products, arithmetic and copies ran while one was open for 1% of the time, Pallas kernels for 38%

profile of v6, /device:TPU:0, one launch (start us, length us, event | category | flops | bytes accessed | tf_op | source)
XLA Modules:
  0.0 234.0 jit_solution(4261337781852728097)
XLA Ops:
  6.5 0.0 all-gather.7.cloned.1.call-start
  6.5 0.7 all-gather.7.cloned.1.call-update
  7.3 0.0 all-gather.11.cloned.1.call-start
  7.3 1.9 pad_maximum_fusion
  9.2 0.0 all-gather.11.cloned.1.call-update
  9.3 2.9 %shard_map.154 = (bf16[16,96,128]{2,1,0:T(8,128)(2,1)}, bf16[4,800,128]{2,1,0:T(8,128)(2,1)}) custom-call(bf16[768,256]{1,0:T(8,128)(2,1)} %q_ref.1, bf16[768,256]{1,0:T(8,128)(2,1)} %k_ref.1, bf16[768,256]{1,0:T(8,128)(2,1)} %v_ref.1, f32[4,768]{1,0:T(4,128)} %bitcast.37), custom_call_target="tpu_custom_call" | custom-call | flops 1000000 | bytes 2500000 | tf_op jit(solution)/shard_map/pallas_call | solution.py:60
  12.1 18.1 %all_to_all.20.refs_2_ = bf16[4,800,128]{2,1,0:T(8,128)(2,1)S(1)} all-to-all(bf16[4,800,128]{2,1,0:T(8,128)(2,1)} %get-tuple-element.20), channel_id=1, replica_groups=mesh['z'=4,'y'=4,'x'=4,'c'=2] {'z'}, dimensions={0} | all-to-all | bytes 1638400 | tf_op jit(solution)/shard_map/all_to_all | solution.py:515
  30.2 0.0 copy-start.1
  30.2 5.2 %all-to-all-start.1 = ((bf16[16,96,128]{2,1,0:T(8,128)(2,1)}), bf16[16,96,128]{2,1,0:T(8,128)(2,1)S(1)}, u32[]{:S(2)}, u32[]{:S(2)}) async-start(bf16[16,96,128]{2,1,0:T(8,128)(2,1)} %get-tuple-element.21), calls=%async_computation.1 | async-start | bytes 786432 | tf_op jit(solution)/shard_map/all_to_all | solution.py:514
  35.4 1.9 collective-permute-start.1
  37.3 1.4 collective-permute-start.2
  38.7 2.1 collective-permute-start
  40.8 18.8 %all-gather.7.cloned.1.call-done = bf16[1024,2048]{1,0:T(8,128)(2,1)} async-done(((bf16[256,2048]{1,0:T(8,128)(2,1)}), bf16[1024,2048]{1,0:T(8,128)(2,1)}) %all-gather.7.cloned.1.call-update) | async-done | bytes 4194320 | tf_op jit(solution)/shard_map/all_gather | solution.py:512
  59.7 0.0 collective-permute-start.3
  59.7 0.0 all-to-all-done.1.refs_3_
  59.7 0.0 copy-start.3
  59.7 0.0 copy-done.1
  59.7 0.7 copy-done.3
  60.4 13.5 %shard_map.155 = (bf16[12,128,256]{2,1,0:T(8,128)(2,1)}, f32[12,8,256]{2,1,0:T(8,128)}, f32[12,80,256]{2,1,0:T(8,128)}) custom-call(s32[4,4,33]{2,1,0:T(4,128)} %constant.19.clone.refs_0_, s32[1]{0:T(128)} %bitcast.3.refs_1_, bf16[4,800,128]{2,1,0:T(8,128)(2,1)} %copy-done.1, bf16[16,96,128]{2,1,0:T(8,128)(2,1)} %copy-done.3), custom_call_target="tpu_custom_call" | custom-call | flops 10400000000 | bytes 3000000 | tf_op jit(solution)/shard_map/pallas_call | solution.py:280
  73.9 0.0 collective-permute-done.1.refs_2_
  73.9 0.0 copy-start.10
  73.9 0.0 collective-permute-done.2.refs_3_
  73.9 0.9 copy-done.10
  74.8 19.2 %shard_map.156 = (f32[12,8,256]{2,1,0:T(8,128)}, f32[12,80,256]{2,1,0:T(8,128)}) custom-call(s32[4,4,59]{2,1,0:T(4,128)} %constant.20.clone.refs_0_, s32[1]{0:T(128)} %bitcast.3.refs_1_, bf16[4,800,128]{2,1,0:T(8,128)(2,1)} %copy-done.10, bf16[4,800,128]{2,1,0:T(8,128)(2,1)} %collective-permute-done.2.refs_3_, ...), custom_call_target="tpu_custom_call" | custom-call | flops 21600000000 | bytes 3000000 | tf_op jit(solution)/shard_map/pallas_call | solution.py:280
  94.0 0.0 collective-permute-done.refs_2_
  94.0 0.9 copy-done.9
  94.9 14.0 %shard_map.157 = bf16[16,96,128]{2,1,0:T(8,128)(2,1)} custom-call(s32[4,4,33]{2,1,0:T(4,128)} %constant.21.clone.refs_0_, s32[1]{0:T(128)} %bitcast.3.refs_1_, bf16[4,800,128]{2,1,0:T(8,128)(2,1)} %copy-done.9, bf16[12,128,256]{2,1,0:T(8,128)(2,1)} %get-tuple-element.22.refs_4_.refs_3_, f32[12,8,256]{2,1,0:T(8,128)} %get-tuple-element.25.refs_4_, ...), custom_call_target="tpu_custom_call" | custom-call | flops 10400000000 | bytes 3000000 | tf_op jit(solution)/shard_map/pallas_call | solution.py:280
  109.0 22.3 %all_to_all.21.o_ref = bf16[16,96,128]{2,1,0:T(8,128)(2,1)} all-to-all(bf16[16,96,128]{2,1,0:T(8,128)(2,1)} %shard_map.157), channel_id=1, replica_groups=mesh['z'=4,'y'=4,'x'=4,'c'=2] {'z','y'}, dimensions={0} | all-to-all | bytes 786432 | tf_op jit(solution)/shard_map/all_to_all | solution.py:525
  131.3 2.0 shard_map.158
  133.3 3.5 %all-to-all-start.3 = ((bf16[8,96,256]{2,1,0:T(8,128)(2,1)}), bf16[8,96,256]{2,1,0:T(8,128)(2,1)S(1)}, u32[]{:S(2)}, u32[]{:S(2)}) async-start(bf16[8,96,256]{2,1,0:T(8,128)(2,1)} %shard_map.158), calls=%async_computation.3 | async-start | bytes 786432 | tf_op jit(solution)/shard_map/all_to_all | solution.py:526
  136.8 0.0 all-gather.9.cloned.1.call-start
  136.8 0.6 pad_add_fusion.place
  137.4 8.2 %all-to-all-done.3.a_ref = bf16[8,96,256]{2,1,0:T(8,128)(2,1)S(1)} async-done(((bf16[8,96,256]{2,1,0:T(8,128)(2,1)}), bf16[8,96,256]{2,1,0:T(8,128)(2,1)S(1)}, u32[]{:S(2)}, u32[]{:S(2)}) %all-to-all-start.3) | async-done | bytes 393248 | tf_op jit(solution)/shard_map/all_to_all | solution.py:526
  145.6 0.0 collective-permute-done.3.other_ref
  145.6 0.7 copy-done
  146.4 7.1 %shard_map.159.n_ref = bf16[96,2048]{1,0:T(8,128)(2,1)} custom-call(s32[3]{0:T(128)} %pad_add_fusion.place, bf16[8,96,256]{2,1,0:T(8,128)(2,1)} %copy-done, bf16[768,2048]{1,0:T(8,128)(2,1)} %stream_ref.1, f32[1,2048]{1,0:T(1,128)} %bitcast.38, f32[1,2048]{1,0:T(1,128)} %bitcast.39, bf16[4,256,2048]{2,1,0:T(8,128)(2,1)} %bitcast.32, ...), custom_call_target="tpu_custom_call" | custom-call | flops 805306368 | bytes 9000000 | tf_op jit(solution)/shard_map/pallas_call | solution.py:348
  153.4 0.0 all-gather.9.cloned.1.call-update
  153.5 0.0 all-gather.11.cloned.1.call-done
  153.5 13.2 %shard_map.160 = (bf16[3,2048,512]{2,1,0:T(8,128)(2,1)}, bf16[16,704,128]{2,1,0:T(8,128)(2,1)}) custom-call(bf16[16,2112,128]{2,1,0:T(8,128)(2,1)} %bitcast.30), custom_call_target="tpu_custom_call" | custom-call | flops 1000000000 | bytes 11000000 | tf_op jit(solution)/shard_map/pallas_call | solution.py:389
  166.7 9.9 %all-gather.9.cloned.1.call-done = bf16[768,2048]{1,0:T(8,128)(2,1)} async-done(((bf16[96,2048]{1,0:T(8,128)(2,1)}), bf16[768,2048]{1,0:T(8,128)(2,1)}) %all-gather.9.cloned.1.call-update) | async-done | bytes 3145744 | tf_op jit(solution)/shard_map/all_gather | solution.py:530
  176.6 7.6 %shard_map.163 = (bf16[1,96,2048]{2,1,0:T(8,128)(2,1)}, bf16[1,96,2048]{2,1,0:T(8,128)(2,1)}) custom-call(s32[3]{0:T(128)} %pad_add_fusion.place, bf16[8,96,2048]{2,1,0:T(8,128)(2,1)} %bitcast.22, bf16[8,96,2048]{2,1,0:T(8,128)(2,1)} %bitcast.23, bf16[3,2048,512]{2,1,0:T(8,128)(2,1)} %get-tuple-element.27.refs_2_.refs_4_, ...), custom_call_target="tpu_custom_call" | custom-call | flops 1660944384 | bytes 10000000 | tf_op jit(solution)/shard_map/pallas_call | solution.py:451
  184.2 0.2 collective-permute-start.8
  184.4 9.6 %shard_map.162 = (bf16[2,96,2048]{2,1,0:T(8,128)(2,1)}, bf16[2,96,2048]{2,1,0:T(8,128)(2,1)}) custom-call(s32[3]{0:T(128)} %pad_add_fusion.place, bf16[8,96,2048]{2,1,0:T(8,128)(2,1)} %bitcast.24, bf16[8,96,2048]{2,1,0:T(8,128)(2,1)} %bitcast.25, bf16[8,96,2048]{2,1,0:T(8,128)(2,1)} %bitcast.26, bf16[8,96,2048]{2,1,0:T(8,128)(2,1)} %bitcast.27, ...), custom_call_target="tpu_custom_call" | custom-call | flops 3321888768 | bytes 10000000 | tf_op jit(solution)/shard_map/pallas_call | solution.py:451
  194.0 0.4 collective-permute-start.5
  194.3 7.6 %shard_map.161 = (bf16[1,96,2048]{2,1,0:T(8,128)(2,1)}, bf16[1,96,2048]{2,1,0:T(8,128)(2,1)}) custom-call(s32[3]{0:T(128)} %pad_add_fusion.place, bf16[8,96,2048]{2,1,0:T(8,128)(2,1)} %bitcast.28, bf16[8,96,2048]{2,1,0:T(8,128)(2,1)} %bitcast.29, bf16[3,2048,512]{2,1,0:T(8,128)(2,1)} %get-tuple-element.27.refs_2_.refs_4_, ...), custom_call_target="tpu_custom_call" | custom-call | flops 1660944384 | bytes 10000000 | tf_op jit(solution)/shard_map/pallas_call | solution.py:451
  201.9 0.4 collective-permute-start.4
  202.2 0.0 collective-permute-done.8
  202.2 0.0 copy-done.4
  202.2 0.1 fusion.2
  202.4 1.7 collective-permute-start.9
  204.0 0.0 collective-permute-done.5
  204.0 0.0 copy-done.2
  204.0 0.3 fusion.1
  204.3 1.0 collective-permute-start.6
  205.3 2.3 collective-permute-start.7
  207.6 0.0 collective-permute-done.4
  207.6 8.3 %collective-permute-done.9.refs_4_ = bf16[96,2048]{1,0:T(8,128)(2,1)S(1)} collective-permute-done((bf16[96,2048]{1,0:T(8,128)(2,1)S(1)}, bf16[96,2048]{1,0:T(8,128)(2,1)S(1)}, u32[]{:S(2)}, u32[]{:S(2)}) %collective-permute-start.9) | collective-permute-done | bytes 393248 | tf_op jit(solution)/shard_map/ppermute | solution.py:506
  216.0 7.6 %collective-permute-done.6.refs_2_ = bf16[96,2048]{1,0:T(8,128)(2,1)S(1)} collective-permute-done((bf16[96,2048]{1,0:T(8,128)(2,1)S(1)}, bf16[96,2048]{1,0:T(8,128)(2,1)S(1)}, u32[]{:S(2)}, u32[]{:S(2)}) %collective-permute-start.6) | collective-permute-done | bytes 393248 | tf_op jit(solution)/shard_map/ppermute | solution.py:506
  223.5 0.0 collective-permute-done.7.refs_3_
  223.5 0.0 copy-done.5
  223.5 0.0 copy-done.6
  223.6 0.7 copy-done.7
  224.3 0.2 copy-done.8
  224.5 3.0 %shard_map.164 = bf16[96,2048]{1,0:T(8,128)(2,1)} custom-call(bf16[96,2048]{1,0:T(8,128)(2,1)} %shard_map.159.n_ref, f32[1,2048]{1,0:T(1,128)} %bitcast.40, f32[1,2048]{1,0:T(1,128)} %bitcast.41, bf16[96,2048]{1,0:T(8,128)(2,1)} %bitcast.33, bf16[96,2048]{1,0:T(8,128)(2,1)} %bitcast.34, bf16[96,2048]{1,0:T(8,128)(2,1)} %copy-done.7, ...), custom_call_target="tpu_custom_call" | custom-call | flops 4000000 | bytes 4000000 | tf_op jit(solution)/shard_map/pallas_call | solution.py:485
  (8 shorter events, 0.0 us)
Async XLA Ops:
  6.5 53.1 %all-gather.7.cloned.1.call-start = ((), (), s32[]{:S(2)}) async-start(), calls=%async_computation.4 | async-start | bytes 5242880 | tf_op jit(solution)/shard_map/all_gather | solution.py:512
  7.3 146.2 %all-gather.11.cloned.1.call-start = ((), (), s32[]{:S(2)}) async-start(), calls=%async_computation.6 | async-start | bytes 9191424 | tf_op jit(solution)/shard_map/all_gather | solution.py:520
  30.2 29.5 %copy-start.1 = (bf16[4,800,128]{2,1,0:T(8,128)(2,1)}, bf16[4,800,128]{2,1,0:T(8,128)(2,1)S(1)}, u32[]{:S(2)}) copy-start(bf16[4,800,128]{2,1,0:T(8,128)(2,1)S(1)} %all_to_all.20.refs_2_) | copy-start | bytes 2457604
  30.2 29.5 %all-to-all-start.1 = ((bf16[16,96,128]{2,1,0:T(8,128)(2,1)}), bf16[16,96,128]{2,1,0:T(8,128)(2,1)S(1)}, u32[]{:S(2)}, u32[]{:S(2)}) async-start(bf16[16,96,128]{2,1,0:T(8,128)(2,1)} %get-tuple-element.21), calls=%async_computation.1 | async-start | bytes 786432 | tf_op jit(solution)/shard_map/all_to_all | solution.py:514
  35.4 38.5 %collective-permute-start.1 = (bf16[4,800,128]{2,1,0:T(8,128)(2,1)S(1)}, bf16[4,800,128]{2,1,0:T(8,128)(2,1)S(1)}, u32[]{:S(2)}, u32[]{:S(2)}) collective-permute-start(bf16[4,800,128]{2,1,0:T(8,128)(2,1)S(1)} %all_to_all.20.refs_2_), channel_id=1, source_target_pairs={{0,8},{8,16},{16,24},{24,0},{1,9},{9,17},{17,25},{25,1},{2,10},{10... | collective-permute-start | bytes 2457608 | tf_op jit(solution)/shard_map/ppermute | solution.py:506
  37.3 36.6 %collective-permute-start.2 = (bf16[4,800,128]{2,1,0:T(8,128)(2,1)S(1)}, bf16[4,800,128]{2,1,0:T(8,128)(2,1)}, u32[]{:S(2)}, u32[]{:S(2)}) collective-permute-start(bf16[4,800,128]{2,1,0:T(8,128)(2,1)S(1)} %all_to_all.20.refs_2_), channel_id=1, source_target_pairs={{0,24},{8,0},{16,8},{24,16},{1,25},{9,1},{17,9},{25,17},{2,26},{10... | collective-permute-start | bytes 2457608 | tf_op jit(solution)/shard_map/ppermute | solution.py:506
  38.7 55.3 %collective-permute-start = (bf16[4,800,128]{2,1,0:T(8,128)(2,1)S(1)}, bf16[4,800,128]{2,1,0:T(8,128)(2,1)S(1)}, u32[]{:S(2)}, u32[]{:S(2)}) collective-permute-start(bf16[4,800,128]{2,1,0:T(8,128)(2,1)S(1)} %all_to_all.20.refs_2_), channel_id=1, source_target_pairs={{0,16},{8,24},{16,0},{24,8},{1,17},{9,25},{17,1},{25,9},{2,18},{10... | collective-permute-start | bytes 2457608 | tf_op jit(solution)/shard_map/ppermute | solution.py:506
  59.7 85.9 %collective-permute-start.3 = (bf16[4,256,2048]{2,1,0:T(8,128)(2,1)}, bf16[4,256,2048]{2,1,0:T(8,128)(2,1)}, u32[]{:S(2)}, u32[]{:S(2)}) collective-permute-start(bf16[4,256,2048]{2,1,0:T(8,128)(2,1)} %bitcast.31), channel_id=1, source_target_pairs={{0,1},{1,0},{2,3},{3,2},{4,5},{5,4},{6,7},{7,6},{8,9},{9,8},{10,11... | collective-permute-start | bytes 12582920 | tf_op jit(solution)/shard_map/ppermute | solution.py:509
  59.7 0.7 copy-start.3
  73.9 0.9 copy-start.10
  94.0 0.9 copy-start.9
  133.3 12.3 %all-to-all-start.3 = ((bf16[8,96,256]{2,1,0:T(8,128)(2,1)}), bf16[8,96,256]{2,1,0:T(8,128)(2,1)S(1)}, u32[]{:S(2)}, u32[]{:S(2)}) async-start(bf16[8,96,256]{2,1,0:T(8,128)(2,1)} %shard_map.158), calls=%async_computation.3 | async-start | bytes 786432 | tf_op jit(solution)/shard_map/all_to_all | solution.py:526
  136.8 39.8 %all-gather.9.cloned.1.call-start = ((), (), s32[]{:S(2)}) async-start(), calls=%async_computation.5 | async-start | bytes 3538944 | tf_op jit(solution)/shard_map/all_gather | solution.py:530
  145.6 0.7 copy-start
  184.2 18.1 %collective-permute-start.8 = (bf16[1,96,2048]{2,1,0:T(8,128)(2,1)}, bf16[1,96,2048]{2,1,0:T(8,128)(2,1)S(1)}, u32[]{:S(2)}, u32[]{:S(2)}) collective-permute-start(bf16[1,96,2048]{2,1,0:T(8,128)(2,1)} %get-tuple-element.34), channel_id=1, source_target_pairs={{0,1},{1,0},{2,3},{3,2},{4,5},{5,4},{6,7},{7,6},{8,9},{9,8},{10,11... | collective-permute-start | bytes 1179656 | tf_op jit(solution)/shard_map/ppermute | solution.py:509
  194.0 8.3 %copy-start.4 = (bf16[1,96,2048]{2,1,0:T(8,128)(2,1)S(1)}, bf16[1,96,2048]{2,1,0:T(8,128)(2,1)}, u32[]{:S(2)}) copy-start(bf16[1,96,2048]{2,1,0:T(8,128)(2,1)} %get-tuple-element.33) | copy-start | bytes 1179652
  194.0 10.1 %copy-start.2 = (bf16[2,96,2048]{2,1,0:T(8,128)(2,1)S(1)}, bf16[2,96,2048]{2,1,0:T(8,128)(2,1)}, u32[]{:S(2)}) copy-start(bf16[2,96,2048]{2,1,0:T(8,128)(2,1)} %get-tuple-element.31) | copy-start | bytes 2359300
  194.0 10.1 %collective-permute-start.5 = (bf16[2,96,2048]{2,1,0:T(8,128)(2,1)}, bf16[2,96,2048]{2,1,0:T(8,128)(2,1)S(1)}, u32[]{:S(2)}, u32[]{:S(2)}) collective-permute-start(bf16[2,96,2048]{2,1,0:T(8,128)(2,1)} %get-tuple-element.32), channel_id=1, source_target_pairs={{0,1},{1,0},{2,3},{3,2},{4,5},{5,4},{6,7},{7,6},{8,9},{9,8},{10,11... | collective-permute-start | bytes 2359304 | tf_op jit(solution)/shard_map/ppermute | solution.py:509
  201.9 5.7 %collective-permute-start.4 = (bf16[1,96,2048]{2,1,0:T(8,128)(2,1)}, bf16[1,96,2048]{2,1,0:T(8,128)(2,1)S(1)}, u32[]{:S(2)}, u32[]{:S(2)}) collective-permute-start(bf16[1,96,2048]{2,1,0:T(8,128)(2,1)} %get-tuple-element.30), channel_id=1, source_target_pairs={{0,1},{1,0},{2,3},{3,2},{4,5},{5,4},{6,7},{7,6},{8,9},{9,8},{10,11... | collective-permute-start | bytes 1179656 | tf_op jit(solution)/shard_map/ppermute | solution.py:509
  202.4 13.6 %collective-permute-start.9 = (bf16[96,2048]{1,0:T(8,128)(2,1)S(1)}, bf16[96,2048]{1,0:T(8,128)(2,1)S(1)}, u32[]{:S(2)}, u32[]{:S(2)}) collective-permute-start(bf16[96,2048]{1,0:T(8,128)(2,1)S(1)} %fusion.2), channel_id=1, source_target_pairs={{0,4},{2,6},{4,0},{6,2},{1,5},{3,7},{5,1},{7,3},{8,12},{10,14},{12... | collective-permute-start | bytes 1179656 | tf_op jit(solution)/shard_map/ppermute | solution.py:506
  204.3 19.2 %collective-permute-start.6 = (bf16[96,2048]{1,0:T(8,128)(2,1)S(1)}, bf16[96,2048]{1,0:T(8,128)(2,1)S(1)}, u32[]{:S(2)}, u32[]{:S(2)}) collective-permute-start(bf16[96,2048]{1,0:T(8,128)(2,1)S(1)} %get-tuple-element.36), channel_id=1, source_target_pairs={{0,2},{2,4},{4,6},{6,0},{1,3},{3,5},{5,7},{7,1},{8,10},{10,12},{12... | collective-permute-start | bytes 1179656 | tf_op jit(solution)/shard_map/ppermute | solution.py:506
  205.3 18.2 %collective-permute-start.7 = (bf16[96,2048]{1,0:T(8,128)(2,1)S(1)}, bf16[96,2048]{1,0:T(8,128)(2,1)S(1)}, u32[]{:S(2)}, u32[]{:S(2)}) collective-permute-start(bf16[96,2048]{1,0:T(8,128)(2,1)S(1)} %get-tuple-element.35), channel_id=1, source_target_pairs={{0,6},{2,0},{4,2},{6,4},{1,7},{3,1},{5,3},{7,5},{8,14},{10,8},{12,... | collective-permute-start | bytes 1179656 | tf_op jit(solution)/shard_map/ppermute | solution.py:506
  207.6 15.9 %copy-start.5 = (bf16[1,96,2048]{2,1,0:T(8,128)(2,1)}, bf16[1,96,2048]{2,1,0:T(8,128)(2,1)S(1)}, u32[]{:S(2)}) copy-start(bf16[1,96,2048]{2,1,0:T(8,128)(2,1)S(1)} %collective-permute-done.4) | copy-start | bytes 1179652
  216.0 7.6 %copy-start.6 = (bf16[96,2048]{1,0:T(8,128)(2,1)}, bf16[96,2048]{1,0:T(8,128)(2,1)S(1)}, u32[]{:S(2)}) copy-start(bf16[96,2048]{1,0:T(8,128)(2,1)S(1)} %collective-permute-done.9.refs_4_) | copy-start | bytes 1179652
  223.5 0.8 copy-start.7
  223.5 0.9 copy-start.8
Sparse Core Ops, SparseCore 0:
  9.0 50.6 all-gather.6
  61.8 77.0 all-gather.10
  153.6 22.9 all-gather.8

commit v7 on v6

--- a/solution.py
+++ b/solution.py
@@ -372,103 +372,62 @@
 BLOCKS = 3
 
 
-def prepare_kernel(w_ref, in_ref, down_ref):
-    down_ref[...] = w_ref[:, 1408:2112, :]
+def ffn_kernel(count, *refs):
+    x_refs = refs[: 2 * count]
+    w_ref, same_ref, other_ref = refs[2 * count :]
+    x = jnp.concatenate([r[...] for r in x_refs], axis=0)
+
+    def rows(at, width):
+        return jnp.concatenate([w_ref[s, at : at + width, :] for s in range(NSH)], axis=1)
+
+    total = None
     for j in range(BLOCKS):
-        live = min(256, 704 - 256 * j)
-        for part in range(2):
-            at = 704 * part + 256 * j
-            in_ref[j, :, 256 * part : 256 * part + live] = w_ref[0, at : at + live, :].T
-            if live < 256:
-                in_ref[j, :, 256 * part + live : 256 * part + 256] = jnp.zeros(
-                    (128, 256 - live), BF16
-                )
-
-
-def prepare(w):
-    return pl.pallas_call(
-        prepare_kernel,
-        out_shape=(
-            jax.ShapeDtypeStruct((BLOCKS, 2048, 512), BF16),
-            jax.ShapeDtypeStruct((NSH, 704, 128), BF16),
-        ),
-        grid=(NSH,),
-        in_specs=[pl.BlockSpec((1, 2112, 128), lambda s: (s, 0, 0))],
-        out_specs=(
-            pl.BlockSpec((BLOCKS, 128, 512), lambda s: (0, s, 0)),
-            pl.BlockSpec((1, 704, 128), lambda s: (s, 0, 0)),
-        ),
-        compiler_params=params(60),
-        cost_estimate=pl.CostEstimate(
-            flops=10**9, bytes_accessed=11 * 10**6, transcendentals=0
-        ),
-    )(w)
-
-
-def ffn_kernel(count, place, *refs):
-    x_refs = refs[: 2 * count]
-    in_ref, out_refs = refs[2 * count], refs[2 * count + 1 : 2 * count + 5]
-    same_ref, other_ref, total = refs[2 * count + 5 :]
-    j = pl.program_id(0)
-    x = jnp.concatenate([r[0] for r in x_refs], axis=0)
-    both = jnp.dot(x, in_ref[0], preferred_element_type=F32)
-    gate, up = both[:, 0:256], both[:, 256:512]
-    hidden = (gate / (1.0 + jnp.exp(-gate)) * up).astype(BF16)
-    rows = [jnp.concatenate([r[s] for s in range(NSH)], axis=1) for r in out_refs]
-    term = jnp.dot(hidden, jnp.concatenate(rows, axis=0), preferred_element_type=F32)
-
-    @pl.when(j == 0)
-    def _():
-        total[...] = term
-
-    @pl.when(j == 1)
-    def _():
-        total[...] += term
-
-    @pl.when(j == BLOCKS - 1)
-    def _():
-        out = (total[...] + term).astype(BF16)
-        for i in range(count):
-            same_ref[i] = out[i * HALF : (i + 1) * HALF]
-            other_ref[i] = out[(count + i) * HALF : (count + i + 1) * HALF]
-
-
-def ffn(steps, place, gathered, w_in, w_down):
-    count = len(steps)
-
-    def block(d, swapped):
-        def at(g, place):
-            x, c = place[2], place[0]
-            return (2 * lax.rem(x + d, 4) + (1 - c if swapped else c), 0, 0)
-
-        return pl.BlockSpec((1, HALF, 2048), at)
-
-    def down(i):
-        return pl.BlockSpec((NSH, 64, 128), lambda g, place: (0, jnp.minimum(4 * g + i, 10), 0))
-
+        width = min(256, 704 - 256 * j)
+        across = (((1,), (1,)), ((), ()))
+        gate = lax.dot_general(x, rows(256 * j, width), across, preferred_element_type=F32)
+        up = lax.dot_general(x, rows(704 + 256 * j, width), across, preferred_element_type=F32)
+        hidden = (gate / (1.0 + jnp.exp(-gate)) * up).astype(BF16)
+        term = jnp.dot(hidden, rows(1408 + 256 * j, width), preferred_element_type=F32)
+        total = term if total is None else total + term
+    out = total.astype(BF16)
+    for i in range(count):
+        same_ref[i] = out[i * HALF : (i + 1) * HALF]
+        other_ref[i] = out[(count + i) * HALF : (count + i + 1) * HALF]
+
+
+def ffn(pieces, w):
+    count = len(pieces) // 2
     shape = jax.ShapeDtypeStruct((count, HALF, 2048), BF16)
     rows = 2 * count * HALF
     return pl.pallas_call(
         functools.partial(ffn_kernel, count),
         out_shape=(shape, shape),
-        grid_spec=pltpu.PrefetchScalarGridSpec(
-            num_scalar_prefetch=1,
-            grid=(BLOCKS,),
-            in_specs=[block(d, swapped) for swapped in (False, True) for d in steps]
-            + [along((2048, 512))]
-            + [down(i) for i in range(4)],
-            out_specs=(whole((count, HALF, 2048)),) * 2,
-            scratch_shapes=[pltpu.VMEM((rows, 2048), F32)],
-        ),
-        compiler_params=params(60),
+        in_specs=[vmem()] * (2 * count + 1),
+        out_specs=(vmem(), vmem()),
+        compiler_params=params(30),
         cost_estimate=pl.CostEstimate(
             flops=6 * rows * 2048 * 704, bytes_accessed=10**7, transcendentals=rows * 704
         ),
-    )(place, *([gathered] * (2 * count)), w_in, *([w_down] * 4))
-
-
-def join(one, two):
-    return (one.astype(F32) + two.astype(F32)).astype(BF16)
+    )(*pieces, w)
+
+
+def join_kernel(count, *refs):
+    same_ref, other_ref = refs[:2]
+    for i in range(count):
+        refs[2 + i][...] = (same_ref[i].astype(F32) + other_ref[i].astype(F32)).astype(BF16)
+
+
+def join(same, other):
+    count = same.shape[0]
+    shape = jax.ShapeDtypeStruct((HALF, 2048), BF16)
+    return pl.pallas_call(
+        functools.partial(join_kernel, count),
+        out_shape=(shape,) * count,
+        in_specs=[vmem()] * 2,
+        out_specs=(vmem(),) * count,
+        compiler_params=params(8),
+        cost_estimate=pl.CostEstimate(flops=10**6, bytes_accessed=10**6, transcendentals=0),
+    )(same, other)
 
 
 def last_kernel(n_ref, gain_ref, bias_ref, *refs):
@@ -527,18 +486,21 @@
         spread(by_shard), ("x", "c"), split_axis=0, concat_axis=0, tiled=True
     )
     normed = mix(place, by_rows, stream_in, mix_gain[None], mix_bias[None], w_same, w_other)
-    gathered = lax.all_gather(normed, ("x", "c"), axis=0, tiled=False)
-    w_in, w_down = prepare(ffn_all)
-
-    far_same, far_other = ffn((2,), place, gathered, w_in, w_down)
+    back, ahead = turn(normed, "x", 1), turn(normed, "x", 3)
+    n_swapped = swap(normed)
+    own_same, own_other = ffn((normed, n_swapped), ffn_all)
+    own_swapped = swap(own_other)
+    far = turn(back, "x", 1)
+    near = (back, ahead, swap(back), swap(ahead))
+    near_same, near_other = ffn(near, ffn_all)
+    near_swapped = swap(near_other)
+    far_other_rows = swap(far)
+    to_back, to_ahead = join(near_same, near_swapped)
+    from_ahead, from_back = turn(to_back, "x", 3), turn(to_ahead, "x", 1)
+    far_same, far_other = ffn((far, far_other_rows), ffn_all)
     far_swapped = swap(far_other)
-    near_same, near_other = ffn((1, 3), place, gathered, w_in, w_down)
-    near_swapped = swap(near_other)
-    own_same, own_other = ffn((0,), place, gathered, w_in, w_down)
-    own_swapped = swap(own_other)
-    from_far = turn(join(far_same[0], far_swapped[0]), "x", 2)
-    near = [join(near_same[i], near_swapped[i]) for i in range(2)]
-    from_back, from_ahead = turn(near[0], "x", 1), turn(near[1], "x", 3)
+    (to_far,) = join(far_same, far_swapped)
+    from_far = turn(to_far, "x", 2)
     parts = [own_same[0], own_swapped[0], from_back, from_ahead, from_far]
     return last(parts, normed, ffn_gain[None], ffn_bias[None])
 

time: 236 us -> 224 us (0.949)
  Pallas kernels: 99.6 us -> 71.8 us
  waiting for transfers between devices: 53.7 us -> 65 us
  local copies, waits for them, and re-layouts: 4.17 us -> 8.16 us
  starting transfers between devices: 20.1 us -> 22.5 us
    ppermute x6 -> x9, waiting for transfers between devices: 15.9 us -> 36.4 us  [turn(): return lax.ppermute(value, axis, [(i, (i + d) % 4) for i in range(4)])]
    pallas_call x3, Pallas kernels: 24.7 us -> 9.49 us  [ffn(): pl.pallas_call(functools.partial(ffn_kernel, count), out_shape=(shape, sh...]
    pallas_call x1 -> x2, Pallas kernels: 13.2 us -> 0.27 us  [join(): pl.pallas_call(functools.partial(join_kernel, count), out_shape=(shape,)...]
    all_gather x1 -> x0, waiting for transfers between devices: 9.91 us -> none  [body(): gathered = lax.all_gather(normed, ('x', 'c'), axis=0, tiled=False)]
    unnamed x22 -> x36, local copies, waits for them, and re-layouts: 4.17 us -> 8.16 us
    ppermute x6 -> x9, starting transfers between devices: 10.4 us -> 12 us  [turn(): return lax.ppermute(value, axis, [(i, (i + d) % 4) for i in range(4)])]
  transfers between devices with their start and end apart: 15 -> 21, of which waited for: 5 -> 6; matrix products, arithmetic and copies ran while one was open for 1% -> 1% of each run, Pallas kernels for 38% -> 31%
where the time goes in v7:
time: 224 us; the launch traced here: 223 us
  Pallas kernels  71.8 us (32%)
  waiting for transfers between devices  65 us (29%)
  blocking collectives  40 us (18%)
  starting transfers between devices  22.5 us (10%)
  between operations  13.6 us (6%)
  local copies, waits for them, and re-layouts  8.16 us (4%)
    pallas_call x3, Pallas kernels, attend(): pl.pallas_call(functools.partial(attend_kernel, chunks, first, final), ou...  47.1 us
    ppermute x9, waiting for transfers between devices, turn(): return lax.ppermute(value, axis, [(i, (i + d) % 4) for i in range(4)])  36.4 us
    all_to_all x1, blocking collectives, body(): lax.all_to_all(attended, ('z', 'y'), split_axis=0, concat_axis=0, tiled=T...  22 us
    all_gather x1, waiting for transfers between devices, body(): w_same = lax.all_gather(out_weight, 'x', axis=0, tiled=False)  19.6 us
    all_to_all x1, blocking collectives, body(): lax.all_to_all(kv_pack, 'z', split_axis=0, concat_axis=0, tiled=True)  18.1 us
    ppermute x9, starting transfers between devices, turn(): return lax.ppermute(value, axis, [(i, (i + d) % 4) for i in range(4)])  12 us
    pallas_call x3, Pallas kernels, ffn(): pl.pallas_call(functools.partial(ffn_kernel, count), out_shape=(shape, sh...  9.49 us
    all_to_all x1, waiting for transfers between devices, body(): lax.all_to_all(spread(by_shard), ('x', 'c'), split_axis=0, concat_axis=0,...  8.3 us
  transfers between devices with their start and end apart: 21, of which 6 were waited for; matrix products, arithmetic and copies ran while one was open for 1% of the time, Pallas kernels for 31%

profile of v7, /device:TPU:0, one launch (start us, length us, event | category | flops | bytes accessed | tf_op | source)
XLA Modules:
  0.0 222.6 jit_solution(13573197646452055993)
XLA Ops:
  6.5 0.7 all-gather.5.cloned.1.call-update
  7.3 0.0 all-gather.7.cloned.1.call-start
  7.3 0.1 copy-done.12
  7.5 0.1 copy-done.11
  7.5 0.1 copy-done.10
  7.6 0.9 pad_maximum_fusion
  8.5 0.0 all-gather.7.cloned.1.call-update
  8.5 2.9 %shard_map.154 = (bf16[16,96,128]{2,1,0:T(8,128)(2,1)}, bf16[4,800,128]{2,1,0:T(8,128)(2,1)}) custom-call(bf16[768,256]{1,0:T(8,128)(2,1)} %q_ref.1, bf16[768,256]{1,0:T(8,128)(2,1)} %k_ref.1, bf16[768,256]{1,0:T(8,128)(2,1)} %v_ref.1, f32[4,768]{1,0:T(4,128)} %bitcast.26), custom_call_target="tpu_custom_call" | custom-call | flops 1000000 | bytes 2500000 | tf_op jit(solution)/shard_map/pallas_call | solution.py:60
  11.4 18.1 %all_to_all.20.refs_2_ = bf16[4,800,128]{2,1,0:T(8,128)(2,1)S(1)} all-to-all(bf16[4,800,128]{2,1,0:T(8,128)(2,1)} %get-tuple-element.20), channel_id=1, replica_groups=mesh['z'=4,'y'=4,'x'=4,'c'=2] {'z'}, dimensions={0} | all-to-all | bytes 1638400 | tf_op jit(solution)/shard_map/all_to_all | solution.py:474
  29.5 5.2 %all-to-all-start.1 = ((bf16[16,96,128]{2,1,0:T(8,128)(2,1)}), bf16[16,96,128]{2,1,0:T(8,128)(2,1)S(1)}, u32[]{:S(2)}, u32[]{:S(2)}) async-start(bf16[16,96,128]{2,1,0:T(8,128)(2,1)} %get-tuple-element.21), calls=%async_computation.1 | async-start | bytes 786432 | tf_op jit(solution)/shard_map/all_to_all | solution.py:473
  34.7 1.9 collective-permute-start.1
  36.6 1.4 collective-permute-start.2
  38.0 2.1 collective-permute-start
  40.1 19.6 %all-gather.5.cloned.1.call-done = bf16[1024,2048]{1,0:T(8,128)(2,1)} async-done(((bf16[256,2048]{1,0:T(8,128)(2,1)}), bf16[1024,2048]{1,0:T(8,128)(2,1)}) %all-gather.5.cloned.1.call-update) | async-done | bytes 4194320 | tf_op jit(solution)/shard_map/all_gather | solution.py:471
  59.7 0.0 collective-permute-start.3
  59.7 0.0 all-to-all-done.1.refs_3_
  59.7 0.7 copy-done.5
  60.4 13.5 %shard_map.155 = (bf16[12,128,256]{2,1,0:T(8,128)(2,1)}, f32[12,8,256]{2,1,0:T(8,128)}, f32[12,80,256]{2,1,0:T(8,128)}) custom-call(s32[4,4,33]{2,1,0:T(4,128)} %constant.19.clone.refs_0_, s32[1]{0:T(128)} %bitcast.3.refs_1_, bf16[4,800,128]{2,1,0:T(8,128)(2,1)} %copy-done.4, bf16[16,96,128]{2,1,0:T(8,128)(2,1)} %copy-done.5), custom_call_target="tpu_custom_call" | custom-call | flops 10400000000 | bytes 3000000 | tf_op jit(solution)/shard_map/pallas_call | solution.py:280
  73.9 0.9 copy-done.14
  74.8 19.3 %shard_map.156 = (f32[12,8,256]{2,1,0:T(8,128)}, f32[12,80,256]{2,1,0:T(8,128)}) custom-call(s32[4,4,59]{2,1,0:T(4,128)} %constant.20.clone.refs_0_, s32[1]{0:T(128)} %bitcast.3.refs_1_, bf16[4,800,128]{2,1,0:T(8,128)(2,1)} %copy-done.14, bf16[4,800,128]{2,1,0:T(8,128)(2,1)} %collective-permute-done.2.refs_3_, ...), custom_call_target="tpu_custom_call" | custom-call | flops 21600000000 | bytes 3000000 | tf_op jit(solution)/shard_map/pallas_call | solution.py:280
  94.1 0.0 collective-permute-done.refs_2_
  94.1 0.9 copy-done.13
  95.0 14.4 %shard_map.157 = bf16[16,96,128]{2,1,0:T(8,128)(2,1)} custom-call(s32[4,4,33]{2,1,0:T(4,128)} %constant.21.clone.refs_0_, s32[1]{0:T(128)} %bitcast.3.refs_1_, bf16[4,800,128]{2,1,0:T(8,128)(2,1)} %copy-done.13, bf16[12,128,256]{2,1,0:T(8,128)(2,1)} %get-tuple-element.22.refs_4_.refs_3_, f32[12,8,256]{2,1,0:T(8,128)} %get-tuple-element.25.refs_4_, ...), custom_call_target="tpu_custom_call" | custom-call | flops 10400000000 | bytes 3000000 | tf_op jit(solution)/shard_map/pallas_call | solution.py:280
  109.4 22.0 %all_to_all.21.o_ref = bf16[16,96,128]{2,1,0:T(8,128)(2,1)} all-to-all(bf16[16,96,128]{2,1,0:T(8,128)(2,1)} %shard_map.157), channel_id=1, replica_groups=mesh['z'=4,'y'=4,'x'=4,'c'=2] {'z','y'}, dimensions={0} | all-to-all | bytes 786432 | tf_op jit(solution)/shard_map/all_to_all | solution.py:484
  131.3 2.0 shard_map.158
  133.4 3.5 %all-to-all-start.3 = ((bf16[8,96,256]{2,1,0:T(8,128)(2,1)}), bf16[8,96,256]{2,1,0:T(8,128)(2,1)S(1)}, u32[]{:S(2)}, u32[]{:S(2)}) async-start(bf16[8,96,256]{2,1,0:T(8,128)(2,1)} %shard_map.158), calls=%async_computation.3 | async-start | bytes 786432 | tf_op jit(solution)/shard_map/all_to_all | solution.py:485
  136.8 0.6 pad_add_fusion.place
  137.4 8.3 %all-to-all-done.3.a_ref = bf16[8,96,256]{2,1,0:T(8,128)(2,1)S(1)} async-done(((bf16[8,96,256]{2,1,0:T(8,128)(2,1)}), bf16[8,96,256]{2,1,0:T(8,128)(2,1)S(1)}, u32[]{:S(2)}, u32[]{:S(2)}) %all-to-all-start.3) | async-done | bytes 393248 | tf_op jit(solution)/shard_map/all_to_all | solution.py:485
  145.7 0.0 collective-permute-done.3.other_ref
  145.7 0.7 copy-done.3
  146.5 7.1 %shard_map.159.refs_0_.n_ref = bf16[96,2048]{1,0:T(8,128)(2,1)} custom-call(s32[3]{0:T(128)} %pad_add_fusion.place, bf16[8,96,256]{2,1,0:T(8,128)(2,1)} %copy-done.3, bf16[768,2048]{1,0:T(8,128)(2,1)} %stream_ref.1, f32[1,2048]{1,0:T(1,128)} %bitcast.27, f32[1,2048]{1,0:T(1,128)} %bitcast.28, bf16[4,256,2048]{2,1,0:T(8,128)(2,1)} %bitcast.22, ...), custom_call_target="tpu_custom_call" | custom-call | flops 805306368 | bytes 9000000 | tf_op jit(solution)/shard_map/pallas_call | solution.py:348
  153.5 0.6 collective-permute-start.6
  154.1 2.7 %collective-permute-start.7 = (bf16[96,2048]{1,0:T(8,128)(2,1)}, bf16[96,2048]{1,0:T(8,128)(2,1)S(1)}, u32[]{:S(2)}, u32[]{:S(2)}) collective-permute-start(bf16[96,2048]{1,0:T(8,128)(2,1)} %shard_map.159.refs_0_.n_ref), channel_id=1, source_target_pairs={{0,6},{2,0},{4,2},{6,4},{1,7},{3,1},{5,3},{7,5},{8,14},{10,8},{12,... | collective-permute-start | bytes 1179656 | tf_op jit(solution)/shard_map/ppermute | solution.py:465
  156.8 8.5 %collective-permute-done.6.refs_0_ = bf16[96,2048]{1,0:T(8,128)(2,1)S(1)} collective-permute-done((bf16[96,2048]{1,0:T(8,128)(2,1)}, bf16[96,2048]{1,0:T(8,128)(2,1)S(1)}, u32[]{:S(2)}, u32[]{:S(2)}) %collective-permute-start.6) | collective-permute-done | bytes 393248 | tf_op jit(solution)/shard_map/ppermute | solution.py:465
  165.3 0.5 collective-permute-start.9
  165.8 10.1 %collective-permute-done.13.refs_0_ = bf16[96,2048]{1,0:T(8,128)(2,1)S(1)} collective-permute-done((bf16[96,2048]{1,0:T(8,128)(2,1)S(1)}, bf16[96,2048]{1,0:T(8,128)(2,1)S(1)}, u32[]{:S(2)}, u32[]{:S(2)}) %collective-permute-start.13) | collective-permute-done | bytes 393248 | tf_op jit(solution)/shard_map/ppermute | solution.py:465
  175.9 0.0 collective-permute-start.14
  175.9 0.0 collective-permute-done.8.refs_2_
  175.9 0.0 collective-permute-done.9.refs_3_
  175.9 0.0 all-gather.7.cloned.1.call-done
  176.0 3.4 %copy-done = bf16[33792,128]{1,0:T(8,128)(2,1)S(1)} copy-done((bf16[33792,128]{1,0:T(8,128)(2,1)S(1)}, bf16[33792,128]{1,0:T(8,128)(2,1)}, u32[]{:S(2)}) %copy-start) | copy-done | bytes 8650776
  179.4 4.0 %shard_map.161 = (bf16[2,96,2048]{2,1,0:T(8,128)(2,1)S(1)}, bf16[2,96,2048]{2,1,0:T(8,128)(2,1)S(1)}) custom-call(bf16[96,2048]{1,0:T(8,128)(2,1)S(1)} %collective-permute-done.6.refs_0_, bf16[96,2048]{1,0:T(8,128)(2,1)S(1)} %collective-permute-done.7.refs_1_, bf16[96,2048]{1,0:T(8,128)(2,1)S(1)} %collective-permute-done.8.refs_2_, ...), custom_call_target="tpu_custom_call" | custom-call | flops 3321888768 | bytes 10000000 | tf_op jit(solution)/shard_map/pallas_call | solution.py:402
  183.4 0.0 slice-start.2
  183.4 0.5 collective-permute-start.10
  184.0 0.1 collective-permute-start.4
  184.1 0.0 collective-permute-done.14.refs_1_
  184.1 2.7 %shard_map.163 = (bf16[1,96,2048]{2,1,0:T(8,128)(2,1)S(1)}, bf16[1,96,2048]{2,1,0:T(8,128)(2,1)S(1)}) custom-call(bf16[96,2048]{1,0:T(8,128)(2,1)S(1)} %collective-permute-done.13.refs_0_, bf16[96,2048]{1,0:T(8,128)(2,1)S(1)} %collective-permute-done.14.refs_1_, bf16[16,2112,128]{2,1,0:T(8,128)(2,1)S(1)} %bitcast.16), custom_call_target="tpu_custom_call" | custom-call | flops 1660944384 | bytes 10000000 | tf_op jit(solution)/shard_map/pallas_call | solution.py:402
  186.8 0.5 collective-permute-start.15
  187.3 0.0 collective-permute-done.4.refs_1_
  187.4 2.8 %shard_map.160 = (bf16[1,96,2048]{2,1,0:T(8,128)(2,1)S(1)}, bf16[1,96,2048]{2,1,0:T(8,128)(2,1)S(1)}) custom-call(bf16[96,2048]{1,0:T(8,128)(2,1)S(1)} %copy-done.1, bf16[96,2048]{1,0:T(8,128)(2,1)S(1)} %collective-permute-done.4.refs_1_, bf16[16,2112,128]{2,1,0:T(8,128)(2,1)S(1)} %bitcast.19), custom_call_target="tpu_custom_call" | custom-call | flops 1660944384 | bytes 10000000 | tf_op jit(solution)/shard_map/pallas_call | solution.py:402
  190.1 0.2 collective-permute-start.5
  190.3 0.0 collective-permute-done.15.refs_1_
  190.3 0.1 shard_map.164
  190.4 0.1 collective-permute-start.16
  190.5 0.0 collective-permute-done.10.refs_1_
  190.5 0.2 shard_map.162
  190.7 0.2 copy-done.2
  190.9 0.3 collective-permute-start.11
  191.2 3.0 %collective-permute-start.12 = (bf16[96,2048]{1,0:T(8,128)(2,1)S(1)}, bf16[96,2048]{1,0:T(8,128)(2,1)S(1)}, u32[]{:S(2)}, u32[]{:S(2)}) collective-permute-start(bf16[96,2048]{1,0:T(8,128)(2,1)S(1)} %get-tuple-element.32), channel_id=1, source_target_pairs={{0,6},{2,0},{4,2},{6,4},{1,7},{3,1},{5,3},{7,5},{8,14},{10,8},{12,... | collective-permute-start | bytes 1179656 | tf_op jit(solution)/shard_map/ppermute | solution.py:465
  194.1 9.9 %collective-permute-done.16.refs_4_ = bf16[96,2048]{1,0:T(8,128)(2,1)S(1)} collective-permute-done((bf16[96,2048]{1,0:T(8,128)(2,1)S(1)}, bf16[96,2048]{1,0:T(8,128)(2,1)S(1)}, u32[]{:S(2)}, u32[]{:S(2)}) %collective-permute-start.16) | collective-permute-done | bytes 393248 | tf_op jit(solution)/shard_map/ppermute | solution.py:465
  204.0 7.8 %collective-permute-done.11.refs_2_ = bf16[96,2048]{1,0:T(8,128)(2,1)S(1)} collective-permute-done((bf16[96,2048]{1,0:T(8,128)(2,1)S(1)}, bf16[96,2048]{1,0:T(8,128)(2,1)S(1)}, u32[]{:S(2)}, u32[]{:S(2)}) %collective-permute-start.11) | collective-permute-done | bytes 393248 | tf_op jit(solution)/shard_map/ppermute | solution.py:465
  211.9 0.7 copy-done.8
  212.6 0.1 copy-done.9
  212.7 3.0 %shard_map.165 = bf16[96,2048]{1,0:T(8,128)(2,1)} custom-call(bf16[96,2048]{1,0:T(8,128)(2,1)} %shard_map.159.refs_0_.n_ref, f32[1,2048]{1,0:T(1,128)} %bitcast.29, f32[1,2048]{1,0:T(1,128)} %bitcast.30, bf16[96,2048]{1,0:T(8,128)(2,1)} %bitcast.20, bf16[96,2048]{1,0:T(8,128)(2,1)} %bitcast.23, bf16[96,2048]{1,0:T(8,128)(2,1)} %copy-done.8, ...), custom_call_target="tpu_custom_call" | custom-call | flops 4000000 | bytes 4000000 | tf_op jit(solution)/shard_map/pallas_call | solution.py:444
  (33 shorter events, 0.1 us)
Async XLA Ops:
  6.5 0.9 copy-start.12
  6.5 1.0 copy-start.11
  6.5 1.1 copy-start.10
  6.5 53.1 %all-gather.5.cloned.1.call-start = ((), (), s32[]{:S(2)}) async-start(), calls=%async_computation.4 | async-start | bytes 5242880 | tf_op jit(solution)/shard_map/all_gather | solution.py:471
  7.3 168.7 %all-gather.7.cloned.1.call-start = ((), (), s32[]{:S(2)}) async-start(), calls=%async_computation.5 | async-start | bytes 9191424 | tf_op jit(solution)/shard_map/all_gather | solution.py:479
  29.5 30.2 %copy-start.4 = (bf16[4,800,128]{2,1,0:T(8,128)(2,1)}, bf16[4,800,128]{2,1,0:T(8,128)(2,1)S(1)}, u32[]{:S(2)}) copy-start(bf16[4,800,128]{2,1,0:T(8,128)(2,1)S(1)} %all_to_all.20.refs_2_) | copy-start | bytes 2457604
  29.5 30.2 %all-to-all-start.1 = ((bf16[16,96,128]{2,1,0:T(8,128)(2,1)}), bf16[16,96,128]{2,1,0:T(8,128)(2,1)S(1)}, u32[]{:S(2)}, u32[]{:S(2)}) async-start(bf16[16,96,128]{2,1,0:T(8,128)(2,1)} %get-tuple-element.21), calls=%async_computation.1 | async-start | bytes 786432 | tf_op jit(solution)/shard_map/all_to_all | solution.py:473
  34.7 39.2 %collective-permute-start.1 = (bf16[4,800,128]{2,1,0:T(8,128)(2,1)S(1)}, bf16[4,800,128]{2,1,0:T(8,128)(2,1)S(1)}, u32[]{:S(2)}, u32[]{:S(2)}) collective-permute-start(bf16[4,800,128]{2,1,0:T(8,128)(2,1)S(1)} %all_to_all.20.refs_2_), channel_id=1, source_target_pairs={{0,8},{8,16},{16,24},{24,0},{1,9},{9,17},{17,25},{25,1},{2,10},{10... | collective-permute-start | bytes 2457608 | tf_op jit(solution)/shard_map/ppermute | solution.py:465
  36.6 37.3 %collective-permute-start.2 = (bf16[4,800,128]{2,1,0:T(8,128)(2,1)S(1)}, bf16[4,800,128]{2,1,0:T(8,128)(2,1)}, u32[]{:S(2)}, u32[]{:S(2)}) collective-permute-start(bf16[4,800,128]{2,1,0:T(8,128)(2,1)S(1)} %all_to_all.20.refs_2_), channel_id=1, source_target_pairs={{0,24},{8,0},{16,8},{24,16},{1,25},{9,1},{17,9},{25,17},{2,26},{10... | collective-permute-start | bytes 2457608 | tf_op jit(solution)/shard_map/ppermute | solution.py:465
  38.0 56.1 %collective-permute-start = (bf16[4,800,128]{2,1,0:T(8,128)(2,1)S(1)}, bf16[4,800,128]{2,1,0:T(8,128)(2,1)S(1)}, u32[]{:S(2)}, u32[]{:S(2)}) collective-permute-start(bf16[4,800,128]{2,1,0:T(8,128)(2,1)S(1)} %all_to_all.20.refs_2_), channel_id=1, source_target_pairs={{0,16},{8,24},{16,0},{24,8},{1,17},{9,25},{17,1},{25,9},{2,18},{10... | collective-permute-start | bytes 2457608 | tf_op jit(solution)/shard_map/ppermute | solution.py:465
  59.7 86.0 %collective-permute-start.3 = (bf16[4,256,2048]{2,1,0:T(8,128)(2,1)}, bf16[4,256,2048]{2,1,0:T(8,128)(2,1)}, u32[]{:S(2)}, u32[]{:S(2)}) collective-permute-start(bf16[4,256,2048]{2,1,0:T(8,128)(2,1)} %bitcast.21), channel_id=1, source_target_pairs={{0,1},{1,0},{2,3},{3,2},{4,5},{5,4},{6,7},{7,6},{8,9},{9,8},{10,11... | collective-permute-start | bytes 12582920 | tf_op jit(solution)/shard_map/ppermute | solution.py:468
  59.7 0.7 copy-start.5
  73.9 0.9 copy-start.14
  94.1 0.9 copy-start.13
  133.4 12.4 %all-to-all-start.3 = ((bf16[8,96,256]{2,1,0:T(8,128)(2,1)}), bf16[8,96,256]{2,1,0:T(8,128)(2,1)S(1)}, u32[]{:S(2)}, u32[]{:S(2)}) async-start(bf16[8,96,256]{2,1,0:T(8,128)(2,1)} %shard_map.158), calls=%async_computation.3 | async-start | bytes 786432 | tf_op jit(solution)/shard_map/all_to_all | solution.py:485
  145.7 0.7 copy-start.3
  153.5 11.7 %collective-permute-start.6 = (bf16[96,2048]{1,0:T(8,128)(2,1)}, bf16[96,2048]{1,0:T(8,128)(2,1)S(1)}, u32[]{:S(2)}, u32[]{:S(2)}) collective-permute-start(bf16[96,2048]{1,0:T(8,128)(2,1)} %shard_map.159.refs_0_.n_ref), channel_id=1, source_target_pairs={{0,2},{2,4},{4,6},{6,0},{1,3},{3,5},{5,7},{7,1},{8,10},{10,12},{12... | collective-permute-start | bytes 1179656 | tf_op jit(solution)/shard_map/ppermute | solution.py:465
  154.1 11.2 %collective-permute-start.7 = (bf16[96,2048]{1,0:T(8,128)(2,1)}, bf16[96,2048]{1,0:T(8,128)(2,1)S(1)}, u32[]{:S(2)}, u32[]{:S(2)}) collective-permute-start(bf16[96,2048]{1,0:T(8,128)(2,1)} %shard_map.159.refs_0_.n_ref), channel_id=1, source_target_pairs={{0,6},{2,0},{4,2},{6,4},{1,7},{3,1},{5,3},{7,5},{8,14},{10,8},{12,... | collective-permute-start | bytes 1179656 | tf_op jit(solution)/shard_map/ppermute | solution.py:465
  165.2 10.7 %collective-permute-start.13 = (bf16[96,2048]{1,0:T(8,128)(2,1)S(1)}, bf16[96,2048]{1,0:T(8,128)(2,1)S(1)}, u32[]{:S(2)}, u32[]{:S(2)}) collective-permute-start(bf16[96,2048]{1,0:T(8,128)(2,1)S(1)} %collective-permute-done.6.refs_0_), channel_id=1, source_target_pairs={{0,2},{2,4},{4,6},{6,0},{1,3},{3,5},{5,7},{7,1},{8,10},{10,12},{12... | collective-permute-start | bytes 1179656 | tf_op jit(solution)/shard_map/ppermute | solution.py:465
  165.3 10.7 %collective-permute-start.8 = (bf16[96,2048]{1,0:T(8,128)(2,1)S(1)}, bf16[96,2048]{1,0:T(8,128)(2,1)S(1)}, u32[]{:S(2)}, u32[]{:S(2)}) collective-permute-start(bf16[96,2048]{1,0:T(8,128)(2,1)S(1)} %collective-permute-done.6.refs_0_), channel_id=1, source_target_pairs={{0,1},{1,0},{2,3},{3,2},{4,5},{5,4},{6,7},{7,6},{8,9},{9,8},{10,11... | collective-permute-start | bytes 1179656 | tf_op jit(solution)/shard_map/ppermute | solution.py:468
  165.3 10.7 %collective-permute-start.9 = (bf16[96,2048]{1,0:T(8,128)(2,1)S(1)}, bf16[96,2048]{1,0:T(8,128)(2,1)S(1)}, u32[]{:S(2)}, u32[]{:S(2)}) collective-permute-start(bf16[96,2048]{1,0:T(8,128)(2,1)S(1)} %collective-permute-done.7.refs_1_), channel_id=1, source_target_pairs={{0,1},{1,0},{2,3},{3,2},{4,5},{5,4},{6,7},{7,6},{8,9},{9,8},{10,11... | collective-permute-start | bytes 1179656 | tf_op jit(solution)/shard_map/ppermute | solution.py:468
  175.9 8.2 %collective-permute-start.14 = (bf16[96,2048]{1,0:T(8,128)(2,1)S(1)}, bf16[96,2048]{1,0:T(8,128)(2,1)S(1)}, u32[]{:S(2)}, u32[]{:S(2)}) collective-permute-start(bf16[96,2048]{1,0:T(8,128)(2,1)S(1)} %collective-permute-done.13.refs_0_), channel_id=1, source_target_pairs={{0,1},{1,0},{2,3},{3,2},{4,5},{5,4},{6,7},{7,6},{8,9},{9,8},{10,11... | collective-permute-start | bytes 1179656 | tf_op jit(solution)/shard_map/ppermute | solution.py:468
  176.0 3.5 %copy-start = (bf16[33792,128]{1,0:T(8,128)(2,1)S(1)}, bf16[33792,128]{1,0:T(8,128)(2,1)}, u32[]{:S(2)}) copy-start(bf16[33792,128]{1,0:T(8,128)(2,1)} %all-gather.7.cloned.1.call-done) | copy-start | bytes 25952260
  179.4 4.6 %copy-start.1 = (bf16[96,2048]{1,0:T(8,128)(2,1)S(1)}, bf16[96,2048]{1,0:T(8,128)(2,1)}, u32[]{:S(2)}) copy-start(bf16[96,2048]{1,0:T(8,128)(2,1)} %shard_map.159.refs_0_.n_ref) | copy-start | bytes 1179652
  179.4 7.9 %slice-start = ((s8[8650752]{0:T(1024)(128)(4,1)}), s8[4194304]{0:T(1024)(128)(4,1)S(1)}, s32[]{:S(2)}) async-start(s8[8650752]{0:T(1024)(128)(4,1)} %bitcast.17), calls=%async_computation.6 | async-start | bytes 8388608
  179.4 7.9 %slice-start.1 = ((s8[8650752]{0:T(1024)(128)(4,1)}), s8[262144]{0:T(1024)(128)(4,1)S(1)}, s32[]{:S(2)}) async-start(s8[8650752]{0:T(1024)(128)(4,1)} %bitcast.17), calls=%async_computation.7 | async-start | bytes 524288
  183.4 3.9 %slice-start.2 = ((s8[8650752]{0:T(1024)(128)(4,1)}), s8[4194304]{0:T(1024)(128)(4,1)S(1)}, s32[]{:S(2)}) async-start(s8[8650752]{0:T(1024)(128)(4,1)} %bitcast.17), calls=%async_computation.8 | async-start | bytes 8388608
  183.4 7.1 %collective-permute-start.10 = (bf16[2,96,2048]{2,1,0:T(8,128)(2,1)S(1)}, bf16[2,96,2048]{2,1,0:T(8,128)(2,1)S(1)}, u32[]{:S(2)}, u32[]{:S(2)}) collective-permute-start(bf16[2,96,2048]{2,1,0:T(8,128)(2,1)S(1)} %get-tuple-element.30), channel_id=1, source_target_pairs={{0,1},{1,0},{2,3},{3,2},{4,5},{5,4},{6,7},{7,6},{8,9},{9,8},{10,11... | collective-permute-start | bytes 2359304 | tf_op jit(solution)/shard_map/ppermute | solution.py:468
  184.0 3.4 %collective-permute-start.4 = (bf16[96,2048]{1,0:T(8,128)(2,1)S(1)}, bf16[96,2048]{1,0:T(8,128)(2,1)S(1)}, u32[]{:S(2)}, u32[]{:S(2)}) collective-permute-start(bf16[96,2048]{1,0:T(8,128)(2,1)S(1)} %copy-done.1), channel_id=1, source_target_pairs={{0,1},{1,0},{2,3},{3,2},{4,5},{5,4},{6,7},{7,6},{8,9},{9,8},{10,11... | collective-permute-start | bytes 1179656 | tf_op jit(solution)/shard_map/ppermute | solution.py:468
  186.8 3.5 %collective-permute-start.15 = (bf16[1,96,2048]{2,1,0:T(8,128)(2,1)S(1)}, bf16[1,96,2048]{2,1,0:T(8,128)(2,1)S(1)}, u32[]{:S(2)}, u32[]{:S(2)}) collective-permute-start(bf16[1,96,2048]{2,1,0:T(8,128)(2,1)S(1)} %get-tuple-element.34), channel_id=1, source_target_pairs={{0,1},{1,0},{2,3},{3,2},{4,5},{5,4},{6,7},{7,6},{8,9},{9,8},{10,11... | collective-permute-start | bytes 1179656 | tf_op jit(solution)/shard_map/ppermute | solution.py:468
  190.1 0.8 copy-start.2
  190.1 4.0 %collective-permute-start.5 = (bf16[1,96,2048]{2,1,0:T(8,128)(2,1)S(1)}, bf16[1,96,2048]{2,1,0:T(8,128)(2,1)S(1)}, u32[]{:S(2)}, u32[]{:S(2)}) collective-permute-start(bf16[1,96,2048]{2,1,0:T(8,128)(2,1)S(1)} %get-tuple-element.28), channel_id=1, source_target_pairs={{0,1},{1,0},{2,3},{3,2},{4,5},{5,4},{6,7},{7,6},{8,9},{9,8},{10,11... | collective-permute-start | bytes 1179656 | tf_op jit(solution)/shard_map/ppermute | solution.py:468
  190.4 13.6 %collective-permute-start.16 = (bf16[96,2048]{1,0:T(8,128)(2,1)S(1)}, bf16[96,2048]{1,0:T(8,128)(2,1)S(1)}, u32[]{:S(2)}, u32[]{:S(2)}) collective-permute-start(bf16[96,2048]{1,0:T(8,128)(2,1)S(1)} %shard_map.164), channel_id=1, source_target_pairs={{0,4},{2,6},{4,0},{6,2},{1,5},{3,7},{5,1},{7,3},{8,12},{10,14},{12... | collective-permute-start | bytes 1179656 | tf_op jit(solution)/shard_map/ppermute | solution.py:465
  190.9 21.0 %collective-permute-start.11 = (bf16[96,2048]{1,0:T(8,128)(2,1)S(1)}, bf16[96,2048]{1,0:T(8,128)(2,1)S(1)}, u32[]{:S(2)}, u32[]{:S(2)}) collective-permute-start(bf16[96,2048]{1,0:T(8,128)(2,1)S(1)} %get-tuple-element.31), channel_id=1, source_target_pairs={{0,2},{2,4},{4,6},{6,0},{1,3},{3,5},{5,7},{7,1},{8,10},{10,12},{12... | collective-permute-start | bytes 1179656 | tf_op jit(solution)/shard_map/ppermute | solution.py:465
  191.2 20.7 %collective-permute-start.12 = (bf16[96,2048]{1,0:T(8,128)(2,1)S(1)}, bf16[96,2048]{1,0:T(8,128)(2,1)S(1)}, u32[]{:S(2)}, u32[]{:S(2)}) collective-permute-start(bf16[96,2048]{1,0:T(8,128)(2,1)S(1)} %get-tuple-element.32), channel_id=1, source_target_pairs={{0,6},{2,0},{4,2},{6,4},{1,7},{3,1},{5,3},{7,5},{8,14},{10,8},{12,... | collective-permute-start | bytes 1179656 | tf_op jit(solution)/shard_map/ppermute | solution.py:465
  194.1 17.7 %copy-start.6 = (bf16[1,96,2048]{2,1,0:T(8,128)(2,1)}, bf16[1,96,2048]{2,1,0:T(8,128)(2,1)S(1)}, u32[]{:S(2)}) copy-start(bf16[1,96,2048]{2,1,0:T(8,128)(2,1)S(1)} %collective-permute-done.5) | copy-start | bytes 1179652
  204.0 7.8 %copy-start.7 = (bf16[96,2048]{1,0:T(8,128)(2,1)}, bf16[96,2048]{1,0:T(8,128)(2,1)S(1)}, u32[]{:S(2)}) copy-start(bf16[96,2048]{1,0:T(8,128)(2,1)S(1)} %collective-permute-done.16.refs_4_) | copy-start | bytes 1179652
  211.8 0.8 copy-start.8
  211.9 0.9 copy-start.9
Sparse Core Ops, SparseCore 0:
  9.0 50.6 all-gather.4
  61.8 76.7 all-gather.6

commit v8 on v7

--- a/solution.py
+++ b/solution.py
@@ -122,7 +122,7 @@
     if final:
         top, acc, oscr = refs[at : at + 3]
     y = y_ref[0]
-    lane = lax.broadcasted_iota(jnp.int32, (128, 128), 1)
+    lane = lax.broadcasted_iota(jnp.int32, (1, 128), 1)
     for i in range(chunks):
         kv_ref = kv_refs[i]
 
@@ -134,12 +134,11 @@
             turned = square.T
             to = i * 4 + s
             for c in range(6):
-                part = kv_ref[s, c * 128 : (c + 1) * 128, :].astype(F32)
+                part = kv_ref[s, c * 128 : (c + 1) * 128, :]
                 mine = (lane == HD + c) | (lane == HD + 6 + c) | (lane == HD + 12 + c)
-                kaug[to, c * 128 : (c + 1) * 128, :] = jnp.where(
-                    lane < HD, part, jnp.where(mine, turned, 0.0)
-                ).astype(BF16)
-                vt[to, :, c * 128 : (c + 1) * 128] = part.T.astype(BF16)
+                biased = jnp.where(mine, turned, 0.0).astype(BF16)
+                kaug[to, c * 128 : (c + 1) * 128, :] = jnp.where(lane < HD, part, biased)
+                vt[to, :, c * 128 : (c + 1) * 128] = part.T
             vt[to, 48:64, :] = jnp.ones((16, ROWS), BF16)
             return carry
 
@@ -411,17 +410,21 @@
     )(*pieces, w)
 
 
-def join_kernel(count, *refs):
+def join_kernel(split, *refs):
     same_ref, other_ref = refs[:2]
-    for i in range(count):
-        refs[2 + i][...] = (same_ref[i].astype(F32) + other_ref[i].astype(F32)).astype(BF16)
-
-
-def join(same, other):
-    count = same.shape[0]
-    shape = jax.ShapeDtypeStruct((HALF, 2048), BF16)
-    return pl.pallas_call(
-        functools.partial(join_kernel, count),
+    outs = refs[2:]
+    for i in range(same_ref.shape[0]):
+        both = (same_ref[i].astype(F32) + other_ref[i].astype(F32)).astype(BF16)
+        for k in range(split):
+            rows = HALF // split
+            outs[i * split + k][...] = both[k * rows : (k + 1) * rows]
+
+
+def join(same, other, split=1):
+    count = same.shape[0] * split
+    shape = jax.ShapeDtypeStruct((HALF // split, 2048), BF16)
+    return pl.pallas_call(
+        functools.partial(join_kernel, split),
         out_shape=(shape,) * count,
         in_specs=[vmem()] * 2,
         out_specs=(vmem(),) * count,
@@ -432,8 +435,8 @@
 
 def last_kernel(n_ref, gain_ref, bias_ref, *refs):
     o_ref = refs[-1]
-    total = refs[0][...].astype(F32)
-    for r in refs[1:-1]:
+    total = jnp.concatenate([r[...].astype(F32) for r in refs[-3:-1]], axis=0)
+    for r in refs[:-3]:
         total = total + r[...].astype(F32)
     lowered = total.astype(BF16).astype(F32)
     matrix = ALPHA * n_ref[...].astype(F32) + lowered
@@ -499,9 +502,10 @@
     from_ahead, from_back = turn(to_back, "x", 3), turn(to_ahead, "x", 1)
     far_same, far_other = ffn((far, far_other_rows), ffn_all)
     far_swapped = swap(far_other)
-    (to_far,) = join(far_same, far_swapped)
+    to_far, to_far_round = join(far_same, far_swapped, 2)
     from_far = turn(to_far, "x", 2)
-    parts = [own_same[0], own_swapped[0], from_back, from_ahead, from_far]
+    from_round = turn(turn(to_far_round, "x", 3), "x", 3)
+    parts = [own_same[0], own_swapped[0], from_back, from_ahead, from_far, from_round]
     return last(parts, normed, ffn_gain[None], ffn_bias[None])
 
 

time: 224 us -> 226 us (level)
    ppermute x9 -> x11, starting transfers between devices: 12 us -> 14 us  [turn(): return lax.ppermute(value, axis, [(i, (i + d) % 4) for i in range(4)])]
    ppermute x9 -> x11, waiting for transfers between devices: 36.4 us -> 37.1 us  [turn(): return lax.ppermute(value, axis, [(i, (i + d) % 4) for i in range(4)])]
    unnamed x36 -> x38, local copies, waits for them, and re-layouts: 8.16 us -> 8.19 us
  transfers between devices with their start and end apart: 21 -> 23, of which waited for: 6 -> 7; matrix products, arithmetic and copies ran while one was open for 1% -> 1% of each run, Pallas kernels for 31% -> 30%
where the time goes in v8:
time: 226 us; the launch traced here: 225 us
  Pallas kernels  71.5 us (32%)
  waiting for transfers between devices  65.8 us (29%)
  blocking collectives  40.1 us (18%)
  starting transfers between devices  24.5 us (11%)
  between operations  13.6 us (6%)
  local copies, waits for them, and re-layouts  8.19 us (4%)
    pallas_call x3, Pallas kernels, attend(): pl.pallas_call(functools.partial(attend_kernel, chunks, first, final), ou...  46.8 us
    ppermute x11, waiting for transfers between devices, turn(): return lax.ppermute(value, axis, [(i, (i + d) % 4) for i in range(4)])  37.1 us
    all_to_all x1, blocking collectives, body(): lax.all_to_all(attended, ('z', 'y'), split_axis=0, concat_axis=0, tiled=T...  22.1 us
    all_gather x1, waiting for transfers between devices, body(): w_same = lax.all_gather(out_weight, 'x', axis=0, tiled=False)  19.6 us
    all_to_all x1, blocking collectives, body(): lax.all_to_all(kv_pack, 'z', split_axis=0, concat_axis=0, tiled=True)  18.1 us
    ppermute x11, starting transfers between devices, turn(): return lax.ppermute(value, axis, [(i, (i + d) % 4) for i in range(4)])  14 us
    pallas_call x3, Pallas kernels, ffn(): pl.pallas_call(functools.partial(ffn_kernel, count), out_shape=(shape, sh...  9.49 us
    all_to_all x1, waiting for transfers between devices, body(): lax.all_to_all(spread(by_shard), ('x', 'c'), split_axis=0, concat_axis=0,...  8.27 us
  transfers between devices with their start and end apart: 23, of which 7 were waited for; matrix products, arithmetic and copies ran while one was open for 1% of the time, Pallas kernels for 30%

profile of v8, /device:TPU:0, one launch (start us, length us, event | category | flops | bytes accessed | tf_op | source)
XLA Modules:
  0.0 225.2 jit_solution(1594503586251540514)
XLA Ops:
  6.5 0.7 all-gather.5.cloned.1.call-update
  7.3 0.0 all-gather.7.cloned.1.call-start
  7.3 0.1 copy-done.13
  7.5 0.1 copy-done.12
  7.5 0.1 copy-done.11
  7.6 0.8 pad_maximum_fusion
  8.5 0.0 all-gather.7.cloned.1.call-update
  8.5 2.9 %shard_map.154 = (bf16[16,96,128]{2,1,0:T(8,128)(2,1)}, bf16[4,800,128]{2,1,0:T(8,128)(2,1)}) custom-call(bf16[768,256]{1,0:T(8,128)(2,1)} %q_ref.1, bf16[768,256]{1,0:T(8,128)(2,1)} %k_ref.1, bf16[768,256]{1,0:T(8,128)(2,1)} %v_ref.1, f32[4,768]{1,0:T(4,128)} %bitcast.26), custom_call_target="tpu_custom_call" | custom-call | flops 1000000 | bytes 2500000 | tf_op jit(solution)/shard_map/pallas_call | solution.py:60
  11.4 18.1 %all_to_all.20.refs_2_ = bf16[4,800,128]{2,1,0:T(8,128)(2,1)S(1)} all-to-all(bf16[4,800,128]{2,1,0:T(8,128)(2,1)} %get-tuple-element.22), channel_id=1, replica_groups=mesh['z'=4,'y'=4,'x'=4,'c'=2] {'z'}, dimensions={0} | all-to-all | bytes 1638400 | tf_op jit(solution)/shard_map/all_to_all | solution.py:477
  29.4 5.2 %all-to-all-start.1 = ((bf16[16,96,128]{2,1,0:T(8,128)(2,1)}), bf16[16,96,128]{2,1,0:T(8,128)(2,1)S(1)}, u32[]{:S(2)}, u32[]{:S(2)}) async-start(bf16[16,96,128]{2,1,0:T(8,128)(2,1)} %get-tuple-element.23), calls=%async_computation.1 | async-start | bytes 786432 | tf_op jit(solution)/shard_map/all_to_all | solution.py:476
  34.6 1.9 collective-permute-start.1
  36.5 1.4 collective-permute-start.2
  37.9 2.1 collective-permute-start
  40.1 19.6 %all-gather.5.cloned.1.call-done = bf16[1024,2048]{1,0:T(8,128)(2,1)} async-done(((bf16[256,2048]{1,0:T(8,128)(2,1)}), bf16[1024,2048]{1,0:T(8,128)(2,1)}) %all-gather.5.cloned.1.call-update) | async-done | bytes 4194320 | tf_op jit(solution)/shard_map/all_gather | solution.py:474
  59.7 0.0 collective-permute-start.3
  59.7 0.0 all-to-all-done.1.refs_3_
  59.7 0.7 copy-done.5
  60.4 13.4 %shard_map.155 = (bf16[12,128,256]{2,1,0:T(8,128)(2,1)}, f32[12,8,256]{2,1,0:T(8,128)}, f32[12,80,256]{2,1,0:T(8,128)}) custom-call(s32[4,4,33]{2,1,0:T(4,128)} %constant.19.clone.refs_0_, s32[1]{0:T(128)} %bitcast.3.refs_1_, bf16[4,800,128]{2,1,0:T(8,128)(2,1)} %copy-done.4, bf16[16,96,128]{2,1,0:T(8,128)(2,1)} %copy-done.5), custom_call_target="tpu_custom_call" | custom-call | flops 10400000000 | bytes 3000000 | tf_op jit(solution)/shard_map/pallas_call | solution.py:279
  73.9 0.0 collective-permute-done.1.refs_2_
  73.9 0.0 collective-permute-done.2.refs_3_
  73.9 0.9 copy-done.15
  74.8 19.2 %shard_map.156 = (f32[12,8,256]{2,1,0:T(8,128)}, f32[12,80,256]{2,1,0:T(8,128)}) custom-call(s32[4,4,59]{2,1,0:T(4,128)} %constant.20.clone.refs_0_, s32[1]{0:T(128)} %bitcast.3.refs_1_, bf16[4,800,128]{2,1,0:T(8,128)(2,1)} %copy-done.15, bf16[4,800,128]{2,1,0:T(8,128)(2,1)} %collective-permute-done.2.refs_3_, ...), custom_call_target="tpu_custom_call" | custom-call | flops 21600000000 | bytes 3000000 | tf_op jit(solution)/shard_map/pallas_call | solution.py:279
  94.0 0.0 collective-permute-done.refs_2_
  94.0 0.9 copy-done.14
  94.9 14.1 %shard_map.157 = bf16[16,96,128]{2,1,0:T(8,128)(2,1)} custom-call(s32[4,4,33]{2,1,0:T(4,128)} %constant.21.clone.refs_0_, s32[1]{0:T(128)} %bitcast.3.refs_1_, bf16[4,800,128]{2,1,0:T(8,128)(2,1)} %copy-done.14, bf16[12,128,256]{2,1,0:T(8,128)(2,1)} %get-tuple-element.24.refs_4_.refs_3_, f32[12,8,256]{2,1,0:T(8,128)} %get-tuple-element.27.refs_4_, ...), custom_call_target="tpu_custom_call" | custom-call | flops 10400000000 | bytes 3000000 | tf_op jit(solution)/shard_map/pallas_call | solution.py:279
  109.0 22.1 %all_to_all.21.o_ref = bf16[16,96,128]{2,1,0:T(8,128)(2,1)} all-to-all(bf16[16,96,128]{2,1,0:T(8,128)(2,1)} %shard_map.157), channel_id=1, replica_groups=mesh['z'=4,'y'=4,'x'=4,'c'=2] {'z','y'}, dimensions={0} | all-to-all | bytes 786432 | tf_op jit(solution)/shard_map/all_to_all | solution.py:487
  131.1 2.0 shard_map.158
  133.1 3.5 %all-to-all-start.3 = ((bf16[8,96,256]{2,1,0:T(8,128)(2,1)}), bf16[8,96,256]{2,1,0:T(8,128)(2,1)S(1)}, u32[]{:S(2)}, u32[]{:S(2)}) async-start(bf16[8,96,256]{2,1,0:T(8,128)(2,1)} %shard_map.158), calls=%async_computation.3 | async-start | bytes 786432 | tf_op jit(solution)/shard_map/all_to_all | solution.py:488
  136.6 0.6 pad_add_fusion.place
  137.2 8.3 %all-to-all-done.3.a_ref = bf16[8,96,256]{2,1,0:T(8,128)(2,1)S(1)} async-done(((bf16[8,96,256]{2,1,0:T(8,128)(2,1)}), bf16[8,96,256]{2,1,0:T(8,128)(2,1)S(1)}, u32[]{:S(2)}, u32[]{:S(2)}) %all-to-all-start.3) | async-done | bytes 393248 | tf_op jit(solution)/shard_map/all_to_all | solution.py:488
  145.5 0.7 copy-done.3
  146.2 7.1 %shard_map.159.refs_0_.n_ref = bf16[96,2048]{1,0:T(8,128)(2,1)} custom-call(s32[3]{0:T(128)} %pad_add_fusion.place, bf16[8,96,256]{2,1,0:T(8,128)(2,1)} %copy-done.3, bf16[768,2048]{1,0:T(8,128)(2,1)} %stream_ref.1, f32[1,2048]{1,0:T(1,128)} %bitcast.27, f32[1,2048]{1,0:T(1,128)} %bitcast.28, bf16[4,256,2048]{2,1,0:T(8,128)(2,1)} %bitcast.22, ...), custom_call_target="tpu_custom_call" | custom-call | flops 805306368 | bytes 9000000 | tf_op jit(solution)/shard_map/pallas_call | solution.py:347
  153.3 0.6 collective-permute-start.6
  153.9 2.7 %collective-permute-start.7 = (bf16[96,2048]{1,0:T(8,128)(2,1)}, bf16[96,2048]{1,0:T(8,128)(2,1)S(1)}, u32[]{:S(2)}, u32[]{:S(2)}) collective-permute-start(bf16[96,2048]{1,0:T(8,128)(2,1)} %shard_map.159.refs_0_.n_ref), channel_id=1, source_target_pairs={{0,6},{2,0},{4,2},{6,4},{1,7},{3,1},{5,3},{7,5},{8,14},{10,8},{12,... | collective-permute-start | bytes 1179656 | tf_op jit(solution)/shard_map/ppermute | solution.py:468
  156.5 8.5 %collective-permute-done.6.refs_0_ = bf16[96,2048]{1,0:T(8,128)(2,1)S(1)} collective-permute-done((bf16[96,2048]{1,0:T(8,128)(2,1)}, bf16[96,2048]{1,0:T(8,128)(2,1)S(1)}, u32[]{:S(2)}, u32[]{:S(2)}) %collective-permute-start.6) | collective-permute-done | bytes 393248 | tf_op jit(solution)/shard_map/ppermute | solution.py:468
  165.0 0.5 collective-permute-start.9
  165.5 10.1 %collective-permute-done.13.refs_0_ = bf16[96,2048]{1,0:T(8,128)(2,1)S(1)} collective-permute-done((bf16[96,2048]{1,0:T(8,128)(2,1)S(1)}, bf16[96,2048]{1,0:T(8,128)(2,1)S(1)}, u32[]{:S(2)}, u32[]{:S(2)}) %collective-permute-start.13) | collective-permute-done | bytes 393248 | tf_op jit(solution)/shard_map/ppermute | solution.py:468
  175.7 0.0 collective-permute-start.14
  175.7 0.0 collective-permute-done.9.refs_3_
  175.7 0.0 all-gather.7.cloned.1.call-done
  175.7 3.4 %copy-done = bf16[33792,128]{1,0:T(8,128)(2,1)S(1)} copy-done((bf16[33792,128]{1,0:T(8,128)(2,1)S(1)}, bf16[33792,128]{1,0:T(8,128)(2,1)}, u32[]{:S(2)}) %copy-start) | copy-done | bytes 8650776
  179.2 4.0 %shard_map.161 = (bf16[2,96,2048]{2,1,0:T(8,128)(2,1)S(1)}, bf16[2,96,2048]{2,1,0:T(8,128)(2,1)S(1)}) custom-call(bf16[96,2048]{1,0:T(8,128)(2,1)S(1)} %collective-permute-done.6.refs_0_, bf16[96,2048]{1,0:T(8,128)(2,1)S(1)} %collective-permute-done.7.refs_1_, bf16[96,2048]{1,0:T(8,128)(2,1)S(1)} %collective-permute-done.8.refs_2_, ...), custom_call_target="tpu_custom_call" | custom-call | flops 3321888768 | bytes 10000000 | tf_op jit(solution)/shard_map/pallas_call | solution.py:401
  183.2 0.6 collective-permute-start.10
  183.8 0.1 collective-permute-start.4
  183.9 2.7 %shard_map.163 = (bf16[1,96,2048]{2,1,0:T(8,128)(2,1)S(1)}, bf16[1,96,2048]{2,1,0:T(8,128)(2,1)S(1)}) custom-call(bf16[96,2048]{1,0:T(8,128)(2,1)S(1)} %collective-permute-done.13.refs_0_, bf16[96,2048]{1,0:T(8,128)(2,1)S(1)} %collective-permute-done.14.refs_1_, bf16[16,2112,128]{2,1,0:T(8,128)(2,1)S(1)} %bitcast.16), custom_call_target="tpu_custom_call" | custom-call | flops 1660944384 | bytes 10000000 | tf_op jit(solution)/shard_map/pallas_call | solution.py:401
  186.6 0.5 collective-permute-start.15
  187.1 2.8 %shard_map.160 = (bf16[1,96,2048]{2,1,0:T(8,128)(2,1)S(1)}, bf16[1,96,2048]{2,1,0:T(8,128)(2,1)S(1)}) custom-call(bf16[96,2048]{1,0:T(8,128)(2,1)S(1)} %copy-done.1, bf16[96,2048]{1,0:T(8,128)(2,1)S(1)} %collective-permute-done.4.refs_1_, bf16[16,2112,128]{2,1,0:T(8,128)(2,1)S(1)} %bitcast.19), custom_call_target="tpu_custom_call" | custom-call | flops 1660944384 | bytes 10000000 | tf_op jit(solution)/shard_map/pallas_call | solution.py:401
  189.9 0.2 collective-permute-start.5
  190.1 0.0 collective-permute-done.15.refs_1_
  190.1 0.1 shard_map.164
  190.2 0.1 collective-permute-start.17
  190.3 0.2 shard_map.162
  190.5 0.2 copy-done.2
  190.7 1.9 collective-permute-start.11
  192.6 1.3 collective-permute-start.12
  193.9 0.8 collective-permute-start.16
  194.7 3.3 %collective-permute-done.17 = bf16[48,2048]{1,0:T(8,128)(2,1)S(1)} collective-permute-done((bf16[48,2048]{1,0:T(8,128)(2,1)S(1)}, bf16[48,2048]{1,0:T(8,128)(2,1)S(1)}, u32[]{:S(2)}, u32[]{:S(2)}) %collective-permute-start.17) | collective-permute-done | bytes 196640 | tf_op jit(solution)/shard_map/ppermute | solution.py:468
  198.0 1.2 collective-permute-start.18
  199.3 6.2 %collective-permute-done.16.refs_4_ = bf16[48,2048]{1,0:T(8,128)(2,1)S(1)} collective-permute-done((bf16[48,2048]{1,0:T(8,128)(2,1)S(1)}, bf16[48,2048]{1,0:T(8,128)(2,1)S(1)}, u32[]{:S(2)}, u32[]{:S(2)}) %collective-permute-start.16) | collective-permute-done | bytes 196640 | tf_op jit(solution)/shard_map/ppermute | solution.py:468
  205.4 8.9 %collective-permute-done.18.refs_5_ = bf16[48,2048]{1,0:T(8,128)(2,1)S(1)} collective-permute-done((bf16[48,2048]{1,0:T(8,128)(2,1)S(1)}, bf16[48,2048]{1,0:T(8,128)(2,1)S(1)}, u32[]{:S(2)}, u32[]{:S(2)}) %collective-permute-start.18) | collective-permute-done | bytes 196640 | tf_op jit(solution)/shard_map/ppermute | solution.py:468
  214.4 0.6 copy-done.10
  215.1 0.1 copy-done.7
  215.2 0.1 copy-done.8
  215.3 3.0 %shard_map.165 = bf16[96,2048]{1,0:T(8,128)(2,1)} custom-call(bf16[96,2048]{1,0:T(8,128)(2,1)} %shard_map.159.refs_0_.n_ref, f32[1,2048]{1,0:T(1,128)} %bitcast.29, f32[1,2048]{1,0:T(1,128)} %bitcast.30, bf16[96,2048]{1,0:T(8,128)(2,1)} %bitcast.20, bf16[96,2048]{1,0:T(8,128)(2,1)} %bitcast.23, bf16[96,2048]{1,0:T(8,128)(2,1)} %copy-done.7, ...), custom_call_target="tpu_custom_call" | custom-call | flops 4000000 | bytes 4000000 | tf_op jit(solution)/shard_map/pallas_call | solution.py:447
  (39 shorter events, 0.1 us)
Async XLA Ops:
  6.5 0.9 copy-start.13
  6.5 1.0 copy-start.12
  6.5 1.1 copy-start.11
  6.5 53.1 %all-gather.5.cloned.1.call-start = ((), (), s32[]{:S(2)}) async-start(), calls=%async_computation.4 | async-start | bytes 5242880 | tf_op jit(solution)/shard_map/all_gather | solution.py:474
  7.3 168.5 %all-gather.7.cloned.1.call-start = ((), (), s32[]{:S(2)}) async-start(), calls=%async_computation.5 | async-start | bytes 9191424 | tf_op jit(solution)/shard_map/all_gather | solution.py:482
  29.4 30.3 %copy-start.4 = (bf16[4,800,128]{2,1,0:T(8,128)(2,1)}, bf16[4,800,128]{2,1,0:T(8,128)(2,1)S(1)}, u32[]{:S(2)}) copy-start(bf16[4,800,128]{2,1,0:T(8,128)(2,1)S(1)} %all_to_all.20.refs_2_) | copy-start | bytes 2457604
  29.4 30.3 %all-to-all-start.1 = ((bf16[16,96,128]{2,1,0:T(8,128)(2,1)}), bf16[16,96,128]{2,1,0:T(8,128)(2,1)S(1)}, u32[]{:S(2)}, u32[]{:S(2)}) async-start(bf16[16,96,128]{2,1,0:T(8,128)(2,1)} %get-tuple-element.23), calls=%async_computation.1 | async-start | bytes 786432 | tf_op jit(solution)/shard_map/all_to_all | solution.py:476
  34.6 39.3 %collective-permute-start.1 = (bf16[4,800,128]{2,1,0:T(8,128)(2,1)S(1)}, bf16[4,800,128]{2,1,0:T(8,128)(2,1)S(1)}, u32[]{:S(2)}, u32[]{:S(2)}) collective-permute-start(bf16[4,800,128]{2,1,0:T(8,128)(2,1)S(1)} %all_to_all.20.refs_2_), channel_id=1, source_target_pairs={{0,8},{8,16},{16,24},{24,0},{1,9},{9,17},{17,25},{25,1},{2,10},{10... | collective-permute-start | bytes 2457608 | tf_op jit(solution)/shard_map/ppermute | solution.py:468
  36.5 37.4 %collective-permute-start.2 = (bf16[4,800,128]{2,1,0:T(8,128)(2,1)S(1)}, bf16[4,800,128]{2,1,0:T(8,128)(2,1)}, u32[]{:S(2)}, u32[]{:S(2)}) collective-permute-start(bf16[4,800,128]{2,1,0:T(8,128)(2,1)S(1)} %all_to_all.20.refs_2_), channel_id=1, source_target_pairs={{0,24},{8,0},{16,8},{24,16},{1,25},{9,1},{17,9},{25,17},{2,26},{10... | collective-permute-start | bytes 2457608 | tf_op jit(solution)/shard_map/ppermute | solution.py:468
  37.9 56.1 %collective-permute-start = (bf16[4,800,128]{2,1,0:T(8,128)(2,1)S(1)}, bf16[4,800,128]{2,1,0:T(8,128)(2,1)S(1)}, u32[]{:S(2)}, u32[]{:S(2)}) collective-permute-start(bf16[4,800,128]{2,1,0:T(8,128)(2,1)S(1)} %all_to_all.20.refs_2_), channel_id=1, source_target_pairs={{0,16},{8,24},{16,0},{24,8},{1,17},{9,25},{17,1},{25,9},{2,18},{10... | collective-permute-start | bytes 2457608 | tf_op jit(solution)/shard_map/ppermute | solution.py:468
  59.7 85.8 %collective-permute-start.3 = (bf16[4,256,2048]{2,1,0:T(8,128)(2,1)}, bf16[4,256,2048]{2,1,0:T(8,128)(2,1)}, u32[]{:S(2)}, u32[]{:S(2)}) collective-permute-start(bf16[4,256,2048]{2,1,0:T(8,128)(2,1)} %bitcast.21), channel_id=1, source_target_pairs={{0,1},{1,0},{2,3},{3,2},{4,5},{5,4},{6,7},{7,6},{8,9},{9,8},{10,11... | collective-permute-start | bytes 12582920 | tf_op jit(solution)/shard_map/ppermute | solution.py:471
  59.7 0.7 copy-start.5
  73.9 0.9 copy-start.15
  94.0 0.9 copy-start.14
  133.1 12.3 %all-to-all-start.3 = ((bf16[8,96,256]{2,1,0:T(8,128)(2,1)}), bf16[8,96,256]{2,1,0:T(8,128)(2,1)S(1)}, u32[]{:S(2)}, u32[]{:S(2)}) async-start(bf16[8,96,256]{2,1,0:T(8,128)(2,1)} %shard_map.158), calls=%async_computation.3 | async-start | bytes 786432 | tf_op jit(solution)/shard_map/all_to_all | solution.py:488
  145.5 0.7 copy-start.3
  153.3 11.7 %collective-permute-start.6 = (bf16[96,2048]{1,0:T(8,128)(2,1)}, bf16[96,2048]{1,0:T(8,128)(2,1)S(1)}, u32[]{:S(2)}, u32[]{:S(2)}) collective-permute-start(bf16[96,2048]{1,0:T(8,128)(2,1)} %shard_map.159.refs_0_.n_ref), channel_id=1, source_target_pairs={{0,2},{2,4},{4,6},{6,0},{1,3},{3,5},{5,7},{7,1},{8,10},{10,12},{12... | collective-permute-start | bytes 1179656 | tf_op jit(solution)/shard_map/ppermute | solution.py:468
  153.9 11.2 %collective-permute-start.7 = (bf16[96,2048]{1,0:T(8,128)(2,1)}, bf16[96,2048]{1,0:T(8,128)(2,1)S(1)}, u32[]{:S(2)}, u32[]{:S(2)}) collective-permute-start(bf16[96,2048]{1,0:T(8,128)(2,1)} %shard_map.159.refs_0_.n_ref), channel_id=1, source_target_pairs={{0,6},{2,0},{4,2},{6,4},{1,7},{3,1},{5,3},{7,5},{8,14},{10,8},{12,... | collective-permute-start | bytes 1179656 | tf_op jit(solution)/shard_map/ppermute | solution.py:468
  165.0 10.7 %collective-permute-start.13 = (bf16[96,2048]{1,0:T(8,128)(2,1)S(1)}, bf16[96,2048]{1,0:T(8,128)(2,1)S(1)}, u32[]{:S(2)}, u32[]{:S(2)}) collective-permute-start(bf16[96,2048]{1,0:T(8,128)(2,1)S(1)} %collective-permute-done.6.refs_0_), channel_id=1, source_target_pairs={{0,2},{2,4},{4,6},{6,0},{1,3},{3,5},{5,7},{7,1},{8,10},{10,12},{12... | collective-permute-start | bytes 1179656 | tf_op jit(solution)/shard_map/ppermute | solution.py:468
  165.0 10.7 %collective-permute-start.8 = (bf16[96,2048]{1,0:T(8,128)(2,1)S(1)}, bf16[96,2048]{1,0:T(8,128)(2,1)S(1)}, u32[]{:S(2)}, u32[]{:S(2)}) collective-permute-start(bf16[96,2048]{1,0:T(8,128)(2,1)S(1)} %collective-permute-done.6.refs_0_), channel_id=1, source_target_pairs={{0,1},{1,0},{2,3},{3,2},{4,5},{5,4},{6,7},{7,6},{8,9},{9,8},{10,11... | collective-permute-start | bytes 1179656 | tf_op jit(solution)/shard_map/ppermute | solution.py:471
  165.0 10.7 %collective-permute-start.9 = (bf16[96,2048]{1,0:T(8,128)(2,1)S(1)}, bf16[96,2048]{1,0:T(8,128)(2,1)S(1)}, u32[]{:S(2)}, u32[]{:S(2)}) collective-permute-start(bf16[96,2048]{1,0:T(8,128)(2,1)S(1)} %collective-permute-done.7.refs_1_), channel_id=1, source_target_pairs={{0,1},{1,0},{2,3},{3,2},{4,5},{5,4},{6,7},{7,6},{8,9},{9,8},{10,11... | collective-permute-start | bytes 1179656 | tf_op jit(solution)/shard_map/ppermute | solution.py:471
  175.7 8.2 %collective-permute-start.14 = (bf16[96,2048]{1,0:T(8,128)(2,1)S(1)}, bf16[96,2048]{1,0:T(8,128)(2,1)S(1)}, u32[]{:S(2)}, u32[]{:S(2)}) collective-permute-start(bf16[96,2048]{1,0:T(8,128)(2,1)S(1)} %collective-permute-done.13.refs_0_), channel_id=1, source_target_pairs={{0,1},{1,0},{2,3},{3,2},{4,5},{5,4},{6,7},{7,6},{8,9},{9,8},{10,11... | collective-permute-start | bytes 1179656 | tf_op jit(solution)/shard_map/ppermute | solution.py:471
  175.7 3.5 %copy-start = (bf16[33792,128]{1,0:T(8,128)(2,1)S(1)}, bf16[33792,128]{1,0:T(8,128)(2,1)}, u32[]{:S(2)}) copy-start(bf16[33792,128]{1,0:T(8,128)(2,1)} %all-gather.7.cloned.1.call-done) | copy-start | bytes 25952260
  179.2 4.6 %copy-start.1 = (bf16[96,2048]{1,0:T(8,128)(2,1)S(1)}, bf16[96,2048]{1,0:T(8,128)(2,1)}, u32[]{:S(2)}) copy-start(bf16[96,2048]{1,0:T(8,128)(2,1)} %shard_map.159.refs_0_.n_ref) | copy-start | bytes 1179652
  179.2 7.9 %slice-start = ((s8[8650752]{0:T(1024)(128)(4,1)}), s8[4194304]{0:T(1024)(128)(4,1)S(1)}, s32[]{:S(2)}) async-start(s8[8650752]{0:T(1024)(128)(4,1)} %bitcast.17), calls=%async_computation.6 | async-start | bytes 8388608
  179.2 7.9 %slice-start.1 = ((s8[8650752]{0:T(1024)(128)(4,1)}), s8[262144]{0:T(1024)(128)(4,1)S(1)}, s32[]{:S(2)}) async-start(s8[8650752]{0:T(1024)(128)(4,1)} %bitcast.17), calls=%async_computation.7 | async-start | bytes 524288
  183.2 3.9 %slice-start.2 = ((s8[8650752]{0:T(1024)(128)(4,1)}), s8[4194304]{0:T(1024)(128)(4,1)S(1)}, s32[]{:S(2)}) async-start(s8[8650752]{0:T(1024)(128)(4,1)} %bitcast.17), calls=%async_computation.8 | async-start | bytes 8388608
  183.2 7.1 %collective-permute-start.10 = (bf16[2,96,2048]{2,1,0:T(8,128)(2,1)S(1)}, bf16[2,96,2048]{2,1,0:T(8,128)(2,1)S(1)}, u32[]{:S(2)}, u32[]{:S(2)}) collective-permute-start(bf16[2,96,2048]{2,1,0:T(8,128)(2,1)S(1)} %get-tuple-element.32), channel_id=1, source_target_pairs={{0,1},{1,0},{2,3},{3,2},{4,5},{5,4},{6,7},{7,6},{8,9},{9,8},{10,11... | collective-permute-start | bytes 2359304 | tf_op jit(solution)/shard_map/ppermute | solution.py:471
  183.8 3.4 %collective-permute-start.4 = (bf16[96,2048]{1,0:T(8,128)(2,1)S(1)}, bf16[96,2048]{1,0:T(8,128)(2,1)S(1)}, u32[]{:S(2)}, u32[]{:S(2)}) collective-permute-start(bf16[96,2048]{1,0:T(8,128)(2,1)S(1)} %copy-done.1), channel_id=1, source_target_pairs={{0,1},{1,0},{2,3},{3,2},{4,5},{5,4},{6,7},{7,6},{8,9},{9,8},{10,11... | collective-permute-start | bytes 1179656 | tf_op jit(solution)/shard_map/ppermute | solution.py:471
  186.6 3.5 %collective-permute-start.15 = (bf16[1,96,2048]{2,1,0:T(8,128)(2,1)S(1)}, bf16[1,96,2048]{2,1,0:T(8,128)(2,1)S(1)}, u32[]{:S(2)}, u32[]{:S(2)}) collective-permute-start(bf16[1,96,2048]{2,1,0:T(8,128)(2,1)S(1)} %get-tuple-element.36), channel_id=1, source_target_pairs={{0,1},{1,0},{2,3},{3,2},{4,5},{5,4},{6,7},{7,6},{8,9},{9,8},{10,11... | collective-permute-start | bytes 1179656 | tf_op jit(solution)/shard_map/ppermute | solution.py:471
  189.9 0.8 copy-start.2
  189.9 9.3 %collective-permute-start.5 = (bf16[1,96,2048]{2,1,0:T(8,128)(2,1)S(1)}, bf16[1,96,2048]{2,1,0:T(8,128)(2,1)S(1)}, u32[]{:S(2)}, u32[]{:S(2)}) collective-permute-start(bf16[1,96,2048]{2,1,0:T(8,128)(2,1)S(1)} %get-tuple-element.30), channel_id=1, source_target_pairs={{0,1},{1,0},{2,3},{3,2},{4,5},{5,4},{6,7},{7,6},{8,9},{9,8},{10,11... | collective-permute-start | bytes 1179656 | tf_op jit(solution)/shard_map/ppermute | solution.py:471
  190.2 7.8 %collective-permute-start.17 = (bf16[48,2048]{1,0:T(8,128)(2,1)S(1)}, bf16[48,2048]{1,0:T(8,128)(2,1)S(1)}, u32[]{:S(2)}, u32[]{:S(2)}) collective-permute-start(bf16[48,2048]{1,0:T(8,128)(2,1)S(1)} %get-tuple-element.38), channel_id=1, source_target_pairs={{0,6},{2,0},{4,2},{6,4},{1,7},{3,1},{5,3},{7,5},{8,14},{10,8},{12,... | collective-permute-start | bytes 589832 | tf_op jit(solution)/shard_map/ppermute | solution.py:468
  190.7 23.7 %collective-permute-start.11 = (bf16[96,2048]{1,0:T(8,128)(2,1)S(1)}, bf16[96,2048]{1,0:T(8,128)(2,1)S(1)}, u32[]{:S(2)}, u32[]{:S(2)}) collective-permute-start(bf16[96,2048]{1,0:T(8,128)(2,1)S(1)} %get-tuple-element.33), channel_id=1, source_target_pairs={{0,2},{2,4},{4,6},{6,0},{1,3},{3,5},{5,7},{7,1},{8,10},{10,12},{12... | collective-permute-start | bytes 1179656 | tf_op jit(solution)/shard_map/ppermute | solution.py:468
  192.6 21.8 %collective-permute-start.12 = (bf16[96,2048]{1,0:T(8,128)(2,1)S(1)}, bf16[96,2048]{1,0:T(8,128)(2,1)S(1)}, u32[]{:S(2)}, u32[]{:S(2)}) collective-permute-start(bf16[96,2048]{1,0:T(8,128)(2,1)S(1)} %get-tuple-element.34), channel_id=1, source_target_pairs={{0,6},{2,0},{4,2},{6,4},{1,7},{3,1},{5,3},{7,5},{8,14},{10,8},{12,... | collective-permute-start | bytes 1179656 | tf_op jit(solution)/shard_map/ppermute | solution.py:468
  193.9 11.5 %collective-permute-start.16 = (bf16[48,2048]{1,0:T(8,128)(2,1)S(1)}, bf16[48,2048]{1,0:T(8,128)(2,1)S(1)}, u32[]{:S(2)}, u32[]{:S(2)}) collective-permute-start(bf16[48,2048]{1,0:T(8,128)(2,1)S(1)} %get-tuple-element.37), channel_id=1, source_target_pairs={{0,4},{2,6},{4,0},{6,2},{1,5},{3,7},{5,1},{7,3},{8,12},{10,14},{12... | collective-permute-start | bytes 589832 | tf_op jit(solution)/shard_map/ppermute | solution.py:468
  198.0 16.3 %collective-permute-start.18 = (bf16[48,2048]{1,0:T(8,128)(2,1)S(1)}, bf16[48,2048]{1,0:T(8,128)(2,1)S(1)}, u32[]{:S(2)}, u32[]{:S(2)}) collective-permute-start(bf16[48,2048]{1,0:T(8,128)(2,1)S(1)} %collective-permute-done.17), channel_id=1, source_target_pairs={{0,6},{2,0},{4,2},{6,4},{1,7},{3,1},{5,3},{7,5},{8,14},{10,8},{12,... | collective-permute-start | bytes 589832 | tf_op jit(solution)/shard_map/ppermute | solution.py:468
  199.3 15.2 %copy-start.6 = (bf16[1,96,2048]{2,1,0:T(8,128)(2,1)}, bf16[1,96,2048]{2,1,0:T(8,128)(2,1)S(1)}, u32[]{:S(2)}) copy-start(bf16[1,96,2048]{2,1,0:T(8,128)(2,1)S(1)} %collective-permute-done.5) | copy-start | bytes 1179652
  205.4 9.0 %copy-start.9 = (bf16[48,2048]{1,0:T(8,128)(2,1)}, bf16[48,2048]{1,0:T(8,128)(2,1)S(1)}, u32[]{:S(2)}) copy-start(bf16[48,2048]{1,0:T(8,128)(2,1)S(1)} %collective-permute-done.16.refs_4_) | copy-start | bytes 589828
  214.4 0.7 copy-start.10
  214.4 0.8 copy-start.7
  214.4 0.9 copy-start.8
Sparse Core Ops, SparseCore 0:
  9.0 50.6 all-gather.4
  61.8 76.8 all-gather.6

commit v9 on v8

--- a/solution.py
+++ b/solution.py
@@ -210,7 +210,9 @@
         top[t, 0:1, :] = high
         al_now[0:1, :] = jnp.exp(old - high)
         scores(u + 1, s_next, mx_next, masked)
-        p_now[...] = jnp.exp(s_now[...] - high).astype(BF16)
+        for k in range(2):
+            part = slice(384 * k, 384 * (k + 1))
+            p_now[part, :] = jnp.exp(s_now[part, :] - high).astype(BF16)
         gather(u - 1, p_before, al_before)
 
     one, two = (s_a, p_a, al_a, mx_a), (s_b, p_b, al_b, mx_b)
@@ -435,8 +437,8 @@
 
 def last_kernel(n_ref, gain_ref, bias_ref, *refs):
     o_ref = refs[-1]
-    total = jnp.concatenate([r[...].astype(F32) for r in refs[-3:-1]], axis=0)
-    for r in refs[:-3]:
+    total = refs[0][...].astype(F32)
+    for r in refs[1:-1]:
         total = total + r[...].astype(F32)
     lowered = total.astype(BF16).astype(F32)
     matrix = ALPHA * n_ref[...].astype(F32) + lowered
@@ -449,7 +451,7 @@
         out_shape=jax.ShapeDtypeStruct((HALF, 2048), BF16),
         in_specs=[vmem()] * (3 + len(parts)),
         out_specs=vmem(),
-        compiler_params=params(60),
+        compiler_params=params(16),
         cost_estimate=pl.CostEstimate(
             flops=4 * 10**6, bytes_accessed=4 * 10**6, transcendentals=0
         ),
@@ -502,10 +504,9 @@
     from_ahead, from_back = turn(to_back, "x", 3), turn(to_ahead, "x", 1)
     far_same, far_other = ffn((far, far_other_rows), ffn_all)
     far_swapped = swap(far_other)
-    to_far, to_far_round = join(far_same, far_swapped, 2)
+    (to_far,) = join(far_same, far_swapped)
     from_far = turn(to_far, "x", 2)
-    from_round = turn(turn(to_far_round, "x", 3), "x", 3)
-    parts = [own_same[0], own_swapped[0], from_back, from_ahead, from_far, from_round]
+    parts = [own_same[0], own_swapped[0], from_back, from_ahead, from_far]
     return last(parts, normed, ffn_gain[None], ffn_bias[None])
 
 

time: 226 us -> 220 us (0.973)
  Pallas kernels: 71.5 us -> 68 us
    ppermute x11 -> x9, starting transfers between devices: 14 us -> 12.1 us  [turn(): return lax.ppermute(value, axis, [(i, (i + d) % 4) for i in range(4)])]
    unnamed x38 -> x30, local copies, waits for them, and re-layouts: 8.19 us -> 7.11 us
    ppermute x11 -> x9, waiting for transfers between devices: 37.1 us -> 36.5 us  [turn(): return lax.ppermute(value, axis, [(i, (i + d) % 4) for i in range(4)])]
  transfers between devices with their start and end apart: 23 -> 21, of which waited for: 7 -> 6; matrix products, arithmetic and copies ran while one was open for 1% -> 1% of each run, Pallas kernels for 30% -> 30%
where the time goes in v9:
time: 220 us; the launch traced here: 219 us
  Pallas kernels  68 us (31%)
  waiting for transfers between devices  65.1 us (30%)
  blocking collectives  40.7 us (19%)
  starting transfers between devices  22.6 us (10%)
  between operations  13.6 us (6%)
  local copies, waits for them, and re-layouts  7.11 us (3%)
    pallas_call x3, Pallas kernels, attend(): pl.pallas_call(functools.partial(attend_kernel, chunks, first, final), ou...  44.9 us
    ppermute x9, waiting for transfers between devices, turn(): return lax.ppermute(value, axis, [(i, (i + d) % 4) for i in range(4)])  36.5 us
    all_to_all x1, blocking collectives, body(): lax.all_to_all(attended, ('z', 'y'), split_axis=0, concat_axis=0, tiled=T...  22.6 us
    all_gather x1, waiting for transfers between devices, body(): w_same = lax.all_gather(out_weight, 'x', axis=0, tiled=False)  19.6 us
    all_to_all x1, blocking collectives, body(): lax.all_to_all(kv_pack, 'z', split_axis=0, concat_axis=0, tiled=True)  18.1 us
    ppermute x9, starting transfers between devices, turn(): return lax.ppermute(value, axis, [(i, (i + d) % 4) for i in range(4)])  12.1 us
    pallas_call x3, Pallas kernels, ffn(): pl.pallas_call(functools.partial(ffn_kernel, count), out_shape=(shape, sh...  9.48 us
    all_to_all x1, waiting for transfers between devices, body(): lax.all_to_all(spread(by_shard), ('x', 'c'), split_axis=0, concat_axis=0,...  8.3 us
  transfers between devices with their start and end apart: 21, of which 6 were waited for; matrix products, arithmetic and copies ran while one was open for 1% of the time, Pallas kernels for 30%

profile of v9, /device:TPU:0, one launch (start us, length us, event | category | flops | bytes accessed | tf_op | source)
XLA Modules:
  0.0 218.6 jit_solution(12714526275871444508)
XLA Ops:
  6.5 0.7 all-gather.5.cloned.1.call-update
  7.3 0.0 all-gather.7.cloned.1.call-start
  7.3 0.1 copy-done.9
  7.5 0.1 copy-done.8
  7.5 0.1 copy-done.7
  7.6 0.9 pad_maximum_fusion
  8.5 0.0 all-gather.7.cloned.1.call-update
  8.5 2.9 %shard_map.154 = (bf16[16,96,128]{2,1,0:T(8,128)(2,1)}, bf16[4,800,128]{2,1,0:T(8,128)(2,1)}) custom-call(bf16[768,256]{1,0:T(8,128)(2,1)} %q_ref.1, bf16[768,256]{1,0:T(8,128)(2,1)} %k_ref.1, bf16[768,256]{1,0:T(8,128)(2,1)} %v_ref.1, f32[4,768]{1,0:T(4,128)} %bitcast.28), custom_call_target="tpu_custom_call" | custom-call | flops 1000000 | bytes 2500000 | tf_op jit(solution)/shard_map/pallas_call | solution.py:60
  11.4 18.1 %all_to_all.20.refs_2_ = bf16[4,800,128]{2,1,0:T(8,128)(2,1)S(1)} all-to-all(bf16[4,800,128]{2,1,0:T(8,128)(2,1)} %get-tuple-element.20), channel_id=1, replica_groups=mesh['z'=4,'y'=4,'x'=4,'c'=2] {'z'}, dimensions={0} | all-to-all | bytes 1638400 | tf_op jit(solution)/shard_map/all_to_all | solution.py:479
  29.5 5.2 %all-to-all-start.1 = ((bf16[16,96,128]{2,1,0:T(8,128)(2,1)}), bf16[16,96,128]{2,1,0:T(8,128)(2,1)S(1)}, u32[]{:S(2)}, u32[]{:S(2)}) async-start(bf16[16,96,128]{2,1,0:T(8,128)(2,1)} %get-tuple-element.21), calls=%async_computation.1 | async-start | bytes 786432 | tf_op jit(solution)/shard_map/all_to_all | solution.py:478
  34.6 1.9 collective-permute-start.1
  36.6 1.4 collective-permute-start.2
  38.0 2.1 collective-permute-start
  40.1 19.6 %all-gather.5.cloned.1.call-done = bf16[1024,2048]{1,0:T(8,128)(2,1)} async-done(((bf16[256,2048]{1,0:T(8,128)(2,1)}), bf16[1024,2048]{1,0:T(8,128)(2,1)}) %all-gather.5.cloned.1.call-update) | async-done | bytes 4194320 | tf_op jit(solution)/shard_map/all_gather | solution.py:476
  59.7 0.0 collective-permute-start.3
  59.7 0.0 all-to-all-done.1.refs_3_
  59.7 0.7 copy-done.6
  60.4 13.0 %shard_map.155 = (bf16[12,128,256]{2,1,0:T(8,128)(2,1)}, f32[12,8,256]{2,1,0:T(8,128)}, f32[12,80,256]{2,1,0:T(8,128)}) custom-call(s32[4,4,33]{2,1,0:T(4,128)} %constant.19.clone.refs_0_, s32[1]{0:T(128)} %bitcast.3.refs_1_, bf16[4,800,128]{2,1,0:T(8,128)(2,1)} %copy-done.5, bf16[16,96,128]{2,1,0:T(8,128)(2,1)} %copy-done.6), custom_call_target="tpu_custom_call" | custom-call | flops 10400000000 | bytes 3000000 | tf_op jit(solution)/shard_map/pallas_call | solution.py:281
  73.5 0.0 collective-permute-done.1.refs_2_
  73.5 0.0 collective-permute-done.2.refs_3_
  73.5 0.9 copy-done.11
  74.4 18.6 %shard_map.156 = (f32[12,8,256]{2,1,0:T(8,128)}, f32[12,80,256]{2,1,0:T(8,128)}) custom-call(s32[4,4,59]{2,1,0:T(4,128)} %constant.20.clone.refs_0_, s32[1]{0:T(128)} %bitcast.3.refs_1_, bf16[4,800,128]{2,1,0:T(8,128)(2,1)} %copy-done.11, bf16[4,800,128]{2,1,0:T(8,128)(2,1)} %collective-permute-done.2.refs_3_, ...), custom_call_target="tpu_custom_call" | custom-call | flops 21600000000 | bytes 3000000 | tf_op jit(solution)/shard_map/pallas_call | solution.py:281
  92.9 0.0 collective-permute-done.refs_2_
  92.9 0.9 copy-done.10
  93.9 13.3 %shard_map.157 = bf16[16,96,128]{2,1,0:T(8,128)(2,1)} custom-call(s32[4,4,33]{2,1,0:T(4,128)} %constant.21.clone.refs_0_, s32[1]{0:T(128)} %bitcast.3.refs_1_, bf16[4,800,128]{2,1,0:T(8,128)(2,1)} %copy-done.10, bf16[12,128,256]{2,1,0:T(8,128)(2,1)} %get-tuple-element.22.refs_4_.refs_3_, f32[12,8,256]{2,1,0:T(8,128)} %get-tuple-element.25.refs_4_, ...), custom_call_target="tpu_custom_call" | custom-call | flops 10400000000 | bytes 3000000 | tf_op jit(solution)/shard_map/pallas_call | solution.py:281
  107.2 22.6 %all_to_all.21.o_ref = bf16[16,96,128]{2,1,0:T(8,128)(2,1)} all-to-all(bf16[16,96,128]{2,1,0:T(8,128)(2,1)} %shard_map.157), channel_id=1, replica_groups=mesh['z'=4,'y'=4,'x'=4,'c'=2] {'z','y'}, dimensions={0} | all-to-all | bytes 786432 | tf_op jit(solution)/shard_map/all_to_all | solution.py:489
  129.8 2.0 shard_map.158
  131.8 3.5 %all-to-all-start.3 = ((bf16[8,96,256]{2,1,0:T(8,128)(2,1)}), bf16[8,96,256]{2,1,0:T(8,128)(2,1)S(1)}, u32[]{:S(2)}, u32[]{:S(2)}) async-start(bf16[8,96,256]{2,1,0:T(8,128)(2,1)} %shard_map.158), calls=%async_computation.3 | async-start | bytes 786432 | tf_op jit(solution)/shard_map/all_to_all | solution.py:490
  135.3 0.6 pad_add_fusion.place
  135.9 8.3 %all-to-all-done.3.a_ref = bf16[8,96,256]{2,1,0:T(8,128)(2,1)S(1)} async-done(((bf16[8,96,256]{2,1,0:T(8,128)(2,1)}), bf16[8,96,256]{2,1,0:T(8,128)(2,1)S(1)}, u32[]{:S(2)}, u32[]{:S(2)}) %all-to-all-start.3) | async-done | bytes 393248 | tf_op jit(solution)/shard_map/all_to_all | solution.py:490
  144.2 0.0 collective-permute-done.3.other_ref
  144.2 0.7 copy-done.4
  144.9 7.1 %shard_map.159.refs_0_.n_ref = bf16[96,2048]{1,0:T(8,128)(2,1)} custom-call(s32[3]{0:T(128)} %pad_add_fusion.place, bf16[8,96,256]{2,1,0:T(8,128)(2,1)} %copy-done.4, bf16[768,2048]{1,0:T(8,128)(2,1)} %stream_ref.1, f32[1,2048]{1,0:T(1,128)} %bitcast.29, f32[1,2048]{1,0:T(1,128)} %bitcast.30, bf16[4,256,2048]{2,1,0:T(8,128)(2,1)} %bitcast.25, ...), custom_call_target="tpu_custom_call" | custom-call | flops 805306368 | bytes 9000000 | tf_op jit(solution)/shard_map/pallas_call | solution.py:349
  152.0 0.6 collective-permute-start.6
  152.5 2.7 %collective-permute-start.7 = (bf16[96,2048]{1,0:T(8,128)(2,1)}, bf16[96,2048]{1,0:T(8,128)(2,1)S(1)}, u32[]{:S(2)}, u32[]{:S(2)}) collective-permute-start(bf16[96,2048]{1,0:T(8,128)(2,1)} %shard_map.159.refs_0_.n_ref), channel_id=1, source_target_pairs={{0,6},{2,0},{4,2},{6,4},{1,7},{3,1},{5,3},{7,5},{8,14},{10,8},{12,... | collective-permute-start | bytes 1179656 | tf_op jit(solution)/shard_map/ppermute | solution.py:470
  155.2 8.5 %collective-permute-done.6.refs_0_ = bf16[96,2048]{1,0:T(8,128)(2,1)S(1)} collective-permute-done((bf16[96,2048]{1,0:T(8,128)(2,1)}, bf16[96,2048]{1,0:T(8,128)(2,1)S(1)}, u32[]{:S(2)}, u32[]{:S(2)}) %collective-permute-start.6) | collective-permute-done | bytes 393248 | tf_op jit(solution)/shard_map/ppermute | solution.py:470
  163.7 0.0 collective-permute-start.13
  163.7 0.0 collective-permute-start.8
  163.7 0.0 collective-permute-done.7.refs_1_
  163.7 0.5 collective-permute-start.9
  164.2 10.1 %collective-permute-done.13.refs_0_ = bf16[96,2048]{1,0:T(8,128)(2,1)S(1)} collective-permute-done((bf16[96,2048]{1,0:T(8,128)(2,1)S(1)}, bf16[96,2048]{1,0:T(8,128)(2,1)S(1)}, u32[]{:S(2)}, u32[]{:S(2)}) %collective-permute-start.13) | collective-permute-done | bytes 393248 | tf_op jit(solution)/shard_map/ppermute | solution.py:470
  174.4 0.0 collective-permute-start.14
  174.4 0.0 collective-permute-done.8.refs_2_
  174.4 0.0 all-gather.7.cloned.1.call-done
  174.4 3.4 %copy-done = bf16[33792,128]{1,0:T(8,128)(2,1)S(1)} copy-done((bf16[33792,128]{1,0:T(8,128)(2,1)S(1)}, bf16[33792,128]{1,0:T(8,128)(2,1)}, u32[]{:S(2)}) %copy-start) | copy-done | bytes 8650776
  177.9 4.0 %shard_map.161 = (bf16[2,96,2048]{2,1,0:T(8,128)(2,1)S(1)}, bf16[2,96,2048]{2,1,0:T(8,128)(2,1)S(1)}) custom-call(bf16[96,2048]{1,0:T(8,128)(2,1)S(1)} %collective-permute-done.6.refs_0_, bf16[96,2048]{1,0:T(8,128)(2,1)S(1)} %collective-permute-done.7.refs_1_, bf16[96,2048]{1,0:T(8,128)(2,1)S(1)} %collective-permute-done.8.refs_2_, ...), custom_call_target="tpu_custom_call" | custom-call | flops 3321888768 | bytes 10000000 | tf_op jit(solution)/shard_map/pallas_call | solution.py:403
  181.9 0.0 slice-start.2
  181.9 0.6 collective-permute-start.10
  182.4 0.1 collective-permute-start.4
  182.5 2.7 %shard_map.163 = (bf16[1,96,2048]{2,1,0:T(8,128)(2,1)S(1)}, bf16[1,96,2048]{2,1,0:T(8,128)(2,1)S(1)}) custom-call(bf16[96,2048]{1,0:T(8,128)(2,1)S(1)} %collective-permute-done.13.refs_0_, bf16[96,2048]{1,0:T(8,128)(2,1)S(1)} %collective-permute-done.14.refs_1_, bf16[16,2112,128]{2,1,0:T(8,128)(2,1)S(1)} %bitcast.16), custom_call_target="tpu_custom_call" | custom-call | flops 1660944384 | bytes 10000000 | tf_op jit(solution)/shard_map/pallas_call | solution.py:403
  185.3 0.5 collective-permute-start.15
  185.8 2.8 %shard_map.160 = (bf16[1,96,2048]{2,1,0:T(8,128)(2,1)S(1)}, bf16[1,96,2048]{2,1,0:T(8,128)(2,1)S(1)}) custom-call(bf16[96,2048]{1,0:T(8,128)(2,1)S(1)} %copy-done.1, bf16[96,2048]{1,0:T(8,128)(2,1)S(1)} %collective-permute-done.4.refs_1_, bf16[16,2112,128]{2,1,0:T(8,128)(2,1)S(1)} %bitcast.19), custom_call_target="tpu_custom_call" | custom-call | flops 1660944384 | bytes 10000000 | tf_op jit(solution)/shard_map/pallas_call | solution.py:403
  188.6 0.2 collective-permute-start.5
  188.8 0.1 shard_map.164
  188.9 0.0 copy-start.2
  188.9 0.0 copy-start.3
  188.9 0.1 collective-permute-start.16
  189.0 0.0 collective-permute-done.10.refs_1_
  189.0 0.2 shard_map.162
  189.2 0.4 collective-permute-start.11
  189.6 2.9 %collective-permute-start.12 = (bf16[96,2048]{1,0:T(8,128)(2,1)S(1)}, bf16[96,2048]{1,0:T(8,128)(2,1)S(1)}, u32[]{:S(2)}, u32[]{:S(2)}) collective-permute-start(bf16[96,2048]{1,0:T(8,128)(2,1)S(1)} %get-tuple-element.32), channel_id=1, source_target_pairs={{0,6},{2,0},{4,2},{6,4},{1,7},{3,1},{5,3},{7,5},{8,14},{10,8},{12,... | collective-permute-start | bytes 1179656 | tf_op jit(solution)/shard_map/ppermute | solution.py:470
  192.5 10.0 %collective-permute-done.16.refs_4_ = bf16[96,2048]{1,0:T(8,128)(2,1)S(1)} collective-permute-done((bf16[96,2048]{1,0:T(8,128)(2,1)S(1)}, bf16[96,2048]{1,0:T(8,128)(2,1)S(1)}, u32[]{:S(2)}, u32[]{:S(2)}) %collective-permute-start.16) | collective-permute-done | bytes 393248 | tf_op jit(solution)/shard_map/ppermute | solution.py:470
  202.5 7.8 %collective-permute-done.11.refs_2_ = bf16[96,2048]{1,0:T(8,128)(2,1)S(1)} collective-permute-done((bf16[96,2048]{1,0:T(8,128)(2,1)S(1)}, bf16[96,2048]{1,0:T(8,128)(2,1)S(1)}, u32[]{:S(2)}, u32[]{:S(2)}) %collective-permute-start.11) | collective-permute-done | bytes 393248 | tf_op jit(solution)/shard_map/ppermute | solution.py:470
  210.3 1.4 shard_map.165
  (27 shorter events, 0.1 us)
Async XLA Ops:
  6.5 0.9 copy-start.9
  6.5 1.0 copy-start.8
  6.5 1.1 copy-start.7
  6.5 53.1 %all-gather.5.cloned.1.call-start = ((), (), s32[]{:S(2)}) async-start(), calls=%async_computation.4 | async-start | bytes 5242880 | tf_op jit(solution)/shard_map/all_gather | solution.py:476
  7.3 167.1 %all-gather.7.cloned.1.call-start = ((), (), s32[]{:S(2)}) async-start(), calls=%async_computation.5 | async-start | bytes 9191424 | tf_op jit(solution)/shard_map/all_gather | solution.py:484
  29.4 30.3 %copy-start.5 = (bf16[4,800,128]{2,1,0:T(8,128)(2,1)}, bf16[4,800,128]{2,1,0:T(8,128)(2,1)S(1)}, u32[]{:S(2)}) copy-start(bf16[4,800,128]{2,1,0:T(8,128)(2,1)S(1)} %all_to_all.20.refs_2_) | copy-start | bytes 2457604
  29.5 30.2 %all-to-all-start.1 = ((bf16[16,96,128]{2,1,0:T(8,128)(2,1)}), bf16[16,96,128]{2,1,0:T(8,128)(2,1)S(1)}, u32[]{:S(2)}, u32[]{:S(2)}) async-start(bf16[16,96,128]{2,1,0:T(8,128)(2,1)} %get-tuple-element.21), calls=%async_computation.1 | async-start | bytes 786432 | tf_op jit(solution)/shard_map/all_to_all | solution.py:478
  34.6 38.8 %collective-permute-start.1 = (bf16[4,800,128]{2,1,0:T(8,128)(2,1)S(1)}, bf16[4,800,128]{2,1,0:T(8,128)(2,1)S(1)}, u32[]{:S(2)}, u32[]{:S(2)}) collective-permute-start(bf16[4,800,128]{2,1,0:T(8,128)(2,1)S(1)} %all_to_all.20.refs_2_), channel_id=1, source_target_pairs={{0,8},{8,16},{16,24},{24,0},{1,9},{9,17},{17,25},{25,1},{2,10},{10... | collective-permute-start | bytes 2457608 | tf_op jit(solution)/shard_map/ppermute | solution.py:470
  36.6 36.9 %collective-permute-start.2 = (bf16[4,800,128]{2,1,0:T(8,128)(2,1)S(1)}, bf16[4,800,128]{2,1,0:T(8,128)(2,1)}, u32[]{:S(2)}, u32[]{:S(2)}) collective-permute-start(bf16[4,800,128]{2,1,0:T(8,128)(2,1)S(1)} %all_to_all.20.refs_2_), channel_id=1, source_target_pairs={{0,24},{8,0},{16,8},{24,16},{1,25},{9,1},{17,9},{25,17},{2,26},{10... | collective-permute-start | bytes 2457608 | tf_op jit(solution)/shard_map/ppermute | solution.py:470
  38.0 55.0 %collective-permute-start = (bf16[4,800,128]{2,1,0:T(8,128)(2,1)S(1)}, bf16[4,800,128]{2,1,0:T(8,128)(2,1)S(1)}, u32[]{:S(2)}, u32[]{:S(2)}) collective-permute-start(bf16[4,800,128]{2,1,0:T(8,128)(2,1)S(1)} %all_to_all.20.refs_2_), channel_id=1, source_target_pairs={{0,16},{8,24},{16,0},{24,8},{1,17},{9,25},{17,1},{25,9},{2,18},{10... | collective-permute-start | bytes 2457608 | tf_op jit(solution)/shard_map/ppermute | solution.py:470
  59.7 84.5 %collective-permute-start.3 = (bf16[4,256,2048]{2,1,0:T(8,128)(2,1)}, bf16[4,256,2048]{2,1,0:T(8,128)(2,1)}, u32[]{:S(2)}, u32[]{:S(2)}) collective-permute-start(bf16[4,256,2048]{2,1,0:T(8,128)(2,1)} %bitcast.24), channel_id=1, source_target_pairs={{0,1},{1,0},{2,3},{3,2},{4,5},{5,4},{6,7},{7,6},{8,9},{9,8},{10,11... | collective-permute-start | bytes 12582920 | tf_op jit(solution)/shard_map/ppermute | solution.py:473
  59.7 0.7 copy-start.6
  73.5 0.9 copy-start.11
  92.9 0.9 copy-start.10
  131.8 12.4 %all-to-all-start.3 = ((bf16[8,96,256]{2,1,0:T(8,128)(2,1)}), bf16[8,96,256]{2,1,0:T(8,128)(2,1)S(1)}, u32[]{:S(2)}, u32[]{:S(2)}) async-start(bf16[8,96,256]{2,1,0:T(8,128)(2,1)} %shard_map.158), calls=%async_computation.3 | async-start | bytes 786432 | tf_op jit(solution)/shard_map/all_to_all | solution.py:490
  144.2 0.7 copy-start.4
  152.0 11.7 %collective-permute-start.6 = (bf16[96,2048]{1,0:T(8,128)(2,1)}, bf16[96,2048]{1,0:T(8,128)(2,1)S(1)}, u32[]{:S(2)}, u32[]{:S(2)}) collective-permute-start(bf16[96,2048]{1,0:T(8,128)(2,1)} %shard_map.159.refs_0_.n_ref), channel_id=1, source_target_pairs={{0,2},{2,4},{4,6},{6,0},{1,3},{3,5},{5,7},{7,1},{8,10},{10,12},{12... | collective-permute-start | bytes 1179656 | tf_op jit(solution)/shard_map/ppermute | solution.py:470
  152.5 11.2 %collective-permute-start.7 = (bf16[96,2048]{1,0:T(8,128)(2,1)}, bf16[96,2048]{1,0:T(8,128)(2,1)S(1)}, u32[]{:S(2)}, u32[]{:S(2)}) collective-permute-start(bf16[96,2048]{1,0:T(8,128)(2,1)} %shard_map.159.refs_0_.n_ref), channel_id=1, source_target_pairs={{0,6},{2,0},{4,2},{6,4},{1,7},{3,1},{5,3},{7,5},{8,14},{10,8},{12,... | collective-permute-start | bytes 1179656 | tf_op jit(solution)/shard_map/ppermute | solution.py:470
  163.7 10.7 %collective-permute-start.13 = (bf16[96,2048]{1,0:T(8,128)(2,1)S(1)}, bf16[96,2048]{1,0:T(8,128)(2,1)S(1)}, u32[]{:S(2)}, u32[]{:S(2)}) collective-permute-start(bf16[96,2048]{1,0:T(8,128)(2,1)S(1)} %collective-permute-done.6.refs_0_), channel_id=1, source_target_pairs={{0,2},{2,4},{4,6},{6,0},{1,3},{3,5},{5,7},{7,1},{8,10},{10,12},{12... | collective-permute-start | bytes 1179656 | tf_op jit(solution)/shard_map/ppermute | solution.py:470
  163.7 10.7 %collective-permute-start.8 = (bf16[96,2048]{1,0:T(8,128)(2,1)S(1)}, bf16[96,2048]{1,0:T(8,128)(2,1)S(1)}, u32[]{:S(2)}, u32[]{:S(2)}) collective-permute-start(bf16[96,2048]{1,0:T(8,128)(2,1)S(1)} %collective-permute-done.6.refs_0_), channel_id=1, source_target_pairs={{0,1},{1,0},{2,3},{3,2},{4,5},{5,4},{6,7},{7,6},{8,9},{9,8},{10,11... | collective-permute-start | bytes 1179656 | tf_op jit(solution)/shard_map/ppermute | solution.py:473
  163.7 10.7 %collective-permute-start.9 = (bf16[96,2048]{1,0:T(8,128)(2,1)S(1)}, bf16[96,2048]{1,0:T(8,128)(2,1)S(1)}, u32[]{:S(2)}, u32[]{:S(2)}) collective-permute-start(bf16[96,2048]{1,0:T(8,128)(2,1)S(1)} %collective-permute-done.7.refs_1_), channel_id=1, source_target_pairs={{0,1},{1,0},{2,3},{3,2},{4,5},{5,4},{6,7},{7,6},{8,9},{9,8},{10,11... | collective-permute-start | bytes 1179656 | tf_op jit(solution)/shard_map/ppermute | solution.py:473
  174.4 8.2 %collective-permute-start.14 = (bf16[96,2048]{1,0:T(8,128)(2,1)S(1)}, bf16[96,2048]{1,0:T(8,128)(2,1)S(1)}, u32[]{:S(2)}, u32[]{:S(2)}) collective-permute-start(bf16[96,2048]{1,0:T(8,128)(2,1)S(1)} %collective-permute-done.13.refs_0_), channel_id=1, source_target_pairs={{0,1},{1,0},{2,3},{3,2},{4,5},{5,4},{6,7},{7,6},{8,9},{9,8},{10,11... | collective-permute-start | bytes 1179656 | tf_op jit(solution)/shard_map/ppermute | solution.py:473
  174.4 3.5 %copy-start = (bf16[33792,128]{1,0:T(8,128)(2,1)S(1)}, bf16[33792,128]{1,0:T(8,128)(2,1)}, u32[]{:S(2)}) copy-start(bf16[33792,128]{1,0:T(8,128)(2,1)} %all-gather.7.cloned.1.call-done) | copy-start | bytes 25952260
  177.9 4.6 %copy-start.1 = (bf16[96,2048]{1,0:T(8,128)(2,1)S(1)}, bf16[96,2048]{1,0:T(8,128)(2,1)}, u32[]{:S(2)}) copy-start(bf16[96,2048]{1,0:T(8,128)(2,1)} %shard_map.159.refs_0_.n_ref) | copy-start | bytes 1179652
  177.9 7.9 %slice-start = ((s8[8650752]{0:T(1024)(128)(4,1)}), s8[4194304]{0:T(1024)(128)(4,1)S(1)}, s32[]{:S(2)}) async-start(s8[8650752]{0:T(1024)(128)(4,1)} %bitcast.17), calls=%async_computation.6 | async-start | bytes 8388608
  177.9 7.9 %slice-start.1 = ((s8[8650752]{0:T(1024)(128)(4,1)}), s8[262144]{0:T(1024)(128)(4,1)S(1)}, s32[]{:S(2)}) async-start(s8[8650752]{0:T(1024)(128)(4,1)} %bitcast.17), calls=%async_computation.7 | async-start | bytes 524288
  181.9 3.9 %slice-start.2 = ((s8[8650752]{0:T(1024)(128)(4,1)}), s8[4194304]{0:T(1024)(128)(4,1)S(1)}, s32[]{:S(2)}) async-start(s8[8650752]{0:T(1024)(128)(4,1)} %bitcast.17), calls=%async_computation.8 | async-start | bytes 8388608
  181.9 7.1 %collective-permute-start.10 = (bf16[2,96,2048]{2,1,0:T(8,128)(2,1)S(1)}, bf16[2,96,2048]{2,1,0:T(8,128)(2,1)S(1)}, u32[]{:S(2)}, u32[]{:S(2)}) collective-permute-start(bf16[2,96,2048]{2,1,0:T(8,128)(2,1)S(1)} %get-tuple-element.30), channel_id=1, source_target_pairs={{0,1},{1,0},{2,3},{3,2},{4,5},{5,4},{6,7},{7,6},{8,9},{9,8},{10,11... | collective-permute-start | bytes 2359304 | tf_op jit(solution)/shard_map/ppermute | solution.py:473
  182.4 3.4 %collective-permute-start.4 = (bf16[96,2048]{1,0:T(8,128)(2,1)S(1)}, bf16[96,2048]{1,0:T(8,128)(2,1)S(1)}, u32[]{:S(2)}, u32[]{:S(2)}) collective-permute-start(bf16[96,2048]{1,0:T(8,128)(2,1)S(1)} %copy-done.1), channel_id=1, source_target_pairs={{0,1},{1,0},{2,3},{3,2},{4,5},{5,4},{6,7},{7,6},{8,9},{9,8},{10,11... | collective-permute-start | bytes 1179656 | tf_op jit(solution)/shard_map/ppermute | solution.py:473
  185.3 3.5 %collective-permute-start.15 = (bf16[1,96,2048]{2,1,0:T(8,128)(2,1)S(1)}, bf16[1,96,2048]{2,1,0:T(8,128)(2,1)S(1)}, u32[]{:S(2)}, u32[]{:S(2)}) collective-permute-start(bf16[1,96,2048]{2,1,0:T(8,128)(2,1)S(1)} %get-tuple-element.34), channel_id=1, source_target_pairs={{0,1},{1,0},{2,3},{3,2},{4,5},{5,4},{6,7},{7,6},{8,9},{9,8},{10,11... | collective-permute-start | bytes 1179656 | tf_op jit(solution)/shard_map/ppermute | solution.py:473
  188.6 3.9 %collective-permute-start.5 = (bf16[1,96,2048]{2,1,0:T(8,128)(2,1)S(1)}, bf16[1,96,2048]{2,1,0:T(8,128)(2,1)S(1)}, u32[]{:S(2)}, u32[]{:S(2)}) collective-permute-start(bf16[1,96,2048]{2,1,0:T(8,128)(2,1)S(1)} %get-tuple-element.28), channel_id=1, source_target_pairs={{0,1},{1,0},{2,3},{3,2},{4,5},{5,4},{6,7},{7,6},{8,9},{9,8},{10,11... | collective-permute-start | bytes 1179656 | tf_op jit(solution)/shard_map/ppermute | solution.py:473
  188.9 21.5 %copy-start.2 = (f32[2048]{0:T(1024)S(1)}, f32[2048]{0:T(1024)}, u32[]{:S(2)}) copy-start(f32[2048]{0:T(1024)} %param.27) | copy-start | bytes 24580
  188.9 21.4 %copy-start.3 = (f32[2048]{0:T(1024)S(1)}, f32[2048]{0:T(1024)}, u32[]{:S(2)}) copy-start(f32[2048]{0:T(1024)} %param.28) | copy-start | bytes 24580
  188.9 13.6 %collective-permute-start.16 = (bf16[96,2048]{1,0:T(8,128)(2,1)S(1)}, bf16[96,2048]{1,0:T(8,128)(2,1)S(1)}, u32[]{:S(2)}, u32[]{:S(2)}) collective-permute-start(bf16[96,2048]{1,0:T(8,128)(2,1)S(1)} %shard_map.164), channel_id=1, source_target_pairs={{0,4},{2,6},{4,0},{6,2},{1,5},{3,7},{5,1},{7,3},{8,12},{10,14},{12... | collective-permute-start | bytes 1179656 | tf_op jit(solution)/shard_map/ppermute | solution.py:470
  189.2 21.1 %collective-permute-start.11 = (bf16[96,2048]{1,0:T(8,128)(2,1)S(1)}, bf16[96,2048]{1,0:T(8,128)(2,1)S(1)}, u32[]{:S(2)}, u32[]{:S(2)}) collective-permute-start(bf16[96,2048]{1,0:T(8,128)(2,1)S(1)} %get-tuple-element.31), channel_id=1, source_target_pairs={{0,2},{2,4},{4,6},{6,0},{1,3},{3,5},{5,7},{7,1},{8,10},{10,12},{12... | collective-permute-start | bytes 1179656 | tf_op jit(solution)/shard_map/ppermute | solution.py:470
  189.6 20.7 %collective-permute-start.12 = (bf16[96,2048]{1,0:T(8,128)(2,1)S(1)}, bf16[96,2048]{1,0:T(8,128)(2,1)S(1)}, u32[]{:S(2)}, u32[]{:S(2)}) collective-permute-start(bf16[96,2048]{1,0:T(8,128)(2,1)S(1)} %get-tuple-element.32), channel_id=1, source_target_pairs={{0,6},{2,0},{4,2},{6,4},{1,7},{3,1},{5,3},{7,5},{8,14},{10,8},{12,... | collective-permute-start | bytes 1179656 | tf_op jit(solution)/shard_map/ppermute | solution.py:470
Sparse Core Ops, SparseCore 0:
  9.0 50.6 all-gather.4
  61.8 76.8 all-gather.6

commit v10 on v9

--- a/solution.py
+++ b/solution.py
@@ -36,11 +36,12 @@
     return pltpu.CompilerParams(vmem_limit_bytes=mb * 1024 * 1024)
 
 
-def pack_kernel(q_ref, k_ref, v_ref, g_ref, qo_ref, kvo_ref):
+def pack_kernel(z_ref, q_ref, k_ref, v_ref, g_ref, qo_ref, *refs):
+    outs, held = refs[:4], refs[4]
     for h in range(4):
         cols = slice(h * HD, (h + 1) * HD)
-        kvo_ref[h, 0:ROWS, 0:HD] = k_ref[:, cols]
-        kvo_ref[h, 0:ROWS, HD : 2 * HD] = v_ref[:, cols]
+        held[h, 0:ROWS, 0:HD] = k_ref[:, cols]
+        held[h, 0:ROWS, HD : 2 * HD] = v_ref[:, cols]
         for y in range(4):
             at = y * SUB
             qo_ref[h * 4 + y, :, 0:HD] = q_ref[at : at + HALF, cols]
@@ -51,23 +52,38 @@
         second = (value - first).astype(BF16).astype(F32)
         third = value - first - second
         rest = jnp.zeros((PACK - ROWS - 18, 128), F32)
-        kvo_ref[h, ROWS:PACK, :] = jnp.concatenate(
-            [first, second, third, rest], axis=0
-        ).astype(BF16)
-
-
-def pack(q, k, v, g):
+        held[h, ROWS:PACK, :] = jnp.concatenate([first, second, third, rest], axis=0).astype(BF16)
+    for d in range(4):
+        outs[d][...] = held[lax.rem(z_ref[0] + d, 4)]
+
+
+def pack(z, q, k, v, g):
+    packet = jax.ShapeDtypeStruct((PACK, 128), BF16)
     return pl.pallas_call(
         pack_kernel,
-        out_shape=(
-            jax.ShapeDtypeStruct((NSH, HALF, 128), BF16),
-            jax.ShapeDtypeStruct((4, PACK, 128), BF16),
-        ),
-        in_specs=[vmem()] * 4,
-        out_specs=(vmem(), vmem()),
+        out_shape=(jax.ShapeDtypeStruct((NSH, HALF, 128), BF16),) + (packet,) * 4,
+        in_specs=[smem()] + [vmem()] * 4,
+        out_specs=(vmem(),) * 5,
+        scratch_shapes=[pltpu.VMEM((4, PACK, 128), BF16)],
         compiler_params=params(60),
         cost_estimate=pl.CostEstimate(flops=10**6, bytes_accessed=2500000, transcendentals=0),
-    )(q, k, v, g)
+    )(z, q, k, v, g)
+
+
+def assemble_kernel(z_ref, *refs):
+    for d in range(4):
+        refs[4][lax.rem(z_ref[0] + 4 - d, 4)] = refs[d][...]
+
+
+def assemble(z, pieces):
+    return pl.pallas_call(
+        assemble_kernel,
+        out_shape=jax.ShapeDtypeStruct((4, PACK, 128), BF16),
+        in_specs=[smem()] + [vmem()] * 4,
+        out_specs=vmem(),
+        compiler_params=params(16),
+        cost_estimate=pl.CostEstimate(flops=10**6, bytes_accessed=1700000, transcendentals=0),
+    )(z, *pieces)
 
 
 def unit_table(steps):
@@ -306,7 +322,7 @@
         out_shape=jax.ShapeDtypeStruct((8, HALF, 256), BF16),
         in_specs=[vmem()],
         out_specs=vmem(),
-        compiler_params=params(60),
+        compiler_params=params(16),
         cost_estimate=pl.CostEstimate(flops=10**5, bytes_accessed=800000, transcendentals=0),
     )(o)
 
@@ -363,7 +379,7 @@
             out_specs=whole((HALF, 2048)),
             scratch_shapes=[pltpu.VMEM((HALF, 2048), F32)],
         ),
-        compiler_params=params(60),
+        compiler_params=params(52),
         cost_estimate=pl.CostEstimate(
             flops=2 * HALF * 2048 * 2048, bytes_accessed=9 * 10**6, transcendentals=0
         ),
@@ -474,9 +490,11 @@
 
     place = jnp.stack([ci, 2 * xi + ci, xi]).astype(jnp.int32)
     w_same = lax.all_gather(out_weight, "x", axis=0, tiled=False)
-    q_pack, kv_pack = pack(queries, key_rows, value_rows, log_forget.T)
+    zi = lax.axis_index("z").astype(jnp.int32)[None]
+    q_pack, *packets = pack(zi, queries, key_rows, value_rows, log_forget.T)
     q_mine = lax.all_to_all(q_pack, ("z", "y"), split_axis=0, concat_axis=0, tiled=True)
-    kv_own = lax.all_to_all(kv_pack, "z", split_axis=0, concat_axis=0, tiled=True)
+    pieces = [packets[0]] + [turn(packets[d], "z", d) for d in (1, 2, 3)]
+    kv_own = assemble(zi, pieces)
     kv_back, kv_ahead = turn(kv_own, "y", 1), turn(kv_own, "y", 3)
     kv_far = turn(kv_own, "y", 2)
     w_other = swap(w_same)

time: 220 us -> 221 us (level)
  blocking collectives: 40.7 us -> 26.1 us
  starting transfers between devices: 22.6 us -> 31.6 us
  waiting for transfers between devices: 65.1 us -> 74 us
    all_to_all x1 -> x0, blocking collectives: 18.1 us -> none  [body(): lax.all_to_all(kv_pack, 'z', split_axis=0, concat_axis=0, tiled=True)]
    ppermute x9 -> x12, waiting for transfers between devices: 36.5 us -> 47.3 us  [turn(): return lax.ppermute(value, axis, [(i, (i + d) % 4) for i in range(4)])]
    ppermute x9 -> x12, starting transfers between devices: 12.1 us -> 17.5 us  [turn(): return lax.ppermute(value, axis, [(i, (i + d) % 4) for i in range(4)])]
    all_to_all x1, blocking collectives: 22.6 us -> 26.1 us  [body(): lax.all_to_all(attended, ('z', 'y'), split_axis=0, concat_axis=0, tiled=T...]
    all_to_all x1, starting transfers between devices: 5.18 us -> 8.16 us  [body(): lax.all_to_all(q_pack, ('z', 'y'), split_axis=0, concat_axis=0, tiled=True)]
    all_gather x1, waiting for transfers between devices: 19.6 us -> 17.1 us  [body(): w_same = lax.all_gather(out_weight, 'x', axis=0, tiled=False)]
    unnamed x30 -> x32, local copies, waits for them, and re-layouts: 7.11 us -> 7.28 us
  transfers between devices with their start and end apart: 21 -> 24, of which waited for: 6 -> 8; matrix products, arithmetic and copies ran while one was open for 1% -> 0% of each run, Pallas kernels for 30% -> 30%
where the time goes in v10:
time: 221 us; the launch traced here: 220 us
  waiting for transfers between devices  74 us (33%)
  Pallas kernels  66.3 us (30%)
  starting transfers between devices  31.6 us (14%)
  blocking collectives  26.1 us (12%)
  between operations  13.6 us (6%)
  local copies, waits for them, and re-layouts  7.28 us (3%)
    ppermute x12, waiting for transfers between devices, turn(): return lax.ppermute(value, axis, [(i, (i + d) % 4) for i in range(4)])  47.3 us
    pallas_call x3, Pallas kernels, attend(): pl.pallas_call(functools.partial(attend_kernel, chunks, first, final), ou...  44.9 us
    all_to_all x1, blocking collectives, body(): lax.all_to_all(attended, ('z', 'y'), split_axis=0, concat_axis=0, tiled=T...  26.1 us
    ppermute x12, starting transfers between devices, turn(): return lax.ppermute(value, axis, [(i, (i + d) % 4) for i in range(4)])  17.5 us
    all_gather x1, waiting for transfers between devices, body(): w_same = lax.all_gather(out_weight, 'x', axis=0, tiled=False)  17.1 us
    pallas_call x3, Pallas kernels, ffn(): pl.pallas_call(functools.partial(ffn_kernel, count), out_shape=(shape, sh...  9.5 us
    all_to_all x1, waiting for transfers between devices, body(): lax.all_to_all(spread(by_shard), ('x', 'c'), split_axis=0, concat_axis=0,...  8.84 us
    all_to_all x1, starting transfers between devices, body(): lax.all_to_all(q_pack, ('z', 'y'), split_axis=0, concat_axis=0, tiled=True)  8.16 us
  transfers between devices with their start and end apart: 24, of which 8 were waited for; matrix products, arithmetic and copies ran while one was open for 0% of the time, Pallas kernels for 30%

profile of v10, /device:TPU:0, one launch (start us, length us, event | category | flops | bytes accessed | tf_op | source)
XLA Modules:
  0.0 219.8 jit_solution(4160215772204988662)
XLA Ops:
  6.5 0.7 all-gather.5.cloned.1.call-update
  7.3 0.0 all-gather.7.cloned.1.call-start
  7.3 0.1 copy-done.10
  7.5 0.1 copy-done.9
  7.5 0.1 copy-done.8
  7.6 0.9 pad_maximum_fusion
  8.5 0.0 all-gather.7.cloned.1.call-update
  8.5 3.1 %shard_map.154 = (bf16[16,96,128]{2,1,0:T(8,128)(2,1)}, bf16[800,128]{1,0:T(8,128)(2,1)}, bf16[800,128]{1,0:T(8,128)(2,1)}, bf16[800,128]{1,0:T(8,128)(2,1)}, bf16[800,128]{1,0:T(8,128)(2,1)}) custom-call(s32[1]{0:T(128)} %bitcast.4.z_ref, bf16[768,256]{1,0:T(8,128)(2,1)} %q_ref.1, bf16[768,256]{1,0:T(8,128)(2,1)} %k_ref.1, bf16[768,256]{1,0:T(8,128)(2,1)} %v_ref.1, ...), custom_call_target="tpu_custom_call" | custom-call | flops 1000000 | bytes 2500000 | tf_op jit(solution)/shard_map/pallas_call | solution.py:62
  11.6 8.2 %all-to-all-start = ((bf16[16,96,128]{2,1,0:T(8,128)(2,1)}), bf16[16,96,128]{2,1,0:T(8,128)(2,1)S(1)}, u32[]{:S(2)}, u32[]{:S(2)}) async-start(bf16[16,96,128]{2,1,0:T(8,128)(2,1)} %get-tuple-element.27), calls=%async_computation | async-start | bytes 786432 | tf_op jit(solution)/shard_map/all_to_all | solution.py:495
  19.8 1.9 collective-permute-start
  21.7 2.7 %collective-permute-start.1 = (bf16[800,128]{1,0:T(8,128)(2,1)}, bf16[800,128]{1,0:T(8,128)(2,1)S(1)}, u32[]{:S(2)}, u32[]{:S(2)}) collective-permute-start(bf16[800,128]{1,0:T(8,128)(2,1)} %get-tuple-element.25), channel_id=1, source_target_pairs={{0,64},{32,96},{64,0},{96,32},{1,65},{33,97},{65,1},{97,33},{2,66}... | collective-permute-start | bytes 614408 | tf_op jit(solution)/shard_map/ppermute | solution.py:486
  24.4 1.5 collective-permute-start.2
  25.9 6.4 %collective-permute-done.refs_1_ = bf16[800,128]{1,0:T(8,128)(2,1)S(1)} collective-permute-done((bf16[800,128]{1,0:T(8,128)(2,1)}, bf16[800,128]{1,0:T(8,128)(2,1)S(1)}, u32[]{:S(2)}, u32[]{:S(2)}) %collective-permute-start) | collective-permute-done | bytes 204832 | tf_op jit(solution)/shard_map/ppermute | solution.py:486
  32.3 4.7 %collective-permute-done.1.refs_2_ = bf16[800,128]{1,0:T(8,128)(2,1)S(1)} collective-permute-done((bf16[800,128]{1,0:T(8,128)(2,1)}, bf16[800,128]{1,0:T(8,128)(2,1)S(1)}, u32[]{:S(2)}, u32[]{:S(2)}) %collective-permute-start.1) | collective-permute-done | bytes 204832 | tf_op jit(solution)/shard_map/ppermute | solution.py:486
  36.9 0.9 copy-done.2
  37.9 0.1 shard_map.155.refs_2_
  37.9 1.5 collective-permute-start.4
  39.5 1.8 collective-permute-start.5
  41.2 1.4 collective-permute-start.3
  42.6 17.1 %all-gather.5.cloned.1.call-done = bf16[1024,2048]{1,0:T(8,128)(2,1)} async-done(((bf16[256,2048]{1,0:T(8,128)(2,1)}), bf16[1024,2048]{1,0:T(8,128)(2,1)}) %all-gather.5.cloned.1.call-update) | async-done | bytes 4194320 | tf_op jit(solution)/shard_map/all_gather | solution.py:492
  59.7 0.7 copy-done.7
  60.4 13.0 %shard_map.156 = (bf16[12,128,256]{2,1,0:T(8,128)(2,1)}, f32[12,8,256]{2,1,0:T(8,128)}, f32[12,80,256]{2,1,0:T(8,128)}) custom-call(s32[4,4,33]{2,1,0:T(4,128)} %constant.23.clone.refs_0_, s32[1]{0:T(128)} %bitcast.3.refs_1_, bf16[4,800,128]{2,1,0:T(8,128)(2,1)} %copy-done.1, bf16[16,96,128]{2,1,0:T(8,128)(2,1)} %copy-done.7), custom_call_target="tpu_custom_call" | custom-call | flops 10400000000 | bytes 3000000 | tf_op jit(solution)/shard_map/pallas_call | solution.py:297
  73.5 0.0 collective-permute-done.4.refs_2_
  73.5 0.0 collective-permute-done.5.refs_3_
  73.5 0.9 copy-done.12
  74.4 18.6 %shard_map.157 = (f32[12,8,256]{2,1,0:T(8,128)}, f32[12,80,256]{2,1,0:T(8,128)}) custom-call(s32[4,4,59]{2,1,0:T(4,128)} %constant.24.clone.refs_0_, s32[1]{0:T(128)} %bitcast.3.refs_1_, bf16[4,800,128]{2,1,0:T(8,128)(2,1)} %copy-done.12, bf16[4,800,128]{2,1,0:T(8,128)(2,1)} %collective-permute-done.5.refs_3_, ...), custom_call_target="tpu_custom_call" | custom-call | flops 21600000000 | bytes 3000000 | tf_op jit(solution)/shard_map/pallas_call | solution.py:297
  92.9 0.0 collective-permute-done.3.refs_2_
  92.9 0.9 copy-done.11
  93.8 13.3 %shard_map.158 = bf16[16,96,128]{2,1,0:T(8,128)(2,1)} custom-call(s32[4,4,33]{2,1,0:T(4,128)} %constant.25.clone.refs_0_, s32[1]{0:T(128)} %bitcast.3.refs_1_, bf16[4,800,128]{2,1,0:T(8,128)(2,1)} %copy-done.11, bf16[12,128,256]{2,1,0:T(8,128)(2,1)} %get-tuple-element.28.refs_4_.refs_3_, f32[12,8,256]{2,1,0:T(8,128)} %get-tuple-element.31.refs_4_, ...), custom_call_target="tpu_custom_call" | custom-call | flops 10400000000 | bytes 3000000 | tf_op jit(solution)/shard_map/pallas_call | solution.py:297
  107.1 26.1 %all_to_all.15.o_ref = bf16[16,96,128]{2,1,0:T(8,128)(2,1)S(1)} all-to-all(bf16[16,96,128]{2,1,0:T(8,128)(2,1)} %shard_map.158), channel_id=1, replica_groups=mesh['z'=4,'y'=4,'x'=4,'c'=2] {'z','y'}, dimensions={0} | all-to-all | bytes 786432 | tf_op jit(solution)/shard_map/all_to_all | solution.py:507
  133.2 1.0 shard_map.159
  134.2 4.1 %all-to-all-start.2 = ((bf16[8,96,256]{2,1,0:T(8,128)(2,1)}), bf16[8,96,256]{2,1,0:T(8,128)(2,1)S(1)}, u32[]{:S(2)}, u32[]{:S(2)}) async-start(bf16[8,96,256]{2,1,0:T(8,128)(2,1)} %shard_map.159), calls=%async_computation.2 | async-start | bytes 786432 | tf_op jit(solution)/shard_map/all_to_all | solution.py:508
  138.3 0.1 pad_add_fusion.place
  138.4 8.8 %all-to-all-done.2.a_ref = bf16[8,96,256]{2,1,0:T(8,128)(2,1)S(1)} async-done(((bf16[8,96,256]{2,1,0:T(8,128)(2,1)}), bf16[8,96,256]{2,1,0:T(8,128)(2,1)S(1)}, u32[]{:S(2)}, u32[]{:S(2)}) %all-to-all-start.2) | async-done | bytes 393248 | tf_op jit(solution)/shard_map/all_to_all | solution.py:508
  147.3 0.0 collective-permute-done.6.other_ref
  147.3 6.0 %shard_map.160.refs_0_.n_ref = bf16[96,2048]{1,0:T(8,128)(2,1)S(1)} custom-call(s32[3]{0:T(128)S(1)} %pad_add_fusion.place, bf16[8,96,256]{2,1,0:T(8,128)(2,1)S(1)} %all-to-all-done.2.a_ref, bf16[768,2048]{1,0:T(8,128)(2,1)} %stream_ref.1, f32[1,2048]{1,0:T(1,128)S(1)} %bitcast.23, f32[1,2048]{1,0:T(1,128)S(1)} %bitcast.24, bf16[4,256,2048]{2,1,0:T(8,128)(2,1)} %bitcast.28, ...), custom_call_target="tpu_custom_call" | custom-call | flops 805306368 | bytes 9000000 | tf_op jit(solution)/shard_map/pallas_call | solution.py:365
  153.3 0.6 collective-permute-start.9
  153.9 2.7 %collective-permute-start.10 = (bf16[96,2048]{1,0:T(8,128)(2,1)S(1)}, bf16[96,2048]{1,0:T(8,128)(2,1)S(1)}, u32[]{:S(2)}, u32[]{:S(2)}) collective-permute-start(bf16[96,2048]{1,0:T(8,128)(2,1)S(1)} %shard_map.160.refs_0_.n_ref), channel_id=1, source_target_pairs={{0,6},{2,0},{4,2},{6,4},{1,7},{3,1},{5,3},{7,5},{8,14},{10,8},{12,... | collective-permute-start | bytes 1179656 | tf_op jit(solution)/shard_map/ppermute | solution.py:486
  156.6 8.3 %collective-permute-done.9.refs_0_ = bf16[96,2048]{1,0:T(8,128)(2,1)S(1)} collective-permute-done((bf16[96,2048]{1,0:T(8,128)(2,1)S(1)}, bf16[96,2048]{1,0:T(8,128)(2,1)S(1)}, u32[]{:S(2)}, u32[]{:S(2)}) %collective-permute-start.9) | collective-permute-done | bytes 393248 | tf_op jit(solution)/shard_map/ppermute | solution.py:486
  164.9 0.0 collective-permute-start.16
  164.9 0.5 collective-permute-start.12
  165.4 10.1 %collective-permute-done.16.refs_0_ = bf16[96,2048]{1,0:T(8,128)(2,1)S(1)} collective-permute-done((bf16[96,2048]{1,0:T(8,128)(2,1)S(1)}, bf16[96,2048]{1,0:T(8,128)(2,1)S(1)}, u32[]{:S(2)}, u32[]{:S(2)}) %collective-permute-start.16) | collective-permute-done | bytes 393248 | tf_op jit(solution)/shard_map/ppermute | solution.py:486
  175.6 0.0 collective-permute-start.17
  175.6 0.0 collective-permute-done.11.refs_2_
  175.6 0.0 collective-permute-done.12.refs_3_
  175.6 0.0 all-gather.7.cloned.1.call-done
  175.6 3.4 %copy-done = bf16[33792,128]{1,0:T(8,128)(2,1)S(1)} copy-done((bf16[33792,128]{1,0:T(8,128)(2,1)S(1)}, bf16[33792,128]{1,0:T(8,128)(2,1)}, u32[]{:S(2)}) %copy-start) | copy-done | bytes 8650776
  179.1 4.0 %shard_map.162 = (bf16[2,96,2048]{2,1,0:T(8,128)(2,1)S(1)}, bf16[2,96,2048]{2,1,0:T(8,128)(2,1)S(1)}) custom-call(bf16[96,2048]{1,0:T(8,128)(2,1)S(1)} %collective-permute-done.9.refs_0_, bf16[96,2048]{1,0:T(8,128)(2,1)S(1)} %collective-permute-done.10.refs_1_, bf16[96,2048]{1,0:T(8,128)(2,1)S(1)} %collective-permute-done.11.refs_2_, ...), custom_call_target="tpu_custom_call" | custom-call | flops 3321888768 | bytes 10000000 | tf_op jit(solution)/shard_map/pallas_call | solution.py:419
  183.1 0.6 collective-permute-start.13
  183.7 0.1 collective-permute-start.7
  183.8 2.7 %shard_map.164 = (bf16[1,96,2048]{2,1,0:T(8,128)(2,1)S(1)}, bf16[1,96,2048]{2,1,0:T(8,128)(2,1)S(1)}) custom-call(bf16[96,2048]{1,0:T(8,128)(2,1)S(1)} %collective-permute-done.16.refs_0_, bf16[96,2048]{1,0:T(8,128)(2,1)S(1)} %collective-permute-done.17.refs_1_, bf16[16,2112,128]{2,1,0:T(8,128)(2,1)S(1)} %bitcast.17), custom_call_target="tpu_custom_call" | custom-call | flops 1660944384 | bytes 10000000 | tf_op jit(solution)/shard_map/pallas_call | solution.py:419
  186.5 0.5 collective-permute-start.18
  187.0 2.8 %shard_map.161 = (bf16[1,96,2048]{2,1,0:T(8,128)(2,1)S(1)}, bf16[1,96,2048]{2,1,0:T(8,128)(2,1)S(1)}) custom-call(bf16[96,2048]{1,0:T(8,128)(2,1)S(1)} %shard_map.160.refs_0_.n_ref, bf16[96,2048]{1,0:T(8,128)(2,1)S(1)} %collective-permute-done.7.refs_1_, bf16[16,2112,128]{2,1,0:T(8,128)(2,1)S(1)} %bitcast.20), custom_call_target="tpu_custom_call" | custom-call | flops 1660944384 | bytes 10000000 | tf_op jit(solution)/shard_map/pallas_call | solution.py:419
  189.8 0.2 collective-permute-start.8
  190.0 0.1 shard_map.165
  190.1 0.0 copy-start.5
  190.1 0.0 copy-start.6
  190.1 0.1 collective-permute-start.19
  190.2 0.2 shard_map.163
  190.4 0.4 collective-permute-start.14
  190.8 2.9 %collective-permute-start.15 = (bf16[96,2048]{1,0:T(8,128)(2,1)S(1)}, bf16[96,2048]{1,0:T(8,128)(2,1)S(1)}, u32[]{:S(2)}, u32[]{:S(2)}) collective-permute-start(bf16[96,2048]{1,0:T(8,128)(2,1)S(1)} %get-tuple-element.38), channel_id=1, source_target_pairs={{0,6},{2,0},{4,2},{6,4},{1,7},{3,1},{5,3},{7,5},{8,14},{10,8},{12,... | collective-permute-start | bytes 1179656 | tf_op jit(solution)/shard_map/ppermute | solution.py:486
  193.7 10.0 %collective-permute-done.19.refs_4_ = bf16[96,2048]{1,0:T(8,128)(2,1)S(1)} collective-permute-done((bf16[96,2048]{1,0:T(8,128)(2,1)S(1)}, bf16[96,2048]{1,0:T(8,128)(2,1)S(1)}, u32[]{:S(2)}, u32[]{:S(2)}) %collective-permute-start.19) | collective-permute-done | bytes 393248 | tf_op jit(solution)/shard_map/ppermute | solution.py:486
  203.7 7.8 %collective-permute-done.14.refs_2_ = bf16[96,2048]{1,0:T(8,128)(2,1)S(1)} collective-permute-done((bf16[96,2048]{1,0:T(8,128)(2,1)S(1)}, bf16[96,2048]{1,0:T(8,128)(2,1)S(1)}, u32[]{:S(2)}, u32[]{:S(2)}) %collective-permute-start.14) | collective-permute-done | bytes 393248 | tf_op jit(solution)/shard_map/ppermute | solution.py:486
  211.5 1.4 shard_map.166
  (35 shorter events, 0.1 us)
Async XLA Ops:
  6.5 0.9 copy-start.10
  6.5 1.0 copy-start.9
  6.5 1.1 copy-start.8
  6.5 53.2 %all-gather.5.cloned.1.call-start = ((), (), s32[]{:S(2)}) async-start(), calls=%async_computation.3 | async-start | bytes 5242880 | tf_op jit(solution)/shard_map/all_gather | solution.py:492
  7.3 168.4 %all-gather.7.cloned.1.call-start = ((), (), s32[]{:S(2)}) async-start(), calls=%async_computation.4 | async-start | bytes 9191424 | tf_op jit(solution)/shard_map/all_gather | solution.py:502
  11.6 48.1 %all-to-all-start = ((bf16[16,96,128]{2,1,0:T(8,128)(2,1)}), bf16[16,96,128]{2,1,0:T(8,128)(2,1)S(1)}, u32[]{:S(2)}, u32[]{:S(2)}) async-start(bf16[16,96,128]{2,1,0:T(8,128)(2,1)} %get-tuple-element.27), calls=%async_computation | async-start | bytes 786432 | tf_op jit(solution)/shard_map/all_to_all | solution.py:495
  19.8 12.4 %collective-permute-start = (bf16[800,128]{1,0:T(8,128)(2,1)}, bf16[800,128]{1,0:T(8,128)(2,1)S(1)}, u32[]{:S(2)}, u32[]{:S(2)}) collective-permute-start(bf16[800,128]{1,0:T(8,128)(2,1)} %get-tuple-element.24), channel_id=1, source_target_pairs={{0,32},{32,64},{64,96},{96,0},{1,33},{33,65},{65,97},{97,1},{2,34}... | collective-permute-start | bytes 614408 | tf_op jit(solution)/shard_map/ppermute | solution.py:486
  21.7 15.2 %collective-permute-start.1 = (bf16[800,128]{1,0:T(8,128)(2,1)}, bf16[800,128]{1,0:T(8,128)(2,1)S(1)}, u32[]{:S(2)}, u32[]{:S(2)}) collective-permute-start(bf16[800,128]{1,0:T(8,128)(2,1)} %get-tuple-element.25), channel_id=1, source_target_pairs={{0,64},{32,96},{64,0},{96,32},{1,65},{33,97},{65,1},{97,33},{2,66}... | collective-permute-start | bytes 614408 | tf_op jit(solution)/shard_map/ppermute | solution.py:486
  24.4 12.5 %collective-permute-start.2 = (bf16[800,128]{1,0:T(8,128)(2,1)}, bf16[800,128]{1,0:T(8,128)(2,1)S(1)}, u32[]{:S(2)}, u32[]{:S(2)}) collective-permute-start(bf16[800,128]{1,0:T(8,128)(2,1)} %get-tuple-element.26), channel_id=1, source_target_pairs={{0,96},{32,0},{64,32},{96,64},{1,97},{33,1},{65,33},{97,65},{2,98}... | collective-permute-start | bytes 614408 | tf_op jit(solution)/shard_map/ppermute | solution.py:486
  36.9 0.9 copy-start.2
  37.9 21.8 %copy-start.1 = (bf16[4,800,128]{2,1,0:T(8,128)(2,1)}, bf16[4,800,128]{2,1,0:T(8,128)(2,1)S(1)}, u32[]{:S(2)}) copy-start(bf16[4,800,128]{2,1,0:T(8,128)(2,1)S(1)} %shard_map.155.refs_2_) | copy-start | bytes 2457604
  37.9 35.5 %collective-permute-start.4 = (bf16[4,800,128]{2,1,0:T(8,128)(2,1)S(1)}, bf16[4,800,128]{2,1,0:T(8,128)(2,1)S(1)}, u32[]{:S(2)}, u32[]{:S(2)}) collective-permute-start(bf16[4,800,128]{2,1,0:T(8,128)(2,1)S(1)} %shard_map.155.refs_2_), channel_id=1, source_target_pairs={{0,8},{8,16},{16,24},{24,0},{1,9},{9,17},{17,25},{25,1},{2,10},{10... | collective-permute-start | bytes 2457608 | tf_op jit(solution)/shard_map/ppermute | solution.py:486
  39.5 34.0 %collective-permute-start.5 = (bf16[4,800,128]{2,1,0:T(8,128)(2,1)S(1)}, bf16[4,800,128]{2,1,0:T(8,128)(2,1)}, u32[]{:S(2)}, u32[]{:S(2)}) collective-permute-start(bf16[4,800,128]{2,1,0:T(8,128)(2,1)S(1)} %shard_map.155.refs_2_), channel_id=1, source_target_pairs={{0,24},{8,0},{16,8},{24,16},{1,25},{9,1},{17,9},{25,17},{2,26},{10... | collective-permute-start | bytes 2457608 | tf_op jit(solution)/shard_map/ppermute | solution.py:486
  41.2 51.7 %collective-permute-start.3 = (bf16[4,800,128]{2,1,0:T(8,128)(2,1)S(1)}, bf16[4,800,128]{2,1,0:T(8,128)(2,1)S(1)}, u32[]{:S(2)}, u32[]{:S(2)}) collective-permute-start(bf16[4,800,128]{2,1,0:T(8,128)(2,1)S(1)} %shard_map.155.refs_2_), channel_id=1, source_target_pairs={{0,16},{8,24},{16,0},{24,8},{1,17},{9,25},{17,1},{25,9},{2,18},{10... | collective-permute-start | bytes 2457608 | tf_op jit(solution)/shard_map/ppermute | solution.py:486
  59.7 87.6 %collective-permute-start.6 = (bf16[4,256,2048]{2,1,0:T(8,128)(2,1)}, bf16[4,256,2048]{2,1,0:T(8,128)(2,1)}, u32[]{:S(2)}, u32[]{:S(2)}) collective-permute-start(bf16[4,256,2048]{2,1,0:T(8,128)(2,1)} %bitcast.27), channel_id=1, source_target_pairs={{0,1},{1,0},{2,3},{3,2},{4,5},{5,4},{6,7},{7,6},{8,9},{9,8},{10,11... | collective-permute-start | bytes 12582920 | tf_op jit(solution)/shard_map/ppermute | solution.py:489
  59.7 0.7 copy-start.7
  73.5 0.9 copy-start.12
  92.9 0.9 copy-start.11
  107.1 40.1 %copy-start.3 = (f32[2048]{0:T(1024)S(1)}, f32[2048]{0:T(1024)}, u32[]{:S(2)}) copy-start(f32[2048]{0:T(1024)} %param.22) | copy-start | bytes 24580
  107.1 40.1 %copy-start.4 = (f32[2048]{0:T(1024)S(1)}, f32[2048]{0:T(1024)}, u32[]{:S(2)}) copy-start(f32[2048]{0:T(1024)} %param.23) | copy-start | bytes 24580
  134.2 13.0 %all-to-all-start.2 = ((bf16[8,96,256]{2,1,0:T(8,128)(2,1)}), bf16[8,96,256]{2,1,0:T(8,128)(2,1)S(1)}, u32[]{:S(2)}, u32[]{:S(2)}) async-start(bf16[8,96,256]{2,1,0:T(8,128)(2,1)} %shard_map.159), calls=%async_computation.2 | async-start | bytes 786432 | tf_op jit(solution)/shard_map/all_to_all | solution.py:508
  153.3 11.6 %collective-permute-start.9 = (bf16[96,2048]{1,0:T(8,128)(2,1)S(1)}, bf16[96,2048]{1,0:T(8,128)(2,1)S(1)}, u32[]{:S(2)}, u32[]{:S(2)}) collective-permute-start(bf16[96,2048]{1,0:T(8,128)(2,1)S(1)} %shard_map.160.refs_0_.n_ref), channel_id=1, source_target_pairs={{0,2},{2,4},{4,6},{6,0},{1,3},{3,5},{5,7},{7,1},{8,10},{10,12},{12... | collective-permute-start | bytes 1179656 | tf_op jit(solution)/shard_map/ppermute | solution.py:486
  153.9 11.0 %collective-permute-start.10 = (bf16[96,2048]{1,0:T(8,128)(2,1)S(1)}, bf16[96,2048]{1,0:T(8,128)(2,1)S(1)}, u32[]{:S(2)}, u32[]{:S(2)}) collective-permute-start(bf16[96,2048]{1,0:T(8,128)(2,1)S(1)} %shard_map.160.refs_0_.n_ref), channel_id=1, source_target_pairs={{0,6},{2,0},{4,2},{6,4},{1,7},{3,1},{5,3},{7,5},{8,14},{10,8},{12,... | collective-permute-start | bytes 1179656 | tf_op jit(solution)/shard_map/ppermute | solution.py:486
  164.9 10.7 %collective-permute-start.16 = (bf16[96,2048]{1,0:T(8,128)(2,1)S(1)}, bf16[96,2048]{1,0:T(8,128)(2,1)S(1)}, u32[]{:S(2)}, u32[]{:S(2)}) collective-permute-start(bf16[96,2048]{1,0:T(8,128)(2,1)S(1)} %collective-permute-done.9.refs_0_), channel_id=1, source_target_pairs={{0,2},{2,4},{4,6},{6,0},{1,3},{3,5},{5,7},{7,1},{8,10},{10,12},{12... | collective-permute-start | bytes 1179656 | tf_op jit(solution)/shard_map/ppermute | solution.py:486
  164.9 10.7 %collective-permute-start.11 = (bf16[96,2048]{1,0:T(8,128)(2,1)S(1)}, bf16[96,2048]{1,0:T(8,128)(2,1)S(1)}, u32[]{:S(2)}, u32[]{:S(2)}) collective-permute-start(bf16[96,2048]{1,0:T(8,128)(2,1)S(1)} %collective-permute-done.9.refs_0_), channel_id=1, source_target_pairs={{0,1},{1,0},{2,3},{3,2},{4,5},{5,4},{6,7},{7,6},{8,9},{9,8},{10,11... | collective-permute-start | bytes 1179656 | tf_op jit(solution)/shard_map/ppermute | solution.py:489
  164.9 10.7 %collective-permute-start.12 = (bf16[96,2048]{1,0:T(8,128)(2,1)S(1)}, bf16[96,2048]{1,0:T(8,128)(2,1)S(1)}, u32[]{:S(2)}, u32[]{:S(2)}) collective-permute-start(bf16[96,2048]{1,0:T(8,128)(2,1)S(1)} %collective-permute-done.10.refs_1_), channel_id=1, source_target_pairs={{0,1},{1,0},{2,3},{3,2},{4,5},{5,4},{6,7},{7,6},{8,9},{9,8},{10,11... | collective-permute-start | bytes 1179656 | tf_op jit(solution)/shard_map/ppermute | solution.py:489
  175.6 8.2 %collective-permute-start.17 = (bf16[96,2048]{1,0:T(8,128)(2,1)S(1)}, bf16[96,2048]{1,0:T(8,128)(2,1)S(1)}, u32[]{:S(2)}, u32[]{:S(2)}) collective-permute-start(bf16[96,2048]{1,0:T(8,128)(2,1)S(1)} %collective-permute-done.16.refs_0_), channel_id=1, source_target_pairs={{0,1},{1,0},{2,3},{3,2},{4,5},{5,4},{6,7},{7,6},{8,9},{9,8},{10,11... | collective-permute-start | bytes 1179656 | tf_op jit(solution)/shard_map/ppermute | solution.py:489
  175.6 3.5 %copy-start = (bf16[33792,128]{1,0:T(8,128)(2,1)S(1)}, bf16[33792,128]{1,0:T(8,128)(2,1)}, u32[]{:S(2)}) copy-start(bf16[33792,128]{1,0:T(8,128)(2,1)} %all-gather.7.cloned.1.call-done) | copy-start | bytes 25952260
  179.1 7.9 %slice-start = ((s8[8650752]{0:T(1024)(128)(4,1)}), s8[4194304]{0:T(1024)(128)(4,1)S(1)}, s32[]{:S(2)}) async-start(s8[8650752]{0:T(1024)(128)(4,1)} %bitcast.18), calls=%async_computation.5 | async-start | bytes 8388608
  179.1 7.9 %slice-start.1 = ((s8[8650752]{0:T(1024)(128)(4,1)}), s8[262144]{0:T(1024)(128)(4,1)S(1)}, s32[]{:S(2)}) async-start(s8[8650752]{0:T(1024)(128)(4,1)} %bitcast.18), calls=%async_computation.6 | async-start | bytes 524288
  183.1 3.9 %slice-start.2 = ((s8[8650752]{0:T(1024)(128)(4,1)}), s8[4194304]{0:T(1024)(128)(4,1)S(1)}, s32[]{:S(2)}) async-start(s8[8650752]{0:T(1024)(128)(4,1)} %bitcast.18), calls=%async_computation.7 | async-start | bytes 8388608
  183.1 7.1 %collective-permute-start.13 = (bf16[2,96,2048]{2,1,0:T(8,128)(2,1)S(1)}, bf16[2,96,2048]{2,1,0:T(8,128)(2,1)S(1)}, u32[]{:S(2)}, u32[]{:S(2)}) collective-permute-start(bf16[2,96,2048]{2,1,0:T(8,128)(2,1)S(1)} %get-tuple-element.36), channel_id=1, source_target_pairs={{0,1},{1,0},{2,3},{3,2},{4,5},{5,4},{6,7},{7,6},{8,9},{9,8},{10,11... | collective-permute-start | bytes 2359304 | tf_op jit(solution)/shard_map/ppermute | solution.py:489
  183.7 3.4 %collective-permute-start.7 = (bf16[96,2048]{1,0:T(8,128)(2,1)S(1)}, bf16[96,2048]{1,0:T(8,128)(2,1)S(1)}, u32[]{:S(2)}, u32[]{:S(2)}) collective-permute-start(bf16[96,2048]{1,0:T(8,128)(2,1)S(1)} %shard_map.160.refs_0_.n_ref), channel_id=1, source_target_pairs={{0,1},{1,0},{2,3},{3,2},{4,5},{5,4},{6,7},{7,6},{8,9},{9,8},{10,11... | collective-permute-start | bytes 1179656 | tf_op jit(solution)/shard_map/ppermute | solution.py:489
  186.5 3.5 %collective-permute-start.18 = (bf16[1,96,2048]{2,1,0:T(8,128)(2,1)S(1)}, bf16[1,96,2048]{2,1,0:T(8,128)(2,1)S(1)}, u32[]{:S(2)}, u32[]{:S(2)}) collective-permute-start(bf16[1,96,2048]{2,1,0:T(8,128)(2,1)S(1)} %get-tuple-element.40), channel_id=1, source_target_pairs={{0,1},{1,0},{2,3},{3,2},{4,5},{5,4},{6,7},{7,6},{8,9},{9,8},{10,11... | collective-permute-start | bytes 1179656 | tf_op jit(solution)/shard_map/ppermute | solution.py:489
  189.8 3.9 %collective-permute-start.8 = (bf16[1,96,2048]{2,1,0:T(8,128)(2,1)S(1)}, bf16[1,96,2048]{2,1,0:T(8,128)(2,1)S(1)}, u32[]{:S(2)}, u32[]{:S(2)}) collective-permute-start(bf16[1,96,2048]{2,1,0:T(8,128)(2,1)S(1)} %get-tuple-element.34), channel_id=1, source_target_pairs={{0,1},{1,0},{2,3},{3,2},{4,5},{5,4},{6,7},{7,6},{8,9},{9,8},{10,11... | collective-permute-start | bytes 1179656 | tf_op jit(solution)/shard_map/ppermute | solution.py:489
  190.1 21.5 %copy-start.5 = (f32[2048]{0:T(1024)S(1)}, f32[2048]{0:T(1024)}, u32[]{:S(2)}) copy-start(f32[2048]{0:T(1024)} %param.27) | copy-start | bytes 24580
  190.1 21.5 %copy-start.6 = (f32[2048]{0:T(1024)S(1)}, f32[2048]{0:T(1024)}, u32[]{:S(2)}) copy-start(f32[2048]{0:T(1024)} %param.28) | copy-start | bytes 24580
  190.1 13.6 %collective-permute-start.19 = (bf16[96,2048]{1,0:T(8,128)(2,1)S(1)}, bf16[96,2048]{1,0:T(8,128)(2,1)S(1)}, u32[]{:S(2)}, u32[]{:S(2)}) collective-permute-start(bf16[96,2048]{1,0:T(8,128)(2,1)S(1)} %shard_map.165), channel_id=1, source_target_pairs={{0,4},{2,6},{4,0},{6,2},{1,5},{3,7},{5,1},{7,3},{8,12},{10,14},{12... | collective-permute-start | bytes 1179656 | tf_op jit(solution)/shard_map/ppermute | solution.py:486
  190.4 21.1 %collective-permute-start.14 = (bf16[96,2048]{1,0:T(8,128)(2,1)S(1)}, bf16[96,2048]{1,0:T(8,128)(2,1)S(1)}, u32[]{:S(2)}, u32[]{:S(2)}) collective-permute-start(bf16[96,2048]{1,0:T(8,128)(2,1)S(1)} %get-tuple-element.37), channel_id=1, source_target_pairs={{0,2},{2,4},{4,6},{6,0},{1,3},{3,5},{5,7},{7,1},{8,10},{10,12},{12... | collective-permute-start | bytes 1179656 | tf_op jit(solution)/shard_map/ppermute | solution.py:486
  190.8 20.7 %collective-permute-start.15 = (bf16[96,2048]{1,0:T(8,128)(2,1)S(1)}, bf16[96,2048]{1,0:T(8,128)(2,1)S(1)}, u32[]{:S(2)}, u32[]{:S(2)}) collective-permute-start(bf16[96,2048]{1,0:T(8,128)(2,1)S(1)} %get-tuple-element.38), channel_id=1, source_target_pairs={{0,6},{2,0},{4,2},{6,4},{1,7},{3,1},{5,3},{7,5},{8,14},{10,8},{12,... | collective-permute-start | bytes 1179656 | tf_op jit(solution)/shard_map/ppermute | solution.py:486
Sparse Core Ops, SparseCore 0:
  9.0 50.6 all-gather.4
  61.8 76.9 all-gather.6
